TPU v7x, 1024 devices: a whole 4x4x32 slice. The times are simulated.
1024 devices in a mesh: tp: 128 (over z, y), dp: 8 (over x, core).
Axes of the slice: x: 4, y: 4, z: 32, core: 2. Of those that a mesh axis runs over, the one named last changes fastest.
Arguments:
- stream: bfloat16 [256, 4096], P(None, ('dp', 'tp')), may hold values from -16 to 16
- lengths: int32 [256], P('dp'), may hold values from 1 to 64, 2048 in all
- prior_state: float32 [2, 256, 4096], P(None, 'dp', 'tp'), may hold values from -6 to 6
- prior_window: bfloat16 [2, 256, 3, 4096], P(None, 'dp', None, 'tp'), may hold values from -6 to 6
- norm_gain: float32 [2, 4096], P(None, 'dp'), may hold values from 0.1 to 1.9
- w_branch: bfloat16 [2, 4096, 4096], P(None, 'dp', 'tp'), may hold values from -0.09375 to 0.09375
- w_gate_branch: bfloat16 [2, 4096, 4096], P(None, 'dp', 'tp'), may hold values from -0.09375 to 0.09375
- conv_taps: bfloat16 [2, 4, 4096], P(None, None, 'tp'), may hold values from -3 to 3
- w_in_gate: bfloat16 [2, 256, 4096], P(None, None, 'tp'), may hold values from -0.375 to 0.375
- w_rec_gate: bfloat16 [2, 256, 4096], P(None, None, 'tp'), may hold values from -0.375 to 0.375
- decay_param: float32 [2, 4096], P(None, 'tp'), may hold values from -1 to 4
- w_out: bfloat16 [2, 4096, 4096], P(None, 'tp', 'dp'), may hold values from -0.5 to 0.5
Outputs:
- mixed_out: bfloat16 [256, 4096], P(None, ('dp', 'tp'))
- new_state: float32 [2, 256, 4096], P(None, 'dp', 'tp')
- new_window: bfloat16 [2, 256, 3, 4096], P(None, 'dp', None, 'tp')
All inputs are finite; a program needn't handle non-finite values. No bound on the sum of `lengths` on one device may be relied on, other than what follows from the above.
Results may differ from a plain program's by a relative error of at most 0.014.
Values may be sent and summed in bfloat16 or wider, within the bound.
No kernel may reach another device: no remote copies, remote signals or barrier semaphores. Data moves between devices by JAX's collectives and lax.ppermute only.
A program may use at most 32 MiB of HBM per device.

v0:
```python
import jax
import jax.numpy as jnp
from jax import lax
from jax.sharding import Mesh
from jax.sharding import PartitionSpec as P

D = 4096
BLOCK = 256
TP = ("tp_0", "tp_1")
DP_TP = ("dp", "tp_0", "tp_1")


epsilon = 1e-06


def laid_out(tiles, dim):
    shape = list(tiles.shape[1:])
    shape[dim] *= tiles.shape[0]
    return jnp.moveaxis(tiles, 0, dim).reshape(shape)


def stacked_from(array, axes, turns):
    tiles = array[None]
    for k in turns:
        tiles = lax.all_gather(tiles, axes[k], axis=0, tiled=True)
    carried = [lax.axis_size(axes[k]) for k in reversed(turns)]
    tiles = tiles.reshape(*carried, *array.shape)
    turned = sorted(range(len(turns)), key=lambda place: turns[len(turns) - 1 - place])
    return tiles.transpose(*turned, *range(len(turns), tiles.ndim)).reshape(-1, *array.shape)


def gathered_by_axis(array, axes, turns, dim):
    return laid_out(stacked_from(array, axes, turns), dim)


def copy_for_each(array, axis):
    devices = lax.axis_size(axis)
    return lax.all_to_all(
        jnp.broadcast_to(array[None], (devices, *array.shape)), axis, 0, 0, tiled=True
    )


def over_copies(array, axis):
    everything = copy_for_each(array, axis)
    return jnp.sum(everything, axis=0)


def from_partner(block, axis, apart):
    count = lax.axis_size(axis)
    route = []
    for low in range(count):
        high = low | 1 << apart
        if high != low and high < count:
            route += [(low, high), (high, low)]
    return lax.ppermute(block, axis, route)


def in_blocks(array, dim, devices):
    before, after = (array.shape[:dim], array.shape[dim + 1 :])
    return jnp.moveaxis(array.reshape(*before, devices, -1, *after), dim, 0)


def summed_on_arrival(array, axis, dim):
    tiles = in_blocks(array, dim, lax.axis_size(axis))
    arrived = lax.all_to_all(tiles, axis, split_axis=0, concat_axis=0, tiled=True)
    return arrived.astype(jnp.float32).sum(axis=0)


def gather_directly(array, axis, dim):
    tiles = copy_for_each(array, axis)
    return laid_out(tiles, dim)


def sum_by_axis(array, axes, dim):
    if not axes:
        return array
    nearer = lax.psum_scatter(array, axes[0], scatter_dimension=dim, tiled=True)
    return sum_by_axis(nearer, axes[1:], dim)


def norm_rows(block_rows, gain_values, squares):
    scaling = lax.rsqrt(squares / D + epsilon)
    return (block_rows.astype(jnp.float32) * scaling * gain_values).astype(jnp.bfloat16)


def normed_input(stream_local, gain_block):
    gathered = gathered_by_axis(stream_local, TP, (0, 1), 1)
    widened = gathered.astype(jnp.float32)
    squares = over_copies(jnp.sum(widened * widened, axis=1, keepdims=True), "dp")
    result = norm_rows(gathered, gain_block, squares)
    return result


def peer_block(convolved):
    col_count = convolved.shape[1]
    group_size = max(BLOCK // col_count, 1)
    device = lax.axis_index(TP)
    grouped = convolved
    for bit_number in range(group_size.bit_length() - 1):
        partner = from_partner(grouped, TP, bit_number)
        is_upper = device // (1 << bit_number) % 2 == 1
        grouped = jnp.where(
            is_upper,
            jnp.concatenate([partner, grouped], axis=1),
            jnp.concatenate([grouped, partner], axis=1),
        )
    return grouped


def block_gates(grouped, weight):
    row_count = grouped.shape[0]
    col_count = weight.shape[1]
    blocks = max(col_count // BLOCK, 1)
    block_cols = min(col_count, BLOCK)
    inputs = grouped.reshape(row_count, blocks, BLOCK)
    tables = weight.reshape(BLOCK, blocks, block_cols)
    mapped = jnp.einsum("rnk,knc->rnc", inputs, tables, preferred_element_type=jnp.float32)
    return mapped.reshape(row_count, col_count)


def recurrent_step(
    normed,
    lengths,
    prior_state,
    prior_window,
    w_branch,
    w_gate_branch,
    conv_taps,
    w_in_gate,
    w_rec_gate,
    decay_param,
    w_out,
    stream_local,
):
    col_count = w_branch.shape[1]
    summed = summed_on_arrival(
        jnp.concatenate(
            [
                jnp.dot(normed, w_branch, preferred_element_type=jnp.float32),
                jnp.dot(normed, w_gate_branch, preferred_element_type=jnp.float32),
            ],
            axis=1,
        ).astype(jnp.bfloat16),
        "dp",
        0,
    )
    branch = summed[:, :col_count].astype(jnp.bfloat16)
    gate_in = summed[:, col_count:].astype(jnp.bfloat16)
    depth = prior_window.shape[1]
    needed = depth + 1 - jnp.arange(depth, dtype=jnp.int32)
    living = lengths[:, None, None] >= needed[None, :, None]
    history = jnp.where(living, prior_window, jnp.zeros_like(prior_window))
    window = jnp.concatenate([history, branch[:, None, :]], axis=1)
    convolved = jnp.sum(
        window.astype(jnp.float32) * conv_taps.astype(jnp.float32)[None], axis=1
    ).astype(jnp.bfloat16)
    grouped = peer_block(convolved)
    input_gate = jax.nn.sigmoid(block_gates(grouped, w_in_gate))
    recur_gate = jax.nn.sigmoid(block_gates(grouped, w_rec_gate))
    log_keep = 8.0 * recur_gate * jax.nn.log_sigmoid(decay_param)
    keeping = jnp.exp(log_keep)
    feeding = jnp.sqrt(-jnp.expm1(2.0 * log_keep))
    earlier = jnp.where(lengths[:, None] >= 2, prior_state, jnp.zeros_like(prior_state))
    state = keeping * earlier + feeding * input_gate * convolved.astype(jnp.float32)
    readout = (state * jax.nn.gelu(gate_in.astype(jnp.float32))).astype(jnp.bfloat16)
    mixed = jnp.dot(gather_directly(readout, "dp", 0), w_out, preferred_element_type=jnp.float32)
    own_width = stream_local.shape[1]
    offset = lax.axis_index(TP) * own_width
    own_cols = lax.dynamic_slice_in_dim(mixed, offset, own_width, 1) + stream_local.astype(
        jnp.float32
    )
    terms = lax.dynamic_update_slice_in_dim(mixed, own_cols, offset, 1)
    return (terms, state, window[:, 1:])


def body(
    stream,
    lengths,
    prior_state,
    prior_window,
    norm_gain,
    w_branch,
    w_gate_branch,
    conv_taps,
    w_in_gate,
    w_rec_gate,
    decay_param,
    w_out,
):
    normed = normed_input(stream, norm_gain[0])
    terms, state_first, window_first = recurrent_step(
        normed,
        lengths,
        prior_state[0],
        prior_window[0],
        w_branch[0],
        w_gate_branch[0],
        conv_taps[0],
        w_in_gate[0],
        w_rec_gate[0],
        decay_param[0],
        w_out[0],
        stream,
    )
    first = sum_by_axis(terms, TP, 1).astype(jnp.bfloat16)
    normed = normed_input(first, norm_gain[1])
    terms, state_second, window_second = recurrent_step(
        normed,
        lengths,
        prior_state[1],
        prior_window[1],
        w_branch[1],
        w_gate_branch[1],
        conv_taps[1],
        w_in_gate[1],
        w_rec_gate[1],
        decay_param[1],
        w_out[1],
        first,
    )
    second = sum_by_axis(terms, TP, 1).astype(jnp.bfloat16)
    return (
        second,
        jnp.stack([state_first, state_second]),
        jnp.stack([window_first, window_second]),
    )


def solution(mesh):
    torus = Mesh(mesh.devices.reshape(32, 4, mesh.shape["dp"]), ("tp_0", "tp_1", "dp"))
    in_specs = (
        P(None, DP_TP),
        P("dp"),
        P(None, "dp", TP),
        P(None, "dp", None, TP),
        P(None, "dp"),
        P(None, "dp", TP),
        P(None, "dp", TP),
        P(None, None, TP),
        P(None, None, TP),
        P(None, None, TP),
        P(None, TP),
        P(None, TP, "dp"),
    )
    out_specs = (P(None, DP_TP), P(None, "dp", TP), P(None, "dp", None, TP))
    return jax.shard_map(body, mesh=torus, in_specs=in_specs, out_specs=out_specs, check_vma=False)
```

profile of v0, /device:TPU:4, one launch (start us, length us, event | category | flops | bytes accessed | tf_op | source)
XLA Modules:
  0.0 568.5 jit_solution(6763780801295925005)
XLA Ops:
  7.2 68.5 %all-gather = bf16[8192,4]{0,1:T(4,128)(2,1)S(1)} all-gather(bf16[256,4]{0,1:T(4,128)(2,1)} %param.12), channel_id=2, replica_groups=mesh['tp_0'=32,'tp_1'=4,'dp'=8] {'tp_0'}, dimensions={0}, use_global_device_ids=true | all-gather | bytes 67584 | tf_op jit(solution)/shard_map/all_gather | solution.py:25
  75.7 12.8 %all_gather.13 = bf16[128,256,4]{1,0,2:T(8,128)(2,1)S(1)} all-gather(bf16[32,256,4]{1,0,2:T(8,128)(2,1)S(1)} %bitcast.189), channel_id=1, replica_groups=mesh['tp_0'=32,'tp_1'=4,'dp'=8] {'tp_1'}, dimensions={0}, use_global_device_ids=true | all-gather | bytes 327680 | tf_op jit(solution)/shard_map/all_gather | solution.py:25
  88.5 0.2 copy.27
  88.7 0.2 fusion.15
  88.9 0.6 broadcast_in_dim.70
  89.5 4.8 all-to-all-start
  94.3 0.7 broadcast_compare_fusion
  95.0 0.8 bitcast_select_fusion.1
  95.9 0.8 slice_reduce_fusion
  96.8 0.5 all-to-all-done
  97.3 0.2 fusion.17
  97.6 0.4 dot_general.34
  98.0 0.7 copy.28
  98.7 0.2 convolution_convert_fusion.2
  99.0 0.2 convolution_convert_fusion.3
  99.3 0.7 reshape.549
  100.0 5.6 all-to-all-start.1
  105.6 3.0 all-to-all-done.1
  108.8 3.2 collective-permute-start
  112.0 2.3 collective-permute-done
  114.5 3.9 collective-permute-start.1
  118.4 3.1 collective-permute-done.1
  121.6 1.9 collective-permute-start.2
  123.5 3.6 collective-permute-done.2
  127.4 0.7 reshape.551
  128.2 5.7 %all-to-all-start.2 = ((bf16[8,2,512]{2,1,0:T(2,128)(2,1)}), bf16[8,2,512]{2,1,0:T(2,128)(2,1)S(1)}, u32[]{:S(2)}, u32[]{:S(2)}) async-start(bf16[8,2,512]{2,1,0:T(2,128)(2,1)} %reshape.551), calls=%async_computation.2 | async-start | bytes 32768 | tf_op jit(solution)/shard_map/all_to_all | solution.py:38
  134.0 2.8 all-to-all-done.2
  136.9 0.2 fusion.22
  137.3 1.1 dynamic_update_slice.6
  138.3 1.0 copy.36
  139.4 1.3 dynamic-slice
  141.3 124.6 %reduce-scatter.9.cloned.1.call-done = f32[16,256]{1,0:T(8,128)} async-done(((f32[512,256]{1,0:T(8,128)}), f32[16,256]{1,0:T(8,128)}) %reduce-scatter.9.cloned.1.call-update) | async-done | bytes 16400
  265.9 0.8 copy.37
  266.7 18.3 %all-reduce = bf16[256,16]{1,0:T(8,128)(2,1)S(1)} all-reduce(f32[256,16]{1,0:T(8,128)S(1)} %copy.37), channel_id=5, replica_groups=mesh['tp_0'=32,'tp_1'=4,'dp'=8] {'tp_1'}, use_global_device_ids=true, to_apply=%region_5.6.clone | all-reduce | flops 4096 | bytes 24576
  285.1 65.0 %all-gather.1 = bf16[8192,4]{1,0:T(8,128)(2,1)S(1)} all-gather(bf16[256,4]{1,0:T(8,128)(2,1)S(1)} %dynamic-slice_convert_fusion.1), channel_id=3, replica_groups=mesh['tp_0'=32,'tp_1'=4,'dp'=8] {'tp_0'}, dimensions={0}, use_global_device_ids=true | all-gather | bytes 67584 | tf_op jit(solution)/shard_map/all_gather | solution.py:25
  350.1 0.9 copy.31
  351.0 12.3 %all_gather.15 = bf16[128,256,4]{1,2,0:T(4,128)(2,1)S(1)} all-gather(bf16[32,256,4]{1,2,0:T(4,128)(2,1)S(1)} %copy.31), channel_id=1, replica_groups=mesh['tp_0'=32,'tp_1'=4,'dp'=8] {'tp_1'}, dimensions={0}, use_global_device_ids=true | all-gather | bytes 327680 | tf_op jit(solution)/shard_map/all_gather | solution.py:25
  363.4 0.2 fusion.12
  363.6 0.6 broadcast_in_dim.75
  364.3 4.8 all-to-all-start.3
  369.2 2.8 all-to-all-done.3
  372.0 0.2 fusion.14
  372.2 0.4 dot_general.40
  372.7 0.7 copy.33
  373.4 0.2 convolution_convert_fusion
  373.6 0.2 convolution_convert_fusion.1
  374.0 7.8 %all_to_all.30 = bf16[8,2,1024]{2,1,0:T(2,128)(2,1)S(1)} all-to-all(bf16[8,2,1024]{2,1,0:T(2,128)(2,1)S(1)} %reshape.553), channel_id=1, replica_groups=mesh['tp_0'=32,'tp_1'=4,'dp'=8] {'dp'}, dimensions={0} | all-to-all | bytes 65536 | tf_op jit(solution)/shard_map/all_to_all | solution.py:65
  382.0 1.9 collective-permute-start.3
  383.9 3.6 collective-permute-done.3
  387.6 3.4 collective-permute-start.4
  391.0 3.7 collective-permute-done.4
  394.7 2.2 collective-permute-start.5
  396.9 3.4 collective-permute-done.5
  400.4 0.1 fusion.43
  400.7 7.8 %all_to_all.31 = bf16[8,2,512]{2,1,0:T(2,128)(2,1)S(1)} all-to-all(bf16[8,2,512]{2,1,0:T(2,128)(2,1)S(1)} %reshape.555), channel_id=1, replica_groups=mesh['tp_0'=32,'tp_1'=4,'dp'=8] {'dp'}, dimensions={0} | all-to-all | bytes 32768 | tf_op jit(solution)/shard_map/all_to_all | solution.py:38
  408.5 0.2 fusion.18
  408.9 1.1 dynamic_update_slice.7
  410.0 1.0 copy.39
  411.0 0.6 pad_maximum_fusion.2
  411.7 0.6 pad_maximum_fusion.5
  412.3 129.3 %reduce-scatter.11.cloned.1.call-done = f32[16,256]{1,0:T(8,128)} async-done(((f32[512,256]{1,0:T(8,128)}), f32[16,256]{1,0:T(8,128)}) %reduce-scatter.11.cloned.1.call-update) | async-done | bytes 16400
  541.6 0.8 copy.40
  542.4 18.4 %all-reduce.1 = bf16[256,16]{1,0:T(8,128)(2,1)S(1)} all-reduce(f32[256,16]{1,0:T(8,128)S(1)} %copy.40), channel_id=7, replica_groups=mesh['tp_0'=32,'tp_1'=4,'dp'=8] {'tp_1'}, use_global_device_ids=true, to_apply=%region_11.12.clone | all-reduce | flops 4096 | bytes 24576
  560.9 0.7 copy.35
  (68 shorter events, 2.8 us)
Async XLA Ops:
  88.7 10.1 %copy-start.1 = (bf16[2,512,32]{1,2,0:T(8,128)(2,1)S(1)}, bf16[2,512,32]{1,2,0:T(8,128)(2,1)}, u32[]{:S(2)}) copy-start(bf16[2,512,32]{1,2,0:T(8,128)(2,1)} %param.18) | copy-start | bytes 196612
  88.9 10.1 %copy-start.2 = (bf16[2,512,32]{1,2,0:T(8,128)(2,1)S(1)}, bf16[2,512,32]{1,2,0:T(8,128)(2,1)}, u32[]{:S(2)}) copy-start(bf16[2,512,32]{1,2,0:T(8,128)(2,1)} %param.17) | copy-start | bytes 196612
  89.5 7.7 %all-to-all-start = ((f32[8,256,1]{1,2,0:T(1,128)}), f32[8,256,1]{1,2,0:T(1,128)S(1)}, u32[]{:S(2)}, u32[]{:S(2)}) async-start(f32[8,256,1]{1,2,0:T(1,128)} %broadcast_in_dim.70), calls=%async_computation | async-start | bytes 16384 | tf_op jit(solution)/shard_map/all_to_all | solution.py:38
  97.3 8.4 %copy-start.5 = (bf16[2,4,32]{2,1,0:T(4,128)(2,1)S(1)}, bf16[2,4,32]{2,1,0:T(4,128)(2,1)}, u32[]{:S(2)}) copy-start(bf16[2,4,32]{2,1,0:T(4,128)(2,1)} %param.19) | copy-start | bytes 1540
  97.5 20.8 %copy-start.6 = (f32[2,32]{1,0:T(2,128)S(1)}, f32[2,32]{1,0:T(2,128)}, u32[]{:S(2)}) copy-start(f32[2,32]{1,0:T(2,128)} %param.22) | copy-start | bytes 772
  97.5 26.0 %copy-start.9 = (s32[32]{0:T(128)S(1)}, s32[32]{0:T(128)}, u32[]{:S(2)}) copy-start(s32[32]{0:T(128)} %param.13) | copy-start | bytes 388
  97.5 29.6 %copy-start.7 = (bf16[2,256,32]{1,2,0:T(8,128)(2,1)S(1)}, bf16[2,256,32]{1,2,0:T(8,128)(2,1)}, u32[]{:S(2)}) copy-start(bf16[2,256,32]{1,2,0:T(8,128)(2,1)} %param.21) | copy-start | bytes 98308
  97.5 29.7 %copy-start.3 = (f32[2,32,32]{2,1,0:T(8,128)S(1)}, f32[2,32,32]{2,1,0:T(8,128)}, u32[]{:S(2)}) copy-start(f32[2,32,32]{2,1,0:T(8,128)} %param.14) | copy-start | bytes 24580
  97.5 29.7 %copy-start.8 = (bf16[2,256,32]{1,2,0:T(8,128)(2,1)S(1)}, bf16[2,256,32]{1,2,0:T(8,128)(2,1)}, u32[]{:S(2)}) copy-start(bf16[2,256,32]{1,2,0:T(8,128)(2,1)} %param.20) | copy-start | bytes 98308
  97.5 36.3 %copy-start.4 = (bf16[256,4]{0,1:T(4,128)(2,1)S(1)}, bf16[256,4]{0,1:T(4,128)(2,1)}, u32[]{:S(2)}) copy-start(bf16[256,4]{0,1:T(4,128)(2,1)} %param.12) | copy-start | bytes 6148
  98.0 38.9 %copy-start = (bf16[2,32,512]{2,1,0:T(8,128)(2,1)S(1)}, bf16[2,32,512]{2,1,0:T(8,128)(2,1)}, u32[]{:S(2)}) copy-start(bf16[2,32,512]{2,1,0:T(8,128)(2,1)} %param.23) | copy-start | bytes 196612
  100.0 8.6 %all-to-all-start.1 = ((bf16[8,2,1024]{2,1,0:T(2,128)(2,1)}), bf16[8,2,1024]{2,1,0:T(2,128)(2,1)S(1)}, u32[]{:S(2)}, u32[]{:S(2)}) async-start(bf16[8,2,1024]{2,1,0:T(2,128)(2,1)} %reshape.549), calls=%async_computation.1 | async-start | bytes 65536 | tf_op jit(solution)/shard_map/all_to_all | solution.py:65
  108.8 5.5 collective-permute-start
  114.5 7.0 %collective-permute-start.1 = (bf16[32,64]{1,0:T(8,128)(2,1)S(1)}, bf16[32,64]{1,0:T(8,128)(2,1)S(1)}, u32[]{:S(2)}, u32[]{:S(2)}) collective-permute-start(bf16[32,64]{1,0:T(8,128)(2,1)S(1)} %maximum_select_fusion.2), channel_id=1, source_target_pairs={{0,16},{16,0},{8,24},{24,8},{32,48},{48,32},{40,56},{56,40},{64,80... | collective-permute-start | bytes 12296 | tf_op jit(solution)/shard_map/ppermute | solution.py:55
  121.6 5.5 collective-permute-start.2
  128.2 8.7 %all-to-all-start.2 = ((bf16[8,2,512]{2,1,0:T(2,128)(2,1)}), bf16[8,2,512]{2,1,0:T(2,128)(2,1)S(1)}, u32[]{:S(2)}, u32[]{:S(2)}) async-start(bf16[8,2,512]{2,1,0:T(2,128)(2,1)} %reshape.551), calls=%async_computation.2 | async-start | bytes 32768 | tf_op jit(solution)/shard_map/all_to_all | solution.py:38
  133.8 132.0 %reduce-scatter.9.cloned.1.call-start = ((), (), s32[]{:S(2)}) async-start(), calls=%async_computation.8 | async-start | bytes 540672
  364.3 7.7 %all-to-all-start.3 = ((f32[8,256,1]{1,2,0:T(1,128)}), f32[8,256,1]{1,2,0:T(1,128)S(1)}, u32[]{:S(2)}, u32[]{:S(2)}) async-start(f32[8,256,1]{1,2,0:T(1,128)} %broadcast_in_dim.75), calls=%async_computation.3 | async-start | bytes 16384 | tf_op jit(solution)/shard_map/all_to_all | solution.py:38
  369.1 172.6 %reduce-scatter.11.cloned.1.call-start = ((), (), s32[]{:S(2)}) async-start(), calls=%async_computation.9 | async-start | bytes 540672
  382.0 5.5 collective-permute-start.3
  387.6 7.0 %collective-permute-start.4 = (bf16[32,64]{1,0:T(8,128)(2,1)S(1)}, bf16[32,64]{1,0:T(8,128)(2,1)S(1)}, u32[]{:S(2)}, u32[]{:S(2)}) collective-permute-start(bf16[32,64]{1,0:T(8,128)(2,1)S(1)} %maximum_select_fusion.4), channel_id=1, source_target_pairs={{0,16},{16,0},{8,24},{24,8},{32,48},{48,32},{40,56},{56,40},{64,80... | collective-permute-start | bytes 12296 | tf_op jit(solution)/shard_map/ppermute | solution.py:55
  394.7 5.5 collective-permute-start.5
Sparse Core Ops, SparseCore 0:
  139.5 126.3 reduce-scatter.8
  411.1 130.4 reduce-scatter.10
where the time goes:
time: 569 us; the launch traced here: 568 us
  waiting for transfers between devices  283 us (50%)
  blocking collectives  211 us (37%)
  starting transfers between devices  37.3 us (7%)
  local copies, waits for them, and re-layouts  15.9 us (3%)
  between operations  15.3 us (3%)
    unnamed x4, waiting for transfers between devices  254 us
    all_gather x4, blocking collectives, stacked_from(): tiles = lax.all_gather(tiles, axes[k], axis=0, tiled=True)  159 us
    unnamed x2, blocking collectives  36.7 us
    ppermute x6, waiting for transfers between devices, from_partner(): return lax.ppermute(block, axis, route)  19.7 us
    ppermute x6, starting transfers between devices, from_partner(): return lax.ppermute(block, axis, route)  16.4 us
    all_to_all x3, starting transfers between devices, copy_for_each(): lax.all_to_all(jnp.broadcast_to(array[None], (devices, *array.shape)), ax...  15.3 us
  transfers between devices with their start and end apart: 12, of which 12 were waited for; matrix products, arithmetic and copies ran while one was open for 1% of the time, Pallas kernels for 0%

commit v1 on v0

--- a/solution.py
+++ b/solution.py
@@ -19,18 +19,14 @@
     return jnp.moveaxis(tiles, 0, dim).reshape(shape)
 
 
-def stacked_from(array, axes, turns):
-    tiles = array[None]
+def gathered_by_axis(array, axes, turns, dim):
     for k in turns:
-        tiles = lax.all_gather(tiles, axes[k], axis=0, tiled=True)
-    carried = [lax.axis_size(axes[k]) for k in reversed(turns)]
-    tiles = tiles.reshape(*carried, *array.shape)
+        array = copy_for_each(array, axes[k])
+    carried = array.shape[: len(turns)]
+    rest = array.shape[len(turns) :]
     turned = sorted(range(len(turns)), key=lambda place: turns[len(turns) - 1 - place])
-    return tiles.transpose(*turned, *range(len(turns), tiles.ndim)).reshape(-1, *array.shape)
-
-
-def gathered_by_axis(array, axes, turns, dim):
-    return laid_out(stacked_from(array, axes, turns), dim)
+    tiles = array.transpose(*turned, *range(len(turns), array.ndim)).reshape(-1, *rest)
+    return laid_out(tiles, dim)
 
 
 def copy_for_each(array, axis):
@@ -71,11 +67,13 @@
     return laid_out(tiles, dim)
 
 
-def sum_by_axis(array, axes, dim):
-    if not axes:
-        return array
-    nearer = lax.psum_scatter(array, axes[0], scatter_dimension=dim, tiled=True)
-    return sum_by_axis(nearer, axes[1:], dim)
+def to_own_features(terms, stream_local):
+    rows, width = terms.shape
+    far, near = (lax.axis_size(axis) for axis in TP)
+    tiles = terms.astype(jnp.bfloat16).reshape(rows, far, near, -1)
+    tiles = summed_on_arrival(tiles, TP[1], 2)[:, :, 0]
+    own = summed_on_arrival(tiles.astype(jnp.bfloat16), TP[0], 1)[:, 0]
+    return (own + stream_local.astype(jnp.float32)).astype(jnp.bfloat16)
 
 
 def norm_rows(block_rows, gain_values, squares):
@@ -164,12 +162,7 @@
     state = keeping * earlier + feeding * input_gate * convolved.astype(jnp.float32)
     readout = (state * jax.nn.gelu(gate_in.astype(jnp.float32))).astype(jnp.bfloat16)
     mixed = jnp.dot(gather_directly(readout, "dp", 0), w_out, preferred_element_type=jnp.float32)
-    own_width = stream_local.shape[1]
-    offset = lax.axis_index(TP) * own_width
-    own_cols = lax.dynamic_slice_in_dim(mixed, offset, own_width, 1) + stream_local.astype(
-        jnp.float32
-    )
-    terms = lax.dynamic_update_slice_in_dim(mixed, own_cols, offset, 1)
+    terms = to_own_features(mixed, stream_local)
     return (terms, state, window[:, 1:])
 
 
@@ -202,7 +195,7 @@
         w_out[0],
         stream,
     )
-    first = sum_by_axis(terms, TP, 1).astype(jnp.bfloat16)
+    first = terms
     normed = normed_input(first, norm_gain[1])
     terms, state_second, window_second = recurrent_step(
         normed,
@@ -218,7 +211,7 @@
         w_out[1],
         first,
     )
-    second = sum_by_axis(terms, TP, 1).astype(jnp.bfloat16)
+    second = terms
     return (
         second,
         jnp.stack([state_first, state_second]),

time: 569 us -> 282 us (0.50)
  the two profiles are of different devices: /device:TPU:4 before, /device:TPU:2 now
where the time goes in v1:
time: 282 us; the launch traced here: 280 us
  blocking collectives  97.2 us (34%)
  waiting for transfers between devices  94.3 us (33%)
  starting transfers between devices  70.4 us (25%)
  local copies, waits for them, and re-layouts  10.9 us (4%)
  other arithmetic  4.74 us (2%)
    all_to_all x4, blocking collectives, copy_for_each(): lax.all_to_all(jnp.broadcast_to(array[None], (devices, *array.shape)), ax...  52.1 us
    all_to_all x3, blocking collectives, summed_on_arrival(): lax.all_to_all(tiles, axis, split_axis=0, concat_axis=0, tiled=True)  45 us
    all_to_all x4, starting transfers between devices, copy_for_each(): lax.all_to_all(jnp.broadcast_to(array[None], (devices, *array.shape)), ax...  43 us
    all_to_all x4, waiting for transfers between devices, copy_for_each(): lax.all_to_all(jnp.broadcast_to(array[None], (devices, *array.shape)), ax...  39.1 us
    all_to_all x3, waiting for transfers between devices, summed_on_arrival(): lax.all_to_all(tiles, axis, split_axis=0, concat_axis=0, tiled=True)  34.5 us
    ppermute x6, waiting for transfers between devices, from_partner(): return lax.ppermute(block, axis, route)  20.7 us
    ppermute x6, starting transfers between devices, from_partner(): return lax.ppermute(block, axis, route)  15.3 us
    all_to_all x3, starting transfers between devices, summed_on_arrival(): lax.all_to_all(tiles, axis, split_axis=0, concat_axis=0, tiled=True)  12.1 us
  transfers between devices with their start and end apart: 13, of which 13 were waited for; matrix products, arithmetic and copies ran while one was open for 1% of the time, Pallas kernels for 0%

profile of v1, /device:TPU:2, one launch (start us, length us, event | category | flops | bytes accessed | tf_op | source)
XLA Modules:
  0.0 280.5 jit_solution(1835935291803614784)
XLA Ops:
  0.6 1.3 broadcast_in_dim.45
  2.0 28.7 %all-to-all-start = ((bf16[32,256,4]{1,2,0:T(4,128)(2,1)}), bf16[32,256,4]{1,2,0:T(4,128)(2,1)S(1)}, u32[]{:S(2)}, u32[]{:S(2)}) async-start(bf16[32,256,4]{1,2,0:T(4,128)(2,1)} %broadcast_in_dim.45), calls=%async_computation | async-start | bytes 131072 | tf_op jit(solution)/shard_map/all_to_all | solution.py:34
  30.7 0.6 copy-done.11
  31.4 25.0 %all-to-all-done = bf16[32,256,4]{1,2,0:T(4,128)(2,1)S(1)} async-done(((bf16[32,256,4]{1,2,0:T(4,128)(2,1)}), bf16[32,256,4]{1,2,0:T(4,128)(2,1)S(1)}, u32[]{:S(2)}, u32[]{:S(2)}) %all-to-all-start) | async-done | bytes 65568 | tf_op jit(solution)/shard_map/all_to_all | solution.py:34
  56.5 0.8 broadcast_in_dim.46
  57.2 4.6 %all-to-all-start.1 = ((bf16[4,32,256,4]{2,3,1,0:T(4,128)(2,1)}), bf16[4,32,256,4]{2,3,1,0:T(4,128)(2,1)S(1)}, u32[]{:S(2)}, u32[]{:S(2)}) async-start(bf16[4,32,256,4]{2,3,1,0:T(4,128)(2,1)} %broadcast_in_dim.46), calls=%async_computation.1 | async-start | bytes 524288 | tf_op jit(solution)/shard_map/all_to_all | solution.py:34
  61.9 6.6 %all-to-all-done.1 = bf16[4,32,256,4]{2,3,1,0:T(4,128)(2,1)S(1)} async-done(((bf16[4,32,256,4]{2,3,1,0:T(4,128)(2,1)}), bf16[4,32,256,4]{2,3,1,0:T(4,128)(2,1)S(1)}, u32[]{:S(2)}, u32[]{:S(2)}) %all-to-all-start.1) | async-done | bytes 262176 | tf_op jit(solution)/shard_map/all_to_all | solution.py:34
  68.6 0.2 fusion.15
  68.8 0.6 broadcast_in_dim.47
  69.5 5.0 %all-to-all-start.2 = ((f32[8,256,1]{1,2,0:T(1,128)}), f32[8,256,1]{1,2,0:T(1,128)S(1)}, u32[]{:S(2)}, u32[]{:S(2)}) async-start(f32[8,256,1]{1,2,0:T(1,128)} %broadcast_in_dim.47), calls=%async_computation.2 | async-start | bytes 16384 | tf_op jit(solution)/shard_map/all_to_all | solution.py:34
  74.6 3.7 %all-to-all-done.2 = f32[8,256,1]{1,2,0:T(1,128)S(1)} async-done(((f32[8,256,1]{1,2,0:T(1,128)}), f32[8,256,1]{1,2,0:T(1,128)S(1)}, u32[]{:S(2)}, u32[]{:S(2)}) %all-to-all-start.2) | async-done | bytes 8224 | tf_op jit(solution)/shard_map/all_to_all | solution.py:34
  78.3 0.2 fusion.17
  78.5 0.4 dot_general.34
  79.0 0.7 copy.36
  79.8 0.2 convolution_convert_fusion.4
  80.0 0.6 copy-done.1
  80.7 0.2 convolution_convert_fusion.5
  81.0 0.7 reshape.541
  81.7 4.8 %all-to-all-start.3 = ((bf16[8,2,1024]{2,1,0:T(2,128)(2,1)}), bf16[8,2,1024]{2,1,0:T(2,128)(2,1)S(1)}, u32[]{:S(2)}, u32[]{:S(2)}) async-start(bf16[8,2,1024]{2,1,0:T(2,128)(2,1)} %reshape.541), calls=%async_computation.3 | async-start | bytes 65536 | tf_op jit(solution)/shard_map/all_to_all | solution.py:61
  86.5 4.0 %all-to-all-done.3 = bf16[8,2,1024]{2,1,0:T(2,128)(2,1)S(1)} async-done(((bf16[8,2,1024]{2,1,0:T(2,128)(2,1)}), bf16[8,2,1024]{2,1,0:T(2,128)(2,1)S(1)}, u32[]{:S(2)}, u32[]{:S(2)}) %all-to-all-start.3) | async-done | bytes 32800 | tf_op jit(solution)/shard_map/all_to_all | solution.py:61
  90.7 2.5 collective-permute-start
  93.2 3.0 %collective-permute-done = bf16[32,32]{1,0:T(8,128)(2,1)S(1)} collective-permute-done((bf16[32,32]{1,0:T(8,128)(2,1)S(1)}, bf16[32,32]{1,0:T(8,128)(2,1)S(1)}, u32[]{:S(2)}, u32[]{:S(2)}) %collective-permute-start) | collective-permute-done | bytes 2080 | tf_op jit(solution)/shard_map/ppermute | solution.py:51
  96.4 2.5 collective-permute-start.1
  99.0 4.4 %collective-permute-done.1 = bf16[32,64]{1,0:T(8,128)(2,1)S(1)} collective-permute-done((bf16[32,64]{1,0:T(8,128)(2,1)S(1)}, bf16[32,64]{1,0:T(8,128)(2,1)S(1)}, u32[]{:S(2)}, u32[]{:S(2)}) %collective-permute-start.1) | collective-permute-done | bytes 4128 | tf_op jit(solution)/shard_map/ppermute | solution.py:51
  103.5 2.6 collective-permute-start.2
  106.2 2.8 %collective-permute-done.2 = bf16[32,128]{1,0:T(8,128)(2,1)S(1)} collective-permute-done((bf16[32,128]{1,0:T(8,128)(2,1)S(1)}, bf16[32,128]{1,0:T(8,128)(2,1)S(1)}, u32[]{:S(2)}, u32[]{:S(2)}) %collective-permute-start.2) | collective-permute-done | bytes 8224 | tf_op jit(solution)/shard_map/ppermute | solution.py:51
  109.2 0.1 fusion.36
  109.5 7.8 %all_to_all.70 = bf16[8,2,512]{2,1,0:T(2,128)(2,1)S(1)} all-to-all(bf16[8,2,512]{2,1,0:T(2,128)(2,1)S(1)} %reshape.543), channel_id=1, replica_groups=mesh['tp_0'=32,'tp_1'=4,'dp'=8] {'dp'}, dimensions={0} | all-to-all | bytes 32768 | tf_op jit(solution)/shard_map/all_to_all | solution.py:34
  117.4 0.2 convolution_convert_fusion.1
  117.6 0.1 copy.38
  117.9 9.3 %all_to_all.71 = bf16[4,256,32,1,4]{1,4,2,3,0:T(4,128)(2,1)S(1)} all-to-all(bf16[4,256,32,1,4]{1,4,2,3,0:T(4,128)(2,1)S(1)} %copy.39), channel_id=1, replica_groups=mesh['tp_0'=32,'tp_1'=4,'dp'=8] {'tp_1'}, dimensions={0} | all-to-all | bytes 524288 | tf_op jit(solution)/shard_map/all_to_all | solution.py:61
  127.2 0.1 reduce_sum.122
  127.4 27.9 %all_to_all.72 = bf16[32,256,1,4]{1,3,2,0:T(4,128)(2,1)S(1)} all-to-all(bf16[32,256,1,4]{1,3,2,0:T(4,128)(2,1)S(1)} %bitcast.180), channel_id=1, replica_groups=mesh['tp_0'=32,'tp_1'=4,'dp'=8] {'tp_0'}, dimensions={0} | all-to-all | bytes 131072 | tf_op jit(solution)/shard_map/all_to_all | solution.py:61
  155.4 0.6 copy-done.5
  156.0 27.5 %all_to_all.73 = bf16[32,256,4]{1,2,0:T(4,128)(2,1)S(1)} all-to-all(bf16[32,256,4]{1,2,0:T(4,128)(2,1)S(1)} %broadcast_in_dim.51), channel_id=1, replica_groups=mesh['tp_0'=32,'tp_1'=4,'dp'=8] {'tp_0'}, dimensions={0} | all-to-all | bytes 131072 | tf_op jit(solution)/shard_map/all_to_all | solution.py:34
  183.6 9.1 %all_to_all.74 = bf16[4,32,256,4]{2,3,1,0:T(4,128)(2,1)S(1)} all-to-all(bf16[4,32,256,4]{2,3,1,0:T(4,128)(2,1)S(1)} %broadcast_in_dim.52), channel_id=1, replica_groups=mesh['tp_0'=32,'tp_1'=4,'dp'=8] {'tp_1'}, dimensions={0} | all-to-all | bytes 524288 | tf_op jit(solution)/shard_map/all_to_all | solution.py:34
  192.8 0.2 fusion.12
  193.0 0.6 broadcast_in_dim.53
  193.6 4.7 %all-to-all-start.9 = ((f32[8,256,1]{1,2,0:T(1,128)}), f32[8,256,1]{1,2,0:T(1,128)S(1)}, u32[]{:S(2)}, u32[]{:S(2)}) async-start(f32[8,256,1]{1,2,0:T(1,128)} %broadcast_in_dim.53), calls=%async_computation.9 | async-start | bytes 16384 | tf_op jit(solution)/shard_map/all_to_all | solution.py:34
  198.4 3.8 %all-to-all-done.9 = f32[8,256,1]{1,2,0:T(1,128)S(1)} async-done(((f32[8,256,1]{1,2,0:T(1,128)}), f32[8,256,1]{1,2,0:T(1,128)S(1)}, u32[]{:S(2)}, u32[]{:S(2)}) %all-to-all-start.9) | async-done | bytes 8224 | tf_op jit(solution)/shard_map/all_to_all | solution.py:34
  202.3 0.2 fusion.14
  202.5 0.4 dot_general.40
  202.9 0.7 copy.43
  203.6 0.2 convolution_convert_fusion.2
  203.8 0.2 convolution_convert_fusion.3
  204.3 7.8 %all_to_all.75 = bf16[8,2,1024]{2,1,0:T(2,128)(2,1)S(1)} all-to-all(bf16[8,2,1024]{2,1,0:T(2,128)(2,1)S(1)} %reshape.545), channel_id=1, replica_groups=mesh['tp_0'=32,'tp_1'=4,'dp'=8] {'dp'}, dimensions={0} | all-to-all | bytes 65536 | tf_op jit(solution)/shard_map/all_to_all | solution.py:61
  212.2 2.5 collective-permute-start.3
  214.7 3.1 %collective-permute-done.3 = bf16[32,32]{1,0:T(8,128)(2,1)S(1)} collective-permute-done((bf16[32,32]{1,0:T(8,128)(2,1)S(1)}, bf16[32,32]{1,0:T(8,128)(2,1)S(1)}, u32[]{:S(2)}, u32[]{:S(2)}) %collective-permute-start.3) | collective-permute-done | bytes 2080 | tf_op jit(solution)/shard_map/ppermute | solution.py:51
  217.9 2.7 collective-permute-start.4
  220.6 4.3 %collective-permute-done.4 = bf16[32,64]{1,0:T(8,128)(2,1)S(1)} collective-permute-done((bf16[32,64]{1,0:T(8,128)(2,1)S(1)}, bf16[32,64]{1,0:T(8,128)(2,1)S(1)}, u32[]{:S(2)}, u32[]{:S(2)}) %collective-permute-start.4) | collective-permute-done | bytes 4128 | tf_op jit(solution)/shard_map/ppermute | solution.py:51
  225.0 2.5 collective-permute-start.5
  227.5 3.1 %collective-permute-done.5 = bf16[32,128]{1,0:T(8,128)(2,1)S(1)} collective-permute-done((bf16[32,128]{1,0:T(8,128)(2,1)S(1)}, bf16[32,128]{1,0:T(8,128)(2,1)S(1)}, u32[]{:S(2)}, u32[]{:S(2)}) %collective-permute-start.5) | collective-permute-done | bytes 8224 | tf_op jit(solution)/shard_map/ppermute | solution.py:51
  230.7 0.1 fusion.41
  231.0 7.7 %all_to_all.76 = bf16[8,2,512]{2,1,0:T(2,128)(2,1)S(1)} all-to-all(bf16[8,2,512]{2,1,0:T(2,128)(2,1)S(1)} %reshape.547), channel_id=1, replica_groups=mesh['tp_0'=32,'tp_1'=4,'dp'=8] {'dp'}, dimensions={0} | all-to-all | bytes 32768 | tf_op jit(solution)/shard_map/all_to_all | solution.py:34
  238.8 0.2 convolution_convert_fusion
  239.2 0.8 copy.46
  240.0 3.4 %all-to-all-start.12 = ((bf16[4,256,32,1,4]{1,4,2,3,0:T(4,128)(2,1)}), bf16[4,256,32,1,4]{1,4,2,3,0:T(4,128)(2,1)S(1)}, u32[]{:S(2)}, u32[]{:S(2)}) async-start(bf16[4,256,32,1,4]{1,4,2,3,0:T(4,128)(2,1)} %copy.46), calls=%async_computation.12 | async-start | bytes 524288 | tf_op jit(solution)/shard_map/all_to_all | solution.py:61
  243.4 6.9 %all-to-all-done.12 = bf16[4,256,32,1,4]{1,4,2,3,0:T(4,128)(2,1)S(1)} async-done(((bf16[4,256,32,1,4]{1,4,2,3,0:T(4,128)(2,1)}), bf16[4,256,32,1,4]{1,4,2,3,0:T(4,128)(2,1)S(1)}, u32[]{:S(2)}, u32[]{:S(2)}) %all-to-all-start.12) | async-done | bytes 262176 | tf_op jit(solution)/shard_map/all_to_all | solution.py:61
  250.3 0.8 reduce_sum.129
  251.0 3.9 %all-to-all-start.13 = ((bf16[32,256,1,4]{1,3,2,0:T(4,128)(2,1)}), bf16[32,256,1,4]{1,3,2,0:T(4,128)(2,1)S(1)}, u32[]{:S(2)}, u32[]{:S(2)}) async-start(bf16[32,256,1,4]{1,3,2,0:T(4,128)(2,1)} %bitcast.39), calls=%async_computation.13 | async-start | bytes 131072 | tf_op jit(solution)/shard_map/all_to_all | solution.py:61
  254.9 0.6 pad_maximum_fusion.2
  255.6 0.6 pad_maximum_fusion.5
  256.2 23.6 %all-to-all-done.13 = bf16[32,256,1,4]{1,3,2,0:T(4,128)(2,1)S(1)} async-done(((bf16[32,256,1,4]{1,3,2,0:T(4,128)(2,1)}), bf16[32,256,1,4]{1,3,2,0:T(4,128)(2,1)S(1)}, u32[]{:S(2)}, u32[]{:S(2)}) %all-to-all-start.13) | async-done | bytes 65568 | tf_op jit(solution)/shard_map/all_to_all | solution.py:61
  279.9 0.6 add_convert_fusion
  (73 shorter events, 3.2 us)
Async XLA Ops:
  2.0 54.5 %all-to-all-start = ((bf16[32,256,4]{1,2,0:T(4,128)(2,1)}), bf16[32,256,4]{1,2,0:T(4,128)(2,1)S(1)}, u32[]{:S(2)}, u32[]{:S(2)}) async-start(bf16[32,256,4]{1,2,0:T(4,128)(2,1)} %broadcast_in_dim.45), calls=%async_computation | async-start | bytes 131072 | tf_op jit(solution)/shard_map/all_to_all | solution.py:34
  30.7 0.7 copy-start.11
  57.2 4.6 %copy-start.3 = (bf16[2,32,3,32]{3,1,2,0:T(8,128)(2,1)S(1)}, bf16[2,32,3,32]{3,1,2,0:T(8,128)(2,1)}, u32[]{:S(2)}) copy-start(bf16[2,32,3,32]{3,1,2,0:T(8,128)(2,1)} %param.15) | copy-start | bytes 36868
  57.2 11.3 %all-to-all-start.1 = ((bf16[4,32,256,4]{2,3,1,0:T(4,128)(2,1)}), bf16[4,32,256,4]{2,3,1,0:T(4,128)(2,1)S(1)}, u32[]{:S(2)}, u32[]{:S(2)}) async-start(bf16[4,32,256,4]{2,3,1,0:T(4,128)(2,1)} %broadcast_in_dim.46), calls=%async_computation.1 | async-start | bytes 524288 | tf_op jit(solution)/shard_map/all_to_all | solution.py:34
  69.5 5.0 %copy-start.6 = (f32[2,512]{1,0:T(2,128)S(1)}, f32[2,512]{1,0:T(2,128)}, u32[]{:S(2)}) copy-start(f32[2,512]{1,0:T(2,128)} %param.16) | copy-start | bytes 12292
  69.5 8.8 %all-to-all-start.2 = ((f32[8,256,1]{1,2,0:T(1,128)}), f32[8,256,1]{1,2,0:T(1,128)S(1)}, u32[]{:S(2)}, u32[]{:S(2)}) async-start(f32[8,256,1]{1,2,0:T(1,128)} %broadcast_in_dim.47), calls=%async_computation.2 | async-start | bytes 16384 | tf_op jit(solution)/shard_map/all_to_all | solution.py:34
  79.0 0.8 copy-start
  79.8 0.8 copy-start.1
  81.7 4.8 %copy-start.7 = (bf16[2,4,32]{2,1,0:T(4,128)(2,1)S(1)}, bf16[2,4,32]{2,1,0:T(4,128)(2,1)}, u32[]{:S(2)}) copy-start(bf16[2,4,32]{2,1,0:T(4,128)(2,1)} %param.19) | copy-start | bytes 1540
  81.7 8.9 %all-to-all-start.3 = ((bf16[8,2,1024]{2,1,0:T(2,128)(2,1)}), bf16[8,2,1024]{2,1,0:T(2,128)(2,1)S(1)}, u32[]{:S(2)}, u32[]{:S(2)}) async-start(bf16[8,2,1024]{2,1,0:T(2,128)(2,1)} %reshape.541), calls=%async_computation.3 | async-start | bytes 65536 | tf_op jit(solution)/shard_map/all_to_all | solution.py:61
  90.7 5.5 %collective-permute-start = (bf16[32,32]{1,0:T(8,128)(2,1)S(1)}, bf16[32,32]{1,0:T(8,128)(2,1)S(1)}, u32[]{:S(2)}, u32[]{:S(2)}) collective-permute-start(bf16[32,32]{1,0:T(8,128)(2,1)S(1)} %multiply_reduce_fusion.1), channel_id=1, source_target_pairs={{0,8},{8,0},{16,24},{24,16},{32,40},{40,32},{48,56},{56,48},{64,72... | collective-permute-start | bytes 6152 | tf_op jit(solution)/shard_map/ppermute | solution.py:51
  93.2 5.7 %copy-start.8 = (f32[2,32]{1,0:T(2,128)S(1)}, f32[2,32]{1,0:T(2,128)}, u32[]{:S(2)}) copy-start(f32[2,32]{1,0:T(2,128)} %param.22) | copy-start | bytes 772
  96.4 7.0 %collective-permute-start.1 = (bf16[32,64]{1,0:T(8,128)(2,1)S(1)}, bf16[32,64]{1,0:T(8,128)(2,1)S(1)}, u32[]{:S(2)}, u32[]{:S(2)}) collective-permute-start(bf16[32,64]{1,0:T(8,128)(2,1)S(1)} %maximum_select_fusion.2), channel_id=1, source_target_pairs={{0,16},{16,0},{8,24},{24,8},{32,48},{48,32},{40,56},{56,40},{64,80... | collective-permute-start | bytes 12296 | tf_op jit(solution)/shard_map/ppermute | solution.py:51
  98.9 10.1 %copy-start.9 = (bf16[2,256,32]{1,2,0:T(8,128)(2,1)S(1)}, bf16[2,256,32]{1,2,0:T(8,128)(2,1)}, u32[]{:S(2)}) copy-start(bf16[2,256,32]{1,2,0:T(8,128)(2,1)} %param.21) | copy-start | bytes 98308
  103.5 5.5 %collective-permute-start.2 = (bf16[32,128]{1,0:T(8,128)(2,1)S(1)}, bf16[32,128]{1,0:T(8,128)(2,1)S(1)}, u32[]{:S(2)}, u32[]{:S(2)}) collective-permute-start(bf16[32,128]{1,0:T(8,128)(2,1)S(1)} %maximum_select_fusion.3), channel_id=1, source_target_pairs={{0,32},{32,0},{8,40},{40,8},{16,48},{48,16},{24,56},{56,24},{64,96... | collective-permute-start | bytes 24584 | tf_op jit(solution)/shard_map/ppermute | solution.py:51
  106.2 3.0 %copy-start.4 = (f32[2,32,32]{2,1,0:T(8,128)S(1)}, f32[2,32,32]{2,1,0:T(8,128)}, u32[]{:S(2)}) copy-start(f32[2,32,32]{2,1,0:T(8,128)} %param.14) | copy-start | bytes 24580
  106.2 3.0 %copy-start.10 = (bf16[2,256,32]{1,2,0:T(8,128)(2,1)S(1)}, bf16[2,256,32]{1,2,0:T(8,128)(2,1)}, u32[]{:S(2)}) copy-start(bf16[2,256,32]{1,2,0:T(8,128)(2,1)} %param.20) | copy-start | bytes 98308
  109.5 8.0 %copy-start.2 = (bf16[2,32,512]{2,1,0:T(8,128)(2,1)S(1)}, bf16[2,32,512]{2,1,0:T(8,128)(2,1)}, u32[]{:S(2)}) copy-start(bf16[2,32,512]{2,1,0:T(8,128)(2,1)} %param.23) | copy-start | bytes 196612
  155.3 0.7 copy-start.5
  193.6 8.6 %all-to-all-start.9 = ((f32[8,256,1]{1,2,0:T(1,128)}), f32[8,256,1]{1,2,0:T(1,128)S(1)}, u32[]{:S(2)}, u32[]{:S(2)}) async-start(f32[8,256,1]{1,2,0:T(1,128)} %broadcast_in_dim.53), calls=%async_computation.9 | async-start | bytes 16384 | tf_op jit(solution)/shard_map/all_to_all | solution.py:34
  212.2 5.5 %collective-permute-start.3 = (bf16[32,32]{1,0:T(8,128)(2,1)S(1)}, bf16[32,32]{1,0:T(8,128)(2,1)S(1)}, u32[]{:S(2)}, u32[]{:S(2)}) collective-permute-start(bf16[32,32]{1,0:T(8,128)(2,1)S(1)} %multiply_reduce_fusion), channel_id=1, source_target_pairs={{0,8},{8,0},{16,24},{24,16},{32,40},{40,32},{48,56},{56,48},{64,72... | collective-permute-start | bytes 6152 | tf_op jit(solution)/shard_map/ppermute | solution.py:51
  217.9 7.0 %collective-permute-start.4 = (bf16[32,64]{1,0:T(8,128)(2,1)S(1)}, bf16[32,64]{1,0:T(8,128)(2,1)S(1)}, u32[]{:S(2)}, u32[]{:S(2)}) collective-permute-start(bf16[32,64]{1,0:T(8,128)(2,1)S(1)} %maximum_select_fusion.4), channel_id=1, source_target_pairs={{0,16},{16,0},{8,24},{24,8},{32,48},{48,32},{40,56},{56,40},{64,80... | collective-permute-start | bytes 12296 | tf_op jit(solution)/shard_map/ppermute | solution.py:51
  225.0 5.5 %collective-permute-start.5 = (bf16[32,128]{1,0:T(8,128)(2,1)S(1)}, bf16[32,128]{1,0:T(8,128)(2,1)S(1)}, u32[]{:S(2)}, u32[]{:S(2)}) collective-permute-start(bf16[32,128]{1,0:T(8,128)(2,1)S(1)} %maximum_select_fusion.5), channel_id=1, source_target_pairs={{0,32},{32,0},{8,40},{40,8},{16,48},{48,16},{24,56},{56,24},{64,96... | collective-permute-start | bytes 24584 | tf_op jit(solution)/shard_map/ppermute | solution.py:51
  240.0 10.3 %all-to-all-start.12 = ((bf16[4,256,32,1,4]{1,4,2,3,0:T(4,128)(2,1)}), bf16[4,256,32,1,4]{1,4,2,3,0:T(4,128)(2,1)S(1)}, u32[]{:S(2)}, u32[]{:S(2)}) async-start(bf16[4,256,32,1,4]{1,4,2,3,0:T(4,128)(2,1)} %copy.46), calls=%async_computation.12 | async-start | bytes 524288 | tf_op jit(solution)/shard_map/all_to_all | solution.py:61
  251.0 28.8 %all-to-all-start.13 = ((bf16[32,256,1,4]{1,3,2,0:T(4,128)(2,1)}), bf16[32,256,1,4]{1,3,2,0:T(4,128)(2,1)S(1)}, u32[]{:S(2)}, u32[]{:S(2)}) async-start(bf16[32,256,1,4]{1,3,2,0:T(4,128)(2,1)} %bitcast.39), calls=%async_computation.13 | async-start | bytes 131072 | tf_op jit(solution)/shard_map/all_to_all | solution.py:61

commit v2 on v1

v2 whole, which is shorter than its diff:
```python
import jax
import jax.numpy as jnp
from jax import lax
from jax.sharding import Mesh
from jax.sharding import PartitionSpec as P

D = 4096
BLOCK = 256
LAYERS = 2
TAPS = 4
AXES = ("zh", "zm", "zl", "y", "x", "core")
Z = ("zh", "zm", "zl")
ZQ = ("zm", "zl")
TP = ("zh", "zm", "zl", "y")
DP = ("x", "core")
PLANE = ("x", "core", "y")
PAIRED = ("zl", "y")
PAIRED_PLANE = ("zl", "y", "x", "core")
bf16 = jnp.bfloat16
f32 = jnp.float32


epsilon = 1e-06


def exchange(tiles, axes):
    return lax.all_to_all(tiles, axes, 0, 0, tiled=True)


def everywhere(array, axes):
    count = lax.axis_size(axes)
    return exchange(jnp.broadcast_to(array[None], (count, *array.shape)), axes)


def contract(a, a_dim, b, b_dim):
    return lax.dot_general(a, b, (((a_dim,), (b_dim,)), ((), ())), preferred_element_type=f32)


def grouped_features(rows_by_feature):
    width = rows_by_feature.shape[1]
    to = jnp.arange(width, dtype=jnp.int32)
    source = (to % 128) // 4 * 16 + to // 128 * 4 + to % 4
    chosen = (jnp.arange(width, dtype=jnp.int32)[:, None] == source[None, :]).astype(bf16)
    return contract(rows_by_feature, 1, chosen, 0).astype(bf16)


def gated_step(layer, branch, gate_in, upper, history, taps, gates, decay, earlier):
    convolved = (
        jnp.sum(history * taps[:3, None], axis=0) + branch.astype(f32) * taps[3]
    ).astype(bf16)
    half = BLOCK // 2
    mapped = [
        contract(convolved[:, :half], 1, gates[kind, 0], 1)
        + contract(convolved[:, half:], 1, gates[kind, 1], 1)
        for kind in range(2)
    ]
    own = jnp.where(upper, convolved[:, half:], convolved[:, :half])
    input_gate = jax.nn.sigmoid(mapped[0])
    recur_gate = jax.nn.sigmoid(mapped[1])
    log_keep = 8.0 * recur_gate * decay
    keeping = jnp.exp(log_keep)
    feeding = jnp.sqrt(-jnp.expm1(2.0 * log_keep))
    state = keeping * earlier + feeding * input_gate * own.astype(f32)
    readout = (state * jax.nn.gelu(gate_in.astype(f32))).astype(bf16)
    own_branch = jnp.where(upper, branch[:, half:], branch[:, :half])
    return state, own_branch, readout


def body(
    stream,
    lengths,
    prior_state,
    prior_window,
    norm_gain,
    w_branch,
    w_gate_branch,
    conv_taps,
    w_in_gate,
    w_rec_gate,
    decay_param,
    w_out,
):
    q = lax.axis_index(ZQ)
    zl = lax.axis_index("zl")
    y = lax.axis_index("y")
    upper = zl == 1

    stream_t = everywhere(stream.T, Z).reshape(128, 256)

    def scaled(weight, layer):
        return (weight[layer].T.astype(f32) * norm_gain[layer]).astype(bf16)

    by_feature = grouped_features(
        jnp.concatenate(
            [
                scaled(w_branch, 0),
                scaled(w_gate_branch, 0),
                scaled(w_branch, 1),
                scaled(w_gate_branch, 1),
                w_out[0],
                w_out[1],
            ],
            axis=0,
        )
    ).reshape(6, 32, 4, 128)
    gate_rows = (
        jnp.stack([w_in_gate, w_rec_gate], axis=1)
        .reshape(LAYERS, 2, 2, 128, 32)
        .transpose(0, 1, 2, 4, 3)
        .reshape(256, 128)
    )
    near = jnp.concatenate(
        [
            by_feature[:2].transpose(2, 0, 1, 3).reshape(4, 64, 128),
            by_feature[5].transpose(1, 0, 2),
            jnp.broadcast_to(gate_rows[None], (4, 256, 128)),
        ],
        axis=1,
    )
    near = exchange(near, "y")
    w_first = near[:, :64].reshape(4, 2, 32, 128).transpose(1, 0, 2, 3).reshape(2, 128, 128)
    w_last = near[:, 64:96].reshape(128, 128)
    gates = (
        near[:, 96:]
        .reshape(4, LAYERS, 2, 2, 32, 128)
        .transpose(1, 2, 3, 0, 4, 5)
        .reshape(LAYERS, 2, 2, 128, 128)
    )

    depth = TAPS - 1
    needed = depth + 1 - jnp.arange(depth, dtype=jnp.int32)
    living = lengths[None, :, None, None] >= needed[None, None, :, None]
    history = jnp.where(living, prior_window, jnp.zeros_like(prior_window))
    earlier = jnp.where(
        lengths[None, :, None] >= 2, prior_state, jnp.zeros_like(prior_state)
    )
    small = jnp.concatenate(
        [
            earlier.reshape(LAYERS, 4, 8, 32).transpose(1, 0, 2, 3).reshape(4, -1),
            history.astype(f32)
            .reshape(LAYERS, 4, 8, depth, 32)
            .transpose(1, 0, 3, 2, 4)
            .reshape(4, -1),
            jnp.broadcast_to(conv_taps.astype(f32).reshape(1, -1), (4, 256)),
            jnp.broadcast_to(jax.nn.log_sigmoid(decay_param).reshape(1, -1), (4, 64)),
            jnp.zeros((4, 64), f32),
        ],
        axis=1,
    ).reshape(1, 4, 19, 128)
    small = exchange(jnp.broadcast_to(small, (2, 4, 19, 128)).reshape(8, 19, 128), PAIRED)
    small = small.reshape(2, 4, -1)

    def own_half(parts):
        return jnp.where(upper, parts[1], parts[0])

    earlier_rows = (
        own_half(small)[:, :512].reshape(4, LAYERS, 8, 32).transpose(1, 2, 0, 3)
    ).reshape(LAYERS, 8, 128)
    history_rows = (
        small[:, :, 512:2048]
        .reshape(8, LAYERS, depth, 8, 32)
        .transpose(1, 2, 3, 0, 4)
        .reshape(LAYERS, depth, 8, 256)
    )
    taps = (
        small[:, :, 2048:2304]
        .reshape(8, LAYERS, TAPS, 32)
        .transpose(1, 2, 0, 3)
        .reshape(LAYERS, TAPS, 256)
    )
    decay = (
        own_half(small)[:, 2304:2368].reshape(4, LAYERS, 32).transpose(1, 0, 2)
    ).reshape(LAYERS, 1, 128)

    w_mid = everywhere(by_feature[4].reshape(32, 512), PLANE)
    w_mid = (
        w_mid.reshape(8, 4, 32, 4, 128).transpose(1, 2, 3, 0, 4).reshape(128, 4096)
    )
    w_second = exchange(by_feature[2:4].transpose(2, 0, 1, 3).reshape(4, 64, 128), ZQ)
    w_second = everywhere(w_second, PLANE)
    w_second = (
        w_second.reshape(8, 4, 4, 2, 32, 128).transpose(2, 3, 1, 4, 0, 5).reshape(1024, 1024)
    )

    stream_rows = stream_t.T.reshape(8, 4, 8, 128).transpose(1, 0, 2, 3)
    products = [
        contract(stream_t, 0, w_first[kind], 1)
        .astype(bf16)
        .reshape(8, 4, 8, 128)
        .transpose(1, 0, 2, 3)
        for kind in range(2)
    ]
    sent = jnp.stack(
        [
            jnp.stack([products[0], jnp.where(upper, stream_rows, products[1])], axis=2),
            jnp.stack([products[0], jnp.where(upper, products[1], stream_rows)], axis=2),
        ]
    )
    came = exchange(sent.reshape(64, 16, 128), PAIRED_PLANE).reshape(2, 32, 2, 8, 128)
    branch = came[:, :, 0].astype(f32).sum(axis=1)
    branch = jnp.concatenate([branch[0], branch[1]], axis=1)
    rows = jnp.where(upper, came[0, :, 1], came[1, :, 1])
    gate_in = jnp.where(upper, came[1, :, 1], came[0, :, 1]).astype(f32).sum(axis=0)
    widened = rows.astype(f32)
    squares = jnp.sum(jnp.sum(widened * widened, axis=0), axis=1, keepdims=True)
    scaling = lax.rsqrt(squares / D + epsilon)
    state_first, branch_first, readout = gated_step(
        0,
        (branch * scaling).astype(bf16),
        (gate_in * scaling).astype(bf16),
        upper,
        history_rows[0],
        taps[0],
        gates[0],
        decay[0],
        earlier_rows[0],
    )
    residual = lax.dynamic_index_in_dim(rows.reshape(4, 8, 8, 128), q, 0, keepdims=False)
    mixed = contract(readout, 1, w_mid, 0).astype(bf16)
    mixed = exchange(mixed.reshape(8, 4, 8, 128).transpose(1, 2, 0, 3), ZQ)
    mixed = mixed.astype(f32).sum(axis=0).astype(bf16)
    mixed = everywhere(mixed, "zh").astype(f32).sum(axis=0)
    first = (mixed + residual.astype(f32)).astype(bf16)

    first_rows = first.transpose(1, 0, 2).reshape(8, 1024)
    widened = first_rows.astype(f32)
    squares = jnp.sum(widened * widened, axis=1, keepdims=True)
    coarse = lax.reduce_precision(squares, 8, 7)
    lane = lax.broadcasted_iota(jnp.int32, (8, 128), 1)
    squares = jnp.where(lane < 64, coarse, squares - coarse).astype(bf16)
    products = contract(first_rows, 1, w_second, 1).astype(bf16)
    products = products.reshape(8, 2, 2, 2, 128)
    sent = jnp.stack(
        [
            jnp.stack(
                [products[:, zm, 0, 0], products[:, zm, 1, 0], products[:, zm, low, 1], squares]
            )
            for zm in range(2)
            for low in range(2)
        ]
    )
    came = exchange(sent, ZQ).astype(f32).sum(axis=0)
    branch = jnp.concatenate([came[0], came[1]], axis=1)
    squares = came[3, :, :1] + came[3, :, 64:65]
    scaling = lax.rsqrt(squares / D + epsilon)
    state_second, branch_second, readout = gated_step(
        1,
        (branch * scaling).astype(bf16),
        (came[2] * scaling).astype(bf16),
        upper,
        history_rows[1],
        taps[1],
        gates[1],
        decay[1],
        earlier_rows[1],
    )
    sent = jnp.stack(
        [
            jnp.broadcast_to(readout[None, None], (8, 4, 8, 128)),
            jnp.broadcast_to(first[:, None], (8, 4, 8, 128)),
        ],
        axis=2,
    )
    came = exchange(sent.reshape(32, 16, 128), PLANE).reshape(32, 2, 8, 128)
    came = jnp.concatenate(
        [came[:, 0].reshape(256, 128), came[:, 1].reshape(256, 128)], axis=1
    )
    adds = (q == y) & (lax.axis_index("zh") == 0)
    index = lax.broadcasted_iota(jnp.int32, (128, 128), 0)
    same = index == lax.broadcasted_iota(jnp.int32, (128, 128), 1)
    same = jnp.where(same & adds, 1.0, 0.0).astype(bf16)
    mixed = contract(jnp.concatenate([w_last, same], axis=0), 0, came, 1).astype(bf16)
    second = exchange(mixed.reshape(32, 4, 256), Z).astype(f32).sum(axis=0).astype(bf16)

    kept = jnp.stack(
        [state_first, state_second, branch_first.astype(f32), branch_second.astype(f32)]
    )
    kept = exchange(kept.reshape(4, 8, 4, 32).transpose(2, 0, 1, 3).reshape(4, 8, 128), "y")
    kept = kept.reshape(4, 4, 8, 32).transpose(1, 0, 2, 3).reshape(2, LAYERS, 32, 32)
    window = jnp.concatenate([history[:, :, 1:], kept[1].astype(bf16)[:, :, None]], axis=2)
    return second.T, kept[0], window


def solution(mesh):
    torus = Mesh(mesh.devices.reshape(8, 2, 2, 4, 4, 2), AXES)
    in_specs = (
        P(None, DP + TP),
        P(DP),
        P(None, DP, TP),
        P(None, DP, None, TP),
        P(None, DP),
        P(None, DP, TP),
        P(None, DP, TP),
        P(None, None, TP),
        P(None, None, TP),
        P(None, None, TP),
        P(None, TP),
        P(None, TP, DP),
    )
    out_specs = (P(None, DP + TP), P(None, DP, TP), P(None, DP, None, TP))
    return jax.shard_map(body, mesh=torus, in_specs=in_specs, out_specs=out_specs, check_vma=False)
```

time: 282 us -> 279 us (0.989)
  blocking collectives: 97.2 us -> 16.9 us
  waiting for transfers between devices: 94.3 us -> 141 us
  local copies, waits for them, and re-layouts: 10.9 us -> 24.7 us
  starting transfers between devices: 70.4 us -> 77.3 us
  other arithmetic: 4.74 us -> 10.7 us
  matrix products: 1.73 us -> 4.63 us
    all_to_all x7 -> x2, blocking collectives: 97.2 us -> 16.9 us  [exchange(): return lax.all_to_all(tiles, axes, 0, 0, tiled=True)]
    all_to_all x7 -> x11, waiting for transfers between devices: 73.6 us -> 141 us  [exchange(): return lax.all_to_all(tiles, axes, 0, 0, tiled=True)]
    all_to_all x7 -> x11, starting transfers between devices: 55.1 us -> 77.3 us  [exchange(): return lax.all_to_all(tiles, axes, 0, 0, tiled=True)]
    ppermute x6 -> x0, waiting for transfers between devices: 20.7 us -> none  [from_partner(): return lax.ppermute(block, axis, route)]
    ppermute x6 -> x0, starting transfers between devices: 15.3 us -> none  [from_partner(): return lax.ppermute(block, axis, route)]
    transpose x2 -> x4, local copies, waits for them, and re-layouts: 0.88 us -> 5.02 us  [the longest x1 3.77 us: body(): w_second.reshape(8, 4, 4, 2, 32, 128).transpose(2, 3, 1, 4, 0, 5)]
    slice x1 -> x20, local copies, waits for them, and re-layouts: 0.02 us -> 3.45 us  [the longest x1 0.77 us: scaled(): return (weight[layer].T.astype(f32) * norm_gain[layer]).astype(bf16)]
    reshape x0 -> x15, local copies, waits for them, and re-layouts: none -> 3.42 us  [the longest x2 0.76 us: body(): w_mid.reshape(8, 4, 32, 4, 128).transpose(1, 2, 3, 0, 4).reshape(128, 4096)]
  transfers between devices with their start and end apart: 13 -> 11, of which waited for: 13 -> 10; matrix products, arithmetic and copies ran while one was open for 1% -> 8% of each run, Pallas kernels for 0% -> 0%
where the time goes in v2:
time: 279 us; the launch traced here: 277 us
  waiting for transfers between devices  141 us (51%)
  starting transfers between devices  77.3 us (28%)
  local copies, waits for them, and re-layouts  24.7 us (9%)
  blocking collectives  16.9 us (6%)
  other arithmetic  10.7 us (4%)
  matrix products  4.63 us (2%)
    all_to_all x11, waiting for transfers between devices, exchange(): return lax.all_to_all(tiles, axes, 0, 0, tiled=True)  141 us
    all_to_all x11, starting transfers between devices, exchange(): return lax.all_to_all(tiles, axes, 0, 0, tiled=True)  77.3 us
    all_to_all x2, blocking collectives, exchange(): return lax.all_to_all(tiles, axes, 0, 0, tiled=True)  16.9 us
  transfers between devices with their start and end apart: 11, of which 10 were waited for; matrix products, arithmetic and copies ran while one was open for 8% of the time, Pallas kernels for 0%

profile of v2, /device:TPU:2, one launch (start us, length us, event | category | flops | bytes accessed | tf_op | source)
XLA Modules:
  0.0 276.8 jit_solution(10422961186151405607)
XLA Ops:
  0.7 0.8 fusion.137
  1.5 0.8 fusion.49
  2.2 0.8 fusion.51
  3.0 0.8 fusion.53
  3.8 0.8 fusion.55
  4.6 0.8 bitcast_dynamic-update-slice_fusion.1
  5.3 0.8 bitcast_dynamic-update-slice_fusion
  6.1 0.4 convolution_convert_fusion.1
  6.5 0.8 stack.87
  7.3 0.8 stack.88
  8.3 0.8 pad_maximum_fusion
  9.0 4.5 %all-to-all-start = ((bf16[4,352,128]{2,1,0:T(8,128)(2,1)}), bf16[4,352,128]{2,1,0:T(8,128)(2,1)S(1)}, u32[]{:S(2)}, u32[]{:S(2)}) async-start(bf16[4,352,128]{2,1,0:T(8,128)(2,1)} %pad_maximum_fusion), calls=%async_computation | async-start | bytes 720896 | tf_op jit(solution)/shard_map/all_to_all | solution.py:27
  13.6 7.6 %all-to-all-done = bf16[4,352,128]{2,1,0:T(8,128)(2,1)S(1)} async-done(((bf16[4,352,128]{2,1,0:T(8,128)(2,1)}), bf16[4,352,128]{2,1,0:T(8,128)(2,1)S(1)}, u32[]{:S(2)}, u32[]{:S(2)}) %all-to-all-start) | async-done | bytes 360480 | tf_op jit(solution)/shard_map/all_to_all | solution.py:27
  21.2 0.7 broadcast_in_dim.131
  21.9 28.7 %all-to-all-start.2 = ((bf16[32,4,256]{2,1,0:T(4,128)(2,1)}), bf16[32,4,256]{2,1,0:T(4,128)(2,1)S(1)}, u32[]{:S(2)}, u32[]{:S(2)}) async-start(bf16[32,4,256]{2,1,0:T(4,128)(2,1)} %broadcast_in_dim.131), calls=%async_computation.2 | async-start | bytes 131072 | tf_op jit(solution)/shard_map/all_to_all | solution.py:27
  51.3 23.8 %all-to-all-done.2 = bf16[32,4,256]{2,1,0:T(4,128)(2,1)S(1)} async-done(((bf16[32,4,256]{2,1,0:T(4,128)(2,1)}), bf16[32,4,256]{2,1,0:T(4,128)(2,1)S(1)}, u32[]{:S(2)}, u32[]{:S(2)}) %all-to-all-start.2) | async-done | bytes 65568 | tf_op jit(solution)/shard_map/all_to_all | solution.py:27
  75.1 8.8 %all_to_all.65 = f32[8,19,128]{2,1,0:T(8,128)S(1)} all-to-all(f32[8,19,128]{2,1,0:T(8,128)S(1)} %bitcast.260), channel_id=1, replica_groups=mesh['zh'=8,'zm'=2,'zl'=2,'y'=4,'x'=4,'core'=2] {'zl','y'}, dimensions={0} | all-to-all | bytes 155648 | tf_op jit(solution)/shard_map/all_to_all | solution.py:27
  84.0 1.1 broadcast_in_dim.132
  85.1 5.6 %all-to-all-start.4 = ((bf16[32,32,512]{2,1,0:T(8,128)(2,1)}), bf16[32,32,512]{2,1,0:T(8,128)(2,1)S(1)}, u32[]{:S(2)}, u32[]{:S(2)}) async-start(bf16[32,32,512]{2,1,0:T(8,128)(2,1)} %broadcast_in_dim.132), calls=%async_computation.4 | async-start | bytes 2097152 | tf_op jit(solution)/shard_map/all_to_all | solution.py:27
  91.5 0.8 copy.91
  92.2 14.1 %all-to-all-done.4 = bf16[32,32,512]{2,1,0:T(8,128)(2,1)S(1)} async-done(((bf16[32,32,512]{2,1,0:T(8,128)(2,1)}), bf16[32,32,512]{2,1,0:T(8,128)(2,1)S(1)}, u32[]{:S(2)}, u32[]{:S(2)}) %all-to-all-start.4) | async-done | bytes 1048608 | tf_op jit(solution)/shard_map/all_to_all | solution.py:27
  106.3 6.4 %all-to-all-start.3 = ((bf16[64,16,128]{2,1,0:T(8,128)(2,1)}), bf16[64,16,128]{2,1,0:T(8,128)(2,1)}, u32[]{:S(2)}, u32[]{:S(2)}) async-start(bf16[64,16,128]{2,1,0:T(8,128)(2,1)} %bitcast.49), calls=%async_computation.3 | async-start | bytes 524288 | tf_op jit(solution)/shard_map/all_to_all | solution.py:27
  112.8 0.6 copy.97
  113.5 0.7 fusion.133
  114.2 0.7 copy.94
  115.0 0.6 fusion.105
  115.6 0.6 mul.247
  116.3 0.6 slice_reduce_fusion
  116.9 0.6 mul.242
  117.6 0.6 fusion.136
  118.2 0.7 squeeze.103
  119.0 0.6 fusion.38
  119.7 0.7 reduce_sum.107
  120.6 1.2 copy.96
  121.9 0.5 reshape.460
  122.4 3.3 %all-to-all-start.7 = ((bf16[4,64,128]{2,1,0:T(8,128)(2,1)}), bf16[4,64,128]{2,1,0:T(8,128)(2,1)S(1)}, u32[]{:S(2)}, u32[]{:S(2)}) async-start(bf16[4,64,128]{2,1,0:T(8,128)(2,1)} %copy.97), calls=%async_computation.7 | async-start | bytes 131072 | tf_op jit(solution)/shard_map/all_to_all | solution.py:27
  125.7 0.9 convert_reduce_fusion.1
  126.7 1.0 multiply_reduce_fusion
  128.4 0.3 convolution_convert_fusion
  128.7 2.7 all-to-all-done.7
  131.4 8.1 %all_to_all.66 = bf16[4,8,8,128]{3,2,1,0:T(8,128)(2,1)S(1)} all-to-all(bf16[4,8,8,128]{3,2,1,0:T(8,128)(2,1)S(1)} %bitcast.271), channel_id=1, replica_groups=mesh['zh'=8,'zm'=2,'zl'=2,'y'=4,'x'=4,'core'=2] {'zm','zl'}, dimensions={0} | all-to-all | bytes 131072 | tf_op jit(solution)/shard_map/all_to_all | solution.py:27
  139.5 1.9 broadcast_in_dim.134
  141.4 7.5 %all-to-all-start.8 = ((bf16[32,4,64,128]{3,2,1,0:T(8,128)(2,1)}), bf16[32,4,64,128]{3,2,1,0:T(8,128)(2,1)S(1)}, u32[]{:S(2)}, u32[]{:S(2)}) async-start(bf16[32,4,64,128]{3,2,1,0:T(8,128)(2,1)} %broadcast_in_dim.134), calls=%async_computation.8 | async-start | bytes 4194304 | tf_op jit(solution)/shard_map/all_to_all | solution.py:27
  148.9 27.2 %all-to-all-done.8 = bf16[32,4,64,128]{3,2,1,0:T(8,128)(2,1)S(1)} async-done(((bf16[32,4,64,128]{3,2,1,0:T(8,128)(2,1)}), bf16[32,4,64,128]{3,2,1,0:T(8,128)(2,1)S(1)}, u32[]{:S(2)}, u32[]{:S(2)}) %all-to-all-start.8) | async-done | bytes 2097184 | tf_op jit(solution)/shard_map/all_to_all | solution.py:27
  176.1 0.7 broadcast_in_dim.133
  176.8 4.0 %all-to-all-start.6 = ((bf16[8,8,8,128]{3,2,1,0:T(8,128)(2,1)}), bf16[8,8,8,128]{3,2,1,0:T(8,128)(2,1)S(1)}, u32[]{:S(2)}, u32[]{:S(2)}) async-start(bf16[8,8,8,128]{3,2,1,0:T(8,128)(2,1)} %broadcast_in_dim.133), calls=%async_computation.6 | async-start | bytes 262144 | tf_op jit(solution)/shard_map/all_to_all | solution.py:27
  180.8 3.8 %copy.98 = bf16[4,2,4,32,8,128]{5,4,3,2,1,0:T(8,128)(2,1)} copy(bf16[4,2,4,32,8,128]{5,3,1,0,2,4:T(8,128)(2,1)S(1)} %bitcast.254) | data formatting | bytes 4194304 | tf_op jit(solution)/shard_map/transpose | solution.py:182
  184.5 24.7 %all-to-all-done.6 = bf16[8,8,8,128]{3,2,1,0:T(8,128)(2,1)S(1)} async-done(((bf16[8,8,8,128]{3,2,1,0:T(8,128)(2,1)}), bf16[8,8,8,128]{3,2,1,0:T(8,128)(2,1)S(1)}, u32[]{:S(2)}, u32[]{:S(2)}) %all-to-all-start.6) | async-done | bytes 131104 | tf_op jit(solution)/shard_map/all_to_all | solution.py:27
  209.4 2.2 fusion.4
  211.8 0.6 pad_maximum_fusion.6
  212.4 3.3 %all-to-all-start.9 = ((bf16[4,4,8,128]{3,2,1,0:T(8,128)(2,1)}), bf16[4,4,8,128]{3,2,1,0:T(8,128)(2,1)S(1)}, u32[]{:S(2)}, u32[]{:S(2)}) async-start(bf16[4,4,8,128]{3,2,1,0:T(8,128)(2,1)} %pad_maximum_fusion.6), calls=%async_computation.9 | async-start | bytes 65536 | tf_op jit(solution)/shard_map/all_to_all | solution.py:27
  216.1 5.2 %all-to-all-done.9 = bf16[4,4,8,128]{3,2,1,0:T(8,128)(2,1)S(1)} async-done(((bf16[4,4,8,128]{3,2,1,0:T(8,128)(2,1)}), bf16[4,4,8,128]{3,2,1,0:T(8,128)(2,1)S(1)}, u32[]{:S(2)}, u32[]{:S(2)}) %all-to-all-start.9) | async-done | bytes 32800 | tf_op jit(solution)/shard_map/all_to_all | solution.py:27
  222.5 0.7 reshape.470
  223.2 3.3 %all-to-all-start.12 = ((f32[4,8,128]{2,1,0:T(8,128)}), f32[4,8,128]{2,1,0:T(8,128)S(1)}, u32[]{:S(2)}, u32[]{:S(2)}) async-start(f32[4,8,128]{2,1,0:T(8,128)} %reshape.470), calls=%async_computation.12 | async-start | bytes 32768 | tf_op jit(solution)/shard_map/all_to_all | solution.py:27
  226.5 0.7 pad_maximum_fusion.4
  227.2 4.6 %all-to-all-done.12 = f32[4,8,128]{2,1,0:T(8,128)S(1)} async-done(((f32[4,8,128]{2,1,0:T(8,128)}), f32[4,8,128]{2,1,0:T(8,128)S(1)}, u32[]{:S(2)}, u32[]{:S(2)}) %all-to-all-start.12) | async-done | bytes 16416 | tf_op jit(solution)/shard_map/all_to_all | solution.py:27
  231.8 5.7 %all-to-all-start.10 = ((bf16[32,16,128]{2,1,0:T(8,128)(2,1)}), bf16[32,16,128]{2,1,0:T(8,128)(2,1)S(1)}, u32[]{:S(2)}, u32[]{:S(2)}) async-start(bf16[32,16,128]{2,1,0:T(8,128)(2,1)} %bitcast.95), calls=%async_computation.10 | async-start | bytes 262144 | tf_op jit(solution)/shard_map/all_to_all | solution.py:27
  237.6 6.5 %all-to-all-done.10 = bf16[32,16,128]{2,1,0:T(8,128)(2,1)S(1)} async-done(((bf16[32,16,128]{2,1,0:T(8,128)(2,1)}), bf16[32,16,128]{2,1,0:T(8,128)(2,1)S(1)}, u32[]{:S(2)}, u32[]{:S(2)}) %all-to-all-start.10) | async-done | bytes 131104 | tf_op jit(solution)/shard_map/all_to_all | solution.py:27
  244.3 0.7 reshape.469
  244.9 5.2 %all-to-all-start.11 = ((bf16[32,4,256]{2,1,0:T(4,128)(2,1)}), bf16[32,4,256]{2,1,0:T(4,128)(2,1)S(1)}, u32[]{:S(2)}, u32[]{:S(2)}) async-start(bf16[32,4,256]{2,1,0:T(4,128)(2,1)} %reshape.469), calls=%async_computation.11 | async-start | bytes 131072 | tf_op jit(solution)/shard_map/all_to_all | solution.py:27
  250.1 0.6 pad_maximum_fusion.5
  250.7 0.6 copy_bitcast_fusion.2
  251.4 24.8 %all-to-all-done.11 = bf16[32,4,256]{2,1,0:T(4,128)(2,1)S(1)} async-done(((bf16[32,4,256]{2,1,0:T(4,128)(2,1)}), bf16[32,4,256]{2,1,0:T(4,128)(2,1)S(1)}, u32[]{:S(2)}, u32[]{:S(2)}) %all-to-all-start.11) | async-done | bytes 65568 | tf_op jit(solution)/shard_map/all_to_all | solution.py:27
  276.2 0.6 reduce_sum.115
  (135 shorter events, 5.4 us)
Async XLA Ops:
  0.6 12.9 %copy-start.13 = (f32[2,32]{1,0:T(2,128)S(1)}, f32[2,32]{1,0:T(2,128)}, u32[]{:S(2)}) copy-start(f32[2,32]{1,0:T(2,128)} %param.22) | copy-start | bytes 772
  0.6 12.9 %copy-start.15 = (s32[32]{0:T(128)S(1)}, s32[32]{0:T(128)}, u32[]{:S(2)}) copy-start(s32[32]{0:T(128)} %param.13) | copy-start | bytes 388
  0.7 12.9 %copy-start.6 = (f32[2,32,32]{2,1,0:T(8,128)S(1)}, f32[2,32,32]{2,1,0:T(8,128)}, u32[]{:S(2)}) copy-start(f32[2,32,32]{2,1,0:T(8,128)} %param.14) | copy-start | bytes 24580
  0.7 20.6 %copy-start.11 = (bf16[256,4]{0,1:T(4,128)(2,1)S(1)}, bf16[256,4]{0,1:T(4,128)(2,1)}, u32[]{:S(2)}) copy-start(bf16[256,4]{0,1:T(4,128)(2,1)} %param.12) | copy-start | bytes 6148
  2.2 48.4 %copy-start.12 = (bf16[2,4,32]{2,1,0:T(4,128)(2,1)S(1)}, bf16[2,4,32]{2,1,0:T(4,128)(2,1)}, u32[]{:S(2)}) copy-start(bf16[2,4,32]{2,1,0:T(4,128)(2,1)} %param.19) | copy-start | bytes 1540
  3.0 48.0 %copy-start.4 = (bf16[2,32,3,32]{3,1,2,0:T(8,128)(2,1)S(1)}, bf16[2,32,3,32]{3,1,2,0:T(8,128)(2,1)}, u32[]{:S(2)}) copy-start(bf16[2,32,3,32]{3,1,2,0:T(8,128)(2,1)} %param.15) | copy-start | bytes 36868
  9.0 12.2 %all-to-all-start = ((bf16[4,352,128]{2,1,0:T(8,128)(2,1)}), bf16[4,352,128]{2,1,0:T(8,128)(2,1)S(1)}, u32[]{:S(2)}, u32[]{:S(2)}) async-start(bf16[4,352,128]{2,1,0:T(8,128)(2,1)} %pad_maximum_fusion), calls=%async_computation | async-start | bytes 720896 | tf_op jit(solution)/shard_map/all_to_all | solution.py:27
  21.9 53.3 %all-to-all-start.2 = ((bf16[32,4,256]{2,1,0:T(4,128)(2,1)}), bf16[32,4,256]{2,1,0:T(4,128)(2,1)S(1)}, u32[]{:S(2)}, u32[]{:S(2)}) async-start(bf16[32,4,256]{2,1,0:T(4,128)(2,1)} %broadcast_in_dim.131), calls=%async_computation.2 | async-start | bytes 131072 | tf_op jit(solution)/shard_map/all_to_all | solution.py:27
  85.1 21.3 %all-to-all-start.4 = ((bf16[32,32,512]{2,1,0:T(8,128)(2,1)}), bf16[32,32,512]{2,1,0:T(8,128)(2,1)S(1)}, u32[]{:S(2)}, u32[]{:S(2)}) async-start(bf16[32,32,512]{2,1,0:T(8,128)(2,1)} %broadcast_in_dim.132), calls=%async_computation.4 | async-start | bytes 2097152 | tf_op jit(solution)/shard_map/all_to_all | solution.py:27
  106.3 16.1 %all-to-all-start.3 = ((bf16[64,16,128]{2,1,0:T(8,128)(2,1)}), bf16[64,16,128]{2,1,0:T(8,128)(2,1)}, u32[]{:S(2)}, u32[]{:S(2)}) async-start(bf16[64,16,128]{2,1,0:T(8,128)(2,1)} %bitcast.49), calls=%async_computation.3 | async-start | bytes 524288 | tf_op jit(solution)/shard_map/all_to_all | solution.py:27
  121.8 5.9 %copy-start.5 = (f32[8,256]{1,0:T(8,128)S(1)}, f32[8,256]{1,0:T(8,128)}, u32[]{:S(2)}) copy-start(f32[8,256]{1,0:T(8,128)} %reduce_sum.107) | copy-start | bytes 24580
  121.9 5.9 %copy-start.10 = (f32[256]{0:T(256)S(1)}, f32[256]{0:T(256)}, u32[]{:S(2)}) copy-start(f32[256]{0:T(256)} %mul.242) | copy-start | bytes 3076
  121.9 5.9 %copy-start.1 = (bf16[1,2,2,4,32,128]{5,4,3,2,1,0:T(8,128)(2,1)S(1)}, bf16[1,2,2,4,32,128]{5,4,3,2,1,0:T(8,128)(2,1)}, u32[]{:S(2)}) copy-start(bf16[1,2,2,4,32,128]{5,4,3,2,1,0:T(8,128)(2,1)} %copy.94) | copy-start | bytes 393220
  121.9 6.2 %copy-start.14 = (f32[128]{0:T(128)S(1)}, f32[128]{0:T(128)}, u32[]{:S(2)}) copy-start(f32[128]{0:T(128)} %mul.247) | copy-start | bytes 1540
  121.9 6.3 %copy-start.9 = (f32[8,128]{1,0:T(8,128)S(1)}, f32[8,128]{1,0:T(8,128)}, u32[]{:S(2)}) copy-start(f32[8,128]{1,0:T(8,128)} %squeeze.103) | copy-start | bytes 12292
  122.4 9.0 %all-to-all-start.7 = ((bf16[4,64,128]{2,1,0:T(8,128)(2,1)}), bf16[4,64,128]{2,1,0:T(8,128)(2,1)S(1)}, u32[]{:S(2)}, u32[]{:S(2)}) async-start(bf16[4,64,128]{2,1,0:T(8,128)(2,1)} %copy.97), calls=%async_computation.7 | async-start | bytes 131072 | tf_op jit(solution)/shard_map/all_to_all | solution.py:27
  141.4 34.7 %all-to-all-start.8 = ((bf16[32,4,64,128]{3,2,1,0:T(8,128)(2,1)}), bf16[32,4,64,128]{3,2,1,0:T(8,128)(2,1)S(1)}, u32[]{:S(2)}, u32[]{:S(2)}) async-start(bf16[32,4,64,128]{3,2,1,0:T(8,128)(2,1)} %broadcast_in_dim.134), calls=%async_computation.8 | async-start | bytes 4194304 | tf_op jit(solution)/shard_map/all_to_all | solution.py:27
  176.8 32.5 %all-to-all-start.6 = ((bf16[8,8,8,128]{3,2,1,0:T(8,128)(2,1)}), bf16[8,8,8,128]{3,2,1,0:T(8,128)(2,1)S(1)}, u32[]{:S(2)}, u32[]{:S(2)}) async-start(bf16[8,8,8,128]{3,2,1,0:T(8,128)(2,1)} %broadcast_in_dim.133), calls=%async_computation.6 | async-start | bytes 262144 | tf_op jit(solution)/shard_map/all_to_all | solution.py:27
  184.5 31.1 %copy-start = (bf16[1,2,2,4,32,128]{5,4,2,1,0,3:T(8,128)(2,1)S(1)}, bf16[1,2,2,4,32,128]{5,4,2,1,0,3:T(8,128)(2,1)}, u32[]{:S(2)}) copy-start(bf16[1,2,2,4,32,128]{5,4,2,1,0,3:T(8,128)(2,1)} %get-tuple-element.19) | copy-start | bytes 393220
  184.5 31.2 %copy-start.8 = (f32[4,32]{1,0:T(4,128)S(1)}, f32[4,32]{1,0:T(4,128)}, u32[]{:S(2)}) copy-start(f32[4,32]{1,0:T(4,128)} %get-tuple-element.7) | copy-start | bytes 1540
  184.5 31.3 %copy-start.7 = (f32[8,32]{1,0:T(8,128)S(1)}, f32[8,32]{1,0:T(8,128)}, u32[]{:S(2)}) copy-start(f32[8,32]{1,0:T(8,128)} %get-tuple-element.5) | copy-start | bytes 3076
  184.5 31.3 %copy-start.3 = (f32[1,8,4,32]{3,1,0,2:T(8,128)S(1)}, f32[1,8,4,32]{3,1,0,2:T(8,128)}, u32[]{:S(2)}) copy-start(f32[1,8,4,32]{3,1,0,2:T(8,128)} %get-tuple-element.34) | copy-start | bytes 12292
  184.5 31.4 %copy-start.2 = (f32[8,8,32]{2,0,1:T(8,128)S(1)}, f32[8,8,32]{2,0,1:T(8,128)}, u32[]{:S(2)}) copy-start(f32[8,8,32]{2,0,1:T(8,128)} %get-tuple-element.3) | copy-start | bytes 24580
  212.4 8.9 %all-to-all-start.9 = ((bf16[4,4,8,128]{3,2,1,0:T(8,128)(2,1)}), bf16[4,4,8,128]{3,2,1,0:T(8,128)(2,1)S(1)}, u32[]{:S(2)}, u32[]{:S(2)}) async-start(bf16[4,4,8,128]{3,2,1,0:T(8,128)(2,1)} %pad_maximum_fusion.6), calls=%async_computation.9 | async-start | bytes 65536 | tf_op jit(solution)/shard_map/all_to_all | solution.py:27
  223.2 8.6 %all-to-all-start.12 = ((f32[4,8,128]{2,1,0:T(8,128)}), f32[4,8,128]{2,1,0:T(8,128)S(1)}, u32[]{:S(2)}, u32[]{:S(2)}) async-start(f32[4,8,128]{2,1,0:T(8,128)} %reshape.470), calls=%async_computation.12 | async-start | bytes 32768 | tf_op jit(solution)/shard_map/all_to_all | solution.py:27
  231.8 12.3 %all-to-all-start.10 = ((bf16[32,16,128]{2,1,0:T(8,128)(2,1)}), bf16[32,16,128]{2,1,0:T(8,128)(2,1)S(1)}, u32[]{:S(2)}, u32[]{:S(2)}) async-start(bf16[32,16,128]{2,1,0:T(8,128)(2,1)} %bitcast.95), calls=%async_computation.10 | async-start | bytes 262144 | tf_op jit(solution)/shard_map/all_to_all | solution.py:27
  244.9 31.3 %all-to-all-start.11 = ((bf16[32,4,256]{2,1,0:T(4,128)(2,1)}), bf16[32,4,256]{2,1,0:T(4,128)(2,1)S(1)}, u32[]{:S(2)}, u32[]{:S(2)}) async-start(bf16[32,4,256]{2,1,0:T(4,128)(2,1)} %reshape.469), calls=%async_computation.11 | async-start | bytes 131072 | tf_op jit(solution)/shard_map/all_to_all | solution.py:27

commit v3 on v2

--- a/solution.py
+++ b/solution.py
@@ -14,7 +14,6 @@
 TP = ("zh", "zm", "zl", "y")
 DP = ("x", "core")
 PLANE = ("x", "core", "y")
-PAIRED = ("zl", "y")
 PAIRED_PLANE = ("zl", "y", "x", "core")
 bf16 = jnp.bfloat16
 f32 = jnp.float32
@@ -30,6 +29,54 @@
 def everywhere(array, axes):
     count = lax.axis_size(axes)
     return exchange(jnp.broadcast_to(array[None], (count, *array.shape)), axes)
+
+
+def passed(piece, axis, step):
+    count = lax.axis_size(axis)
+    return lax.ppermute(piece, axis, [(at, (at + step) % count) for at in range(count)])
+
+
+def traded(tiles, axis):
+    count = lax.axis_size(axis)
+    here = lax.axis_index(axis)
+    pieces = []
+    for step in range(count):
+        piece = lax.dynamic_index_in_dim(tiles, (here + step) % count, 0, keepdims=False)
+        pieces.append(passed(piece, axis, step) if step else piece)
+    return pieces
+
+
+def collected(piece, axis):
+    return [piece] + [passed(piece, axis, k) for k in range(1, lax.axis_size(axis))]
+
+
+def in_order(pieces, axis):
+    backward = jnp.stack(pieces[::-1] + pieces[::-1])
+    count = len(pieces)
+    return lax.dynamic_slice_in_dim(backward, count - 1 - lax.axis_index(axis), count, 0)
+
+
+def relative(tiles):
+    parts = tiles.reshape(4, 2, *tiles.shape[1:])
+    parts = jnp.concatenate([parts, parts])[::-1]
+    parts = lax.dynamic_slice_in_dim(parts, 3 - lax.axis_index("x"), 4, 0)
+    return jnp.where(lax.axis_index("core") == 1, parts[:, ::-1], parts).reshape(tiles.shape)
+
+
+def parts_of(value):
+    coarse = lax.reduce_precision(value, 8, 7)
+    rest = value - coarse
+    middle = lax.reduce_precision(rest, 8, 7)
+    return [coarse.astype(bf16), middle.astype(bf16), (rest - middle).astype(bf16)]
+
+
+def whole_of(coarse, middle, fine):
+    return coarse.astype(f32) + (middle.astype(f32) + fine.astype(f32))
+
+
+def over_dp(piece):
+    pieces = jnp.stack(collected(piece, "x"))
+    return [pieces, passed(pieces, "core", 1)]
 
 
 def contract(a, a_dim, b, b_dim):
@@ -109,24 +156,6 @@
         .transpose(0, 1, 2, 4, 3)
         .reshape(256, 128)
     )
-    near = jnp.concatenate(
-        [
-            by_feature[:2].transpose(2, 0, 1, 3).reshape(4, 64, 128),
-            by_feature[5].transpose(1, 0, 2),
-            jnp.broadcast_to(gate_rows[None], (4, 256, 128)),
-        ],
-        axis=1,
-    )
-    near = exchange(near, "y")
-    w_first = near[:, :64].reshape(4, 2, 32, 128).transpose(1, 0, 2, 3).reshape(2, 128, 128)
-    w_last = near[:, 64:96].reshape(128, 128)
-    gates = (
-        near[:, 96:]
-        .reshape(4, LAYERS, 2, 2, 32, 128)
-        .transpose(1, 2, 3, 0, 4, 5)
-        .reshape(LAYERS, 2, 2, 128, 128)
-    )
-
     depth = TAPS - 1
     needed = depth + 1 - jnp.arange(depth, dtype=jnp.int32)
     living = lengths[None, :, None, None] >= needed[None, None, :, None]
@@ -134,53 +163,74 @@
     earlier = jnp.where(
         lengths[None, :, None] >= 2, prior_state, jnp.zeros_like(prior_state)
     )
+    earlier = earlier.reshape(LAYERS, 4, 8, 32).transpose(1, 0, 2, 3).reshape(4, -1)
+    decay = jnp.broadcast_to(jax.nn.log_sigmoid(decay_param).reshape(1, -1), (4, 64))
     small = jnp.concatenate(
-        [
-            earlier.reshape(LAYERS, 4, 8, 32).transpose(1, 0, 2, 3).reshape(4, -1),
-            history.astype(f32)
-            .reshape(LAYERS, 4, 8, depth, 32)
-            .transpose(1, 0, 3, 2, 4)
-            .reshape(4, -1),
-            jnp.broadcast_to(conv_taps.astype(f32).reshape(1, -1), (4, 256)),
-            jnp.broadcast_to(jax.nn.log_sigmoid(decay_param).reshape(1, -1), (4, 64)),
-            jnp.zeros((4, 64), f32),
+        parts_of(earlier)
+        + parts_of(decay)
+        + [
+            history.reshape(LAYERS, 4, 8, depth, 32).transpose(1, 0, 3, 2, 4).reshape(4, -1),
+            jnp.broadcast_to(conv_taps.reshape(1, -1), (4, 256)),
+            jnp.zeros((4, 64), bf16),
         ],
         axis=1,
-    ).reshape(1, 4, 19, 128)
-    small = exchange(jnp.broadcast_to(small, (2, 4, 19, 128)).reshape(8, 19, 128), PAIRED)
-    small = small.reshape(2, 4, -1)
-
-    def own_half(parts):
-        return jnp.where(upper, parts[1], parts[0])
+    ).reshape(4, 28, 128)
+    near = jnp.concatenate(
+        [
+            by_feature[:2].transpose(2, 0, 1, 3).reshape(4, 64, 128),
+            by_feature[5].transpose(1, 0, 2),
+            jnp.broadcast_to(gate_rows[None], (4, 256, 128)),
+            jnp.broadcast_to(by_feature[4].transpose(1, 0, 2).reshape(1, 128, 128), (4, 128, 128)),
+            small,
+        ],
+        axis=1,
+    )
+    near = in_order(traded(near, "y"), "y")
+    w_first = near[:, :64].reshape(4, 2, 32, 128).transpose(1, 0, 2, 3).reshape(2, 128, 128)
+    w_last = near[:, 64:96].reshape(128, 128)
+    gates = (
+        near[:, 96:352]
+        .reshape(4, LAYERS, 2, 2, 32, 128)
+        .transpose(1, 2, 3, 0, 4, 5)
+        .reshape(LAYERS, 2, 2, 128, 128)
+    )
+    w_mid = near[:, 352:480].reshape(4, 4, 32, 128).transpose(1, 0, 2, 3).reshape(4, 128, 128)
+    small = near[:, 480:].reshape(4, 3584)
 
     earlier_rows = (
-        own_half(small)[:, :512].reshape(4, LAYERS, 8, 32).transpose(1, 2, 0, 3)
-    ).reshape(LAYERS, 8, 128)
-    history_rows = (
-        small[:, :, 512:2048]
-        .reshape(8, LAYERS, depth, 8, 32)
-        .transpose(1, 2, 3, 0, 4)
-        .reshape(LAYERS, depth, 8, 256)
-    )
-    taps = (
-        small[:, :, 2048:2304]
-        .reshape(8, LAYERS, TAPS, 32)
+        whole_of(small[:, :512], small[:, 512:1024], small[:, 1024:1536])
+        .reshape(4, LAYERS, 8, 32)
         .transpose(1, 2, 0, 3)
-        .reshape(LAYERS, TAPS, 256)
+        .reshape(LAYERS, 8, 128)
     )
     decay = (
-        own_half(small)[:, 2304:2368].reshape(4, LAYERS, 32).transpose(1, 0, 2)
-    ).reshape(LAYERS, 1, 128)
-
-    w_mid = everywhere(by_feature[4].reshape(32, 512), PLANE)
-    w_mid = (
-        w_mid.reshape(8, 4, 32, 4, 128).transpose(1, 2, 3, 0, 4).reshape(128, 4096)
-    )
-    w_second = exchange(by_feature[2:4].transpose(2, 0, 1, 3).reshape(4, 64, 128), ZQ)
-    w_second = everywhere(w_second, PLANE)
+        whole_of(small[:, 1536:1600], small[:, 1600:1664], small[:, 1664:1728])
+        .reshape(4, LAYERS, 32)
+        .transpose(1, 0, 2)
+        .reshape(LAYERS, 1, 128)
+    )
+    windows = jnp.concatenate(
+        [
+            small[:, 1728:3264].reshape(4, 48, 32).transpose(1, 0, 2).reshape(48, 128),
+            small[:, 3264:3520].reshape(4, 8, 32).transpose(1, 0, 2).reshape(8, 128),
+        ],
+        axis=0,
+    )
+    partner = passed(windows, "zl", 1)
+    windows = jnp.concatenate(
+        [jnp.where(upper, partner, windows), jnp.where(upper, windows, partner)], axis=1
+    ).astype(f32)
+    history_rows = windows[:48].reshape(LAYERS, depth, 8, 256)
+    taps = windows[48:].reshape(LAYERS, TAPS, 256)
+
+    w_mid = over_dp(w_mid)
+    w_second = by_feature[2:4].transpose(2, 0, 1, 3).reshape(4, 64, 128)
+    w_second = in_order(traded(w_second, ZQ), ZQ).reshape(256, 128)
+    w_second = in_order(collected(w_second, "y"), "y")
     w_second = (
-        w_second.reshape(8, 4, 4, 2, 32, 128).transpose(2, 3, 1, 4, 0, 5).reshape(1024, 1024)
-    )
+        w_second.reshape(4, 4, 2, 32, 128).transpose(1, 2, 0, 3, 4).reshape(1024, 128)
+    )
+    w_second = over_dp(w_second)
 
     stream_rows = stream_t.T.reshape(8, 4, 8, 128).transpose(1, 0, 2, 3)
     products = [
@@ -216,19 +266,33 @@
         earlier_rows[0],
     )
     residual = lax.dynamic_index_in_dim(rows.reshape(4, 8, 8, 128), q, 0, keepdims=False)
-    mixed = contract(readout, 1, w_mid, 0).astype(bf16)
-    mixed = exchange(mixed.reshape(8, 4, 8, 128).transpose(1, 2, 0, 3), ZQ)
+    residual = relative(residual)
+    mixed = jnp.stack(
+        [
+            jnp.stack(
+                [
+                    jnp.stack([contract(readout, 1, w_mid[core][x, part], 0) for core in range(2)])
+                    for x in range(4)
+                ]
+            )
+            for part in range(4)
+        ]
+    ).astype(bf16)
+    mixed = exchange(mixed.reshape(4, 8, 8, 128), ZQ)
     mixed = mixed.astype(f32).sum(axis=0).astype(bf16)
     mixed = everywhere(mixed, "zh").astype(f32).sum(axis=0)
     first = (mixed + residual.astype(f32)).astype(bf16)
 
-    first_rows = first.transpose(1, 0, 2).reshape(8, 1024)
-    widened = first_rows.astype(f32)
-    squares = jnp.sum(widened * widened, axis=1, keepdims=True)
+    widened = first.astype(f32)
+    squares = jnp.sum(jnp.sum(widened * widened, axis=0), axis=1, keepdims=True)
     coarse = lax.reduce_precision(squares, 8, 7)
     lane = lax.broadcasted_iota(jnp.int32, (8, 128), 1)
     squares = jnp.where(lane < 64, coarse, squares - coarse).astype(bf16)
-    products = contract(first_rows, 1, w_second, 1).astype(bf16)
+    products = sum(
+        contract(first[2 * x + core], 1, w_second[core][x], 1)
+        for core in range(2)
+        for x in range(4)
+    ).astype(bf16)
     products = products.reshape(8, 2, 2, 2, 128)
     sent = jnp.stack(
         [
@@ -257,7 +321,7 @@
     sent = jnp.stack(
         [
             jnp.broadcast_to(readout[None, None], (8, 4, 8, 128)),
-            jnp.broadcast_to(first[:, None], (8, 4, 8, 128)),
+            jnp.broadcast_to(relative(first)[:, None], (8, 4, 8, 128)),
         ],
         axis=2,
     )
@@ -275,7 +339,8 @@
     kept = jnp.stack(
         [state_first, state_second, branch_first.astype(f32), branch_second.astype(f32)]
     )
-    kept = exchange(kept.reshape(4, 8, 4, 32).transpose(2, 0, 1, 3).reshape(4, 8, 128), "y")
+    kept = kept.reshape(4, 8, 4, 32).transpose(2, 0, 1, 3).reshape(4, 8, 128)
+    kept = in_order(traded(kept, "y"), "y")
     kept = kept.reshape(4, 4, 8, 32).transpose(1, 0, 2, 3).reshape(2, LAYERS, 32, 32)
     window = jnp.concatenate([history[:, :, 1:], kept[1].astype(bf16)[:, :, None]], axis=2)
     return second.T, kept[0], window

time: 279 us -> 246 us (0.88)
  waiting for transfers between devices: 141 us -> 66.5 us
  starting transfers between devices: 77.3 us -> 146 us
  blocking collectives: 16.9 us -> 0 us
  local copies, waits for them, and re-layouts: 24.7 us -> 15.9 us
  other arithmetic: 10.7 us -> 6.35 us
  matrix products: 4.63 us -> 7.73 us
    all_to_all x11 -> x7, waiting for transfers between devices: 141 us -> 60.9 us  [exchange(): return lax.all_to_all(tiles, axes, 0, 0, tiled=True)]
    ppermute x0 -> x21, starting transfers between devices: none -> 71 us  [passed(): lax.ppermute(piece, axis, [(at, (at + step) % count) for at in range(coun...]
    all_to_all x2 -> x0, blocking collectives: 16.9 us -> none  [exchange(): return lax.all_to_all(tiles, axes, 0, 0, tiled=True)]
    unnamed x35 -> x64, local copies, waits for them, and re-layouts: 0.85 us -> 6.85 us
    ppermute x0 -> x21, waiting for transfers between devices: none -> 5.63 us  [passed(): lax.ppermute(piece, axis, [(at, (at + step) % count) for at in range(coun...]
    transpose x2 -> x4, local copies, waits for them, and re-layouts: 4.99 us -> 0.13 us  [the longest x1 0.09 us: body(): small[:, 1728:3264].reshape(4, 48, 32).transpose(1, 0, 2).reshape(48, 128)]
    dot_general x14 -> x52, matrix products: 4.63 us -> 7.73 us  [contract(): lax.dot_general(a, b, (((a_dim,), (b_dim,)), ((), ())), preferred_element...]
    unnamed x5 -> x4, other arithmetic: 3.1 us -> 0.04 us
  transfers between devices with their start and end apart: 11 -> 28, of which waited for: 10 -> 6; matrix products, arithmetic and copies ran while one was open for 8% -> 5% of each run, Pallas kernels for 0% -> 0%
where the time goes in v3:
time: 246 us; the launch traced here: 245 us
  starting transfers between devices  146 us (59%)
  waiting for transfers between devices  66.5 us (27%)
  local copies, waits for them, and re-layouts  15.9 us (6%)
  matrix products  7.73 us (3%)
  other arithmetic  6.35 us (3%)
    all_to_all x7, starting transfers between devices, exchange(): return lax.all_to_all(tiles, axes, 0, 0, tiled=True)  74.9 us
    ppermute x21, starting transfers between devices, passed(): lax.ppermute(piece, axis, [(at, (at + step) % count) for at in range(coun...  71 us
    all_to_all x7, waiting for transfers between devices, exchange(): return lax.all_to_all(tiles, axes, 0, 0, tiled=True)  60.9 us
    dot_general x52, matrix products, contract(): lax.dot_general(a, b, (((a_dim,), (b_dim,)), ((), ())), preferred_element...  7.73 us
    unnamed x64, local copies, waits for them, and re-layouts  6.85 us
    ppermute x21, waiting for transfers between devices, passed(): lax.ppermute(piece, axis, [(at, (at + step) % count) for at in range(coun...  5.63 us
  transfers between devices with their start and end apart: 28, of which 6 were waited for; matrix products, arithmetic and copies ran while one was open for 5% of the time, Pallas kernels for 0%

profile of v3, /device:TPU:2, one launch (start us, length us, event | category | flops | bytes accessed | tf_op | source)
XLA Modules:
  0.0 244.6 jit_solution(10051562679948132306)
XLA Ops:
  0.6 1.3 broadcast_in_dim.121
  1.9 28.7 %all-to-all-start = ((bf16[32,4,256]{2,1,0:T(4,128)(2,1)}), bf16[32,4,256]{2,1,0:T(4,128)(2,1)S(1)}, u32[]{:S(2)}, u32[]{:S(2)}) async-start(bf16[32,4,256]{2,1,0:T(4,128)(2,1)} %broadcast_in_dim.121), calls=%async_computation | async-start | bytes 131072 | tf_op jit(solution)/shard_map/all_to_all | solution.py:26
  30.8 0.6 copy-done.10
  31.6 0.8 copy-done.4
  32.4 0.4 convolution_convert_fusion
  32.9 3.7 %collective-permute-start.10 = (bf16[64,128]{1,0:T(8,128)(2,1)S(1)}, bf16[64,128]{1,0:T(8,128)(2,1)S(1)}, u32[]{:S(2)}, u32[]{:S(2)}) collective-permute-start(bf16[64,128]{1,0:T(8,128)(2,1)S(1)} %get-tuple-element.29), channel_id=1, source_target_pairs={{0,32},{32,64},{64,96},{96,0},{1,33},{33,65},{65,97},{97,1},{2,34}... | collective-permute-start | bytes 49160 | tf_op jit(solution)/shard_map/ppermute | solution.py:36
  36.6 4.3 %collective-permute-start.9 = (bf16[64,128]{1,0:T(8,128)(2,1)S(1)}, bf16[64,128]{1,0:T(8,128)(2,1)S(1)}, u32[]{:S(2)}, u32[]{:S(2)}) collective-permute-start(bf16[64,128]{1,0:T(8,128)(2,1)S(1)} %get-tuple-element.30), channel_id=1, source_target_pairs={{0,64},{32,96},{64,0},{96,32},{1,65},{33,97},{65,1},{97,33},{2,66}... | collective-permute-start | bytes 49160 | tf_op jit(solution)/shard_map/ppermute | solution.py:36
  40.9 3.4 %collective-permute-start.8 = (bf16[64,128]{1,0:T(8,128)(2,1)S(1)}, bf16[64,128]{1,0:T(8,128)(2,1)S(1)}, u32[]{:S(2)}, u32[]{:S(2)}) collective-permute-start(bf16[64,128]{1,0:T(8,128)(2,1)S(1)} %get-tuple-element.31), channel_id=1, source_target_pairs={{0,96},{32,0},{64,32},{96,64},{1,97},{33,1},{65,33},{97,65},{2,98}... | collective-permute-start | bytes 49160 | tf_op jit(solution)/shard_map/ppermute | solution.py:36
  44.3 0.6 copy-done.11
  45.1 0.6 copy-done.13
  45.7 0.6 copy-done.12
  46.6 0.7 copy-done.6
  47.3 0.7 copy-done.7
  48.2 0.8 copy-done
  49.8 4.9 %collective-permute-start.11 = (bf16[256,128]{1,0:T(8,128)(2,1)S(1)}, bf16[256,128]{1,0:T(8,128)(2,1)S(1)}, u32[]{:S(2)}, u32[]{:S(2)}) collective-permute-start(bf16[256,128]{1,0:T(8,128)(2,1)S(1)} %bitcast.606), channel_id=1, source_target_pairs={{0,24},{8,0},{16,8},{24,16},{1,25},{9,1},{17,9},{25,17},{2,26},{10... | collective-permute-start | bytes 196616 | tf_op jit(solution)/shard_map/ppermute | solution.py:36
  54.8 1.9 collective-permute-start.2
  56.7 4.1 %collective-permute-start.1 = (bf16[508,128]{1,0:T(8,128)(2,1)S(1)}, bf16[508,128]{1,0:T(8,128)(2,1)S(1)}, u32[]{:S(2)}, u32[]{:S(2)}) collective-permute-start(bf16[508,128]{1,0:T(8,128)(2,1)S(1)} %get-tuple-element.16), channel_id=1, source_target_pairs={{0,16},{8,24},{16,0},{24,8},{1,17},{9,25},{17,1},{25,9},{2,18},{10... | collective-permute-start | bytes 390152 | tf_op jit(solution)/shard_map/ppermute | solution.py:36
  60.8 3.0 %collective-permute-start = (bf16[508,128]{1,0:T(8,128)(2,1)S(1)}, bf16[508,128]{1,0:T(8,128)(2,1)S(1)}, u32[]{:S(2)}, u32[]{:S(2)}) collective-permute-start(bf16[508,128]{1,0:T(8,128)(2,1)S(1)} %get-tuple-element.17), channel_id=1, source_target_pairs={{0,24},{8,0},{16,8},{24,16},{1,25},{9,1},{17,9},{25,17},{2,26},{10... | collective-permute-start | bytes 390152 | tf_op jit(solution)/shard_map/ppermute | solution.py:36
  63.8 2.9 %collective-permute-start.13 = (bf16[256,128]{1,0:T(8,128)(2,1)S(1)}, bf16[256,128]{1,0:T(8,128)(2,1)S(1)}, u32[]{:S(2)}, u32[]{:S(2)}) collective-permute-start(bf16[256,128]{1,0:T(8,128)(2,1)S(1)} %bitcast.607), channel_id=1, source_target_pairs={{0,8},{8,16},{16,24},{24,0},{1,9},{9,17},{17,25},{25,1},{2,10},{10... | collective-permute-start | bytes 196616 | tf_op jit(solution)/shard_map/ppermute | solution.py:36
  66.7 3.9 %collective-permute-start.12 = (bf16[256,128]{1,0:T(8,128)(2,1)S(1)}, bf16[256,128]{1,0:T(8,128)(2,1)S(1)}, u32[]{:S(2)}, u32[]{:S(2)}) collective-permute-start(bf16[256,128]{1,0:T(8,128)(2,1)S(1)} %bitcast.608), channel_id=1, source_target_pairs={{0,16},{8,24},{16,0},{24,8},{1,17},{9,25},{17,1},{25,9},{2,18},{10... | collective-permute-start | bytes 196616 | tf_op jit(solution)/shard_map/ppermute | solution.py:36
  70.6 3.8 %collective-permute-done.12 = bf16[256,128]{1,0:T(8,128)(2,1)S(1)} collective-permute-done((bf16[256,128]{1,0:T(8,128)(2,1)S(1)}, bf16[256,128]{1,0:T(8,128)(2,1)S(1)}, u32[]{:S(2)}, u32[]{:S(2)}) %collective-permute-start.12) | collective-permute-done | bytes 65568 | tf_op jit(solution)/shard_map/ppermute | solution.py:36
  75.6 0.7 copy.110
  76.4 7.1 %all-to-all-start.1 = ((bf16[64,16,128]{2,1,0:T(8,128)(2,1)}), bf16[64,16,128]{2,1,0:T(8,128)(2,1)S(1)}, u32[]{:S(2)}, u32[]{:S(2)}) async-start(bf16[64,16,128]{2,1,0:T(8,128)(2,1)} %bitcast.57), calls=%async_computation.1 | async-start | bytes 524288 | tf_op jit(solution)/shard_map/all_to_all | solution.py:26
  83.7 2.4 collective-permute-start.6
  86.0 4.4 %collective-permute-start.5 = (bf16[4,128,128]{2,1,0:T(8,128)(2,1)S(1)}, bf16[4,128,128]{2,1,0:T(8,128)(2,1)S(1)}, u32[]{:S(2)}, u32[]{:S(2)}) collective-permute-start(bf16[4,128,128]{2,1,0:T(8,128)(2,1)S(1)} %bitcast.592), channel_id=1, source_target_pairs={{0,4},{2,6},{4,0},{6,2},{1,5},{3,7},{5,1},{7,3},{8,12},{10,14},{12... | collective-permute-start | bytes 393224 | tf_op jit(solution)/shard_map/ppermute | solution.py:36
  90.4 3.7 %collective-permute-start.4 = (bf16[4,128,128]{2,1,0:T(8,128)(2,1)S(1)}, bf16[4,128,128]{2,1,0:T(8,128)(2,1)S(1)}, u32[]{:S(2)}, u32[]{:S(2)}) collective-permute-start(bf16[4,128,128]{2,1,0:T(8,128)(2,1)S(1)} %bitcast.593), channel_id=1, source_target_pairs={{0,2},{2,4},{4,6},{6,0},{1,3},{3,5},{5,7},{7,1},{8,10},{10,12},{12... | collective-permute-start | bytes 393224 | tf_op jit(solution)/shard_map/ppermute | solution.py:36
  94.8 3.5 %collective-permute-start.3 = (bf16[56,128]{1,0:T(8,128)(2,1)S(1)}, bf16[56,128]{1,0:T(8,128)(2,1)S(1)}, u32[]{:S(2)}, u32[]{:S(2)}) collective-permute-start(bf16[56,128]{1,0:T(8,128)(2,1)S(1)} %pad_maximum_fusion.19), channel_id=1, source_target_pairs={{0,32},{32,0},{1,33},{33,1},{2,34},{34,2},{3,35},{35,3},{4,36},{36... | collective-permute-start | bytes 43016 | tf_op jit(solution)/shard_map/ppermute | solution.py:36
  98.7 1.8 collective-permute-done.3
  100.6 1.9 collective-permute-start.7
  102.6 0.8 multiply_reduce_fusion
  103.9 0.2 fusion.119
  108.5 0.6 pad_maximum_fusion.6
  109.2 3.3 %all-to-all-start.2 = ((bf16[4,8,8,128]{3,2,1,0:T(8,128)(2,1)}), bf16[4,8,8,128]{3,2,1,0:T(8,128)(2,1)S(1)}, u32[]{:S(2)}, u32[]{:S(2)}) async-start(bf16[4,8,8,128]{3,2,1,0:T(8,128)(2,1)} %pad_maximum_fusion.6), calls=%async_computation.2 | async-start | bytes 131072 | tf_op jit(solution)/shard_map/all_to_all | solution.py:26
  112.6 2.2 collective-permute-start.16
  114.8 3.1 %collective-permute-start.15 = (bf16[1024,128]{1,0:T(8,128)(2,1)S(1)}, bf16[1024,128]{1,0:T(8,128)(2,1)S(1)}, u32[]{:S(2)}, u32[]{:S(2)}) collective-permute-start(bf16[1024,128]{1,0:T(8,128)(2,1)S(1)} %bitcast.587), channel_id=1, source_target_pairs={{0,4},{2,6},{4,0},{6,2},{1,5},{3,7},{5,1},{7,3},{8,12},{10,14},{12... | collective-permute-start | bytes 786440 | tf_op jit(solution)/shard_map/ppermute | solution.py:36
  117.9 4.5 %collective-permute-start.14 = (bf16[1024,128]{1,0:T(8,128)(2,1)S(1)}, bf16[1024,128]{1,0:T(8,128)(2,1)S(1)}, u32[]{:S(2)}, u32[]{:S(2)}) collective-permute-start(bf16[1024,128]{1,0:T(8,128)(2,1)S(1)} %bitcast.588), channel_id=1, source_target_pairs={{0,2},{2,4},{4,6},{6,0},{1,3},{3,5},{5,7},{7,1},{8,10},{10,12},{12... | collective-permute-start | bytes 786440 | tf_op jit(solution)/shard_map/ppermute | solution.py:36
  122.5 0.6 select_convert_fusion
  123.3 0.6 constant_dynamic-slice_fusion.2
  123.9 0.7 broadcast_in_dim.122
  124.6 20.6 %all-to-all-start.3 = ((bf16[8,8,8,128]{3,2,1,0:T(8,128)(2,1)}), bf16[8,8,8,128]{3,2,1,0:T(8,128)(2,1)S(1)}, u32[]{:S(2)}, u32[]{:S(2)}) async-start(bf16[8,8,8,128]{3,2,1,0:T(8,128)(2,1)} %broadcast_in_dim.122), calls=%async_computation.3 | async-start | bytes 262144 | tf_op jit(solution)/shard_map/all_to_all | solution.py:26
  145.4 1.9 collective-permute-start.17
  147.4 0.7 constant_dynamic-slice_fusion.12
  148.2 24.8 %all-to-all-done.3 = bf16[8,8,8,128]{3,2,1,0:T(8,128)(2,1)S(1)} async-done(((bf16[8,8,8,128]{3,2,1,0:T(8,128)(2,1)}), bf16[8,8,8,128]{3,2,1,0:T(8,128)(2,1)S(1)}, u32[]{:S(2)}, u32[]{:S(2)}) %all-to-all-start.3) | async-done | bytes 131104 | tf_op jit(solution)/shard_map/all_to_all | solution.py:26
  174.5 0.2 fusion.6
  174.8 0.6 pad_maximum_fusion.9
  175.4 5.5 %all-to-all-start.4 = ((bf16[4,4,8,128]{3,2,1,0:T(8,128)(2,1)}), bf16[4,4,8,128]{3,2,1,0:T(8,128)(2,1)S(1)}, u32[]{:S(2)}, u32[]{:S(2)}) async-start(bf16[4,4,8,128]{3,2,1,0:T(8,128)(2,1)} %pad_maximum_fusion.9), calls=%async_computation.4 | async-start | bytes 65536 | tf_op jit(solution)/shard_map/all_to_all | solution.py:26
  180.9 5.6 %all-to-all-done.4 = bf16[4,4,8,128]{3,2,1,0:T(8,128)(2,1)S(1)} async-done(((bf16[4,4,8,128]{3,2,1,0:T(8,128)(2,1)}), bf16[4,4,8,128]{3,2,1,0:T(8,128)(2,1)S(1)}, u32[]{:S(2)}, u32[]{:S(2)}) %all-to-all-start.4) | async-done | bytes 32800 | tf_op jit(solution)/shard_map/all_to_all | solution.py:26
  186.6 0.2 fusion.132
  187.4 0.2 fusion.126
  187.8 3.4 %collective-permute-start.20 = (f32[8,128]{1,0:T(8,128)S(1)}, f32[8,128]{1,0:T(8,128)S(1)}, u32[]{:S(2)}, u32[]{:S(2)}) collective-permute-start(f32[8,128]{1,0:T(8,128)S(1)} %get-tuple-element.44), channel_id=1, source_target_pairs={{0,8},{8,16},{16,24},{24,0},{1,9},{9,17},{17,25},{25,1},{2,10},{10... | collective-permute-start | bytes 12296 | tf_op jit(solution)/shard_map/ppermute | solution.py:36
  191.2 4.7 %collective-permute-start.19 = (f32[8,128]{1,0:T(8,128)S(1)}, f32[8,128]{1,0:T(8,128)S(1)}, u32[]{:S(2)}, u32[]{:S(2)}) collective-permute-start(f32[8,128]{1,0:T(8,128)S(1)} %get-tuple-element.45), channel_id=1, source_target_pairs={{0,16},{8,24},{16,0},{24,8},{1,17},{9,25},{17,1},{25,9},{2,18},{10... | collective-permute-start | bytes 12296 | tf_op jit(solution)/shard_map/ppermute | solution.py:36
  195.9 3.3 %collective-permute-start.18 = (f32[8,128]{1,0:T(8,128)S(1)}, f32[8,128]{1,0:T(8,128)S(1)}, u32[]{:S(2)}, u32[]{:S(2)}) collective-permute-start(f32[8,128]{1,0:T(8,128)S(1)} %get-tuple-element.46), channel_id=1, source_target_pairs={{0,24},{8,0},{16,8},{24,16},{1,25},{9,1},{17,9},{25,17},{2,26},{10... | collective-permute-start | bytes 12296 | tf_op jit(solution)/shard_map/ppermute | solution.py:36
  199.3 0.7 pad_maximum_fusion.5
  199.9 4.8 %all-to-all-start.5 = ((bf16[32,16,128]{2,1,0:T(8,128)(2,1)}), bf16[32,16,128]{2,1,0:T(8,128)(2,1)S(1)}, u32[]{:S(2)}, u32[]{:S(2)}) async-start(bf16[32,16,128]{2,1,0:T(8,128)(2,1)} %bitcast.224), calls=%async_computation.5 | async-start | bytes 262144 | tf_op jit(solution)/shard_map/all_to_all | solution.py:26
  204.9 6.4 %all-to-all-done.5 = bf16[32,16,128]{2,1,0:T(8,128)(2,1)S(1)} async-done(((bf16[32,16,128]{2,1,0:T(8,128)(2,1)}), bf16[32,16,128]{2,1,0:T(8,128)(2,1)S(1)}, u32[]{:S(2)}, u32[]{:S(2)}) %all-to-all-start.5) | async-done | bytes 131104 | tf_op jit(solution)/shard_map/all_to_all | solution.py:26
  211.3 0.7 copy-done.8
  212.1 0.2 convolution_convert_fusion.3
  212.3 0.6 reshape.473
  212.9 5.0 %all-to-all-start.6 = ((bf16[32,4,256]{2,1,0:T(4,128)(2,1)}), bf16[32,4,256]{2,1,0:T(4,128)(2,1)S(1)}, u32[]{:S(2)}, u32[]{:S(2)}) async-start(bf16[32,4,256]{2,1,0:T(4,128)(2,1)} %reshape.473), calls=%async_computation.6 | async-start | bytes 131072 | tf_op jit(solution)/shard_map/all_to_all | solution.py:26
  217.9 0.7 slice-done
  218.6 0.6 pad_maximum_fusion.7
  219.3 0.6 copy_bitcast_fusion.2
  219.9 24.1 %all-to-all-done.6 = bf16[32,4,256]{2,1,0:T(4,128)(2,1)S(1)} async-done(((bf16[32,4,256]{2,1,0:T(4,128)(2,1)}), bf16[32,4,256]{2,1,0:T(4,128)(2,1)S(1)}, u32[]{:S(2)}, u32[]{:S(2)}) %all-to-all-start.6) | async-done | bytes 65568 | tf_op jit(solution)/shard_map/all_to_all | solution.py:26
  244.0 0.6 reduce_sum.116
  (276 shorter events, 12.0 us)
Async XLA Ops:
  1.9 72.9 %all-to-all-start = ((bf16[32,4,256]{2,1,0:T(4,128)(2,1)}), bf16[32,4,256]{2,1,0:T(4,128)(2,1)S(1)}, u32[]{:S(2)}, u32[]{:S(2)}) async-start(bf16[32,4,256]{2,1,0:T(4,128)(2,1)} %broadcast_in_dim.121), calls=%async_computation | async-start | bytes 131072 | tf_op jit(solution)/shard_map/all_to_all | solution.py:26
  30.7 0.8 copy-start.2
  30.7 0.7 copy-start.10
  30.7 0.9 copy-start.3
  31.6 0.8 copy-start.4
  32.9 16.8 %collective-permute-start.10 = (bf16[64,128]{1,0:T(8,128)(2,1)S(1)}, bf16[64,128]{1,0:T(8,128)(2,1)S(1)}, u32[]{:S(2)}, u32[]{:S(2)}) collective-permute-start(bf16[64,128]{1,0:T(8,128)(2,1)S(1)} %get-tuple-element.29), channel_id=1, source_target_pairs={{0,32},{32,64},{64,96},{96,0},{1,33},{33,65},{65,97},{97,1},{2,34}... | collective-permute-start | bytes 49160 | tf_op jit(solution)/shard_map/ppermute | solution.py:36
  36.6 13.0 %collective-permute-start.9 = (bf16[64,128]{1,0:T(8,128)(2,1)S(1)}, bf16[64,128]{1,0:T(8,128)(2,1)S(1)}, u32[]{:S(2)}, u32[]{:S(2)}) collective-permute-start(bf16[64,128]{1,0:T(8,128)(2,1)S(1)} %get-tuple-element.30), channel_id=1, source_target_pairs={{0,64},{32,96},{64,0},{96,32},{1,65},{33,97},{65,1},{97,33},{2,66}... | collective-permute-start | bytes 49160 | tf_op jit(solution)/shard_map/ppermute | solution.py:36
  40.9 8.7 %collective-permute-start.8 = (bf16[64,128]{1,0:T(8,128)(2,1)S(1)}, bf16[64,128]{1,0:T(8,128)(2,1)S(1)}, u32[]{:S(2)}, u32[]{:S(2)}) collective-permute-start(bf16[64,128]{1,0:T(8,128)(2,1)S(1)} %get-tuple-element.31), channel_id=1, source_target_pairs={{0,96},{32,0},{64,32},{96,64},{1,97},{33,1},{65,33},{97,65},{2,98}... | collective-permute-start | bytes 49160 | tf_op jit(solution)/shard_map/ppermute | solution.py:36
  44.3 0.7 copy-start.11
  44.3 2.1 copy-start.5
  45.0 0.7 copy-start.13
  45.6 0.7 copy-start.12
  46.5 0.8 copy-start.6
  47.3 0.8 copy-start.7
  48.1 0.8 copy-start
  49.8 16.9 %collective-permute-start.11 = (bf16[256,128]{1,0:T(8,128)(2,1)S(1)}, bf16[256,128]{1,0:T(8,128)(2,1)S(1)}, u32[]{:S(2)}, u32[]{:S(2)}) collective-permute-start(bf16[256,128]{1,0:T(8,128)(2,1)S(1)} %bitcast.606), channel_id=1, source_target_pairs={{0,24},{8,0},{16,8},{24,16},{1,25},{9,1},{17,9},{25,17},{2,26},{10... | collective-permute-start | bytes 196616 | tf_op jit(solution)/shard_map/ppermute | solution.py:36
  54.8 19.8 %collective-permute-start.2 = (bf16[508,128]{1,0:T(8,128)(2,1)S(1)}, bf16[508,128]{1,0:T(8,128)(2,1)S(1)}, u32[]{:S(2)}, u32[]{:S(2)}) collective-permute-start(bf16[508,128]{1,0:T(8,128)(2,1)S(1)} %get-tuple-element.15), channel_id=1, source_target_pairs={{0,8},{8,16},{16,24},{24,0},{1,9},{9,17},{17,25},{25,1},{2,10},{10... | collective-permute-start | bytes 390152 | tf_op jit(solution)/shard_map/ppermute | solution.py:36
  56.7 17.8 %collective-permute-start.1 = (bf16[508,128]{1,0:T(8,128)(2,1)S(1)}, bf16[508,128]{1,0:T(8,128)(2,1)S(1)}, u32[]{:S(2)}, u32[]{:S(2)}) collective-permute-start(bf16[508,128]{1,0:T(8,128)(2,1)S(1)} %get-tuple-element.16), channel_id=1, source_target_pairs={{0,16},{8,24},{16,0},{24,8},{1,17},{9,25},{17,1},{25,9},{2,18},{10... | collective-permute-start | bytes 390152 | tf_op jit(solution)/shard_map/ppermute | solution.py:36
  60.8 13.7 %collective-permute-start = (bf16[508,128]{1,0:T(8,128)(2,1)S(1)}, bf16[508,128]{1,0:T(8,128)(2,1)S(1)}, u32[]{:S(2)}, u32[]{:S(2)}) collective-permute-start(bf16[508,128]{1,0:T(8,128)(2,1)S(1)} %get-tuple-element.17), channel_id=1, source_target_pairs={{0,24},{8,0},{16,8},{24,16},{1,25},{9,1},{17,9},{25,17},{2,26},{10... | collective-permute-start | bytes 390152 | tf_op jit(solution)/shard_map/ppermute | solution.py:36
  63.8 10.6 %collective-permute-start.13 = (bf16[256,128]{1,0:T(8,128)(2,1)S(1)}, bf16[256,128]{1,0:T(8,128)(2,1)S(1)}, u32[]{:S(2)}, u32[]{:S(2)}) collective-permute-start(bf16[256,128]{1,0:T(8,128)(2,1)S(1)} %bitcast.607), channel_id=1, source_target_pairs={{0,8},{8,16},{16,24},{24,0},{1,9},{9,17},{17,25},{25,1},{2,10},{10... | collective-permute-start | bytes 196616 | tf_op jit(solution)/shard_map/ppermute | solution.py:36
  66.7 7.7 %collective-permute-start.12 = (bf16[256,128]{1,0:T(8,128)(2,1)S(1)}, bf16[256,128]{1,0:T(8,128)(2,1)S(1)}, u32[]{:S(2)}, u32[]{:S(2)}) collective-permute-start(bf16[256,128]{1,0:T(8,128)(2,1)S(1)} %bitcast.608), channel_id=1, source_target_pairs={{0,16},{8,24},{16,0},{24,8},{1,17},{9,25},{17,1},{25,9},{2,18},{10... | collective-permute-start | bytes 196616 | tf_op jit(solution)/shard_map/ppermute | solution.py:36
  76.4 26.2 %all-to-all-start.1 = ((bf16[64,16,128]{2,1,0:T(8,128)(2,1)}), bf16[64,16,128]{2,1,0:T(8,128)(2,1)S(1)}, u32[]{:S(2)}, u32[]{:S(2)}) async-start(bf16[64,16,128]{2,1,0:T(8,128)(2,1)} %bitcast.57), calls=%async_computation.1 | async-start | bytes 524288 | tf_op jit(solution)/shard_map/all_to_all | solution.py:26
  83.7 16.9 %collective-permute-start.6 = (bf16[4,128,128]{2,1,0:T(8,128)(2,1)S(1)}, bf16[4,128,128]{2,1,0:T(8,128)(2,1)S(1)}, u32[]{:S(2)}, u32[]{:S(2)}) collective-permute-start(bf16[4,128,128]{2,1,0:T(8,128)(2,1)S(1)} %bitcast.591), channel_id=1, source_target_pairs={{0,6},{2,0},{4,2},{6,4},{1,7},{3,1},{5,3},{7,5},{8,14},{10,8},{12,... | collective-permute-start | bytes 393224 | tf_op jit(solution)/shard_map/ppermute | solution.py:36
  86.0 14.5 %collective-permute-start.5 = (bf16[4,128,128]{2,1,0:T(8,128)(2,1)S(1)}, bf16[4,128,128]{2,1,0:T(8,128)(2,1)S(1)}, u32[]{:S(2)}, u32[]{:S(2)}) collective-permute-start(bf16[4,128,128]{2,1,0:T(8,128)(2,1)S(1)} %bitcast.592), channel_id=1, source_target_pairs={{0,4},{2,6},{4,0},{6,2},{1,5},{3,7},{5,1},{7,3},{8,12},{10,14},{12... | collective-permute-start | bytes 393224 | tf_op jit(solution)/shard_map/ppermute | solution.py:36
  90.4 10.1 %collective-permute-start.4 = (bf16[4,128,128]{2,1,0:T(8,128)(2,1)S(1)}, bf16[4,128,128]{2,1,0:T(8,128)(2,1)S(1)}, u32[]{:S(2)}, u32[]{:S(2)}) collective-permute-start(bf16[4,128,128]{2,1,0:T(8,128)(2,1)S(1)} %bitcast.593), channel_id=1, source_target_pairs={{0,2},{2,4},{4,6},{6,0},{1,3},{3,5},{5,7},{7,1},{8,10},{10,12},{12... | collective-permute-start | bytes 393224 | tf_op jit(solution)/shard_map/ppermute | solution.py:36
  94.8 5.6 %collective-permute-start.3 = (bf16[56,128]{1,0:T(8,128)(2,1)S(1)}, bf16[56,128]{1,0:T(8,128)(2,1)S(1)}, u32[]{:S(2)}, u32[]{:S(2)}) collective-permute-start(bf16[56,128]{1,0:T(8,128)(2,1)S(1)} %pad_maximum_fusion.19), channel_id=1, source_target_pairs={{0,32},{32,0},{1,33},{33,1},{2,34},{34,2},{3,35},{35,3},{4,36},{36... | collective-permute-start | bytes 43016 | tf_op jit(solution)/shard_map/ppermute | solution.py:36
  100.6 5.6 %collective-permute-start.7 = (bf16[4,4,128,128]{3,2,1,0:T(8,128)(2,1)S(1)}, bf16[4,4,128,128]{3,2,1,0:T(8,128)(2,1)S(1)}, u32[]{:S(2)}, u32[]{:S(2)}) collective-permute-start(bf16[4,4,128,128]{3,2,1,0:T(8,128)(2,1)S(1)} %pad_maximum_fusion.1), channel_id=1, source_target_pairs={{0,1},{1,0},{2,3},{3,2},{4,5},{5,4},{6,7},{7,6},{8,9},{9,8},{10,11... | collective-permute-start | bytes 1572872 | tf_op jit(solution)/shard_map/ppermute | solution.py:36
  109.2 14.7 %all-to-all-start.2 = ((bf16[4,8,8,128]{3,2,1,0:T(8,128)(2,1)}), bf16[4,8,8,128]{3,2,1,0:T(8,128)(2,1)S(1)}, u32[]{:S(2)}, u32[]{:S(2)}) async-start(bf16[4,8,8,128]{3,2,1,0:T(8,128)(2,1)} %pad_maximum_fusion.6), calls=%async_computation.2 | async-start | bytes 131072 | tf_op jit(solution)/shard_map/all_to_all | solution.py:26
  112.6 9.9 %copy-start.1 = (bf16[2,32,3,32]{3,1,2,0:T(8,128)(2,1)}, bf16[2,32,3,32]{3,1,2,0:T(8,128)(2,1)S(1)}, u32[]{:S(2)}) copy-start(bf16[2,32,3,32]{3,1,2,0:T(8,128)(2,1)S(1)} %broadcast_select_fusion.1) | copy-start | bytes 36868
  112.6 32.6 %collective-permute-start.16 = (bf16[1024,128]{1,0:T(8,128)(2,1)S(1)}, bf16[1024,128]{1,0:T(8,128)(2,1)S(1)}, u32[]{:S(2)}, u32[]{:S(2)}) collective-permute-start(bf16[1024,128]{1,0:T(8,128)(2,1)S(1)} %bitcast.586), channel_id=1, source_target_pairs={{0,6},{2,0},{4,2},{6,4},{1,7},{3,1},{5,3},{7,5},{8,14},{10,8},{12,... | collective-permute-start | bytes 786440 | tf_op jit(solution)/shard_map/ppermute | solution.py:36
  114.8 30.4 %collective-permute-start.15 = (bf16[1024,128]{1,0:T(8,128)(2,1)S(1)}, bf16[1024,128]{1,0:T(8,128)(2,1)S(1)}, u32[]{:S(2)}, u32[]{:S(2)}) collective-permute-start(bf16[1024,128]{1,0:T(8,128)(2,1)S(1)} %bitcast.587), channel_id=1, source_target_pairs={{0,4},{2,6},{4,0},{6,2},{1,5},{3,7},{5,1},{7,3},{8,12},{10,14},{12... | collective-permute-start | bytes 786440 | tf_op jit(solution)/shard_map/ppermute | solution.py:36
  117.9 27.3 %collective-permute-start.14 = (bf16[1024,128]{1,0:T(8,128)(2,1)S(1)}, bf16[1024,128]{1,0:T(8,128)(2,1)S(1)}, u32[]{:S(2)}, u32[]{:S(2)}) collective-permute-start(bf16[1024,128]{1,0:T(8,128)(2,1)S(1)} %bitcast.588), channel_id=1, source_target_pairs={{0,2},{2,4},{4,6},{6,0},{1,3},{3,5},{5,7},{7,1},{8,10},{10,12},{12... | collective-permute-start | bytes 786440 | tf_op jit(solution)/shard_map/ppermute | solution.py:36
  124.6 48.4 %all-to-all-start.3 = ((bf16[8,8,8,128]{3,2,1,0:T(8,128)(2,1)}), bf16[8,8,8,128]{3,2,1,0:T(8,128)(2,1)S(1)}, u32[]{:S(2)}, u32[]{:S(2)}) async-start(bf16[8,8,8,128]{3,2,1,0:T(8,128)(2,1)} %broadcast_in_dim.122), calls=%async_computation.3 | async-start | bytes 262144 | tf_op jit(solution)/shard_map/all_to_all | solution.py:26
  145.4 28.2 %collective-permute-start.17 = (bf16[4,1024,128]{2,1,0:T(8,128)(2,1)S(1)}, bf16[4,1024,128]{2,1,0:T(8,128)(2,1)S(1)}, u32[]{:S(2)}, u32[]{:S(2)}) collective-permute-start(bf16[4,1024,128]{2,1,0:T(8,128)(2,1)S(1)} %pad_maximum_fusion), channel_id=1, source_target_pairs={{0,1},{1,0},{2,3},{3,2},{4,5},{5,4},{6,7},{7,6},{8,9},{9,8},{10,11... | collective-permute-start | bytes 3145736 | tf_op jit(solution)/shard_map/ppermute | solution.py:36
  175.4 11.2 %all-to-all-start.4 = ((bf16[4,4,8,128]{3,2,1,0:T(8,128)(2,1)}), bf16[4,4,8,128]{3,2,1,0:T(8,128)(2,1)S(1)}, u32[]{:S(2)}, u32[]{:S(2)}) async-start(bf16[4,4,8,128]{3,2,1,0:T(8,128)(2,1)} %pad_maximum_fusion.9), calls=%async_computation.4 | async-start | bytes 65536 | tf_op jit(solution)/shard_map/all_to_all | solution.py:26
  187.8 17.0 %collective-permute-start.20 = (f32[8,128]{1,0:T(8,128)S(1)}, f32[8,128]{1,0:T(8,128)S(1)}, u32[]{:S(2)}, u32[]{:S(2)}) collective-permute-start(f32[8,128]{1,0:T(8,128)S(1)} %get-tuple-element.44), channel_id=1, source_target_pairs={{0,8},{8,16},{16,24},{24,0},{1,9},{9,17},{17,25},{25,1},{2,10},{10... | collective-permute-start | bytes 12296 | tf_op jit(solution)/shard_map/ppermute | solution.py:36
  191.2 13.5 %collective-permute-start.19 = (f32[8,128]{1,0:T(8,128)S(1)}, f32[8,128]{1,0:T(8,128)S(1)}, u32[]{:S(2)}, u32[]{:S(2)}) collective-permute-start(f32[8,128]{1,0:T(8,128)S(1)} %get-tuple-element.45), channel_id=1, source_target_pairs={{0,16},{8,24},{16,0},{24,8},{1,17},{9,25},{17,1},{25,9},{2,18},{10... | collective-permute-start | bytes 12296 | tf_op jit(solution)/shard_map/ppermute | solution.py:36
  195.9 8.8 %collective-permute-start.18 = (f32[8,128]{1,0:T(8,128)S(1)}, f32[8,128]{1,0:T(8,128)S(1)}, u32[]{:S(2)}, u32[]{:S(2)}) collective-permute-start(f32[8,128]{1,0:T(8,128)S(1)} %get-tuple-element.46), channel_id=1, source_target_pairs={{0,24},{8,0},{16,8},{24,16},{1,25},{9,1},{17,9},{25,17},{2,26},{10... | collective-permute-start | bytes 12296 | tf_op jit(solution)/shard_map/ppermute | solution.py:36
  199.9 11.4 %all-to-all-start.5 = ((bf16[32,16,128]{2,1,0:T(8,128)(2,1)}), bf16[32,16,128]{2,1,0:T(8,128)(2,1)S(1)}, u32[]{:S(2)}, u32[]{:S(2)}) async-start(bf16[32,16,128]{2,1,0:T(8,128)(2,1)} %bitcast.224), calls=%async_computation.5 | async-start | bytes 262144 | tf_op jit(solution)/shard_map/all_to_all | solution.py:26
  211.3 0.8 copy-start.8
  211.3 0.8 copy-start.9
  212.9 31.1 %all-to-all-start.6 = ((bf16[32,4,256]{2,1,0:T(4,128)(2,1)}), bf16[32,4,256]{2,1,0:T(4,128)(2,1)S(1)}, u32[]{:S(2)}, u32[]{:S(2)}) async-start(bf16[32,4,256]{2,1,0:T(4,128)(2,1)} %reshape.473), calls=%async_computation.6 | async-start | bytes 131072 | tf_op jit(solution)/shard_map/all_to_all | solution.py:26
  217.9 0.8 slice-start

commit v4 on v3

--- a/solution.py
+++ b/solution.py
@@ -3,6 +3,7 @@
 from jax import lax
 from jax.sharding import Mesh
 from jax.sharding import PartitionSpec as P
+
 
 D = 4096
 BLOCK = 256
@@ -46,21 +47,10 @@
     return pieces
 
 
-def collected(piece, axis):
-    return [piece] + [passed(piece, axis, k) for k in range(1, lax.axis_size(axis))]
-
-
 def in_order(pieces, axis):
     backward = jnp.stack(pieces[::-1] + pieces[::-1])
     count = len(pieces)
     return lax.dynamic_slice_in_dim(backward, count - 1 - lax.axis_index(axis), count, 0)
-
-
-def relative(tiles):
-    parts = tiles.reshape(4, 2, *tiles.shape[1:])
-    parts = jnp.concatenate([parts, parts])[::-1]
-    parts = lax.dynamic_slice_in_dim(parts, 3 - lax.axis_index("x"), 4, 0)
-    return jnp.where(lax.axis_index("core") == 1, parts[:, ::-1], parts).reshape(tiles.shape)
 
 
 def parts_of(value):
@@ -72,11 +62,6 @@
 
 def whole_of(coarse, middle, fine):
     return coarse.astype(f32) + (middle.astype(f32) + fine.astype(f32))
-
-
-def over_dp(piece):
-    pieces = jnp.stack(collected(piece, "x"))
-    return [pieces, passed(pieces, "core", 1)]
 
 
 def contract(a, a_dim, b, b_dim):
@@ -91,7 +76,7 @@
     return contract(rows_by_feature, 1, chosen, 0).astype(bf16)
 
 
-def gated_step(layer, branch, gate_in, upper, history, taps, gates, decay, earlier):
+def gated_step(branch, gate_in, upper, history, taps, gates, decay, earlier):
     convolved = (
         jnp.sum(history * taps[:3, None], axis=0) + branch.astype(f32) * taps[3]
     ).astype(bf16)
@@ -113,7 +98,7 @@
     return state, own_branch, readout
 
 
-def body(
+def both_blocks(
     stream,
     lengths,
     prior_state,
@@ -127,9 +112,7 @@
     decay_param,
     w_out,
 ):
-    q = lax.axis_index(ZQ)
     zl = lax.axis_index("zl")
-    y = lax.axis_index("y")
     upper = zl == 1
 
     stream_t = everywhere(stream.T, Z).reshape(128, 256)
@@ -180,7 +163,9 @@
             by_feature[:2].transpose(2, 0, 1, 3).reshape(4, 64, 128),
             by_feature[5].transpose(1, 0, 2),
             jnp.broadcast_to(gate_rows[None], (4, 256, 128)),
-            jnp.broadcast_to(by_feature[4].transpose(1, 0, 2).reshape(1, 128, 128), (4, 128, 128)),
+            jnp.broadcast_to(
+                by_feature[2:5].transpose(2, 0, 1, 3).reshape(1, 384, 128), (4, 384, 128)
+            ),
             small,
         ],
         axis=1,
@@ -194,9 +179,10 @@
         .transpose(1, 2, 3, 0, 4, 5)
         .reshape(LAYERS, 2, 2, 128, 128)
     )
-    w_mid = near[:, 352:480].reshape(4, 4, 32, 128).transpose(1, 0, 2, 3).reshape(4, 128, 128)
-    small = near[:, 480:].reshape(4, 3584)
-
+    middle = (
+        near[:, 352:736].reshape(4, 4, 3, 32, 128).transpose(1, 2, 0, 3, 4).reshape(4, 384, 128)
+    )
+    small = near[:, 736:].reshape(4, 3584)
     earlier_rows = (
         whole_of(small[:, :512], small[:, 512:1024], small[:, 1024:1536])
         .reshape(4, LAYERS, 8, 32)
@@ -223,14 +209,9 @@
     history_rows = windows[:48].reshape(LAYERS, depth, 8, 256)
     taps = windows[48:].reshape(LAYERS, TAPS, 256)
 
-    w_mid = over_dp(w_mid)
-    w_second = by_feature[2:4].transpose(2, 0, 1, 3).reshape(4, 64, 128)
-    w_second = in_order(traded(w_second, ZQ), ZQ).reshape(256, 128)
-    w_second = in_order(collected(w_second, "y"), "y")
-    w_second = (
-        w_second.reshape(4, 4, 2, 32, 128).transpose(1, 2, 0, 3, 4).reshape(1024, 128)
-    )
-    w_second = over_dp(w_second)
+    middle = in_order(traded(middle, ZQ), ZQ)
+    w_second = middle[:, :256].reshape(1024, 128)
+    w_mid = middle[:, 256:].reshape(512, 128)
 
     stream_rows = stream_t.T.reshape(8, 4, 8, 128).transpose(1, 0, 2, 3)
     products = [
@@ -255,7 +236,6 @@
     squares = jnp.sum(jnp.sum(widened * widened, axis=0), axis=1, keepdims=True)
     scaling = lax.rsqrt(squares / D + epsilon)
     state_first, branch_first, readout = gated_step(
-        0,
         (branch * scaling).astype(bf16),
         (gate_in * scaling).astype(bf16),
         upper,
@@ -265,50 +245,43 @@
         decay[0],
         earlier_rows[0],
     )
-    residual = lax.dynamic_index_in_dim(rows.reshape(4, 8, 8, 128), q, 0, keepdims=False)
-    residual = relative(residual)
-    mixed = jnp.stack(
+    sent = jnp.stack(
+        [jnp.broadcast_to(readout[None], (32, 8, 128)), rows], axis=1
+    )
+    came = exchange(sent.reshape(32, 16, 128), ZQ + DP).reshape(4, 8, 2, 8, 128)
+    residual = came[0, :, 1].reshape(64, 128).astype(f32)
+    came = came[:, :, 0].reshape(4, 64, 128)
+    came = jnp.concatenate([came[at] for at in range(4)], axis=1)
+    mixed = contract(came, 1, w_mid, 0).astype(bf16)
+    mixed = everywhere(mixed, "zh").astype(f32).sum(axis=0)
+    first = (mixed + residual).astype(bf16)
+
+    products = contract(first, 1, w_second, 1).astype(bf16)
+    products = [products[:, 128 * at : 128 * (at + 1)].reshape(8, 8, 128) for at in range(8)]
+    own_rows = first.reshape(8, 8, 128)
+    sent = jnp.stack(
         [
             jnp.stack(
                 [
-                    jnp.stack([contract(readout, 1, w_mid[core][x, part], 0) for core in range(2)])
-                    for x in range(4)
-                ]
-            )
-            for part in range(4)
-        ]
-    ).astype(bf16)
-    mixed = exchange(mixed.reshape(4, 8, 8, 128), ZQ)
-    mixed = mixed.astype(f32).sum(axis=0).astype(bf16)
-    mixed = everywhere(mixed, "zh").astype(f32).sum(axis=0)
-    first = (mixed + residual.astype(f32)).astype(bf16)
-
-    widened = first.astype(f32)
-    squares = jnp.sum(jnp.sum(widened * widened, axis=0), axis=1, keepdims=True)
-    coarse = lax.reduce_precision(squares, 8, 7)
-    lane = lax.broadcasted_iota(jnp.int32, (8, 128), 1)
-    squares = jnp.where(lane < 64, coarse, squares - coarse).astype(bf16)
-    products = sum(
-        contract(first[2 * x + core], 1, w_second[core][x], 1)
-        for core in range(2)
-        for x in range(4)
-    ).astype(bf16)
-    products = products.reshape(8, 2, 2, 2, 128)
-    sent = jnp.stack(
-        [
-            jnp.stack(
-                [products[:, zm, 0, 0], products[:, zm, 1, 0], products[:, zm, low, 1], squares]
+                    products[4 * zm],
+                    products[4 * zm + 2],
+                    products[4 * zm + 2 * low + 1],
+                    own_rows,
+                ],
+                axis=1,
             )
             for zm in range(2)
             for low in range(2)
         ]
     )
-    came = exchange(sent, ZQ).astype(f32).sum(axis=0)
+    came = exchange(sent.reshape(32, 32, 128), ZQ + DP).reshape(32, 4, 8, 128)
+    rows = came[:, 3]
+    came = came[:, :3].astype(f32).sum(axis=0)
+    widened = rows.astype(f32)
+    squares = jnp.sum(jnp.sum(widened * widened, axis=0), axis=1, keepdims=True)
     branch = jnp.concatenate([came[0], came[1]], axis=1)
-    squares = came[3, :, :1] + came[3, :, 64:65]
     scaling = lax.rsqrt(squares / D + epsilon)
     state_second, branch_second, readout = gated_step(
-        1,
         (branch * scaling).astype(bf16),
         (came[2] * scaling).astype(bf16),
         upper,
@@ -320,21 +293,18 @@
     )
     sent = jnp.stack(
         [
-            jnp.broadcast_to(readout[None, None], (8, 4, 8, 128)),
-            jnp.broadcast_to(relative(first)[:, None], (8, 4, 8, 128)),
+            jnp.broadcast_to(readout[None], (32, 8, 128)),
+            rows.reshape(4, 8, 8, 128).transpose(1, 0, 2, 3).reshape(32, 8, 128),
         ],
-        axis=2,
+        axis=1,
     )
     came = exchange(sent.reshape(32, 16, 128), PLANE).reshape(32, 2, 8, 128)
-    came = jnp.concatenate(
-        [came[:, 0].reshape(256, 128), came[:, 1].reshape(256, 128)], axis=1
-    )
-    adds = (q == y) & (lax.axis_index("zh") == 0)
-    index = lax.broadcasted_iota(jnp.int32, (128, 128), 0)
-    same = index == lax.broadcasted_iota(jnp.int32, (128, 128), 1)
-    same = jnp.where(same & adds, 1.0, 0.0).astype(bf16)
-    mixed = contract(jnp.concatenate([w_last, same], axis=0), 0, came, 1).astype(bf16)
-    second = exchange(mixed.reshape(32, 4, 256), Z).astype(f32).sum(axis=0).astype(bf16)
+    mixed = contract(w_last, 0, came[:, 0].reshape(256, 128), 1).astype(bf16)
+    own = lax.broadcasted_iota(jnp.int32, (4, 128), 0) + 4 * lax.axis_index(Z)
+    own = (own == lax.broadcasted_iota(jnp.int32, (4, 128), 1)).astype(bf16)
+    residual = contract(own, 1, came[:, 1].reshape(256, 128), 1)
+    second = exchange(mixed.reshape(32, 4, 256), Z).astype(f32).sum(axis=0)
+    second = (second + residual).astype(bf16)
 
     kept = jnp.stack(
         [state_first, state_second, branch_first.astype(f32), branch_second.astype(f32)]
@@ -363,4 +333,6 @@
         P(None, TP, DP),
     )
     out_specs = (P(None, DP + TP), P(None, DP, TP), P(None, DP, None, TP))
-    return jax.shard_map(body, mesh=torus, in_specs=in_specs, out_specs=out_specs, check_vma=False)
+    return jax.shard_map(
+        both_blocks, mesh=torus, in_specs=in_specs, out_specs=out_specs, check_vma=False
+    )

time: 246 us -> 223 us (0.907)
  starting transfers between devices: 146 us -> 96.4 us
  waiting for transfers between devices: 66.5 us -> 97.1 us
  matrix products: 7.73 us -> 3.15 us
    ppermute x21 -> x10, starting transfers between devices: 71 us -> 33 us  [passed(): lax.ppermute(piece, axis, [(at, (at + step) % count) for at in range(coun...]
    all_to_all x7, waiting for transfers between devices: 60.9 us -> 92 us  [exchange(): return lax.all_to_all(tiles, axes, 0, 0, tiled=True)]
    all_to_all x7, starting transfers between devices: 74.9 us -> 63.3 us  [exchange(): return lax.all_to_all(tiles, axes, 0, 0, tiled=True)]
    dot_general x52 -> x15, matrix products: 7.73 us -> 3.15 us  [contract(): lax.dot_general(a, b, (((a_dim,), (b_dim,)), ((), ())), preferred_element...]
    unnamed x4, other arithmetic: 0.04 us -> 3.06 us
    unnamed x64 -> x44, local copies, waits for them, and re-layouts: 6.85 us -> 5.71 us
    ppermute x21 -> x10, waiting for transfers between devices: 5.63 us -> 5.01 us  [passed(): lax.ppermute(piece, axis, [(at, (at + step) % count) for at in range(coun...]
  transfers between devices with their start and end apart: 28 -> 17, of which waited for: 6 -> 8; matrix products, arithmetic and copies ran while one was open for 5% -> 6% of each run, Pallas kernels for 0% -> 0%
where the time goes in v4:
time: 223 us; the launch traced here: 222 us
  waiting for transfers between devices  97.1 us (44%)
  starting transfers between devices  96.4 us (43%)
  local copies, waits for them, and re-layouts  16.9 us (8%)
  other arithmetic  6.45 us (3%)
  matrix products  3.15 us (1%)
    all_to_all x7, waiting for transfers between devices, exchange(): return lax.all_to_all(tiles, axes, 0, 0, tiled=True)  92 us
    all_to_all x7, starting transfers between devices, exchange(): return lax.all_to_all(tiles, axes, 0, 0, tiled=True)  63.3 us
    ppermute x10, starting transfers between devices, passed(): lax.ppermute(piece, axis, [(at, (at + step) % count) for at in range(coun...  33 us
    unnamed x44, local copies, waits for them, and re-layouts  5.71 us
    ppermute x10, waiting for transfers between devices, passed(): lax.ppermute(piece, axis, [(at, (at + step) % count) for at in range(coun...  5.01 us
  transfers between devices with their start and end apart: 17, of which 8 were waited for; matrix products, arithmetic and copies ran while one was open for 6% of the time, Pallas kernels for 0%

profile of v4, /device:TPU:2, one launch (start us, length us, event | category | flops | bytes accessed | tf_op | source)
XLA Modules:
  0.0 221.8 jit_solution(14375293099803805989)
XLA Ops:
  0.8 0.8 fusion.124
  1.5 0.8 constant_dynamic-update-slice_fusion.5
  2.3 0.8 constant_dynamic-update-slice_fusion.4
  3.1 0.8 constant_dynamic-update-slice_fusion.3
  3.8 0.8 constant_dynamic-update-slice_fusion.2
  4.6 0.8 constant_dynamic-update-slice_fusion.1
  5.4 0.8 constant_dynamic-update-slice_fusion
  6.1 0.4 convolution_convert_fusion
  8.0 4.9 %collective-permute-start = (bf16[764,128]{1,0:T(8,128)(2,1)S(1)}, bf16[764,128]{1,0:T(8,128)(2,1)S(1)}, u32[]{:S(2)}, u32[]{:S(2)}) collective-permute-start(bf16[764,128]{1,0:T(8,128)(2,1)S(1)} %get-tuple-element.15), channel_id=1, source_target_pairs={{0,24},{8,0},{16,8},{24,16},{1,25},{9,1},{17,9},{25,17},{2,26},{10... | collective-permute-start | bytes 586760 | tf_op jit(solution)/shard_map/ppermute | solution.py:37
  12.9 2.5 %collective-permute-start.1 = (bf16[764,128]{1,0:T(8,128)(2,1)S(1)}, bf16[764,128]{1,0:T(8,128)(2,1)S(1)}, u32[]{:S(2)}, u32[]{:S(2)}) collective-permute-start(bf16[764,128]{1,0:T(8,128)(2,1)S(1)} %get-tuple-element.14), channel_id=1, source_target_pairs={{0,16},{8,24},{16,0},{24,8},{1,17},{9,25},{17,1},{25,9},{2,18},{10... | collective-permute-start | bytes 586760 | tf_op jit(solution)/shard_map/ppermute | solution.py:37
  15.5 2.9 %collective-permute-start.2 = (bf16[764,128]{1,0:T(8,128)(2,1)S(1)}, bf16[764,128]{1,0:T(8,128)(2,1)S(1)}, u32[]{:S(2)}, u32[]{:S(2)}) collective-permute-start(bf16[764,128]{1,0:T(8,128)(2,1)S(1)} %get-tuple-element.13), channel_id=1, source_target_pairs={{0,8},{8,16},{16,24},{24,0},{1,9},{9,17},{17,25},{25,1},{2,10},{10... | collective-permute-start | bytes 586760 | tf_op jit(solution)/shard_map/ppermute | solution.py:37
  18.4 0.6 broadcast_in_dim.96
  19.0 28.7 %all-to-all-start = ((bf16[32,4,256]{2,1,0:T(4,128)(2,1)}), bf16[32,4,256]{2,1,0:T(4,128)(2,1)S(1)}, u32[]{:S(2)}, u32[]{:S(2)}) async-start(bf16[32,4,256]{2,1,0:T(4,128)(2,1)} %broadcast_in_dim.96), calls=%async_computation | async-start | bytes 131072 | tf_op jit(solution)/shard_map/all_to_all | solution.py:27
  48.9 3.7 %collective-permute-start.3 = (bf16[56,128]{1,0:T(8,128)(2,1)S(1)}, bf16[56,128]{1,0:T(8,128)(2,1)S(1)}, u32[]{:S(2)}, u32[]{:S(2)}) collective-permute-start(bf16[56,128]{1,0:T(8,128)(2,1)S(1)} %pad_maximum_fusion.12), channel_id=1, source_target_pairs={{0,32},{32,0},{1,33},{33,1},{2,34},{34,2},{3,35},{35,3},{4,36},{36... | collective-permute-start | bytes 43016 | tf_op jit(solution)/shard_map/ppermute | solution.py:37
  52.7 20.3 %all-to-all-done = bf16[32,4,256]{2,1,0:T(4,128)(2,1)S(1)} async-done(((bf16[32,4,256]{2,1,0:T(4,128)(2,1)}), bf16[32,4,256]{2,1,0:T(4,128)(2,1)S(1)}, u32[]{:S(2)}, u32[]{:S(2)}) %all-to-all-start) | async-done | bytes 65568 | tf_op jit(solution)/shard_map/all_to_all | solution.py:27
  73.0 0.2 select_bitcast_fusion.1
  73.4 0.1 fusion
  73.8 0.8 copy.116
  74.5 7.1 %all-to-all-start.1 = ((bf16[64,16,128]{2,1,0:T(8,128)(2,1)}), bf16[64,16,128]{2,1,0:T(8,128)(2,1)S(1)}, u32[]{:S(2)}, u32[]{:S(2)}) async-start(bf16[64,16,128]{2,1,0:T(8,128)(2,1)} %bitcast.57), calls=%async_computation.1 | async-start | bytes 524288 | tf_op jit(solution)/shard_map/all_to_all | solution.py:27
  82.2 3.5 %collective-permute-start.4 = (bf16[384,128]{1,0:T(8,128)(2,1)S(1)}, bf16[384,128]{1,0:T(8,128)(2,1)S(1)}, u32[]{:S(2)}, u32[]{:S(2)}) collective-permute-start(bf16[384,128]{1,0:T(8,128)(2,1)S(1)} %get-tuple-element.18), channel_id=1, source_target_pairs={{0,96},{32,0},{64,32},{96,64},{1,97},{33,1},{65,33},{97,65},{2,98}... | collective-permute-start | bytes 294920 | tf_op jit(solution)/shard_map/ppermute | solution.py:37
  85.6 3.4 %collective-permute-start.5 = (bf16[384,128]{1,0:T(8,128)(2,1)S(1)}, bf16[384,128]{1,0:T(8,128)(2,1)S(1)}, u32[]{:S(2)}, u32[]{:S(2)}) collective-permute-start(bf16[384,128]{1,0:T(8,128)(2,1)S(1)} %get-tuple-element.17), channel_id=1, source_target_pairs={{0,64},{32,96},{64,0},{96,32},{1,65},{33,97},{65,1},{97,33},{2,66}... | collective-permute-start | bytes 294920 | tf_op jit(solution)/shard_map/ppermute | solution.py:37
  89.0 1.9 collective-permute-start.6
  91.1 0.6 bitcast_dynamic-update-slice_fusion.10
  91.7 3.3 %collective-permute-done.5 = bf16[384,128]{1,0:T(8,128)(2,1)S(1)} collective-permute-done((bf16[384,128]{1,0:T(8,128)(2,1)S(1)}, bf16[384,128]{1,0:T(8,128)(2,1)S(1)}, u32[]{:S(2)}, u32[]{:S(2)}) %collective-permute-start.5) | collective-permute-done | bytes 98336 | tf_op jit(solution)/shard_map/ppermute | solution.py:37
  95.0 0.6 bitcast_dynamic-update-slice_fusion.8
  95.6 1.7 collective-permute-done.6
  97.3 0.6 bitcast_dynamic-update-slice_fusion.6
  98.0 0.1 convert_reduce_fusion.4
  98.4 0.1 fusion.53
  98.7 0.2 fusion.83
  98.9 0.7 maximum_bitcast_fusion
  99.6 5.0 %all-to-all-start.2 = ((bf16[32,16,128]{2,1,0:T(8,128)(2,1)}), bf16[32,16,128]{2,1,0:T(8,128)(2,1)S(1)}, u32[]{:S(2)}, u32[]{:S(2)}) async-start(bf16[32,16,128]{2,1,0:T(8,128)(2,1)} %maximum_bitcast_fusion), calls=%async_computation.2 | async-start | bytes 262144 | tf_op jit(solution)/shard_map/all_to_all | solution.py:27
  104.6 0.6 dynamic-slice_dynamic-update-slice_fusion.2
  105.2 0.6 bitcast_dynamic-update-slice_fusion.11
  105.9 0.7 bitcast_dynamic-update-slice_fusion.9
  106.5 0.6 bitcast_dynamic-update-slice_fusion.7
  107.1 0.6 dynamic-slice_dynamic-update-slice_fusion.3
  107.8 0.9 constant_dynamic-slice_fusion
  108.7 3.2 %all-to-all-done.2 = bf16[32,16,128]{2,1,0:T(8,128)(2,1)S(1)} async-done(((bf16[32,16,128]{2,1,0:T(8,128)(2,1)}), bf16[32,16,128]{2,1,0:T(8,128)(2,1)S(1)}, u32[]{:S(2)}, u32[]{:S(2)}) %all-to-all-start.2) | async-done | bytes 131104 | tf_op jit(solution)/shard_map/all_to_all | solution.py:27
  112.0 0.2 convolution_convert_fusion.5
  112.1 0.7 broadcast_in_dim.97
  112.8 5.2 %all-to-all-start.3 = ((bf16[8,64,128]{2,1,0:T(8,128)(2,1)}), bf16[8,64,128]{2,1,0:T(8,128)(2,1)S(1)}, u32[]{:S(2)}, u32[]{:S(2)}) async-start(bf16[8,64,128]{2,1,0:T(8,128)(2,1)} %broadcast_in_dim.97), calls=%async_computation.3 | async-start | bytes 262144 | tf_op jit(solution)/shard_map/all_to_all | solution.py:27
  118.0 1.0 constant_dynamic-slice_fusion.9
  118.9 28.4 %all-to-all-done.3 = bf16[8,64,128]{2,1,0:T(8,128)(2,1)S(1)} async-done(((bf16[8,64,128]{2,1,0:T(8,128)(2,1)}), bf16[8,64,128]{2,1,0:T(8,128)(2,1)S(1)}, u32[]{:S(2)}, u32[]{:S(2)}) %all-to-all-start.3) | async-done | bytes 131104 | tf_op jit(solution)/shard_map/all_to_all | solution.py:27
  147.4 0.2 convolution_convert_fusion.1
  147.7 0.7 copy.123
  148.5 6.1 %all-to-all-start.4 = ((bf16[32,32,128]{2,1,0:T(8,128)(2,1)}), bf16[32,32,128]{2,1,0:T(8,128)(2,1)S(1)}, u32[]{:S(2)}, u32[]{:S(2)}) async-start(bf16[32,32,128]{2,1,0:T(8,128)(2,1)} %bitcast.106), calls=%async_computation.4 | async-start | bytes 524288 | tf_op jit(solution)/shard_map/all_to_all | solution.py:27
  155.1 8.9 %all-to-all-done.4 = bf16[32,32,128]{2,1,0:T(8,128)(2,1)S(1)} async-done(((bf16[32,32,128]{2,1,0:T(8,128)(2,1)}), bf16[32,32,128]{2,1,0:T(8,128)(2,1)S(1)}, u32[]{:S(2)}, u32[]{:S(2)}) %all-to-all-start.4) | async-done | bytes 262176 | tf_op jit(solution)/shard_map/all_to_all | solution.py:27
  164.0 0.1 multiply_reduce_fusion
  164.4 0.1 fusion.51
  164.7 0.2 fusion.90
  165.2 4.8 %collective-permute-start.7 = (f32[8,128]{1,0:T(8,128)S(1)}, f32[8,128]{1,0:T(8,128)S(1)}, u32[]{:S(2)}, u32[]{:S(2)}) collective-permute-start(f32[8,128]{1,0:T(8,128)S(1)} %get-tuple-element.53), channel_id=1, source_target_pairs={{0,24},{8,0},{16,8},{24,16},{1,25},{9,1},{17,9},{25,17},{2,26},{10... | collective-permute-start | bytes 12296 | tf_op jit(solution)/shard_map/ppermute | solution.py:37
  169.9 2.7 %collective-permute-start.8 = (f32[8,128]{1,0:T(8,128)S(1)}, f32[8,128]{1,0:T(8,128)S(1)}, u32[]{:S(2)}, u32[]{:S(2)}) collective-permute-start(f32[8,128]{1,0:T(8,128)S(1)} %get-tuple-element.52), channel_id=1, source_target_pairs={{0,16},{8,24},{16,0},{24,8},{1,17},{9,25},{17,1},{25,9},{2,18},{10... | collective-permute-start | bytes 12296 | tf_op jit(solution)/shard_map/ppermute | solution.py:37
  172.6 2.8 %collective-permute-start.9 = (f32[8,128]{1,0:T(8,128)S(1)}, f32[8,128]{1,0:T(8,128)S(1)}, u32[]{:S(2)}, u32[]{:S(2)}) collective-permute-start(f32[8,128]{1,0:T(8,128)S(1)} %get-tuple-element.51), channel_id=1, source_target_pairs={{0,8},{8,16},{16,24},{24,0},{1,9},{9,17},{17,25},{25,1},{2,10},{10... | collective-permute-start | bytes 12296 | tf_op jit(solution)/shard_map/ppermute | solution.py:37
  175.5 0.7 copy_bitcast_fusion
  176.1 6.4 %all-to-all-start.5 = ((bf16[32,16,128]{2,1,0:T(8,128)(2,1)}), bf16[32,16,128]{2,1,0:T(8,128)(2,1)S(1)}, u32[]{:S(2)}, u32[]{:S(2)}) async-start(bf16[32,16,128]{2,1,0:T(8,128)(2,1)} %copy_bitcast_fusion), calls=%async_computation.5 | async-start | bytes 262144 | tf_op jit(solution)/shard_map/all_to_all | solution.py:27
  182.8 6.4 %all-to-all-done.5 = bf16[32,16,128]{2,1,0:T(8,128)(2,1)S(1)} async-done(((bf16[32,16,128]{2,1,0:T(8,128)(2,1)}), bf16[32,16,128]{2,1,0:T(8,128)(2,1)S(1)}, u32[]{:S(2)}, u32[]{:S(2)}) %all-to-all-start.5) | async-done | bytes 131104 | tf_op jit(solution)/shard_map/all_to_all | solution.py:27
  189.1 0.2 convolution_convert_fusion.2
  189.3 0.6 reshape.408
  190.0 4.9 %all-to-all-start.6 = ((bf16[32,4,256]{2,1,0:T(4,128)(2,1)}), bf16[32,4,256]{2,1,0:T(4,128)(2,1)S(1)}, u32[]{:S(2)}, u32[]{:S(2)}) async-start(bf16[32,4,256]{2,1,0:T(4,128)(2,1)} %reshape.408), calls=%async_computation.6 | async-start | bytes 131072 | tf_op jit(solution)/shard_map/all_to_all | solution.py:27
  194.9 0.6 pad_maximum_fusion.11
  195.5 0.6 copy_bitcast_fusion.2
  196.1 24.8 %all-to-all-done.6 = bf16[32,4,256]{2,1,0:T(4,128)(2,1)S(1)} async-done(((bf16[32,4,256]{2,1,0:T(4,128)(2,1)}), bf16[32,4,256]{2,1,0:T(4,128)(2,1)S(1)}, u32[]{:S(2)}, u32[]{:S(2)}) %all-to-all-start.6) | async-done | bytes 65568 | tf_op jit(solution)/shard_map/all_to_all | solution.py:27
  221.0 0.8 fusion.25
  (164 shorter events, 5.2 us)
Async XLA Ops:
  0.6 6.0 %copy-start.1 = (bf16[2,256,32]{1,2,0:T(8,128)(2,1)S(1)}, bf16[2,256,32]{1,2,0:T(8,128)(2,1)}, u32[]{:S(2)}) copy-start(bf16[2,256,32]{1,2,0:T(8,128)(2,1)} %param.20) | copy-start | bytes 98308
  0.6 6.0 %copy-start.2 = (bf16[2,256,32]{1,2,0:T(8,128)(2,1)S(1)}, bf16[2,256,32]{1,2,0:T(8,128)(2,1)}, u32[]{:S(2)}) copy-start(bf16[2,256,32]{1,2,0:T(8,128)(2,1)} %param.21) | copy-start | bytes 98308
  0.7 6.2 %copy-start.7 = (s32[32]{0:T(128)S(1)}, s32[32]{0:T(128)}, u32[]{:S(2)}) copy-start(s32[32]{0:T(128)} %param.13) | copy-start | bytes 388
  0.7 6.2 %copy-start.3 = (f32[2,32,32]{2,1,0:T(8,128)S(1)}, f32[2,32,32]{2,1,0:T(8,128)}, u32[]{:S(2)}) copy-start(f32[2,32,32]{2,1,0:T(8,128)} %param.14) | copy-start | bytes 24580
  0.7 6.4 %copy-start.6 = (f32[2,32]{1,0:T(2,128)S(1)}, f32[2,32]{1,0:T(2,128)}, u32[]{:S(2)}) copy-start(f32[2,32]{1,0:T(2,128)} %param.22) | copy-start | bytes 772
  0.7 6.6 %copy-start = (bf16[2,32,3,32]{3,1,2,0:T(8,128)(2,1)S(1)}, bf16[2,32,3,32]{3,1,2,0:T(8,128)(2,1)}, u32[]{:S(2)}) copy-start(bf16[2,32,3,32]{3,1,2,0:T(8,128)(2,1)} %param.15) | copy-start | bytes 36868
  0.7 6.8 %copy-start.5 = (bf16[2,4,32]{2,1,0:T(4,128)(2,1)S(1)}, bf16[2,4,32]{2,1,0:T(4,128)(2,1)}, u32[]{:S(2)}) copy-start(bf16[2,4,32]{2,1,0:T(4,128)(2,1)} %param.19) | copy-start | bytes 1540
  6.7 11.7 %copy-start.4 = (bf16[256,4]{0,1:T(4,128)(2,1)S(1)}, bf16[256,4]{0,1:T(4,128)(2,1)}, u32[]{:S(2)}) copy-start(bf16[256,4]{0,1:T(4,128)(2,1)} %param.12) | copy-start | bytes 6148
  8.0 39.8 %collective-permute-start = (bf16[764,128]{1,0:T(8,128)(2,1)S(1)}, bf16[764,128]{1,0:T(8,128)(2,1)S(1)}, u32[]{:S(2)}, u32[]{:S(2)}) collective-permute-start(bf16[764,128]{1,0:T(8,128)(2,1)S(1)} %get-tuple-element.15), channel_id=1, source_target_pairs={{0,24},{8,0},{16,8},{24,16},{1,25},{9,1},{17,9},{25,17},{2,26},{10... | collective-permute-start | bytes 586760 | tf_op jit(solution)/shard_map/ppermute | solution.py:37
  12.9 34.9 %collective-permute-start.1 = (bf16[764,128]{1,0:T(8,128)(2,1)S(1)}, bf16[764,128]{1,0:T(8,128)(2,1)S(1)}, u32[]{:S(2)}, u32[]{:S(2)}) collective-permute-start(bf16[764,128]{1,0:T(8,128)(2,1)S(1)} %get-tuple-element.14), channel_id=1, source_target_pairs={{0,16},{8,24},{16,0},{24,8},{1,17},{9,25},{17,1},{25,9},{2,18},{10... | collective-permute-start | bytes 586760 | tf_op jit(solution)/shard_map/ppermute | solution.py:37
  15.5 32.4 %collective-permute-start.2 = (bf16[764,128]{1,0:T(8,128)(2,1)S(1)}, bf16[764,128]{1,0:T(8,128)(2,1)S(1)}, u32[]{:S(2)}, u32[]{:S(2)}) collective-permute-start(bf16[764,128]{1,0:T(8,128)(2,1)S(1)} %get-tuple-element.13), channel_id=1, source_target_pairs={{0,8},{8,16},{16,24},{24,0},{1,9},{9,17},{17,25},{25,1},{2,10},{10... | collective-permute-start | bytes 586760 | tf_op jit(solution)/shard_map/ppermute | solution.py:37
  19.0 54.0 %all-to-all-start = ((bf16[32,4,256]{2,1,0:T(4,128)(2,1)}), bf16[32,4,256]{2,1,0:T(4,128)(2,1)S(1)}, u32[]{:S(2)}, u32[]{:S(2)}) async-start(bf16[32,4,256]{2,1,0:T(4,128)(2,1)} %broadcast_in_dim.96), calls=%async_computation | async-start | bytes 131072 | tf_op jit(solution)/shard_map/all_to_all | solution.py:27
  48.9 42.0 %collective-permute-start.3 = (bf16[56,128]{1,0:T(8,128)(2,1)S(1)}, bf16[56,128]{1,0:T(8,128)(2,1)S(1)}, u32[]{:S(2)}, u32[]{:S(2)}) collective-permute-start(bf16[56,128]{1,0:T(8,128)(2,1)S(1)} %pad_maximum_fusion.12), channel_id=1, source_target_pairs={{0,32},{32,0},{1,33},{33,1},{2,34},{34,2},{3,35},{35,3},{4,36},{36... | collective-permute-start | bytes 43016 | tf_op jit(solution)/shard_map/ppermute | solution.py:37
  74.5 23.5 %all-to-all-start.1 = ((bf16[64,16,128]{2,1,0:T(8,128)(2,1)}), bf16[64,16,128]{2,1,0:T(8,128)(2,1)S(1)}, u32[]{:S(2)}, u32[]{:S(2)}) async-start(bf16[64,16,128]{2,1,0:T(8,128)(2,1)} %bitcast.57), calls=%async_computation.1 | async-start | bytes 524288 | tf_op jit(solution)/shard_map/all_to_all | solution.py:27
  82.2 8.9 %collective-permute-start.4 = (bf16[384,128]{1,0:T(8,128)(2,1)S(1)}, bf16[384,128]{1,0:T(8,128)(2,1)S(1)}, u32[]{:S(2)}, u32[]{:S(2)}) collective-permute-start(bf16[384,128]{1,0:T(8,128)(2,1)S(1)} %get-tuple-element.18), channel_id=1, source_target_pairs={{0,96},{32,0},{64,32},{96,64},{1,97},{33,1},{65,33},{97,65},{2,98}... | collective-permute-start | bytes 294920 | tf_op jit(solution)/shard_map/ppermute | solution.py:37
  85.6 9.3 %collective-permute-start.5 = (bf16[384,128]{1,0:T(8,128)(2,1)S(1)}, bf16[384,128]{1,0:T(8,128)(2,1)S(1)}, u32[]{:S(2)}, u32[]{:S(2)}) collective-permute-start(bf16[384,128]{1,0:T(8,128)(2,1)S(1)} %get-tuple-element.17), channel_id=1, source_target_pairs={{0,64},{32,96},{64,0},{96,32},{1,65},{33,97},{65,1},{97,33},{2,66}... | collective-permute-start | bytes 294920 | tf_op jit(solution)/shard_map/ppermute | solution.py:37
  89.0 8.3 %collective-permute-start.6 = (bf16[384,128]{1,0:T(8,128)(2,1)S(1)}, bf16[384,128]{1,0:T(8,128)(2,1)S(1)}, u32[]{:S(2)}, u32[]{:S(2)}) collective-permute-start(bf16[384,128]{1,0:T(8,128)(2,1)S(1)} %get-tuple-element.16), channel_id=1, source_target_pairs={{0,32},{32,64},{64,96},{96,0},{1,33},{33,65},{65,97},{97,1},{2,34}... | collective-permute-start | bytes 294920 | tf_op jit(solution)/shard_map/ppermute | solution.py:37
  99.6 12.3 %all-to-all-start.2 = ((bf16[32,16,128]{2,1,0:T(8,128)(2,1)}), bf16[32,16,128]{2,1,0:T(8,128)(2,1)S(1)}, u32[]{:S(2)}, u32[]{:S(2)}) async-start(bf16[32,16,128]{2,1,0:T(8,128)(2,1)} %maximum_bitcast_fusion), calls=%async_computation.2 | async-start | bytes 262144 | tf_op jit(solution)/shard_map/all_to_all | solution.py:27
  112.8 34.6 %all-to-all-start.3 = ((bf16[8,64,128]{2,1,0:T(8,128)(2,1)}), bf16[8,64,128]{2,1,0:T(8,128)(2,1)S(1)}, u32[]{:S(2)}, u32[]{:S(2)}) async-start(bf16[8,64,128]{2,1,0:T(8,128)(2,1)} %broadcast_in_dim.97), calls=%async_computation.3 | async-start | bytes 262144 | tf_op jit(solution)/shard_map/all_to_all | solution.py:27
  148.5 15.5 %all-to-all-start.4 = ((bf16[32,32,128]{2,1,0:T(8,128)(2,1)}), bf16[32,32,128]{2,1,0:T(8,128)(2,1)S(1)}, u32[]{:S(2)}, u32[]{:S(2)}) async-start(bf16[32,32,128]{2,1,0:T(8,128)(2,1)} %bitcast.106), calls=%async_computation.4 | async-start | bytes 524288 | tf_op jit(solution)/shard_map/all_to_all | solution.py:27
  165.2 17.4 %collective-permute-start.7 = (f32[8,128]{1,0:T(8,128)S(1)}, f32[8,128]{1,0:T(8,128)S(1)}, u32[]{:S(2)}, u32[]{:S(2)}) collective-permute-start(f32[8,128]{1,0:T(8,128)S(1)} %get-tuple-element.53), channel_id=1, source_target_pairs={{0,24},{8,0},{16,8},{24,16},{1,25},{9,1},{17,9},{25,17},{2,26},{10... | collective-permute-start | bytes 12296 | tf_op jit(solution)/shard_map/ppermute | solution.py:37
  169.9 12.6 %collective-permute-start.8 = (f32[8,128]{1,0:T(8,128)S(1)}, f32[8,128]{1,0:T(8,128)S(1)}, u32[]{:S(2)}, u32[]{:S(2)}) collective-permute-start(f32[8,128]{1,0:T(8,128)S(1)} %get-tuple-element.52), channel_id=1, source_target_pairs={{0,16},{8,24},{16,0},{24,8},{1,17},{9,25},{17,1},{25,9},{2,18},{10... | collective-permute-start | bytes 12296 | tf_op jit(solution)/shard_map/ppermute | solution.py:37
  172.6 10.0 %collective-permute-start.9 = (f32[8,128]{1,0:T(8,128)S(1)}, f32[8,128]{1,0:T(8,128)S(1)}, u32[]{:S(2)}, u32[]{:S(2)}) collective-permute-start(f32[8,128]{1,0:T(8,128)S(1)} %get-tuple-element.51), channel_id=1, source_target_pairs={{0,8},{8,16},{16,24},{24,0},{1,9},{9,17},{17,25},{25,1},{2,10},{10... | collective-permute-start | bytes 12296 | tf_op jit(solution)/shard_map/ppermute | solution.py:37
  176.1 13.0 %all-to-all-start.5 = ((bf16[32,16,128]{2,1,0:T(8,128)(2,1)}), bf16[32,16,128]{2,1,0:T(8,128)(2,1)S(1)}, u32[]{:S(2)}, u32[]{:S(2)}) async-start(bf16[32,16,128]{2,1,0:T(8,128)(2,1)} %copy_bitcast_fusion), calls=%async_computation.5 | async-start | bytes 262144 | tf_op jit(solution)/shard_map/all_to_all | solution.py:27
  190.0 31.0 %all-to-all-start.6 = ((bf16[32,4,256]{2,1,0:T(4,128)(2,1)}), bf16[32,4,256]{2,1,0:T(4,128)(2,1)S(1)}, u32[]{:S(2)}, u32[]{:S(2)}) async-start(bf16[32,4,256]{2,1,0:T(4,128)(2,1)} %reshape.408), calls=%async_computation.6 | async-start | bytes 131072 | tf_op jit(solution)/shard_map/all_to_all | solution.py:27

commit v5 on v4

--- a/solution.py
+++ b/solution.py
@@ -42,15 +42,16 @@
     here = lax.axis_index(axis)
     pieces = []
     for step in range(count):
-        piece = lax.dynamic_index_in_dim(tiles, (here + step) % count, 0, keepdims=False)
+        piece = lax.dynamic_slice_in_dim(tiles, (here + step) & 3, 1)[0]
         pieces.append(passed(piece, axis, step) if step else piece)
     return pieces
 
 
-def in_order(pieces, axis):
-    backward = jnp.stack(pieces[::-1] + pieces[::-1])
-    count = len(pieces)
-    return lax.dynamic_slice_in_dim(backward, count - 1 - lax.axis_index(axis), count, 0)
+def counted_back(pieces, axis):
+    here = lax.axis_index(axis)
+    pieces = [pieces[-k % 4] for k in range(4)]
+    pieces = [jnp.where((here & 1) == 1, pieces[k - 1], pieces[k]) for k in range(4)]
+    return [jnp.where(here > 1, pieces[k - 2], pieces[k]) for k in range(4)]
 
 
 def parts_of(value):
@@ -115,24 +116,20 @@
     zl = lax.axis_index("zl")
     upper = zl == 1
 
-    stream_t = everywhere(stream.T, Z).reshape(128, 256)
-
-    def scaled(weight, layer):
-        return (weight[layer].T.astype(f32) * norm_gain[layer]).astype(bf16)
-
-    by_feature = grouped_features(
-        jnp.concatenate(
-            [
-                scaled(w_branch, 0),
-                scaled(w_gate_branch, 0),
-                scaled(w_branch, 1),
-                scaled(w_gate_branch, 1),
-                w_out[0],
-                w_out[1],
-            ],
-            axis=0,
-        )
-    ).reshape(6, 32, 4, 128)
+    stream_t = everywhere(stream.T, Z).reshape(128, 2, 128).transpose(1, 0, 2)
+
+    def scaled(weight):
+        return (weight.transpose(0, 2, 1).astype(f32) * norm_gain[:, None]).astype(bf16)
+
+    by_feature = [
+        grouped_features(weight.reshape(64, 512)).reshape(2, 32, 4, 128)
+        for weight in (scaled(w_branch), scaled(w_gate_branch), w_out)
+    ]
+    w_first = jnp.concatenate([by_feature[0][0], by_feature[1][0]]).reshape(64, 512)
+    place = lax.axis_index("y") * 128 + zl * 64 + lax.broadcasted_iota(jnp.int32, (64, 512), 0)
+    kept_rows = (place == lax.broadcasted_iota(jnp.int32, (64, 512), 1)).astype(bf16)
+    w_first = jnp.concatenate([w_first, kept_rows])
+    second_weights = jnp.stack([by_feature[0][1], by_feature[1][1]])
     gate_rows = (
         jnp.stack([w_in_gate, w_rec_gate], axis=1)
         .reshape(LAYERS, 2, 2, 128, 32)
@@ -149,40 +146,74 @@
     earlier = earlier.reshape(LAYERS, 4, 8, 32).transpose(1, 0, 2, 3).reshape(4, -1)
     decay = jnp.broadcast_to(jax.nn.log_sigmoid(decay_param).reshape(1, -1), (4, 64))
     small = jnp.concatenate(
-        parts_of(earlier)
-        + parts_of(decay)
-        + [
+        parts_of(earlier) + parts_of(decay) + [jnp.zeros((4, 64), bf16)], axis=1
+    ).reshape(4, 14, 128)
+    windows = jnp.concatenate(
+        [
             history.reshape(LAYERS, 4, 8, depth, 32).transpose(1, 0, 3, 2, 4).reshape(4, -1),
             jnp.broadcast_to(conv_taps.reshape(1, -1), (4, 256)),
-            jnp.zeros((4, 64), bf16),
-        ],
-        axis=1,
-    ).reshape(4, 28, 128)
+        ],
+        axis=1,
+    ).reshape(4, 14, 128)
+
+    def for_each(rows):
+        return jnp.broadcast_to(rows.reshape(1, -1, 128), (4, rows.size // 128, 128))
+
+    shared = jnp.concatenate(
+        [
+            by_feature[2][0].transpose(1, 0, 2),
+            second_weights.transpose(2, 0, 1, 3).reshape(4, 64, 128),
+            for_each(windows),
+        ],
+        axis=1,
+    )
+    shared = traded(shared, ZQ)
+    partner = jnp.where(upper, shared[1][96:], shared[3][96:]).reshape(4, 14, 128)
+    shared = counted_back([piece[:96] for piece in shared], ZQ)
     near = jnp.concatenate(
         [
-            by_feature[:2].transpose(2, 0, 1, 3).reshape(4, 64, 128),
-            by_feature[5].transpose(1, 0, 2),
-            jnp.broadcast_to(gate_rows[None], (4, 256, 128)),
-            jnp.broadcast_to(
-                by_feature[2:5].transpose(2, 0, 1, 3).reshape(1, 384, 128), (4, 384, 128)
-            ),
+            for_each(gate_rows[:128]),
+            for_each(jnp.concatenate([piece[:32] for piece in shared])),
             small,
-        ],
-        axis=1,
-    )
-    near = in_order(traded(near, "y"), "y")
-    w_first = near[:, :64].reshape(4, 2, 32, 128).transpose(1, 0, 2, 3).reshape(2, 128, 128)
-    w_last = near[:, 64:96].reshape(128, 128)
-    gates = (
-        near[:, 96:352]
-        .reshape(4, LAYERS, 2, 2, 32, 128)
-        .transpose(1, 2, 3, 0, 4, 5)
-        .reshape(LAYERS, 2, 2, 128, 128)
-    )
-    middle = (
-        near[:, 352:736].reshape(4, 4, 3, 32, 128).transpose(1, 2, 0, 3, 4).reshape(4, 384, 128)
-    )
-    small = near[:, 736:].reshape(4, 3584)
+            jnp.where(upper, partner, windows),
+            jnp.where(upper, windows, partner),
+        ],
+        axis=1,
+    )
+    near, w_first = lax.optimization_barrier((near, w_first))
+    near = jnp.concatenate([for_each(stream_t), near], axis=1)
+    near = exchange(near, "y")
+    stream_t = near[:, :256].reshape(4, 2, 128, 128).transpose(1, 0, 2, 3).reshape(2, 512, 128)
+
+    def gates_of(rows):
+        return (
+            rows.reshape(4, 2, 2, 32, 128).transpose(1, 2, 0, 3, 4).reshape(2, 2, 128, 128)
+        )
+
+    gates = gates_of(near[:, 256:384])
+    w_mid = (
+        near[:, 384:512].reshape(4, 4, 32, 128).transpose(1, 0, 2, 3).reshape(512, 128)
+    )
+    small = near[:, 512:526].reshape(4, 1792)
+    windows = near[:, 526:].reshape(4, 2, 1792)
+    later_rows = jnp.concatenate(
+        [
+            for_each(gate_rows[128:]),
+            for_each(jnp.concatenate([piece[32:] for piece in shared])),
+            by_feature[2][1].transpose(1, 0, 2),
+        ],
+        axis=1,
+    )
+    later_rows = jnp.stack(counted_back(traded(later_rows, "y"), "y"))
+    gates_second = gates_of(later_rows[:, :128])
+    w_second = (
+        later_rows[:, 128:384]
+        .reshape(4, 4, 2, 32, 128)
+        .transpose(1, 2, 0, 3, 4)
+        .reshape(1024, 128)
+    )
+    w_last = later_rows[:, 384:].reshape(128, 128)
+
     earlier_rows = (
         whole_of(small[:, :512], small[:, 512:1024], small[:, 1024:1536])
         .reshape(4, LAYERS, 8, 32)
@@ -195,45 +226,36 @@
         .transpose(1, 0, 2)
         .reshape(LAYERS, 1, 128)
     )
-    windows = jnp.concatenate(
-        [
-            small[:, 1728:3264].reshape(4, 48, 32).transpose(1, 0, 2).reshape(48, 128),
-            small[:, 3264:3520].reshape(4, 8, 32).transpose(1, 0, 2).reshape(8, 128),
-        ],
-        axis=0,
-    )
-    partner = passed(windows, "zl", 1)
-    windows = jnp.concatenate(
-        [jnp.where(upper, partner, windows), jnp.where(upper, windows, partner)], axis=1
-    ).astype(f32)
-    history_rows = windows[:48].reshape(LAYERS, depth, 8, 256)
-    taps = windows[48:].reshape(LAYERS, TAPS, 256)
-
-    middle = in_order(traded(middle, ZQ), ZQ)
-    w_second = middle[:, :256].reshape(1024, 128)
-    w_mid = middle[:, 256:].reshape(512, 128)
-
-    stream_rows = stream_t.T.reshape(8, 4, 8, 128).transpose(1, 0, 2, 3)
-    products = [
-        contract(stream_t, 0, w_first[kind], 1)
-        .astype(bf16)
-        .reshape(8, 4, 8, 128)
-        .transpose(1, 0, 2, 3)
-        for kind in range(2)
-    ]
-    sent = jnp.stack(
-        [
-            jnp.stack([products[0], jnp.where(upper, stream_rows, products[1])], axis=2),
-            jnp.stack([products[0], jnp.where(upper, products[1], stream_rows)], axis=2),
-        ]
-    )
-    came = exchange(sent.reshape(64, 16, 128), PAIRED_PLANE).reshape(2, 32, 2, 8, 128)
-    branch = came[:, :, 0].astype(f32).sum(axis=1)
-    branch = jnp.concatenate([branch[0], branch[1]], axis=1)
-    rows = jnp.where(upper, came[0, :, 1], came[1, :, 1])
-    gate_in = jnp.where(upper, came[1, :, 1], came[0, :, 1]).astype(f32).sum(axis=0)
+    history_rows = (
+        windows[:, :, :1536]
+        .reshape(4, 2, LAYERS * depth * 8, 32)
+        .transpose(2, 1, 0, 3)
+        .reshape(LAYERS, depth, 8, 256)
+        .astype(f32)
+    )
+    taps = (
+        windows[:, :, 1536:]
+        .reshape(4, 2, LAYERS * TAPS, 32)
+        .transpose(2, 1, 0, 3)
+        .reshape(LAYERS, TAPS, 256)
+        .astype(f32)
+    )
+
+    products = jnp.concatenate(
+        [contract(stream_t[half], 0, w_first, 1).astype(bf16) for half in range(2)]
+    )
+    products = products.reshape(8, 4, 8, 128).transpose(1, 0, 2, 3).reshape(1, 32, 8, 128)
+    sent = jnp.broadcast_to(products, (2, 32, 8, 128)).reshape(64, 8, 128)
+    came = exchange(sent, PAIRED_PLANE).reshape(2, 4, 8, 8, 128)
+    later = (history_rows[1], taps[1], decay[1], earlier_rows[1], history)
+    came, w_mid, later = lax.optimization_barrier((came, w_mid, later))
+    summed = came.astype(f32).sum(axis=2)
+    branch = summed[:, :, :, :32].transpose(2, 0, 1, 3).reshape(8, 256)
+    gate_in = jnp.where(upper, summed[1], summed[0])[:, :, 32:64].transpose(1, 0, 2).reshape(8, 128)
+    rows = came[:, :, :, :, 64:]
     widened = rows.astype(f32)
-    squares = jnp.sum(jnp.sum(widened * widened, axis=0), axis=1, keepdims=True)
+    squares = jnp.sum(widened * widened, axis=(0, 1, 2, 4))[:, None]
+    rows = jnp.concatenate([rows[0], rows[1]], axis=3).reshape(32, 8, 128)
     scaling = lax.rsqrt(squares / D + epsilon)
     state_first, branch_first, readout = gated_step(
         (branch * scaling).astype(bf16),
@@ -241,19 +263,21 @@
         upper,
         history_rows[0],
         taps[0],
-        gates[0],
+        gates,
         decay[0],
         earlier_rows[0],
     )
-    sent = jnp.stack(
-        [jnp.broadcast_to(readout[None], (32, 8, 128)), rows], axis=1
-    )
+    sent = jnp.stack([jnp.broadcast_to(readout[None], (32, 8, 128)), rows], axis=1)
     came = exchange(sent.reshape(32, 16, 128), ZQ + DP).reshape(4, 8, 2, 8, 128)
     residual = came[0, :, 1].reshape(64, 128).astype(f32)
     came = came[:, :, 0].reshape(4, 64, 128)
     came = jnp.concatenate([came[at] for at in range(4)], axis=1)
     mixed = contract(came, 1, w_mid, 0).astype(bf16)
-    mixed = everywhere(mixed, "zh").astype(f32).sum(axis=0)
+    mixed = everywhere(mixed, "zh")
+    mixed, w_second, gates_second, w_last = lax.optimization_barrier(
+        (mixed, w_second, gates_second, w_last)
+    )
+    mixed = mixed.astype(f32).sum(axis=0)
     first = (mixed + residual).astype(bf16)
 
     products = contract(first, 1, w_second, 1).astype(bf16)
@@ -285,11 +309,11 @@
         (branch * scaling).astype(bf16),
         (came[2] * scaling).astype(bf16),
         upper,
-        history_rows[1],
-        taps[1],
-        gates[1],
-        decay[1],
-        earlier_rows[1],
+        later[0],
+        later[1],
+        gates_second,
+        later[2],
+        later[3],
     )
     sent = jnp.stack(
         [
@@ -300,19 +324,20 @@
     )
     came = exchange(sent.reshape(32, 16, 128), PLANE).reshape(32, 2, 8, 128)
     mixed = contract(w_last, 0, came[:, 0].reshape(256, 128), 1).astype(bf16)
+    mixed = mixed.reshape(32, 4, 256)
     own = lax.broadcasted_iota(jnp.int32, (4, 128), 0) + 4 * lax.axis_index(Z)
     own = (own == lax.broadcasted_iota(jnp.int32, (4, 128), 1)).astype(bf16)
     residual = contract(own, 1, came[:, 1].reshape(256, 128), 1)
-    second = exchange(mixed.reshape(32, 4, 256), Z).astype(f32).sum(axis=0)
+    second = exchange(mixed, Z).astype(f32).sum(axis=0)
     second = (second + residual).astype(bf16)
 
     kept = jnp.stack(
         [state_first, state_second, branch_first.astype(f32), branch_second.astype(f32)]
     )
     kept = kept.reshape(4, 8, 4, 32).transpose(2, 0, 1, 3).reshape(4, 8, 128)
-    kept = in_order(traded(kept, "y"), "y")
+    kept = jnp.stack(counted_back(traded(kept, "y"), "y"))
     kept = kept.reshape(4, 4, 8, 32).transpose(1, 0, 2, 3).reshape(2, LAYERS, 32, 32)
-    window = jnp.concatenate([history[:, :, 1:], kept[1].astype(bf16)[:, :, None]], axis=2)
+    window = jnp.concatenate([later[4][:, :, 1:], kept[1].astype(bf16)[:, :, None]], axis=2)
     return second.T, kept[0], window
 
 

time: 223 us -> 223 us (level)
  waiting for transfers between devices: 97.1 us -> 106 us
  local copies, waits for them, and re-layouts: 16.9 us -> 8.7 us
    all_to_all x7 -> x8, waiting for transfers between devices: 92 us -> 100 us  [exchange(): return lax.all_to_all(tiles, axes, 0, 0, tiled=True)]
    unnamed x44 -> x20, local copies, waits for them, and re-layouts: 5.71 us -> 0.07 us
    ppermute x10 -> x9, starting transfers between devices: 33 us -> 28 us  [passed(): lax.ppermute(piece, axis, [(at, (at + step) % count) for at in range(coun...]
    all_to_all x7 -> x8, starting transfers between devices: 63.3 us -> 66.5 us  [exchange(): return lax.all_to_all(tiles, axes, 0, 0, tiled=True)]
    unnamed x4 -> x0, other arithmetic: 3.06 us -> none
    slice x21 -> x31, local copies, waits for them, and re-layouts: 3.03 us -> 0.45 us  [the longest x1 0.1 us: both_blocks(): rows = jnp.concatenate([rows[0], rows[1]], axis=3).reshape(32, 8, 128)]
    ppermute x10 -> x9, waiting for transfers between devices: 5.01 us -> 5.82 us  [passed(): lax.ppermute(piece, axis, [(at, (at + step) % count) for at in range(coun...]
  transfers between devices with their start and end apart: 17 -> 17, of which waited for: 8 -> 10; matrix products, arithmetic and copies ran while one was open for 6% -> 3% of each run, Pallas kernels for 0% -> 0%
where the time goes in v5:
time: 223 us; the launch traced here: 222 us
  waiting for transfers between devices  106 us (48%)
  starting transfers between devices  94.5 us (42%)
  local copies, waits for them, and re-layouts  8.7 us (4%)
  other arithmetic  7.06 us (3%)
  matrix products  3.87 us (2%)
    all_to_all x8, waiting for transfers between devices, exchange(): return lax.all_to_all(tiles, axes, 0, 0, tiled=True)  100 us
    all_to_all x8, starting transfers between devices, exchange(): return lax.all_to_all(tiles, axes, 0, 0, tiled=True)  66.5 us
    ppermute x9, starting transfers between devices, passed(): lax.ppermute(piece, axis, [(at, (at + step) % count) for at in range(coun...  28 us
    ppermute x9, waiting for transfers between devices, passed(): lax.ppermute(piece, axis, [(at, (at + step) % count) for at in range(coun...  5.82 us
  transfers between devices with their start and end apart: 17, of which 10 were waited for; matrix products, arithmetic and copies ran while one was open for 3% of the time, Pallas kernels for 0%

profile of v5, /device:TPU:2, one launch (start us, length us, event | category | flops | bytes accessed | tf_op | source)
XLA Modules:
  0.0 222.2 jit_solution(5653635881036152353)
XLA Ops:
  0.7 0.7 broadcast_compare_fusion
  1.4 0.9 copy_bitcast_fusion.1
  2.4 0.8 reshape.452
  3.2 0.9 multiply_convert_fusion.1
  4.1 0.3 convolution_convert_fusion.2
  4.5 0.3 convolution_convert_fusion.3
  4.9 0.3 fusion
  5.4 5.2 %collective-permute-start.1 = (bf16[152,128]{1,0:T(8,128)(2,1)S(1)}, bf16[152,128]{1,0:T(8,128)(2,1)S(1)}, u32[]{:S(2)}, u32[]{:S(2)}) collective-permute-start(bf16[152,128]{1,0:T(8,128)(2,1)S(1)} %get-tuple-element.54), channel_id=1, source_target_pairs={{0,64},{32,96},{64,0},{96,32},{1,65},{33,97},{65,1},{97,33},{2,66}... | collective-permute-start | bytes 116744 | tf_op jit(solution)/shard_map/ppermute | solution.py:37
  10.6 3.3 %collective-permute-start = (bf16[152,128]{1,0:T(8,128)(2,1)S(1)}, bf16[152,128]{1,0:T(8,128)(2,1)S(1)}, u32[]{:S(2)}, u32[]{:S(2)}) collective-permute-start(bf16[152,128]{1,0:T(8,128)(2,1)S(1)} %get-tuple-element.52), channel_id=1, source_target_pairs={{0,96},{32,0},{64,32},{96,64},{1,97},{33,1},{65,33},{97,65},{2,98}... | collective-permute-start | bytes 116744 | tf_op jit(solution)/shard_map/ppermute | solution.py:37
  13.9 2.6 %collective-permute-start.2 = (bf16[152,128]{1,0:T(8,128)(2,1)S(1)}, bf16[152,128]{1,0:T(8,128)(2,1)S(1)}, u32[]{:S(2)}, u32[]{:S(2)}) collective-permute-start(bf16[152,128]{1,0:T(8,128)(2,1)S(1)} %get-tuple-element.53), channel_id=1, source_target_pairs={{0,32},{32,64},{64,96},{96,0},{1,33},{33,65},{65,97},{97,1},{2,34}... | collective-permute-start | bytes 116744 | tf_op jit(solution)/shard_map/ppermute | solution.py:37
  16.5 0.6 broadcast_in_dim.62
  17.1 27.4 %all-to-all-start = ((bf16[32,4,256]{2,1,0:T(4,128)(2,1)}), bf16[32,4,256]{2,1,0:T(4,128)(2,1)S(1)}, u32[]{:S(2)}, u32[]{:S(2)}) async-start(bf16[32,4,256]{2,1,0:T(4,128)(2,1)} %broadcast_in_dim.62), calls=%async_computation | async-start | bytes 131072 | tf_op jit(solution)/shard_map/all_to_all | solution.py:27
  45.6 0.4 concatenate.57
  45.9 23.6 %all-to-all-done = bf16[32,4,256]{2,1,0:T(4,128)(2,1)S(1)} async-done(((bf16[32,4,256]{2,1,0:T(4,128)(2,1)}), bf16[32,4,256]{2,1,0:T(4,128)(2,1)S(1)}, u32[]{:S(2)}, u32[]{:S(2)}) %all-to-all-start) | async-done | bytes 65568 | tf_op jit(solution)/shard_map/all_to_all | solution.py:27
  69.6 0.9 pad_maximum_fusion
  70.5 4.6 %all-to-all-start.1 = ((bf16[4,554,128]{2,1,0:T(8,128)(2,1)}), bf16[4,554,128]{2,1,0:T(8,128)(2,1)S(1)}, u32[]{:S(2)}, u32[]{:S(2)}) async-start(bf16[4,554,128]{2,1,0:T(8,128)(2,1)} %pad_maximum_fusion), calls=%async_computation.1 | async-start | bytes 1146880 | tf_op jit(solution)/shard_map/all_to_all | solution.py:27
  75.2 8.2 %all-to-all-done.1 = bf16[4,554,128]{2,1,0:T(8,128)(2,1)S(1)} async-done(((bf16[4,554,128]{2,1,0:T(8,128)(2,1)}), bf16[4,554,128]{2,1,0:T(8,128)(2,1)S(1)}, u32[]{:S(2)}, u32[]{:S(2)}) %all-to-all-start.1) | async-done | bytes 567328 | tf_op jit(solution)/shard_map/all_to_all | solution.py:27
  83.8 0.2 convolution_convert_fusion.5
  84.0 0.2 convolution_convert_fusion.6
  84.3 0.6 broadcast_in_dim.138
  84.9 6.0 %all-to-all-start.2 = ((bf16[64,8,128]{2,1,0:T(8,128)(2,1)}), bf16[64,8,128]{2,1,0:T(8,128)(2,1)S(1)}, u32[]{:S(2)}, u32[]{:S(2)}) async-start(bf16[64,8,128]{2,1,0:T(8,128)(2,1)} %bitcast.33), calls=%async_computation.2 | async-start | bytes 262144 | tf_op jit(solution)/shard_map/all_to_all | solution.py:27
  91.0 0.1 reshape.439
  91.2 0.1 squeeze.129
  92.0 0.1 squeeze.126
  92.3 6.1 %all-to-all-done.2 = bf16[64,8,128]{2,1,0:T(8,128)(2,1)S(1)} async-done(((bf16[64,8,128]{2,1,0:T(8,128)(2,1)}), bf16[64,8,128]{2,1,0:T(8,128)(2,1)S(1)}, u32[]{:S(2)}, u32[]{:S(2)}) %all-to-all-start.2) | async-done | bytes 131104 | tf_op jit(solution)/shard_map/all_to_all | solution.py:27
  98.6 0.2 multiply_reduce_fusion
  99.0 0.1 fusion.45
  99.2 0.1 fusion.46
  99.5 0.1 fusion.24
  99.6 0.2 fusion.77
  99.8 0.7 maximum_bitcast_fusion
  100.6 4.9 %all-to-all-start.3 = ((bf16[32,16,128]{2,1,0:T(8,128)(2,1)}), bf16[32,16,128]{2,1,0:T(8,128)(2,1)S(1)}, u32[]{:S(2)}, u32[]{:S(2)}) async-start(bf16[32,16,128]{2,1,0:T(8,128)(2,1)} %maximum_bitcast_fusion), calls=%async_computation.3 | async-start | bytes 262144 | tf_op jit(solution)/shard_map/all_to_all | solution.py:27
  105.6 7.4 %all-to-all-done.3 = bf16[32,16,128]{2,1,0:T(8,128)(2,1)S(1)} async-done(((bf16[32,16,128]{2,1,0:T(8,128)(2,1)}), bf16[32,16,128]{2,1,0:T(8,128)(2,1)S(1)}, u32[]{:S(2)}, u32[]{:S(2)}) %all-to-all-start.3) | async-done | bytes 131104 | tf_op jit(solution)/shard_map/all_to_all | solution.py:27
  113.0 0.2 convolution_convert_fusion.7
  113.2 0.7 broadcast_in_dim.139
  113.8 3.7 %all-to-all-start.4 = ((bf16[8,64,128]{2,1,0:T(8,128)(2,1)}), bf16[8,64,128]{2,1,0:T(8,128)(2,1)S(1)}, u32[]{:S(2)}, u32[]{:S(2)}) async-start(bf16[8,64,128]{2,1,0:T(8,128)(2,1)} %broadcast_in_dim.139), calls=%async_computation.4 | async-start | bytes 262144 | tf_op jit(solution)/shard_map/all_to_all | solution.py:27
  117.6 3.1 %collective-permute-start.3 = (bf16[416,128]{1,0:T(8,128)(2,1)S(1)}, bf16[416,128]{1,0:T(8,128)(2,1)S(1)}, u32[]{:S(2)}, u32[]{:S(2)}) collective-permute-start(bf16[416,128]{1,0:T(8,128)(2,1)S(1)} %get-tuple-element.41), channel_id=1, source_target_pairs={{0,24},{8,0},{16,8},{24,16},{1,25},{9,1},{17,9},{25,17},{2,26},{10... | collective-permute-start | bytes 319496 | tf_op jit(solution)/shard_map/ppermute | solution.py:37
  120.8 3.4 %collective-permute-start.4 = (bf16[416,128]{1,0:T(8,128)(2,1)S(1)}, bf16[416,128]{1,0:T(8,128)(2,1)S(1)}, u32[]{:S(2)}, u32[]{:S(2)}) collective-permute-start(bf16[416,128]{1,0:T(8,128)(2,1)S(1)} %get-tuple-element.43), channel_id=1, source_target_pairs={{0,16},{8,24},{16,0},{24,8},{1,17},{9,25},{17,1},{25,9},{2,18},{10... | collective-permute-start | bytes 319496 | tf_op jit(solution)/shard_map/ppermute | solution.py:37
  124.2 2.0 collective-permute-start.5
  126.2 2.8 %collective-permute-done.4 = bf16[416,128]{1,0:T(8,128)(2,1)S(1)} collective-permute-done((bf16[416,128]{1,0:T(8,128)(2,1)S(1)}, bf16[416,128]{1,0:T(8,128)(2,1)S(1)}, u32[]{:S(2)}, u32[]{:S(2)}) %collective-permute-start.4) | collective-permute-done | bytes 106528 | tf_op jit(solution)/shard_map/ppermute | solution.py:37
  129.0 3.0 %collective-permute-done.5 = bf16[416,128]{1,0:T(8,128)(2,1)S(1)} collective-permute-done((bf16[416,128]{1,0:T(8,128)(2,1)S(1)}, bf16[416,128]{1,0:T(8,128)(2,1)S(1)}, u32[]{:S(2)}, u32[]{:S(2)}) %collective-permute-start.5) | collective-permute-done | bytes 106528 | tf_op jit(solution)/shard_map/ppermute | solution.py:37
  132.2 14.7 %all-to-all-done.4 = bf16[8,64,128]{2,1,0:T(8,128)(2,1)S(1)} async-done(((bf16[8,64,128]{2,1,0:T(8,128)(2,1)}), bf16[8,64,128]{2,1,0:T(8,128)(2,1)S(1)}, u32[]{:S(2)}, u32[]{:S(2)}) %all-to-all-start.4) | async-done | bytes 131104 | tf_op jit(solution)/shard_map/all_to_all | solution.py:27
  146.9 0.2 convolution_convert_fusion
  147.3 0.7 copy.106
  148.0 6.1 %all-to-all-start.5 = ((bf16[32,32,128]{2,1,0:T(8,128)(2,1)}), bf16[32,32,128]{2,1,0:T(8,128)(2,1)S(1)}, u32[]{:S(2)}, u32[]{:S(2)}) async-start(bf16[32,32,128]{2,1,0:T(8,128)(2,1)} %bitcast.91), calls=%async_computation.5 | async-start | bytes 524288 | tf_op jit(solution)/shard_map/all_to_all | solution.py:27
  154.2 9.2 %all-to-all-done.5 = bf16[32,32,128]{2,1,0:T(8,128)(2,1)S(1)} async-done(((bf16[32,32,128]{2,1,0:T(8,128)(2,1)}), bf16[32,32,128]{2,1,0:T(8,128)(2,1)S(1)}, u32[]{:S(2)}, u32[]{:S(2)}) %all-to-all-start.5) | async-done | bytes 262176 | tf_op jit(solution)/shard_map/all_to_all | solution.py:27
  163.6 0.1 multiply_reduce_fusion.1
  163.8 0.1 fusion.48
  163.9 0.1 fusion.51
  164.3 0.1 fusion.12
  164.4 0.2 fusion.84
  164.8 3.6 %collective-permute-start.6 = (f32[8,128]{1,0:T(8,128)S(1)}, f32[8,128]{1,0:T(8,128)S(1)}, u32[]{:S(2)}, u32[]{:S(2)}) collective-permute-start(f32[8,128]{1,0:T(8,128)S(1)} %get-tuple-element.89), channel_id=1, source_target_pairs={{0,24},{8,0},{16,8},{24,16},{1,25},{9,1},{17,9},{25,17},{2,26},{10... | collective-permute-start | bytes 12296 | tf_op jit(solution)/shard_map/ppermute | solution.py:37
  168.4 2.9 %collective-permute-start.7 = (f32[8,128]{1,0:T(8,128)S(1)}, f32[8,128]{1,0:T(8,128)S(1)}, u32[]{:S(2)}, u32[]{:S(2)}) collective-permute-start(f32[8,128]{1,0:T(8,128)S(1)} %get-tuple-element.91), channel_id=1, source_target_pairs={{0,16},{8,24},{16,0},{24,8},{1,17},{9,25},{17,1},{25,9},{2,18},{10... | collective-permute-start | bytes 12296 | tf_op jit(solution)/shard_map/ppermute | solution.py:37
  171.4 2.0 collective-permute-start.8
  173.4 0.7 copy_bitcast_fusion
  174.0 7.5 %all-to-all-start.6 = ((bf16[32,16,128]{2,1,0:T(8,128)(2,1)}), bf16[32,16,128]{2,1,0:T(8,128)(2,1)S(1)}, u32[]{:S(2)}, u32[]{:S(2)}) async-start(bf16[32,16,128]{2,1,0:T(8,128)(2,1)} %copy_bitcast_fusion), calls=%async_computation.6 | async-start | bytes 262144 | tf_op jit(solution)/shard_map/all_to_all | solution.py:27
  181.9 6.2 %all-to-all-done.6 = bf16[32,16,128]{2,1,0:T(8,128)(2,1)S(1)} async-done(((bf16[32,16,128]{2,1,0:T(8,128)(2,1)}), bf16[32,16,128]{2,1,0:T(8,128)(2,1)S(1)}, u32[]{:S(2)}, u32[]{:S(2)}) %all-to-all-start.6) | async-done | bytes 131104 | tf_op jit(solution)/shard_map/all_to_all | solution.py:27
  188.1 0.2 convolution_convert_fusion.1
  188.3 0.6 reshape.433
  189.0 6.3 %all-to-all-start.7 = ((bf16[32,4,256]{2,1,0:T(4,128)(2,1)}), bf16[32,4,256]{2,1,0:T(4,128)(2,1)S(1)}, u32[]{:S(2)}, u32[]{:S(2)}) async-start(bf16[32,4,256]{2,1,0:T(4,128)(2,1)} %reshape.433), calls=%async_computation.7 | async-start | bytes 131072 | tf_op jit(solution)/shard_map/all_to_all | solution.py:27
  195.3 0.6 pad_maximum_fusion.16
  195.9 0.6 slice_bitcast_fusion.4
  196.6 24.8 %all-to-all-done.7 = bf16[32,4,256]{2,1,0:T(4,128)(2,1)S(1)} async-done(((bf16[32,4,256]{2,1,0:T(4,128)(2,1)}), bf16[32,4,256]{2,1,0:T(4,128)(2,1)S(1)}, u32[]{:S(2)}, u32[]{:S(2)}) %all-to-all-start.7) | async-done | bytes 65568 | tf_op jit(solution)/shard_map/all_to_all | solution.py:27
  221.4 0.8 fusion.25
  (185 shorter events, 4.6 us)
Async XLA Ops:
  0.6 4.3 %copy-start = (bf16[2,32,512]{2,1,0:T(8,128)(2,1)S(1)}, bf16[2,32,512]{2,1,0:T(8,128)(2,1)}, u32[]{:S(2)}) copy-start(bf16[2,32,512]{2,1,0:T(8,128)(2,1)} %param.23) | copy-start | bytes 196612
  4.9 11.5 %copy-start.6 = (bf16[256,4]{0,1:T(4,128)(2,1)S(1)}, bf16[256,4]{0,1:T(4,128)(2,1)}, u32[]{:S(2)}) copy-start(bf16[256,4]{0,1:T(4,128)(2,1)} %param.12) | copy-start | bytes 6148
  5.2 39.2 %copy-start.8 = (s32[32]{0:T(128)S(1)}, s32[32]{0:T(128)}, u32[]{:S(2)}) copy-start(s32[32]{0:T(128)} %param.13) | copy-start | bytes 388
  5.2 39.3 %copy-start.3 = (bf16[2,256,32]{1,2,0:T(8,128)(2,1)S(1)}, bf16[2,256,32]{1,2,0:T(8,128)(2,1)}, u32[]{:S(2)}) copy-start(bf16[2,256,32]{1,2,0:T(8,128)(2,1)} %param.21) | copy-start | bytes 98308
  5.3 39.3 %copy-start.4 = (bf16[2,256,32]{1,2,0:T(8,128)(2,1)S(1)}, bf16[2,256,32]{1,2,0:T(8,128)(2,1)}, u32[]{:S(2)}) copy-start(bf16[2,256,32]{1,2,0:T(8,128)(2,1)} %param.20) | copy-start | bytes 98308
  5.3 39.4 %copy-start.5 = (f32[2,32,32]{2,1,0:T(8,128)S(1)}, f32[2,32,32]{2,1,0:T(8,128)}, u32[]{:S(2)}) copy-start(f32[2,32,32]{2,1,0:T(8,128)} %param.14) | copy-start | bytes 24580
  5.3 39.6 %copy-start.7 = (f32[2,32]{1,0:T(2,128)S(1)}, f32[2,32]{1,0:T(2,128)}, u32[]{:S(2)}) copy-start(f32[2,32]{1,0:T(2,128)} %param.22) | copy-start | bytes 772
  5.4 40.0 %collective-permute-start.1 = (bf16[152,128]{1,0:T(8,128)(2,1)S(1)}, bf16[152,128]{1,0:T(8,128)(2,1)S(1)}, u32[]{:S(2)}, u32[]{:S(2)}) collective-permute-start(bf16[152,128]{1,0:T(8,128)(2,1)S(1)} %get-tuple-element.54), channel_id=1, source_target_pairs={{0,64},{32,96},{64,0},{96,32},{1,65},{33,97},{65,1},{97,33},{2,66}... | collective-permute-start | bytes 116744 | tf_op jit(solution)/shard_map/ppermute | solution.py:37
  10.6 34.8 %collective-permute-start = (bf16[152,128]{1,0:T(8,128)(2,1)S(1)}, bf16[152,128]{1,0:T(8,128)(2,1)S(1)}, u32[]{:S(2)}, u32[]{:S(2)}) collective-permute-start(bf16[152,128]{1,0:T(8,128)(2,1)S(1)} %get-tuple-element.52), channel_id=1, source_target_pairs={{0,96},{32,0},{64,32},{96,64},{1,97},{33,1},{65,33},{97,65},{2,98}... | collective-permute-start | bytes 116744 | tf_op jit(solution)/shard_map/ppermute | solution.py:37
  13.9 31.5 %collective-permute-start.2 = (bf16[152,128]{1,0:T(8,128)(2,1)S(1)}, bf16[152,128]{1,0:T(8,128)(2,1)S(1)}, u32[]{:S(2)}, u32[]{:S(2)}) collective-permute-start(bf16[152,128]{1,0:T(8,128)(2,1)S(1)} %get-tuple-element.53), channel_id=1, source_target_pairs={{0,32},{32,64},{64,96},{96,0},{1,33},{33,65},{65,97},{97,1},{2,34}... | collective-permute-start | bytes 116744 | tf_op jit(solution)/shard_map/ppermute | solution.py:37
  17.1 52.5 %all-to-all-start = ((bf16[32,4,256]{2,1,0:T(4,128)(2,1)}), bf16[32,4,256]{2,1,0:T(4,128)(2,1)S(1)}, u32[]{:S(2)}, u32[]{:S(2)}) async-start(bf16[32,4,256]{2,1,0:T(4,128)(2,1)} %broadcast_in_dim.62), calls=%async_computation | async-start | bytes 131072 | tf_op jit(solution)/shard_map/all_to_all | solution.py:27
  70.5 4.6 %copy-start.1 = (bf16[2,32,3,32]{3,1,2,0:T(8,128)(2,1)S(1)}, bf16[2,32,3,32]{3,1,2,0:T(8,128)(2,1)}, u32[]{:S(2)}) copy-start(bf16[2,32,3,32]{3,1,2,0:T(8,128)(2,1)} %param.15) | copy-start | bytes 36868
  70.5 12.9 %all-to-all-start.1 = ((bf16[4,554,128]{2,1,0:T(8,128)(2,1)}), bf16[4,554,128]{2,1,0:T(8,128)(2,1)S(1)}, u32[]{:S(2)}, u32[]{:S(2)}) async-start(bf16[4,554,128]{2,1,0:T(8,128)(2,1)} %pad_maximum_fusion), calls=%async_computation.1 | async-start | bytes 1146880 | tf_op jit(solution)/shard_map/all_to_all | solution.py:27
  75.2 79.0 %copy-start.2 = (bf16[2,32,3,32]{3,1,2,0:T(8,128)(2,1)}, bf16[2,32,3,32]{3,1,2,0:T(8,128)(2,1)S(1)}, u32[]{:S(2)}) copy-start(bf16[2,32,3,32]{3,1,2,0:T(8,128)(2,1)S(1)} %broadcast_select_fusion.2) | copy-start | bytes 36868
  84.9 13.5 %all-to-all-start.2 = ((bf16[64,8,128]{2,1,0:T(8,128)(2,1)}), bf16[64,8,128]{2,1,0:T(8,128)(2,1)S(1)}, u32[]{:S(2)}, u32[]{:S(2)}) async-start(bf16[64,8,128]{2,1,0:T(8,128)(2,1)} %bitcast.33), calls=%async_computation.2 | async-start | bytes 262144 | tf_op jit(solution)/shard_map/all_to_all | solution.py:27
  100.6 12.4 %all-to-all-start.3 = ((bf16[32,16,128]{2,1,0:T(8,128)(2,1)}), bf16[32,16,128]{2,1,0:T(8,128)(2,1)S(1)}, u32[]{:S(2)}, u32[]{:S(2)}) async-start(bf16[32,16,128]{2,1,0:T(8,128)(2,1)} %maximum_bitcast_fusion), calls=%async_computation.3 | async-start | bytes 262144 | tf_op jit(solution)/shard_map/all_to_all | solution.py:27
  113.8 33.1 %all-to-all-start.4 = ((bf16[8,64,128]{2,1,0:T(8,128)(2,1)}), bf16[8,64,128]{2,1,0:T(8,128)(2,1)S(1)}, u32[]{:S(2)}, u32[]{:S(2)}) async-start(bf16[8,64,128]{2,1,0:T(8,128)(2,1)} %broadcast_in_dim.139), calls=%async_computation.4 | async-start | bytes 262144 | tf_op jit(solution)/shard_map/all_to_all | solution.py:27
  117.6 8.5 %collective-permute-start.3 = (bf16[416,128]{1,0:T(8,128)(2,1)S(1)}, bf16[416,128]{1,0:T(8,128)(2,1)S(1)}, u32[]{:S(2)}, u32[]{:S(2)}) collective-permute-start(bf16[416,128]{1,0:T(8,128)(2,1)S(1)} %get-tuple-element.41), channel_id=1, source_target_pairs={{0,24},{8,0},{16,8},{24,16},{1,25},{9,1},{17,9},{25,17},{2,26},{10... | collective-permute-start | bytes 319496 | tf_op jit(solution)/shard_map/ppermute | solution.py:37
  120.8 8.2 %collective-permute-start.4 = (bf16[416,128]{1,0:T(8,128)(2,1)S(1)}, bf16[416,128]{1,0:T(8,128)(2,1)S(1)}, u32[]{:S(2)}, u32[]{:S(2)}) collective-permute-start(bf16[416,128]{1,0:T(8,128)(2,1)S(1)} %get-tuple-element.43), channel_id=1, source_target_pairs={{0,16},{8,24},{16,0},{24,8},{1,17},{9,25},{17,1},{25,9},{2,18},{10... | collective-permute-start | bytes 319496 | tf_op jit(solution)/shard_map/ppermute | solution.py:37
  124.2 7.8 %collective-permute-start.5 = (bf16[416,128]{1,0:T(8,128)(2,1)S(1)}, bf16[416,128]{1,0:T(8,128)(2,1)S(1)}, u32[]{:S(2)}, u32[]{:S(2)}) collective-permute-start(bf16[416,128]{1,0:T(8,128)(2,1)S(1)} %get-tuple-element.42), channel_id=1, source_target_pairs={{0,8},{8,16},{16,24},{24,0},{1,9},{9,17},{17,25},{25,1},{2,10},{10... | collective-permute-start | bytes 319496 | tf_op jit(solution)/shard_map/ppermute | solution.py:37
  148.0 15.5 %all-to-all-start.5 = ((bf16[32,32,128]{2,1,0:T(8,128)(2,1)}), bf16[32,32,128]{2,1,0:T(8,128)(2,1)S(1)}, u32[]{:S(2)}, u32[]{:S(2)}) async-start(bf16[32,32,128]{2,1,0:T(8,128)(2,1)} %bitcast.91), calls=%async_computation.5 | async-start | bytes 524288 | tf_op jit(solution)/shard_map/all_to_all | solution.py:27
  164.8 16.7 %collective-permute-start.6 = (f32[8,128]{1,0:T(8,128)S(1)}, f32[8,128]{1,0:T(8,128)S(1)}, u32[]{:S(2)}, u32[]{:S(2)}) collective-permute-start(f32[8,128]{1,0:T(8,128)S(1)} %get-tuple-element.89), channel_id=1, source_target_pairs={{0,24},{8,0},{16,8},{24,16},{1,25},{9,1},{17,9},{25,17},{2,26},{10... | collective-permute-start | bytes 12296 | tf_op jit(solution)/shard_map/ppermute | solution.py:37
  168.4 13.1 %collective-permute-start.7 = (f32[8,128]{1,0:T(8,128)S(1)}, f32[8,128]{1,0:T(8,128)S(1)}, u32[]{:S(2)}, u32[]{:S(2)}) collective-permute-start(f32[8,128]{1,0:T(8,128)S(1)} %get-tuple-element.91), channel_id=1, source_target_pairs={{0,16},{8,24},{16,0},{24,8},{1,17},{9,25},{17,1},{25,9},{2,18},{10... | collective-permute-start | bytes 12296 | tf_op jit(solution)/shard_map/ppermute | solution.py:37
  171.4 10.2 %collective-permute-start.8 = (f32[8,128]{1,0:T(8,128)S(1)}, f32[8,128]{1,0:T(8,128)S(1)}, u32[]{:S(2)}, u32[]{:S(2)}) collective-permute-start(f32[8,128]{1,0:T(8,128)S(1)} %get-tuple-element.90), channel_id=1, source_target_pairs={{0,8},{8,16},{16,24},{24,0},{1,9},{9,17},{17,25},{25,1},{2,10},{10... | collective-permute-start | bytes 12296 | tf_op jit(solution)/shard_map/ppermute | solution.py:37
  173.4 21.9 %slice-start = ((bf16[2,32,3,32]{3,1,2,0:T(8,128)(2,1)}), bf16[2,32,2,32]{3,1,2,0:T(8,128)(2,1)S(1)}, s32[]{:S(2)}) async-start(bf16[2,32,3,32]{3,1,2,0:T(8,128)(2,1)} %copy-done.2), calls=%async_computation.8 | async-start | bytes 65536 | tf_op jit(solution)/shard_map/slice | solution.py:340
  174.0 14.1 %all-to-all-start.6 = ((bf16[32,16,128]{2,1,0:T(8,128)(2,1)}), bf16[32,16,128]{2,1,0:T(8,128)(2,1)S(1)}, u32[]{:S(2)}, u32[]{:S(2)}) async-start(bf16[32,16,128]{2,1,0:T(8,128)(2,1)} %copy_bitcast_fusion), calls=%async_computation.6 | async-start | bytes 262144 | tf_op jit(solution)/shard_map/all_to_all | solution.py:27
  189.0 32.4 %all-to-all-start.7 = ((bf16[32,4,256]{2,1,0:T(4,128)(2,1)}), bf16[32,4,256]{2,1,0:T(4,128)(2,1)S(1)}, u32[]{:S(2)}, u32[]{:S(2)}) async-start(bf16[32,4,256]{2,1,0:T(4,128)(2,1)} %reshape.433), calls=%async_computation.7 | async-start | bytes 131072 | tf_op jit(solution)/shard_map/all_to_all | solution.py:27

commit v6 on v5

--- a/solution.py
+++ b/solution.py
@@ -27,9 +27,20 @@
     return lax.all_to_all(tiles, axes, 0, 0, tiled=True)
 
 
+def exchange_far(tiles, axes):
+    count = lax.axis_size(axes)
+    first = count * 3 // 4
+    order = [(first + at) % count for at in range(count)]
+    tiles = lax.all_to_all(
+        jnp.roll(tiles, -first, axis=0), axes, 0, 0, axis_index_groups=[order], tiled=True
+    )
+    return jnp.roll(tiles, first, axis=0)
+
+
 def everywhere(array, axes):
     count = lax.axis_size(axes)
-    return exchange(jnp.broadcast_to(array[None], (count, *array.shape)), axes)
+    tiles = jnp.broadcast_to(array[None], (count, *array.shape))
+    return exchange_far(tiles, axes)
 
 
 def passed(piece, axis, step):
@@ -328,7 +339,7 @@
     own = lax.broadcasted_iota(jnp.int32, (4, 128), 0) + 4 * lax.axis_index(Z)
     own = (own == lax.broadcasted_iota(jnp.int32, (4, 128), 1)).astype(bf16)
     residual = contract(own, 1, came[:, 1].reshape(256, 128), 1)
-    second = exchange(mixed, Z).astype(f32).sum(axis=0)
+    second = exchange_far(mixed, Z).astype(f32).sum(axis=0)
     second = (second + residual).astype(bf16)
 
     kept = jnp.stack(

time: 223 us -> 214 us (0.960)
  waiting for transfers between devices: 106 us -> 78.1 us
  starting transfers between devices: 94.5 us -> 113 us
    all_to_all x8 -> x5, waiting for transfers between devices: 100 us -> 37.3 us  [exchange(): return lax.all_to_all(tiles, axes, 0, 0, tiled=True)]
    all_to_all x0 -> x3, starting transfers between devices: none -> 56.1 us  [exchange_far(): lax.all_to_all(jnp.roll(tiles, -first, axis=0), axes, 0, 0, axis_index_gr...]
    all_to_all x8 -> x5, starting transfers between devices: 66.5 us -> 29 us  [exchange(): return lax.all_to_all(tiles, axes, 0, 0, tiled=True)]
    all_to_all x0 -> x3, waiting for transfers between devices: none -> 35 us  [exchange_far(): lax.all_to_all(jnp.roll(tiles, -first, axis=0), axes, 0, 0, axis_index_gr...]
where the time goes in v6:
time: 214 us; the launch traced here: 213 us
  starting transfers between devices  113 us (53%)
  waiting for transfers between devices  78.1 us (36%)
  other arithmetic  9.12 us (4%)
  local copies, waits for them, and re-layouts  6.89 us (3%)
  matrix products  3.87 us (2%)
    all_to_all x3, starting transfers between devices, exchange_far(): lax.all_to_all(jnp.roll(tiles, -first, axis=0), axes, 0, 0, axis_index_gr...  56.1 us
    all_to_all x5, waiting for transfers between devices, exchange(): return lax.all_to_all(tiles, axes, 0, 0, tiled=True)  37.3 us
    all_to_all x3, waiting for transfers between devices, exchange_far(): lax.all_to_all(jnp.roll(tiles, -first, axis=0), axes, 0, 0, axis_index_gr...  35 us
    all_to_all x5, starting transfers between devices, exchange(): return lax.all_to_all(tiles, axes, 0, 0, tiled=True)  29 us
    ppermute x9, starting transfers between devices, passed(): lax.ppermute(piece, axis, [(at, (at + step) % count) for at in range(coun...  28 us
    ppermute x9, waiting for transfers between devices, passed(): lax.ppermute(piece, axis, [(at, (at + step) % count) for at in range(coun...  5.82 us
  transfers between devices with their start and end apart: 17, of which 10 were waited for; matrix products, arithmetic and copies ran while one was open for 3% of the time, Pallas kernels for 0%

profile of v6, /device:TPU:2, one launch (start us, length us, event | category | flops | bytes accessed | tf_op | source)
XLA Modules:
  0.0 213.1 jit_solution(16717410806266583367)
XLA Ops:
  0.7 0.7 broadcast_compare_fusion
  1.4 0.9 copy_bitcast_fusion.1
  2.4 0.8 reshape.451
  3.2 0.9 multiply_convert_fusion.1
  4.1 0.3 convolution_convert_fusion.2
  4.5 0.3 convolution_convert_fusion.3
  4.9 0.3 fusion
  5.4 5.2 %collective-permute-start.1 = (bf16[152,128]{1,0:T(8,128)(2,1)S(1)}, bf16[152,128]{1,0:T(8,128)(2,1)S(1)}, u32[]{:S(2)}, u32[]{:S(2)}) collective-permute-start(bf16[152,128]{1,0:T(8,128)(2,1)S(1)} %get-tuple-element.54), channel_id=1, source_target_pairs={{0,64},{32,96},{64,0},{96,32},{1,65},{33,97},{65,1},{97,33},{2,66}... | collective-permute-start | bytes 116744 | tf_op jit(solution)/shard_map/ppermute | solution.py:48
  10.6 3.3 %collective-permute-start = (bf16[152,128]{1,0:T(8,128)(2,1)S(1)}, bf16[152,128]{1,0:T(8,128)(2,1)S(1)}, u32[]{:S(2)}, u32[]{:S(2)}) collective-permute-start(bf16[152,128]{1,0:T(8,128)(2,1)S(1)} %get-tuple-element.52), channel_id=1, source_target_pairs={{0,96},{32,0},{64,32},{96,64},{1,97},{33,1},{65,33},{97,65},{2,98}... | collective-permute-start | bytes 116744 | tf_op jit(solution)/shard_map/ppermute | solution.py:48
  13.9 2.6 %collective-permute-start.2 = (bf16[152,128]{1,0:T(8,128)(2,1)S(1)}, bf16[152,128]{1,0:T(8,128)(2,1)S(1)}, u32[]{:S(2)}, u32[]{:S(2)}) collective-permute-start(bf16[152,128]{1,0:T(8,128)(2,1)S(1)} %get-tuple-element.53), channel_id=1, source_target_pairs={{0,32},{32,64},{64,96},{96,0},{1,33},{33,65},{65,97},{97,1},{2,34}... | collective-permute-start | bytes 116744 | tf_op jit(solution)/shard_map/ppermute | solution.py:48
  16.5 0.7 pad_maximum_fusion.14
  17.2 27.7 %all-to-all-start = ((bf16[32,4,256]{2,1,0:T(4,128)(2,1)}), bf16[32,4,256]{2,1,0:T(4,128)(2,1)S(1)}, u32[]{:S(2)}, u32[]{:S(2)}) async-start(bf16[32,4,256]{2,1,0:T(4,128)(2,1)} %pad_maximum_fusion.14), calls=%async_computation | async-start | bytes 131072 | tf_op jit(solution)/shard_map/all_to_all | solution.py:34
  46.0 0.4 concatenate.81
  46.3 13.6 %all-to-all-done = bf16[32,4,256]{2,1,0:T(4,128)(2,1)S(1)} async-done(((bf16[32,4,256]{2,1,0:T(4,128)(2,1)}), bf16[32,4,256]{2,1,0:T(4,128)(2,1)S(1)}, u32[]{:S(2)}, u32[]{:S(2)}) %all-to-all-start) | async-done | bytes 65568 | tf_op jit(solution)/shard_map/all_to_all | solution.py:34
  60.1 0.9 pad_maximum_fusion
  60.9 4.6 %all-to-all-start.1 = ((bf16[4,554,128]{2,1,0:T(8,128)(2,1)}), bf16[4,554,128]{2,1,0:T(8,128)(2,1)S(1)}, u32[]{:S(2)}, u32[]{:S(2)}) async-start(bf16[4,554,128]{2,1,0:T(8,128)(2,1)} %pad_maximum_fusion), calls=%async_computation.1 | async-start | bytes 1146880 | tf_op jit(solution)/shard_map/all_to_all | solution.py:27
  65.6 8.2 %all-to-all-done.1 = bf16[4,554,128]{2,1,0:T(8,128)(2,1)S(1)} async-done(((bf16[4,554,128]{2,1,0:T(8,128)(2,1)}), bf16[4,554,128]{2,1,0:T(8,128)(2,1)S(1)}, u32[]{:S(2)}, u32[]{:S(2)}) %all-to-all-start.1) | async-done | bytes 567328 | tf_op jit(solution)/shard_map/all_to_all | solution.py:27
  74.2 0.2 convolution_convert_fusion.5
  74.5 0.2 convolution_convert_fusion.6
  74.7 0.6 broadcast_in_dim.133
  75.4 6.9 %all-to-all-start.2 = ((bf16[64,8,128]{2,1,0:T(8,128)(2,1)}), bf16[64,8,128]{2,1,0:T(8,128)(2,1)S(1)}, u32[]{:S(2)}, u32[]{:S(2)}) async-start(bf16[64,8,128]{2,1,0:T(8,128)(2,1)} %bitcast.33), calls=%async_computation.2 | async-start | bytes 262144 | tf_op jit(solution)/shard_map/all_to_all | solution.py:27
  82.3 0.1 reshape.438
  82.5 0.1 squeeze.129
  83.2 0.1 squeeze.126
  83.6 6.1 %all-to-all-done.2 = bf16[64,8,128]{2,1,0:T(8,128)(2,1)S(1)} async-done(((bf16[64,8,128]{2,1,0:T(8,128)(2,1)}), bf16[64,8,128]{2,1,0:T(8,128)(2,1)S(1)}, u32[]{:S(2)}, u32[]{:S(2)}) %all-to-all-start.2) | async-done | bytes 131104 | tf_op jit(solution)/shard_map/all_to_all | solution.py:27
  89.9 0.2 multiply_reduce_fusion
  90.3 0.1 fusion.45
  90.4 0.1 fusion.46
  90.8 0.1 fusion.24
  90.9 0.2 fusion.77
  91.1 0.7 maximum_bitcast_fusion
  91.9 4.9 %all-to-all-start.3 = ((bf16[32,16,128]{2,1,0:T(8,128)(2,1)}), bf16[32,16,128]{2,1,0:T(8,128)(2,1)S(1)}, u32[]{:S(2)}, u32[]{:S(2)}) async-start(bf16[32,16,128]{2,1,0:T(8,128)(2,1)} %maximum_bitcast_fusion), calls=%async_computation.3 | async-start | bytes 262144 | tf_op jit(solution)/shard_map/all_to_all | solution.py:27
  96.9 7.4 %all-to-all-done.3 = bf16[32,16,128]{2,1,0:T(8,128)(2,1)S(1)} async-done(((bf16[32,16,128]{2,1,0:T(8,128)(2,1)}), bf16[32,16,128]{2,1,0:T(8,128)(2,1)S(1)}, u32[]{:S(2)}, u32[]{:S(2)}) %all-to-all-start.3) | async-done | bytes 131104 | tf_op jit(solution)/shard_map/all_to_all | solution.py:27
  104.3 0.2 convolution_convert_fusion.7
  104.5 0.7 pad_maximum_fusion.7
  105.1 13.1 %all-to-all-start.4 = ((bf16[8,64,128]{2,1,0:T(8,128)(2,1)}), bf16[8,64,128]{2,1,0:T(8,128)(2,1)S(1)}, u32[]{:S(2)}, u32[]{:S(2)}) async-start(bf16[8,64,128]{2,1,0:T(8,128)(2,1)} %pad_maximum_fusion.7), calls=%async_computation.4 | async-start | bytes 262144 | tf_op jit(solution)/shard_map/all_to_all | solution.py:34
  118.4 3.1 %collective-permute-start.3 = (bf16[416,128]{1,0:T(8,128)(2,1)S(1)}, bf16[416,128]{1,0:T(8,128)(2,1)S(1)}, u32[]{:S(2)}, u32[]{:S(2)}) collective-permute-start(bf16[416,128]{1,0:T(8,128)(2,1)S(1)} %get-tuple-element.41), channel_id=1, source_target_pairs={{0,24},{8,0},{16,8},{24,16},{1,25},{9,1},{17,9},{25,17},{2,26},{10... | collective-permute-start | bytes 319496 | tf_op jit(solution)/shard_map/ppermute | solution.py:48
  121.5 3.4 %collective-permute-start.4 = (bf16[416,128]{1,0:T(8,128)(2,1)S(1)}, bf16[416,128]{1,0:T(8,128)(2,1)S(1)}, u32[]{:S(2)}, u32[]{:S(2)}) collective-permute-start(bf16[416,128]{1,0:T(8,128)(2,1)S(1)} %get-tuple-element.43), channel_id=1, source_target_pairs={{0,16},{8,24},{16,0},{24,8},{1,17},{9,25},{17,1},{25,9},{2,18},{10... | collective-permute-start | bytes 319496 | tf_op jit(solution)/shard_map/ppermute | solution.py:48
  124.9 2.0 collective-permute-start.5
  126.9 2.7 %collective-permute-done.4 = bf16[416,128]{1,0:T(8,128)(2,1)S(1)} collective-permute-done((bf16[416,128]{1,0:T(8,128)(2,1)S(1)}, bf16[416,128]{1,0:T(8,128)(2,1)S(1)}, u32[]{:S(2)}, u32[]{:S(2)}) %collective-permute-start.4) | collective-permute-done | bytes 106528 | tf_op jit(solution)/shard_map/ppermute | solution.py:48
  129.6 3.2 %collective-permute-done.5 = bf16[416,128]{1,0:T(8,128)(2,1)S(1)} collective-permute-done((bf16[416,128]{1,0:T(8,128)(2,1)S(1)}, bf16[416,128]{1,0:T(8,128)(2,1)S(1)}, u32[]{:S(2)}, u32[]{:S(2)}) %collective-permute-start.5) | collective-permute-done | bytes 106528 | tf_op jit(solution)/shard_map/ppermute | solution.py:48
  132.9 6.5 %all-to-all-done.4 = bf16[8,64,128]{2,1,0:T(8,128)(2,1)S(1)} async-done(((bf16[8,64,128]{2,1,0:T(8,128)(2,1)}), bf16[8,64,128]{2,1,0:T(8,128)(2,1)S(1)}, u32[]{:S(2)}, u32[]{:S(2)}) %all-to-all-start.4) | async-done | bytes 131104 | tf_op jit(solution)/shard_map/all_to_all | solution.py:34
  139.6 0.2 convolution_convert_fusion
  139.9 0.7 copy.106
  140.6 5.0 %all-to-all-start.5 = ((bf16[32,32,128]{2,1,0:T(8,128)(2,1)}), bf16[32,32,128]{2,1,0:T(8,128)(2,1)S(1)}, u32[]{:S(2)}, u32[]{:S(2)}) async-start(bf16[32,32,128]{2,1,0:T(8,128)(2,1)} %bitcast.91), calls=%async_computation.5 | async-start | bytes 524288 | tf_op jit(solution)/shard_map/all_to_all | solution.py:27
  145.8 9.3 %all-to-all-done.5 = bf16[32,32,128]{2,1,0:T(8,128)(2,1)S(1)} async-done(((bf16[32,32,128]{2,1,0:T(8,128)(2,1)}), bf16[32,32,128]{2,1,0:T(8,128)(2,1)S(1)}, u32[]{:S(2)}, u32[]{:S(2)}) %all-to-all-start.5) | async-done | bytes 262176 | tf_op jit(solution)/shard_map/all_to_all | solution.py:27
  155.2 0.1 multiply_reduce_fusion.1
  155.4 0.1 fusion.48
  155.5 0.1 fusion.51
  155.9 0.1 fusion.12
  156.0 0.2 fusion.84
  156.4 3.3 %collective-permute-start.6 = (f32[8,128]{1,0:T(8,128)S(1)}, f32[8,128]{1,0:T(8,128)S(1)}, u32[]{:S(2)}, u32[]{:S(2)}) collective-permute-start(f32[8,128]{1,0:T(8,128)S(1)} %get-tuple-element.89), channel_id=1, source_target_pairs={{0,24},{8,0},{16,8},{24,16},{1,25},{9,1},{17,9},{25,17},{2,26},{10... | collective-permute-start | bytes 12296 | tf_op jit(solution)/shard_map/ppermute | solution.py:48
  159.8 3.2 %collective-permute-start.7 = (f32[8,128]{1,0:T(8,128)S(1)}, f32[8,128]{1,0:T(8,128)S(1)}, u32[]{:S(2)}, u32[]{:S(2)}) collective-permute-start(f32[8,128]{1,0:T(8,128)S(1)} %get-tuple-element.91), channel_id=1, source_target_pairs={{0,16},{8,24},{16,0},{24,8},{1,17},{9,25},{17,1},{25,9},{2,18},{10... | collective-permute-start | bytes 12296 | tf_op jit(solution)/shard_map/ppermute | solution.py:48
  163.0 2.0 collective-permute-start.8
  165.0 0.7 copy_bitcast_fusion
  165.6 7.6 %all-to-all-start.6 = ((bf16[32,16,128]{2,1,0:T(8,128)(2,1)}), bf16[32,16,128]{2,1,0:T(8,128)(2,1)S(1)}, u32[]{:S(2)}, u32[]{:S(2)}) async-start(bf16[32,16,128]{2,1,0:T(8,128)(2,1)} %copy_bitcast_fusion), calls=%async_computation.6 | async-start | bytes 262144 | tf_op jit(solution)/shard_map/all_to_all | solution.py:27
  173.6 6.2 %all-to-all-done.6 = bf16[32,16,128]{2,1,0:T(8,128)(2,1)S(1)} async-done(((bf16[32,16,128]{2,1,0:T(8,128)(2,1)}), bf16[32,16,128]{2,1,0:T(8,128)(2,1)S(1)}, u32[]{:S(2)}, u32[]{:S(2)}) %all-to-all-start.6) | async-done | bytes 131104 | tf_op jit(solution)/shard_map/all_to_all | solution.py:27
  179.9 0.2 convolution_convert_fusion.1
  180.1 0.7 pad_maximum_fusion.20
  180.8 15.3 %all-to-all-start.7 = ((bf16[32,4,256]{2,1,0:T(4,128)(2,1)}), bf16[32,4,256]{2,1,0:T(4,128)(2,1)S(1)}, u32[]{:S(2)}, u32[]{:S(2)}) async-start(bf16[32,4,256]{2,1,0:T(4,128)(2,1)} %pad_maximum_fusion.20), calls=%async_computation.7 | async-start | bytes 131072 | tf_op jit(solution)/shard_map/all_to_all | solution.py:34
  196.1 0.6 pad_maximum_fusion.21
  196.7 0.6 slice_bitcast_fusion.4
  197.3 14.9 %all-to-all-done.7 = bf16[32,4,256]{2,1,0:T(4,128)(2,1)S(1)} async-done(((bf16[32,4,256]{2,1,0:T(4,128)(2,1)}), bf16[32,4,256]{2,1,0:T(4,128)(2,1)S(1)}, u32[]{:S(2)}, u32[]{:S(2)}) %all-to-all-start.7) | async-done | bytes 65568 | tf_op jit(solution)/shard_map/all_to_all | solution.py:34
  212.3 0.8 fusion.25
  (201 shorter events, 4.8 us)
Async XLA Ops:
  0.6 4.3 %copy-start = (bf16[2,32,512]{2,1,0:T(8,128)(2,1)S(1)}, bf16[2,32,512]{2,1,0:T(8,128)(2,1)}, u32[]{:S(2)}) copy-start(bf16[2,32,512]{2,1,0:T(8,128)(2,1)} %param.23) | copy-start | bytes 196612
  4.9 11.5 %copy-start.6 = (bf16[256,4]{0,1:T(4,128)(2,1)S(1)}, bf16[256,4]{0,1:T(4,128)(2,1)}, u32[]{:S(2)}) copy-start(bf16[256,4]{0,1:T(4,128)(2,1)} %param.12) | copy-start | bytes 6148
  5.2 39.6 %copy-start.8 = (s32[32]{0:T(128)S(1)}, s32[32]{0:T(128)}, u32[]{:S(2)}) copy-start(s32[32]{0:T(128)} %param.13) | copy-start | bytes 388
  5.2 39.6 %copy-start.3 = (bf16[2,256,32]{1,2,0:T(8,128)(2,1)S(1)}, bf16[2,256,32]{1,2,0:T(8,128)(2,1)}, u32[]{:S(2)}) copy-start(bf16[2,256,32]{1,2,0:T(8,128)(2,1)} %param.21) | copy-start | bytes 98308
  5.3 39.7 %copy-start.4 = (bf16[2,256,32]{1,2,0:T(8,128)(2,1)S(1)}, bf16[2,256,32]{1,2,0:T(8,128)(2,1)}, u32[]{:S(2)}) copy-start(bf16[2,256,32]{1,2,0:T(8,128)(2,1)} %param.20) | copy-start | bytes 98308
  5.3 39.8 %copy-start.5 = (f32[2,32,32]{2,1,0:T(8,128)S(1)}, f32[2,32,32]{2,1,0:T(8,128)}, u32[]{:S(2)}) copy-start(f32[2,32,32]{2,1,0:T(8,128)} %param.14) | copy-start | bytes 24580
  5.4 39.9 %copy-start.7 = (f32[2,32]{1,0:T(2,128)S(1)}, f32[2,32]{1,0:T(2,128)}, u32[]{:S(2)}) copy-start(f32[2,32]{1,0:T(2,128)} %param.22) | copy-start | bytes 772
  5.4 40.4 %collective-permute-start.1 = (bf16[152,128]{1,0:T(8,128)(2,1)S(1)}, bf16[152,128]{1,0:T(8,128)(2,1)S(1)}, u32[]{:S(2)}, u32[]{:S(2)}) collective-permute-start(bf16[152,128]{1,0:T(8,128)(2,1)S(1)} %get-tuple-element.54), channel_id=1, source_target_pairs={{0,64},{32,96},{64,0},{96,32},{1,65},{33,97},{65,1},{97,33},{2,66}... | collective-permute-start | bytes 116744 | tf_op jit(solution)/shard_map/ppermute | solution.py:48
  10.6 35.2 %collective-permute-start = (bf16[152,128]{1,0:T(8,128)(2,1)S(1)}, bf16[152,128]{1,0:T(8,128)(2,1)S(1)}, u32[]{:S(2)}, u32[]{:S(2)}) collective-permute-start(bf16[152,128]{1,0:T(8,128)(2,1)S(1)} %get-tuple-element.52), channel_id=1, source_target_pairs={{0,96},{32,0},{64,32},{96,64},{1,97},{33,1},{65,33},{97,65},{2,98}... | collective-permute-start | bytes 116744 | tf_op jit(solution)/shard_map/ppermute | solution.py:48
  13.9 31.9 %collective-permute-start.2 = (bf16[152,128]{1,0:T(8,128)(2,1)S(1)}, bf16[152,128]{1,0:T(8,128)(2,1)S(1)}, u32[]{:S(2)}, u32[]{:S(2)}) collective-permute-start(bf16[152,128]{1,0:T(8,128)(2,1)S(1)} %get-tuple-element.53), channel_id=1, source_target_pairs={{0,32},{32,64},{64,96},{96,0},{1,33},{33,65},{65,97},{97,1},{2,34}... | collective-permute-start | bytes 116744 | tf_op jit(solution)/shard_map/ppermute | solution.py:48
  17.2 42.7 %all-to-all-start = ((bf16[32,4,256]{2,1,0:T(4,128)(2,1)}), bf16[32,4,256]{2,1,0:T(4,128)(2,1)S(1)}, u32[]{:S(2)}, u32[]{:S(2)}) async-start(bf16[32,4,256]{2,1,0:T(4,128)(2,1)} %pad_maximum_fusion.14), calls=%async_computation | async-start | bytes 131072 | tf_op jit(solution)/shard_map/all_to_all | solution.py:34
  60.9 4.6 %copy-start.1 = (bf16[2,32,3,32]{3,1,2,0:T(8,128)(2,1)S(1)}, bf16[2,32,3,32]{3,1,2,0:T(8,128)(2,1)}, u32[]{:S(2)}) copy-start(bf16[2,32,3,32]{3,1,2,0:T(8,128)(2,1)} %param.15) | copy-start | bytes 36868
  60.9 12.9 %all-to-all-start.1 = ((bf16[4,554,128]{2,1,0:T(8,128)(2,1)}), bf16[4,554,128]{2,1,0:T(8,128)(2,1)S(1)}, u32[]{:S(2)}, u32[]{:S(2)}) async-start(bf16[4,554,128]{2,1,0:T(8,128)(2,1)} %pad_maximum_fusion), calls=%async_computation.1 | async-start | bytes 1146880 | tf_op jit(solution)/shard_map/all_to_all | solution.py:27
  65.6 80.1 %copy-start.2 = (bf16[2,32,3,32]{3,1,2,0:T(8,128)(2,1)}, bf16[2,32,3,32]{3,1,2,0:T(8,128)(2,1)S(1)}, u32[]{:S(2)}) copy-start(bf16[2,32,3,32]{3,1,2,0:T(8,128)(2,1)S(1)} %broadcast_select_fusion.2) | copy-start | bytes 36868
  75.4 14.3 %all-to-all-start.2 = ((bf16[64,8,128]{2,1,0:T(8,128)(2,1)}), bf16[64,8,128]{2,1,0:T(8,128)(2,1)S(1)}, u32[]{:S(2)}, u32[]{:S(2)}) async-start(bf16[64,8,128]{2,1,0:T(8,128)(2,1)} %bitcast.33), calls=%async_computation.2 | async-start | bytes 262144 | tf_op jit(solution)/shard_map/all_to_all | solution.py:27
  91.9 12.4 %all-to-all-start.3 = ((bf16[32,16,128]{2,1,0:T(8,128)(2,1)}), bf16[32,16,128]{2,1,0:T(8,128)(2,1)S(1)}, u32[]{:S(2)}, u32[]{:S(2)}) async-start(bf16[32,16,128]{2,1,0:T(8,128)(2,1)} %maximum_bitcast_fusion), calls=%async_computation.3 | async-start | bytes 262144 | tf_op jit(solution)/shard_map/all_to_all | solution.py:27
  105.1 34.3 %all-to-all-start.4 = ((bf16[8,64,128]{2,1,0:T(8,128)(2,1)}), bf16[8,64,128]{2,1,0:T(8,128)(2,1)S(1)}, u32[]{:S(2)}, u32[]{:S(2)}) async-start(bf16[8,64,128]{2,1,0:T(8,128)(2,1)} %pad_maximum_fusion.7), calls=%async_computation.4 | async-start | bytes 262144 | tf_op jit(solution)/shard_map/all_to_all | solution.py:34
  118.4 8.5 %collective-permute-start.3 = (bf16[416,128]{1,0:T(8,128)(2,1)S(1)}, bf16[416,128]{1,0:T(8,128)(2,1)S(1)}, u32[]{:S(2)}, u32[]{:S(2)}) collective-permute-start(bf16[416,128]{1,0:T(8,128)(2,1)S(1)} %get-tuple-element.41), channel_id=1, source_target_pairs={{0,24},{8,0},{16,8},{24,16},{1,25},{9,1},{17,9},{25,17},{2,26},{10... | collective-permute-start | bytes 319496 | tf_op jit(solution)/shard_map/ppermute | solution.py:48
  121.5 8.1 %collective-permute-start.4 = (bf16[416,128]{1,0:T(8,128)(2,1)S(1)}, bf16[416,128]{1,0:T(8,128)(2,1)S(1)}, u32[]{:S(2)}, u32[]{:S(2)}) collective-permute-start(bf16[416,128]{1,0:T(8,128)(2,1)S(1)} %get-tuple-element.43), channel_id=1, source_target_pairs={{0,16},{8,24},{16,0},{24,8},{1,17},{9,25},{17,1},{25,9},{2,18},{10... | collective-permute-start | bytes 319496 | tf_op jit(solution)/shard_map/ppermute | solution.py:48
  124.9 7.8 %collective-permute-start.5 = (bf16[416,128]{1,0:T(8,128)(2,1)S(1)}, bf16[416,128]{1,0:T(8,128)(2,1)S(1)}, u32[]{:S(2)}, u32[]{:S(2)}) collective-permute-start(bf16[416,128]{1,0:T(8,128)(2,1)S(1)} %get-tuple-element.42), channel_id=1, source_target_pairs={{0,8},{8,16},{16,24},{24,0},{1,9},{9,17},{17,25},{25,1},{2,10},{10... | collective-permute-start | bytes 319496 | tf_op jit(solution)/shard_map/ppermute | solution.py:48
  140.6 14.5 %all-to-all-start.5 = ((bf16[32,32,128]{2,1,0:T(8,128)(2,1)}), bf16[32,32,128]{2,1,0:T(8,128)(2,1)S(1)}, u32[]{:S(2)}, u32[]{:S(2)}) async-start(bf16[32,32,128]{2,1,0:T(8,128)(2,1)} %bitcast.91), calls=%async_computation.5 | async-start | bytes 524288 | tf_op jit(solution)/shard_map/all_to_all | solution.py:27
  156.4 16.8 %collective-permute-start.6 = (f32[8,128]{1,0:T(8,128)S(1)}, f32[8,128]{1,0:T(8,128)S(1)}, u32[]{:S(2)}, u32[]{:S(2)}) collective-permute-start(f32[8,128]{1,0:T(8,128)S(1)} %get-tuple-element.89), channel_id=1, source_target_pairs={{0,24},{8,0},{16,8},{24,16},{1,25},{9,1},{17,9},{25,17},{2,26},{10... | collective-permute-start | bytes 12296 | tf_op jit(solution)/shard_map/ppermute | solution.py:48
  159.8 13.5 %collective-permute-start.7 = (f32[8,128]{1,0:T(8,128)S(1)}, f32[8,128]{1,0:T(8,128)S(1)}, u32[]{:S(2)}, u32[]{:S(2)}) collective-permute-start(f32[8,128]{1,0:T(8,128)S(1)} %get-tuple-element.91), channel_id=1, source_target_pairs={{0,16},{8,24},{16,0},{24,8},{1,17},{9,25},{17,1},{25,9},{2,18},{10... | collective-permute-start | bytes 12296 | tf_op jit(solution)/shard_map/ppermute | solution.py:48
  163.0 10.3 %collective-permute-start.8 = (f32[8,128]{1,0:T(8,128)S(1)}, f32[8,128]{1,0:T(8,128)S(1)}, u32[]{:S(2)}, u32[]{:S(2)}) collective-permute-start(f32[8,128]{1,0:T(8,128)S(1)} %get-tuple-element.90), channel_id=1, source_target_pairs={{0,8},{8,16},{16,24},{24,0},{1,9},{9,17},{17,25},{25,1},{2,10},{10... | collective-permute-start | bytes 12296 | tf_op jit(solution)/shard_map/ppermute | solution.py:48
  165.6 30.4 %slice-start = ((bf16[2,32,3,32]{3,1,2,0:T(8,128)(2,1)}), bf16[2,32,2,32]{3,1,2,0:T(8,128)(2,1)S(1)}, s32[]{:S(2)}) async-start(bf16[2,32,3,32]{3,1,2,0:T(8,128)(2,1)} %copy-done.2), calls=%async_computation.8 | async-start | bytes 65536 | tf_op jit(solution)/shard_map/slice | solution.py:351
  165.6 14.2 %all-to-all-start.6 = ((bf16[32,16,128]{2,1,0:T(8,128)(2,1)}), bf16[32,16,128]{2,1,0:T(8,128)(2,1)S(1)}, u32[]{:S(2)}, u32[]{:S(2)}) async-start(bf16[32,16,128]{2,1,0:T(8,128)(2,1)} %copy_bitcast_fusion), calls=%async_computation.6 | async-start | bytes 262144 | tf_op jit(solution)/shard_map/all_to_all | solution.py:27
  180.8 31.4 %all-to-all-start.7 = ((bf16[32,4,256]{2,1,0:T(4,128)(2,1)}), bf16[32,4,256]{2,1,0:T(4,128)(2,1)S(1)}, u32[]{:S(2)}, u32[]{:S(2)}) async-start(bf16[32,4,256]{2,1,0:T(4,128)(2,1)} %pad_maximum_fusion.20), calls=%async_computation.7 | async-start | bytes 131072 | tf_op jit(solution)/shard_map/all_to_all | solution.py:34

commit v7 on v5

--- a/solution.py
+++ b/solution.py
@@ -16,6 +16,9 @@
 DP = ("x", "core")
 PLANE = ("x", "core", "y")
 PAIRED_PLANE = ("zl", "y", "x", "core")
+FIRST_GATHER = 24
+FIRST_REDUCE = 4
+FIRST_LAST = 20
 bf16 = jnp.bfloat16
 f32 = jnp.float32
 
@@ -27,31 +30,32 @@
     return lax.all_to_all(tiles, axes, 0, 0, tiled=True)
 
 
-def everywhere(array, axes):
+def exchange_far(tiles, axes, first):
     count = lax.axis_size(axes)
-    return exchange(jnp.broadcast_to(array[None], (count, *array.shape)), axes)
-
-
-def passed(piece, axis, step):
-    count = lax.axis_size(axis)
-    return lax.ppermute(piece, axis, [(at, (at + step) % count) for at in range(count)])
+    order = [(first + at) % count for at in range(count)]
+    return lax.all_to_all(tiles, axes, 0, 0, axis_index_groups=[order], tiled=True)
+
+
+def everywhere(array, axes, first):
+    count = lax.axis_size(axes)
+    tiles = jnp.broadcast_to(array[None], (count, *array.shape))
+    return exchange_far(tiles, axes, first)
+
+
+def passed(piece, axis, flip):
+    return lax.ppermute(piece, axis, [(at, at ^ flip) for at in range(lax.axis_size(axis))])
 
 
 def traded(tiles, axis):
-    count = lax.axis_size(axis)
     here = lax.axis_index(axis)
-    pieces = []
-    for step in range(count):
-        piece = lax.dynamic_slice_in_dim(tiles, (here + step) & 3, 1)[0]
-        pieces.append(passed(piece, axis, step) if step else piece)
-    return pieces
-
-
-def counted_back(pieces, axis):
+    pieces = [lax.dynamic_slice_in_dim(tiles, here ^ flip, 1)[0] for flip in range(4)]
+    return pieces[:1] + [passed(pieces[flip], axis, flip) for flip in range(1, 4)]
+
+
+def in_order(pieces, axis):
     here = lax.axis_index(axis)
-    pieces = [pieces[-k % 4] for k in range(4)]
-    pieces = [jnp.where((here & 1) == 1, pieces[k - 1], pieces[k]) for k in range(4)]
-    return [jnp.where(here > 1, pieces[k - 2], pieces[k]) for k in range(4)]
+    pieces = [jnp.where((here & 1) == 1, pieces[k ^ 1], pieces[k]) for k in range(4)]
+    return [jnp.where(here > 1, pieces[k ^ 2], pieces[k]) for k in range(4)]
 
 
 def parts_of(value):
@@ -69,10 +73,10 @@
     return lax.dot_general(a, b, (((a_dim,), (b_dim,)), ((), ())), preferred_element_type=f32)
 
 
-def grouped_features(rows_by_feature):
+def grouped_features(rows_by_feature, first):
     width = rows_by_feature.shape[1]
     to = jnp.arange(width, dtype=jnp.int32)
-    source = (to % 128) // 4 * 16 + to // 128 * 4 + to % 4
+    source = ((to % 128) // 4 + first) % 32 * 16 + to // 128 * 4 + to % 4
     chosen = (jnp.arange(width, dtype=jnp.int32)[:, None] == source[None, :]).astype(bf16)
     return contract(rows_by_feature, 1, chosen, 0).astype(bf16)
 
@@ -116,20 +120,11 @@
     zl = lax.axis_index("zl")
     upper = zl == 1
 
-    stream_t = everywhere(stream.T, Z).reshape(128, 2, 128).transpose(1, 0, 2)
-
-    def scaled(weight):
-        return (weight.transpose(0, 2, 1).astype(f32) * norm_gain[:, None]).astype(bf16)
-
-    by_feature = [
-        grouped_features(weight.reshape(64, 512)).reshape(2, 32, 4, 128)
-        for weight in (scaled(w_branch), scaled(w_gate_branch), w_out)
-    ]
-    w_first = jnp.concatenate([by_feature[0][0], by_feature[1][0]]).reshape(64, 512)
-    place = lax.axis_index("y") * 128 + zl * 64 + lax.broadcasted_iota(jnp.int32, (64, 512), 0)
-    kept_rows = (place == lax.broadcasted_iota(jnp.int32, (64, 512), 1)).astype(bf16)
-    w_first = jnp.concatenate([w_first, kept_rows])
-    second_weights = jnp.stack([by_feature[0][1], by_feature[1][1]])
+    stream_t = everywhere(stream.T, Z, FIRST_GATHER).reshape(128, 2, 128).transpose(1, 0, 2)
+
+    def by_quarter(weight):
+        return weight.reshape(32, 4, 128).transpose(1, 0, 2)
+
     gate_rows = (
         jnp.stack([w_in_gate, w_rec_gate], axis=1)
         .reshape(LAYERS, 2, 2, 128, 32)
@@ -143,33 +138,42 @@
     earlier = jnp.where(
         lengths[None, :, None] >= 2, prior_state, jnp.zeros_like(prior_state)
     )
-    earlier = earlier.reshape(LAYERS, 4, 8, 32).transpose(1, 0, 2, 3).reshape(4, -1)
-    decay = jnp.broadcast_to(jax.nn.log_sigmoid(decay_param).reshape(1, -1), (4, 64))
-    small = jnp.concatenate(
-        parts_of(earlier) + parts_of(decay) + [jnp.zeros((4, 64), bf16)], axis=1
-    ).reshape(4, 14, 128)
-    windows = jnp.concatenate(
-        [
-            history.reshape(LAYERS, 4, 8, depth, 32).transpose(1, 0, 3, 2, 4).reshape(4, -1),
-            jnp.broadcast_to(conv_taps.reshape(1, -1), (4, 256)),
-        ],
-        axis=1,
-    ).reshape(4, 14, 128)
+
+    def by_rows(groups):
+        packed = jnp.concatenate(groups, axis=1).reshape(4, 8, -1, 128)
+        return packed.transpose(0, 2, 1, 3).reshape(4, -1, 128)
+
+    def for_all(rows):
+        return jnp.broadcast_to(rows[None], (4, 8, 32)).reshape(32, 32)
+
+    decay = jnp.concatenate(
+        parts_of(jax.nn.log_sigmoid(decay_param)) + [jnp.zeros((2, 32), bf16)]
+    )
+    none = jnp.zeros((32, 32), bf16)
+    small = by_rows(
+        [part[layer] for layer in range(LAYERS) for part in parts_of(earlier)]
+        + [for_all(decay), none]
+    )
+    windows = by_rows(
+        [history[layer, :, tap] for layer in range(LAYERS) for tap in range(depth)]
+        + [for_all(conv_taps.reshape(8, 32)), none]
+    )
 
     def for_each(rows):
         return jnp.broadcast_to(rows.reshape(1, -1, 128), (4, rows.size // 128, 128))
 
     shared = jnp.concatenate(
         [
-            by_feature[2][0].transpose(1, 0, 2),
-            second_weights.transpose(2, 0, 1, 3).reshape(4, 64, 128),
+            by_quarter(w_out[0]),
+            by_quarter(w_branch[1].T),
+            by_quarter(w_gate_branch[1].T),
             for_each(windows),
         ],
         axis=1,
     )
     shared = traded(shared, ZQ)
-    partner = jnp.where(upper, shared[1][96:], shared[3][96:]).reshape(4, 14, 128)
-    shared = counted_back([piece[:96] for piece in shared], ZQ)
+    partner = shared[1][96:].reshape(4, 16, 128)
+    shared = in_order([piece[:96] for piece in shared], ZQ)
     near = jnp.concatenate(
         [
             for_each(gate_rows[:128]),
@@ -180,9 +184,17 @@
         ],
         axis=1,
     )
-    near, w_first = lax.optimization_barrier((near, w_first))
+    stream_t, near, first_weights = lax.optimization_barrier(
+        (stream_t, near, (w_branch[0], w_gate_branch[0], norm_gain[0]))
+    )
     near = jnp.concatenate([for_each(stream_t), near], axis=1)
     near = exchange(near, "y")
+    w_first = jnp.concatenate([first_weights[0].T, first_weights[1].T]).astype(f32)
+    w_first = grouped_features((w_first * first_weights[2]).astype(bf16), FIRST_GATHER)
+    place = (zl * 4 + lax.axis_index("y")) * 64 + lax.broadcasted_iota(jnp.int32, (64, 512), 0)
+    place = (place % 16) // 4 * 128 + (place // 16 - FIRST_GATHER) % 32 * 4 + place % 4
+    kept_rows = (place == lax.broadcasted_iota(jnp.int32, (64, 512), 1)).astype(bf16)
+    w_first = jnp.concatenate([w_first, kept_rows])
     stream_t = near[:, :256].reshape(4, 2, 128, 128).transpose(1, 0, 2, 3).reshape(2, 512, 128)
 
     def gates_of(rows):
@@ -194,17 +206,17 @@
     w_mid = (
         near[:, 384:512].reshape(4, 4, 32, 128).transpose(1, 0, 2, 3).reshape(512, 128)
     )
-    small = near[:, 512:526].reshape(4, 1792)
-    windows = near[:, 526:].reshape(4, 2, 1792)
+    groups = near[:, 512:].reshape(4, 6, 8, 4, 32).transpose(1, 3, 2, 0, 4).reshape(24, 8, 128)
+    windows = jnp.concatenate([groups[8:16], groups[16:]], axis=2).astype(f32)
     later_rows = jnp.concatenate(
         [
             for_each(gate_rows[128:]),
             for_each(jnp.concatenate([piece[32:] for piece in shared])),
-            by_feature[2][1].transpose(1, 0, 2),
+            by_quarter(grouped_features(w_out[1], FIRST_LAST)),
         ],
         axis=1,
     )
-    later_rows = jnp.stack(counted_back(traded(later_rows, "y"), "y"))
+    later_rows = jnp.stack(in_order(traded(later_rows, "y"), "y"))
     gates_second = gates_of(later_rows[:, :128])
     w_second = (
         later_rows[:, 128:384]
@@ -214,32 +226,10 @@
     )
     w_last = later_rows[:, 384:].reshape(128, 128)
 
-    earlier_rows = (
-        whole_of(small[:, :512], small[:, 512:1024], small[:, 1024:1536])
-        .reshape(4, LAYERS, 8, 32)
-        .transpose(1, 2, 0, 3)
-        .reshape(LAYERS, 8, 128)
-    )
-    decay = (
-        whole_of(small[:, 1536:1600], small[:, 1600:1664], small[:, 1664:1728])
-        .reshape(4, LAYERS, 32)
-        .transpose(1, 0, 2)
-        .reshape(LAYERS, 1, 128)
-    )
-    history_rows = (
-        windows[:, :, :1536]
-        .reshape(4, 2, LAYERS * depth * 8, 32)
-        .transpose(2, 1, 0, 3)
-        .reshape(LAYERS, depth, 8, 256)
-        .astype(f32)
-    )
-    taps = (
-        windows[:, :, 1536:]
-        .reshape(4, 2, LAYERS * TAPS, 32)
-        .transpose(2, 1, 0, 3)
-        .reshape(LAYERS, TAPS, 256)
-        .astype(f32)
-    )
+    earlier_rows = [whole_of(*groups[3 * layer : 3 * layer + 3]) for layer in range(LAYERS)]
+    decay = whole_of(groups[6][:2], groups[6][2:4], groups[6][4:6])[:, None]
+    history_rows = windows[:6].reshape(LAYERS, depth, 8, 256)
+    taps = windows[6].reshape(LAYERS, TAPS, 256)
 
     products = jnp.concatenate(
         [contract(stream_t[half], 0, w_first, 1).astype(bf16) for half in range(2)]
@@ -255,7 +245,8 @@
     rows = came[:, :, :, :, 64:]
     widened = rows.astype(f32)
     squares = jnp.sum(widened * widened, axis=(0, 1, 2, 4))[:, None]
-    rows = jnp.concatenate([rows[0], rows[1]], axis=3).reshape(32, 8, 128)
+    rows = rows.reshape(4, 2, 8, 8, 64)
+    rows = jnp.concatenate([rows[:, 0], rows[:, 1]], axis=3).reshape(32, 8, 128)
     scaling = lax.rsqrt(squares / D + epsilon)
     state_first, branch_first, readout = gated_step(
         (branch * scaling).astype(bf16),
@@ -273,14 +264,16 @@
     came = came[:, :, 0].reshape(4, 64, 128)
     came = jnp.concatenate([came[at] for at in range(4)], axis=1)
     mixed = contract(came, 1, w_mid, 0).astype(bf16)
-    mixed = everywhere(mixed, "zh")
+    mixed = everywhere(mixed, "zh", FIRST_REDUCE)
     mixed, w_second, gates_second, w_last = lax.optimization_barrier(
         (mixed, w_second, gates_second, w_last)
     )
     mixed = mixed.astype(f32).sum(axis=0)
     first = (mixed + residual).astype(bf16)
 
-    products = contract(first, 1, w_second, 1).astype(bf16)
+    gain = lax.dynamic_slice_in_dim(norm_gain[1], lax.axis_index(ZQ) * 128, 128)
+    scaled = (first.astype(f32) * gain).astype(bf16)
+    products = contract(scaled, 1, w_second, 1).astype(bf16)
     products = [products[:, 128 * at : 128 * (at + 1)].reshape(8, 8, 128) for at in range(8)]
     own_rows = first.reshape(8, 8, 128)
     sent = jnp.stack(
@@ -315,27 +308,29 @@
         later[2],
         later[3],
     )
+    rows = lax.dynamic_slice_in_dim(rows.reshape(4, 8, 1, 8, 128), lax.axis_index("zh") // 2, 1)
     sent = jnp.stack(
         [
             jnp.broadcast_to(readout[None], (32, 8, 128)),
-            rows.reshape(4, 8, 8, 128).transpose(1, 0, 2, 3).reshape(32, 8, 128),
+            jnp.broadcast_to(rows[0], (8, 4, 8, 128)).reshape(32, 8, 128),
         ],
         axis=1,
     )
     came = exchange(sent.reshape(32, 16, 128), PLANE).reshape(32, 2, 8, 128)
     mixed = contract(w_last, 0, came[:, 0].reshape(256, 128), 1).astype(bf16)
     mixed = mixed.reshape(32, 4, 256)
-    own = lax.broadcasted_iota(jnp.int32, (4, 128), 0) + 4 * lax.axis_index(Z)
+    own = (lax.axis_index(Z) & 7) * 16 + lax.axis_index("y") * 4
+    own = lax.broadcasted_iota(jnp.int32, (4, 128), 0) + own
     own = (own == lax.broadcasted_iota(jnp.int32, (4, 128), 1)).astype(bf16)
     residual = contract(own, 1, came[:, 1].reshape(256, 128), 1)
-    second = exchange(mixed, Z).astype(f32).sum(axis=0)
+    second = exchange_far(mixed, Z, FIRST_LAST).astype(f32).sum(axis=0)
     second = (second + residual).astype(bf16)
 
     kept = jnp.stack(
         [state_first, state_second, branch_first.astype(f32), branch_second.astype(f32)]
     )
     kept = kept.reshape(4, 8, 4, 32).transpose(2, 0, 1, 3).reshape(4, 8, 128)
-    kept = jnp.stack(counted_back(traded(kept, "y"), "y"))
+    kept = jnp.stack(in_order(traded(kept, "y"), "y"))
     kept = kept.reshape(4, 4, 8, 32).transpose(1, 0, 2, 3).reshape(2, LAYERS, 32, 32)
     window = jnp.concatenate([later[4][:, :, 1:], kept[1].astype(bf16)[:, :, None]], axis=2)
     return second.T, kept[0], window

time: 223 us -> 204 us (0.915)
  the two profiles are of different devices: /device:TPU:2 before, /device:TPU:1 now
where the time goes in v7:
time: 204 us; the launch traced here: 203 us
  starting transfers between devices  126 us (62%)
  waiting for transfers between devices  56.5 us (28%)
  local copies, waits for them, and re-layouts  8.45 us (4%)
  other arithmetic  6.11 us (3%)
  matrix products  3.55 us (2%)
    all_to_all x3, starting transfers between devices, exchange_far(): lax.all_to_all(tiles, axes, 0, 0, axis_index_groups=[order], tiled=True)  70 us
    all_to_all x5, waiting for transfers between devices, exchange(): return lax.all_to_all(tiles, axes, 0, 0, tiled=True)  41 us
    all_to_all x5, starting transfers between devices, exchange(): return lax.all_to_all(tiles, axes, 0, 0, tiled=True)  29 us
    ppermute x9, starting transfers between devices, passed(): lax.ppermute(piece, axis, [(at, at ^ flip) for at in range(lax.axis_size(...  27 us
    all_to_all x3, waiting for transfers between devices, exchange_far(): lax.all_to_all(tiles, axes, 0, 0, axis_index_groups=[order], tiled=True)  10 us
    ppermute x9, waiting for transfers between devices, passed(): lax.ppermute(piece, axis, [(at, at ^ flip) for at in range(lax.axis_size(...  5.56 us
  transfers between devices with their start and end apart: 17, of which 10 were waited for; matrix products, arithmetic and copies ran while one was open for 4% of the time, Pallas kernels for 0%

profile of v7, /device:TPU:1, one launch (start us, length us, event | category | flops | bytes accessed | tf_op | source)
XLA Modules:
  0.0 202.6 jit_solution(10619319821410058626)
XLA Ops:
  0.7 1.3 broadcast_in_dim.62
  2.0 29.3 %all-to-all-start = ((bf16[32,4,256]{2,1,0:T(4,128)(2,1)}), bf16[32,4,256]{2,1,0:T(4,128)(2,1)S(1)}, u32[]{:S(2)}, u32[]{:S(2)}) async-start(bf16[32,4,256]{2,1,0:T(4,128)(2,1)} %broadcast_in_dim.62), calls=%async_computation | async-start | bytes 131072 | tf_op jit(solution)/shard_map/all_to_all | solution.py:36
  31.4 0.7 broadcast_compare_fusion
  32.1 0.9 broadcast_select_fusion.2
  33.0 0.8 slice_bitcast_fusion.14
  34.2 4.0 %collective-permute-start.1 = (bf16[160,128]{1,0:T(8,128)(2,1)S(1)}, bf16[160,128]{1,0:T(8,128)(2,1)S(1)}, u32[]{:S(2)}, u32[]{:S(2)}) collective-permute-start(bf16[160,128]{1,0:T(8,128)(2,1)S(1)} %get-tuple-element.59), channel_id=1, source_target_pairs={{0,64},{32,96},{64,0},{96,32},{1,65},{33,97},{65,1},{97,33},{2,66}... | collective-permute-start | bytes 122888 | tf_op jit(solution)/shard_map/ppermute | solution.py:46
  38.2 3.1 %collective-permute-start = (bf16[160,128]{1,0:T(8,128)(2,1)S(1)}, bf16[160,128]{1,0:T(8,128)(2,1)S(1)}, u32[]{:S(2)}, u32[]{:S(2)}) collective-permute-start(bf16[160,128]{1,0:T(8,128)(2,1)S(1)} %get-tuple-element.60), channel_id=1, source_target_pairs={{0,96},{32,64},{64,32},{96,0},{1,97},{33,65},{65,33},{97,1},{2,98}... | collective-permute-start | bytes 122888 | tf_op jit(solution)/shard_map/ppermute | solution.py:46
  41.3 1.9 collective-permute-start.2
  44.1 1.3 collective-permute-done
  45.3 1.2 collective-permute-done.2
  46.8 0.9 pad_maximum_fusion
  47.7 4.2 %all-to-all-start.1 = ((bf16[4,560,128]{2,1,0:T(8,128)(2,1)}), bf16[4,560,128]{2,1,0:T(8,128)(2,1)S(1)}, u32[]{:S(2)}, u32[]{:S(2)}) async-start(bf16[4,560,128]{2,1,0:T(8,128)(2,1)} %pad_maximum_fusion), calls=%async_computation.1 | async-start | bytes 1146880 | tf_op jit(solution)/shard_map/all_to_all | solution.py:30
  51.8 0.1 fusion.39
  52.0 0.3 convolution_convert_fusion.2
  52.3 6.7 %all-to-all-done.1 = bf16[4,560,128]{2,1,0:T(8,128)(2,1)S(1)} async-done(((bf16[4,560,128]{2,1,0:T(8,128)(2,1)}), bf16[4,560,128]{2,1,0:T(8,128)(2,1)S(1)}, u32[]{:S(2)}, u32[]{:S(2)}) %all-to-all-start.1) | async-done | bytes 573472 | tf_op jit(solution)/shard_map/all_to_all | solution.py:30
  59.1 0.1 reshape.423
  59.3 0.1 slice.416
  59.7 0.2 convolution_convert_fusion.4
  59.9 0.2 convolution_convert_fusion.5
  60.2 0.7 broadcast_in_dim.140
  60.8 9.7 %all-to-all-start.2 = ((bf16[64,8,128]{2,1,0:T(8,128)(2,1)}), bf16[64,8,128]{2,1,0:T(8,128)(2,1)S(1)}, u32[]{:S(2)}, u32[]{:S(2)}) async-start(bf16[64,8,128]{2,1,0:T(8,128)(2,1)} %bitcast.56), calls=%async_computation.2 | async-start | bytes 262144 | tf_op jit(solution)/shard_map/all_to_all | solution.py:30
  70.6 0.2 copy.85
  70.8 0.1 reshape.430
  71.0 8.0 %all-to-all-done.2 = bf16[64,8,128]{2,1,0:T(8,128)(2,1)S(1)} async-done(((bf16[64,8,128]{2,1,0:T(8,128)(2,1)}), bf16[64,8,128]{2,1,0:T(8,128)(2,1)S(1)}, u32[]{:S(2)}, u32[]{:S(2)}) %all-to-all-start.2) | async-done | bytes 131104 | tf_op jit(solution)/shard_map/all_to_all | solution.py:30
  79.0 0.1 slice.431
  79.2 0.2 multiply_reduce_fusion
  79.6 0.1 fusion.60
  79.8 0.1 fusion.61
  80.1 0.1 fusion.24
  80.3 0.2 fusion.97
  80.5 0.7 maximum_bitcast_fusion
  81.2 4.6 %all-to-all-start.3 = ((bf16[32,16,128]{2,1,0:T(8,128)(2,1)}), bf16[32,16,128]{2,1,0:T(8,128)(2,1)S(1)}, u32[]{:S(2)}, u32[]{:S(2)}) async-start(bf16[32,16,128]{2,1,0:T(8,128)(2,1)} %maximum_bitcast_fusion), calls=%async_computation.3 | async-start | bytes 262144 | tf_op jit(solution)/shard_map/all_to_all | solution.py:30
  85.8 0.3 fusion
  86.2 8.1 %all-to-all-done.3 = bf16[32,16,128]{2,1,0:T(8,128)(2,1)S(1)} async-done(((bf16[32,16,128]{2,1,0:T(8,128)(2,1)}), bf16[32,16,128]{2,1,0:T(8,128)(2,1)S(1)}, u32[]{:S(2)}, u32[]{:S(2)}) %all-to-all-start.3) | async-done | bytes 131104 | tf_op jit(solution)/shard_map/all_to_all | solution.py:30
  94.3 0.2 convolution_convert_fusion.6
  94.5 0.7 broadcast_in_dim.141
  95.1 21.1 %all-to-all-start.4 = ((bf16[8,64,128]{2,1,0:T(8,128)(2,1)}), bf16[8,64,128]{2,1,0:T(8,128)(2,1)S(1)}, u32[]{:S(2)}, u32[]{:S(2)}) async-start(bf16[8,64,128]{2,1,0:T(8,128)(2,1)} %broadcast_in_dim.141), calls=%async_computation.4 | async-start | bytes 262144 | tf_op jit(solution)/shard_map/all_to_all | solution.py:36
  116.3 2.7 %collective-permute-start.3 = (bf16[416,128]{1,0:T(8,128)(2,1)S(1)}, bf16[416,128]{1,0:T(8,128)(2,1)S(1)}, u32[]{:S(2)}, u32[]{:S(2)}) collective-permute-start(bf16[416,128]{1,0:T(8,128)(2,1)S(1)} %get-tuple-element.49), channel_id=1, source_target_pairs={{0,24},{8,16},{16,8},{24,0},{1,25},{9,17},{17,9},{25,1},{2,26},{10... | collective-permute-start | bytes 319496 | tf_op jit(solution)/shard_map/ppermute | solution.py:46
  119.1 3.2 %collective-permute-start.4 = (bf16[416,128]{1,0:T(8,128)(2,1)S(1)}, bf16[416,128]{1,0:T(8,128)(2,1)S(1)}, u32[]{:S(2)}, u32[]{:S(2)}) collective-permute-start(bf16[416,128]{1,0:T(8,128)(2,1)S(1)} %get-tuple-element.48), channel_id=1, source_target_pairs={{0,16},{8,24},{16,0},{24,8},{1,17},{9,25},{17,1},{25,9},{2,18},{10... | collective-permute-start | bytes 319496 | tf_op jit(solution)/shard_map/ppermute | solution.py:46
  122.3 3.0 %collective-permute-start.5 = (bf16[416,128]{1,0:T(8,128)(2,1)S(1)}, bf16[416,128]{1,0:T(8,128)(2,1)S(1)}, u32[]{:S(2)}, u32[]{:S(2)}) collective-permute-start(bf16[416,128]{1,0:T(8,128)(2,1)S(1)} %get-tuple-element.47), channel_id=1, source_target_pairs={{0,8},{8,0},{16,24},{24,16},{1,9},{9,1},{17,25},{25,17},{2,10},{10... | collective-permute-start | bytes 319496 | tf_op jit(solution)/shard_map/ppermute | solution.py:46
  125.4 0.9 collective-permute-done.4
  126.3 2.1 %collective-permute-done.5 = bf16[416,128]{1,0:T(8,128)(2,1)S(1)} collective-permute-done((bf16[416,128]{1,0:T(8,128)(2,1)S(1)}, bf16[416,128]{1,0:T(8,128)(2,1)S(1)}, u32[]{:S(2)}, u32[]{:S(2)}) %collective-permute-start.5) | collective-permute-done | bytes 106528 | tf_op jit(solution)/shard_map/ppermute | solution.py:46
  128.7 0.2 convolution_convert_fusion
  129.1 0.7 copy.95
  129.8 5.4 %all-to-all-start.5 = ((bf16[32,32,128]{2,1,0:T(8,128)(2,1)}), bf16[32,32,128]{2,1,0:T(8,128)(2,1)S(1)}, u32[]{:S(2)}, u32[]{:S(2)}) async-start(bf16[32,32,128]{2,1,0:T(8,128)(2,1)} %bitcast.123), calls=%async_computation.5 | async-start | bytes 524288 | tf_op jit(solution)/shard_map/all_to_all | solution.py:30
  135.5 10.9 %all-to-all-done.5 = bf16[32,32,128]{2,1,0:T(8,128)(2,1)S(1)} async-done(((bf16[32,32,128]{2,1,0:T(8,128)(2,1)}), bf16[32,32,128]{2,1,0:T(8,128)(2,1)S(1)}, u32[]{:S(2)}, u32[]{:S(2)}) %all-to-all-start.5) | async-done | bytes 262176 | tf_op jit(solution)/shard_map/all_to_all | solution.py:30
  146.4 0.1 multiply_reduce_fusion.1
  146.7 0.1 fusion.63
  146.8 0.1 fusion.66
  147.0 0.2 fusion.12
  147.2 0.2 fusion.104
  147.6 2.9 %collective-permute-start.6 = (f32[8,128]{1,0:T(8,128)S(1)}, f32[8,128]{1,0:T(8,128)S(1)}, u32[]{:S(2)}, u32[]{:S(2)}) collective-permute-start(f32[8,128]{1,0:T(8,128)S(1)} %get-tuple-element.102), channel_id=1, source_target_pairs={{0,24},{8,16},{16,8},{24,0},{1,25},{9,17},{17,9},{25,1},{2,26},{10... | collective-permute-start | bytes 12296 | tf_op jit(solution)/shard_map/ppermute | solution.py:46
  150.5 3.8 %collective-permute-start.7 = (f32[8,128]{1,0:T(8,128)S(1)}, f32[8,128]{1,0:T(8,128)S(1)}, u32[]{:S(2)}, u32[]{:S(2)}) collective-permute-start(f32[8,128]{1,0:T(8,128)S(1)} %get-tuple-element.101), channel_id=1, source_target_pairs={{0,16},{8,24},{16,0},{24,8},{1,17},{9,25},{17,1},{25,9},{2,18},{10... | collective-permute-start | bytes 12296 | tf_op jit(solution)/shard_map/ppermute | solution.py:46
  154.3 2.3 %collective-permute-start.8 = (f32[8,128]{1,0:T(8,128)S(1)}, f32[8,128]{1,0:T(8,128)S(1)}, u32[]{:S(2)}, u32[]{:S(2)}) collective-permute-start(f32[8,128]{1,0:T(8,128)S(1)} %get-tuple-element.100), channel_id=1, source_target_pairs={{0,8},{8,0},{16,24},{24,16},{1,9},{9,1},{17,25},{25,17},{2,10},{10... | collective-permute-start | bytes 12296 | tf_op jit(solution)/shard_map/ppermute | solution.py:46
  156.7 0.7 maximum_bitcast_fusion.1
  157.4 5.1 %all-to-all-start.6 = ((bf16[32,16,128]{2,1,0:T(8,128)(2,1)}), bf16[32,16,128]{2,1,0:T(8,128)(2,1)S(1)}, u32[]{:S(2)}, u32[]{:S(2)}) async-start(bf16[32,16,128]{2,1,0:T(8,128)(2,1)} %maximum_bitcast_fusion.1), calls=%async_computation.6 | async-start | bytes 262144 | tf_op jit(solution)/shard_map/all_to_all | solution.py:30
  162.9 7.2 %all-to-all-done.6 = bf16[32,16,128]{2,1,0:T(8,128)(2,1)S(1)} async-done(((bf16[32,16,128]{2,1,0:T(8,128)(2,1)}), bf16[32,16,128]{2,1,0:T(8,128)(2,1)S(1)}, u32[]{:S(2)}, u32[]{:S(2)}) %all-to-all-start.6) | async-done | bytes 131104 | tf_op jit(solution)/shard_map/all_to_all | solution.py:30
  170.1 0.2 convolution_convert_fusion.1
  170.3 0.6 reshape.448
  170.9 19.6 %all-to-all-start.7 = ((bf16[32,4,256]{2,1,0:T(4,128)(2,1)}), bf16[32,4,256]{2,1,0:T(4,128)(2,1)S(1)}, u32[]{:S(2)}, u32[]{:S(2)}) async-start(bf16[32,4,256]{2,1,0:T(4,128)(2,1)} %reshape.448), calls=%async_computation.7 | async-start | bytes 131072 | tf_op jit(solution)/shard_map/all_to_all | solution.py:36
  190.5 0.6 pad_maximum_fusion.17
  191.2 0.6 slice_bitcast_fusion.4
  191.8 10.0 %all-to-all-done.7 = bf16[32,4,256]{2,1,0:T(4,128)(2,1)S(1)} async-done(((bf16[32,4,256]{2,1,0:T(4,128)(2,1)}), bf16[32,4,256]{2,1,0:T(4,128)(2,1)S(1)}, u32[]{:S(2)}, u32[]{:S(2)}) %all-to-all-start.7) | async-done | bytes 65568 | tf_op jit(solution)/shard_map/all_to_all | solution.py:36
  201.8 0.8 fusion.25
  (172 shorter events, 3.5 us)
Async XLA Ops:
  0.6 32.4 %copy-start = (bf16[2,4,32]{2,1,0:T(4,128)(2,1)S(1)}, bf16[2,4,32]{2,1,0:T(4,128)(2,1)}, u32[]{:S(2)}) copy-start(bf16[2,4,32]{2,1,0:T(4,128)(2,1)} %param.19) | copy-start | bytes 1540
  0.6 33.2 %copy-start.3 = (bf16[2,512,32]{1,2,0:T(8,128)(2,1)S(1)}, bf16[2,512,32]{1,2,0:T(8,128)(2,1)}, u32[]{:S(2)}) copy-start(bf16[2,512,32]{1,2,0:T(8,128)(2,1)} %param.17) | copy-start | bytes 196612
  0.7 33.2 %slice-start.1 = ((bf16[2,32,512]{2,1,0:T(8,128)(2,1)}), bf16[1,32,512]{2,1,0:T(8,128)(2,1)S(1)}, s32[]{:S(2)}) async-start(bf16[2,32,512]{2,1,0:T(8,128)(2,1)} %param.23), calls=%async_computation.9 | async-start | bytes 65536 | tf_op jit(solution)/shard_map/slice | solution.py:167
  2.0 44.7 %all-to-all-start = ((bf16[32,4,256]{2,1,0:T(4,128)(2,1)}), bf16[32,4,256]{2,1,0:T(4,128)(2,1)S(1)}, u32[]{:S(2)}, u32[]{:S(2)}) async-start(bf16[32,4,256]{2,1,0:T(4,128)(2,1)} %broadcast_in_dim.62), calls=%async_computation | async-start | bytes 131072 | tf_op jit(solution)/shard_map/all_to_all | solution.py:36
  33.0 102.4 %copy-start.1 = (bf16[2,32,3,32]{3,1,2,0:T(8,128)(2,1)}, bf16[2,32,3,32]{3,1,2,0:T(8,128)(2,1)S(1)}, u32[]{:S(2)}) copy-start(bf16[2,32,3,32]{3,1,2,0:T(8,128)(2,1)S(1)} %broadcast_select_fusion.2) | copy-start | bytes 36868
  33.8 9.4 %copy-start.9 = (s32[32]{0:T(128)S(1)}, s32[32]{0:T(128)}, u32[]{:S(2)}) copy-start(s32[32]{0:T(128)} %param.13) | copy-start | bytes 388
  33.8 9.5 %copy-start.4 = (bf16[2,256,32]{1,2,0:T(8,128)(2,1)S(1)}, bf16[2,256,32]{1,2,0:T(8,128)(2,1)}, u32[]{:S(2)}) copy-start(bf16[2,256,32]{1,2,0:T(8,128)(2,1)} %param.21) | copy-start | bytes 98308
  33.9 9.5 %copy-start.5 = (bf16[2,256,32]{1,2,0:T(8,128)(2,1)S(1)}, bf16[2,256,32]{1,2,0:T(8,128)(2,1)}, u32[]{:S(2)}) copy-start(bf16[2,256,32]{1,2,0:T(8,128)(2,1)} %param.20) | copy-start | bytes 98308
  34.1 9.5 %copy-start.6 = (f32[2,32,32]{2,1,0:T(8,128)S(1)}, f32[2,32,32]{2,1,0:T(8,128)}, u32[]{:S(2)}) copy-start(f32[2,32,32]{2,1,0:T(8,128)} %param.14) | copy-start | bytes 24580
  34.1 9.6 %copy-start.8 = (f32[2,32]{1,0:T(2,128)S(1)}, f32[2,32]{1,0:T(2,128)}, u32[]{:S(2)}) copy-start(f32[2,32]{1,0:T(2,128)} %param.22) | copy-start | bytes 772
  34.1 9.8 %copy-start.7 = (f32[2,512]{1,0:T(2,128)S(1)}, f32[2,512]{1,0:T(2,128)}, u32[]{:S(2)}) copy-start(f32[2,512]{1,0:T(2,128)} %param.16) | copy-start | bytes 12292
  34.2 9.9 %collective-permute-start.1 = (bf16[160,128]{1,0:T(8,128)(2,1)S(1)}, bf16[160,128]{1,0:T(8,128)(2,1)S(1)}, u32[]{:S(2)}, u32[]{:S(2)}) collective-permute-start(bf16[160,128]{1,0:T(8,128)(2,1)S(1)} %get-tuple-element.59), channel_id=1, source_target_pairs={{0,64},{32,96},{64,0},{96,32},{1,65},{33,97},{65,1},{97,33},{2,66}... | collective-permute-start | bytes 122888 | tf_op jit(solution)/shard_map/ppermute | solution.py:46
  38.2 7.2 %collective-permute-start = (bf16[160,128]{1,0:T(8,128)(2,1)S(1)}, bf16[160,128]{1,0:T(8,128)(2,1)S(1)}, u32[]{:S(2)}, u32[]{:S(2)}) collective-permute-start(bf16[160,128]{1,0:T(8,128)(2,1)S(1)} %get-tuple-element.60), channel_id=1, source_target_pairs={{0,96},{32,64},{64,32},{96,0},{1,97},{33,65},{65,33},{97,1},{2,98}... | collective-permute-start | bytes 122888 | tf_op jit(solution)/shard_map/ppermute | solution.py:46
  41.3 5.2 %collective-permute-start.2 = (bf16[160,128]{1,0:T(8,128)(2,1)S(1)}, bf16[160,128]{1,0:T(8,128)(2,1)S(1)}, u32[]{:S(2)}, u32[]{:S(2)}) collective-permute-start(bf16[160,128]{1,0:T(8,128)(2,1)S(1)} %get-tuple-element.58), channel_id=1, source_target_pairs={{0,32},{32,0},{64,96},{96,64},{1,33},{33,1},{65,97},{97,65},{2,34}... | collective-permute-start | bytes 122888 | tf_op jit(solution)/shard_map/ppermute | solution.py:46
  47.7 11.4 %all-to-all-start.1 = ((bf16[4,560,128]{2,1,0:T(8,128)(2,1)}), bf16[4,560,128]{2,1,0:T(8,128)(2,1)S(1)}, u32[]{:S(2)}, u32[]{:S(2)}) async-start(bf16[4,560,128]{2,1,0:T(8,128)(2,1)} %pad_maximum_fusion), calls=%async_computation.1 | async-start | bytes 1146880 | tf_op jit(solution)/shard_map/all_to_all | solution.py:30
  60.8 18.2 %all-to-all-start.2 = ((bf16[64,8,128]{2,1,0:T(8,128)(2,1)}), bf16[64,8,128]{2,1,0:T(8,128)(2,1)S(1)}, u32[]{:S(2)}, u32[]{:S(2)}) async-start(bf16[64,8,128]{2,1,0:T(8,128)(2,1)} %bitcast.56), calls=%async_computation.2 | async-start | bytes 262144 | tf_op jit(solution)/shard_map/all_to_all | solution.py:30
  79.9 5.9 %copy-start.2 = (bf16[2,32,512]{2,1,0:T(8,128)(2,1)S(1)}, bf16[2,32,512]{2,1,0:T(8,128)(2,1)}, u32[]{:S(2)}) copy-start(bf16[2,32,512]{2,1,0:T(8,128)(2,1)} %param.23) | copy-start | bytes 196612
  81.2 13.1 %all-to-all-start.3 = ((bf16[32,16,128]{2,1,0:T(8,128)(2,1)}), bf16[32,16,128]{2,1,0:T(8,128)(2,1)S(1)}, u32[]{:S(2)}, u32[]{:S(2)}) async-start(bf16[32,16,128]{2,1,0:T(8,128)(2,1)} %maximum_bitcast_fusion), calls=%async_computation.3 | async-start | bytes 262144 | tf_op jit(solution)/shard_map/all_to_all | solution.py:30
  95.1 33.5 %all-to-all-start.4 = ((bf16[8,64,128]{2,1,0:T(8,128)(2,1)}), bf16[8,64,128]{2,1,0:T(8,128)(2,1)S(1)}, u32[]{:S(2)}, u32[]{:S(2)}) async-start(bf16[8,64,128]{2,1,0:T(8,128)(2,1)} %broadcast_in_dim.141), calls=%async_computation.4 | async-start | bytes 262144 | tf_op jit(solution)/shard_map/all_to_all | solution.py:36
  116.3 9.0 %collective-permute-start.3 = (bf16[416,128]{1,0:T(8,128)(2,1)S(1)}, bf16[416,128]{1,0:T(8,128)(2,1)S(1)}, u32[]{:S(2)}, u32[]{:S(2)}) collective-permute-start(bf16[416,128]{1,0:T(8,128)(2,1)S(1)} %get-tuple-element.49), channel_id=1, source_target_pairs={{0,24},{8,16},{16,8},{24,0},{1,25},{9,17},{17,9},{25,1},{2,26},{10... | collective-permute-start | bytes 319496 | tf_op jit(solution)/shard_map/ppermute | solution.py:46
  119.1 7.2 %collective-permute-start.4 = (bf16[416,128]{1,0:T(8,128)(2,1)S(1)}, bf16[416,128]{1,0:T(8,128)(2,1)S(1)}, u32[]{:S(2)}, u32[]{:S(2)}) collective-permute-start(bf16[416,128]{1,0:T(8,128)(2,1)S(1)} %get-tuple-element.48), channel_id=1, source_target_pairs={{0,16},{8,24},{16,0},{24,8},{1,17},{9,25},{17,1},{25,9},{2,18},{10... | collective-permute-start | bytes 319496 | tf_op jit(solution)/shard_map/ppermute | solution.py:46
  122.3 6.1 %collective-permute-start.5 = (bf16[416,128]{1,0:T(8,128)(2,1)S(1)}, bf16[416,128]{1,0:T(8,128)(2,1)S(1)}, u32[]{:S(2)}, u32[]{:S(2)}) collective-permute-start(bf16[416,128]{1,0:T(8,128)(2,1)S(1)} %get-tuple-element.47), channel_id=1, source_target_pairs={{0,8},{8,0},{16,24},{24,16},{1,9},{9,1},{17,25},{25,17},{2,10},{10... | collective-permute-start | bytes 319496 | tf_op jit(solution)/shard_map/ppermute | solution.py:46
  129.8 16.6 %all-to-all-start.5 = ((bf16[32,32,128]{2,1,0:T(8,128)(2,1)}), bf16[32,32,128]{2,1,0:T(8,128)(2,1)S(1)}, u32[]{:S(2)}, u32[]{:S(2)}) async-start(bf16[32,32,128]{2,1,0:T(8,128)(2,1)} %bitcast.123), calls=%async_computation.5 | async-start | bytes 524288 | tf_op jit(solution)/shard_map/all_to_all | solution.py:30
  147.6 14.9 %collective-permute-start.6 = (f32[8,128]{1,0:T(8,128)S(1)}, f32[8,128]{1,0:T(8,128)S(1)}, u32[]{:S(2)}, u32[]{:S(2)}) collective-permute-start(f32[8,128]{1,0:T(8,128)S(1)} %get-tuple-element.102), channel_id=1, source_target_pairs={{0,24},{8,16},{16,8},{24,0},{1,25},{9,17},{17,9},{25,1},{2,26},{10... | collective-permute-start | bytes 12296 | tf_op jit(solution)/shard_map/ppermute | solution.py:46
  150.5 12.0 %collective-permute-start.7 = (f32[8,128]{1,0:T(8,128)S(1)}, f32[8,128]{1,0:T(8,128)S(1)}, u32[]{:S(2)}, u32[]{:S(2)}) collective-permute-start(f32[8,128]{1,0:T(8,128)S(1)} %get-tuple-element.101), channel_id=1, source_target_pairs={{0,16},{8,24},{16,0},{24,8},{1,17},{9,25},{17,1},{25,9},{2,18},{10... | collective-permute-start | bytes 12296 | tf_op jit(solution)/shard_map/ppermute | solution.py:46
  154.3 8.2 %collective-permute-start.8 = (f32[8,128]{1,0:T(8,128)S(1)}, f32[8,128]{1,0:T(8,128)S(1)}, u32[]{:S(2)}, u32[]{:S(2)}) collective-permute-start(f32[8,128]{1,0:T(8,128)S(1)} %get-tuple-element.100), channel_id=1, source_target_pairs={{0,8},{8,0},{16,24},{24,16},{1,9},{9,1},{17,25},{25,17},{2,10},{10... | collective-permute-start | bytes 12296 | tf_op jit(solution)/shard_map/ppermute | solution.py:46
  156.7 33.8 %slice-start = ((bf16[2,32,3,32]{3,1,2,0:T(8,128)(2,1)}), bf16[2,32,2,32]{3,1,2,0:T(8,128)(2,1)S(1)}, s32[]{:S(2)}) async-start(bf16[2,32,3,32]{3,1,2,0:T(8,128)(2,1)} %copy-done.1), calls=%async_computation.8 | async-start | bytes 65536 | tf_op jit(solution)/shard_map/slice | solution.py:335
  157.4 12.7 %all-to-all-start.6 = ((bf16[32,16,128]{2,1,0:T(8,128)(2,1)}), bf16[32,16,128]{2,1,0:T(8,128)(2,1)S(1)}, u32[]{:S(2)}, u32[]{:S(2)}) async-start(bf16[32,16,128]{2,1,0:T(8,128)(2,1)} %maximum_bitcast_fusion.1), calls=%async_computation.6 | async-start | bytes 262144 | tf_op jit(solution)/shard_map/all_to_all | solution.py:30
  170.9 30.9 %all-to-all-start.7 = ((bf16[32,4,256]{2,1,0:T(4,128)(2,1)}), bf16[32,4,256]{2,1,0:T(4,128)(2,1)S(1)}, u32[]{:S(2)}, u32[]{:S(2)}) async-start(bf16[32,4,256]{2,1,0:T(4,128)(2,1)} %reshape.448), calls=%async_computation.7 | async-start | bytes 131072 | tf_op jit(solution)/shard_map/all_to_all | solution.py:36

commit v8 on v7

--- a/solution.py
+++ b/solution.py
@@ -120,10 +120,17 @@
     zl = lax.axis_index("zl")
     upper = zl == 1
 
-    stream_t = everywhere(stream.T, Z, FIRST_GATHER).reshape(128, 2, 128).transpose(1, 0, 2)
-
-    def by_quarter(weight):
-        return weight.reshape(32, 4, 128).transpose(1, 0, 2)
+    stream_t = everywhere(stream.T, Z, FIRST_GATHER).reshape(128, 256)
+
+    def scaled(weight, layer):
+        return (weight[layer].T.astype(f32) * norm_gain[layer]).astype(bf16)
+
+    def grouped(*weights):
+        rows = grouped_features(jnp.concatenate(weights), FIRST_GATHER)
+        return rows.reshape(-1, 4, 128).transpose(1, 0, 2)
+
+    first_weights = grouped(scaled(w_branch, 0), scaled(w_gate_branch, 0), w_out[0])
+    second_weights = grouped(scaled(w_branch, 1), scaled(w_gate_branch, 1))
 
     gate_rows = (
         jnp.stack([w_in_gate, w_rec_gate], axis=1)
@@ -162,57 +169,51 @@
     def for_each(rows):
         return jnp.broadcast_to(rows.reshape(1, -1, 128), (4, rows.size // 128, 128))
 
-    shared = jnp.concatenate(
-        [
-            by_quarter(w_out[0]),
-            by_quarter(w_branch[1].T),
-            by_quarter(w_gate_branch[1].T),
-            for_each(windows),
+    near = jnp.concatenate(
+        [
+            first_weights[:, :64],
+            for_each(gate_rows[:128]),
+            for_each(first_weights[:, 64:]),
+            small,
+            windows,
         ],
         axis=1,
     )
-    shared = traded(shared, ZQ)
-    partner = shared[1][96:].reshape(4, 16, 128)
-    shared = in_order([piece[:96] for piece in shared], ZQ)
-    near = jnp.concatenate(
-        [
-            for_each(gate_rows[:128]),
-            for_each(jnp.concatenate([piece[:32] for piece in shared])),
-            small,
-            jnp.where(upper, partner, windows),
-            jnp.where(upper, windows, partner),
-        ],
-        axis=1,
-    )
-    stream_t, near, first_weights = lax.optimization_barrier(
-        (stream_t, near, (w_branch[0], w_gate_branch[0], norm_gain[0]))
-    )
-    near = jnp.concatenate([for_each(stream_t), near], axis=1)
-    near = exchange(near, "y")
-    w_first = jnp.concatenate([first_weights[0].T, first_weights[1].T]).astype(f32)
-    w_first = grouped_features((w_first * first_weights[2]).astype(bf16), FIRST_GATHER)
-    place = (zl * 4 + lax.axis_index("y")) * 64 + lax.broadcasted_iota(jnp.int32, (64, 512), 0)
-    place = (place % 16) // 4 * 128 + (place // 16 - FIRST_GATHER) % 32 * 4 + place % 4
-    kept_rows = (place == lax.broadcasted_iota(jnp.int32, (64, 512), 1)).astype(bf16)
-    w_first = jnp.concatenate([w_first, kept_rows])
-    stream_t = near[:, :256].reshape(4, 2, 128, 128).transpose(1, 0, 2, 3).reshape(2, 512, 128)
+    near = jnp.stack(in_order(traded(near, "y"), "y"))
+    w_first = near[:, :64].reshape(4, 2, 32, 128).transpose(1, 0, 2, 3).reshape(2, 128, 128)
 
     def gates_of(rows):
         return (
             rows.reshape(4, 2, 2, 32, 128).transpose(1, 2, 0, 3, 4).reshape(2, 2, 128, 128)
         )
 
-    gates = gates_of(near[:, 256:384])
-    w_mid = (
-        near[:, 384:512].reshape(4, 4, 32, 128).transpose(1, 0, 2, 3).reshape(512, 128)
-    )
-    groups = near[:, 512:].reshape(4, 6, 8, 4, 32).transpose(1, 3, 2, 0, 4).reshape(24, 8, 128)
-    windows = jnp.concatenate([groups[8:16], groups[16:]], axis=2).astype(f32)
+    gates = gates_of(near[:, 64:192])
+
+    def by_group(rows):
+        rows = rows.reshape(4, -1, 8, 4, 32).transpose(1, 3, 2, 0, 4)
+        return rows.reshape(-1, 8, 128)
+
+    groups = by_group(near[:, 320:])
+    shared = jnp.concatenate(
+        [
+            near[:, 192:320].reshape(4, 4, 32, 128).transpose(1, 0, 2, 3).reshape(4, 128, 128),
+            second_weights,
+            for_each(near[:, 336:]),
+        ],
+        axis=1,
+    )
+    shared = traded(shared, ZQ)
+    partner = by_group(shared[1][192:].reshape(4, 16, 128))
+    windows = jnp.concatenate(
+        [jnp.where(upper, partner, groups[8:]), jnp.where(upper, groups[8:], partner)], axis=2
+    ).astype(f32)
+    shared = in_order([piece[:192] for piece in shared], ZQ)
+    w_mid = jnp.concatenate([piece[:128] for piece in shared])
     later_rows = jnp.concatenate(
         [
             for_each(gate_rows[128:]),
-            for_each(jnp.concatenate([piece[32:] for piece in shared])),
-            by_quarter(grouped_features(w_out[1], FIRST_LAST)),
+            for_each(jnp.concatenate([piece[128:] for piece in shared])),
+            grouped_features(w_out[1], FIRST_LAST).reshape(32, 4, 128).transpose(1, 0, 2),
         ],
         axis=1,
     )
@@ -231,22 +232,27 @@
     history_rows = windows[:6].reshape(LAYERS, depth, 8, 256)
     taps = windows[6].reshape(LAYERS, TAPS, 256)
 
-    products = jnp.concatenate(
-        [contract(stream_t[half], 0, w_first, 1).astype(bf16) for half in range(2)]
-    )
-    products = products.reshape(8, 4, 8, 128).transpose(1, 0, 2, 3).reshape(1, 32, 8, 128)
-    sent = jnp.broadcast_to(products, (2, 32, 8, 128)).reshape(64, 8, 128)
-    came = exchange(sent, PAIRED_PLANE).reshape(2, 4, 8, 8, 128)
+    products = [
+        contract(stream_t, 0, w_first[kind], 1).astype(bf16).reshape(8, 4, 8, 128)
+        for kind in range(2)
+    ]
+    products.append(stream_t.T.reshape(8, 4, 8, 128))
+    branch, gate_in, rows = [part.transpose(1, 0, 2, 3) for part in products]
+    sent = jnp.stack(
+        [
+            jnp.stack([branch, jnp.where(upper, rows, gate_in)], axis=2),
+            jnp.stack([branch, jnp.where(upper, gate_in, rows)], axis=2),
+        ]
+    )
+    came = exchange(sent.reshape(64, 16, 128), PAIRED_PLANE)
+    came = came.reshape(2, 32, 2, 8, 128)
     later = (history_rows[1], taps[1], decay[1], earlier_rows[1], history)
-    came, w_mid, later = lax.optimization_barrier((came, w_mid, later))
-    summed = came.astype(f32).sum(axis=2)
-    branch = summed[:, :, :, :32].transpose(2, 0, 1, 3).reshape(8, 256)
-    gate_in = jnp.where(upper, summed[1], summed[0])[:, :, 32:64].transpose(1, 0, 2).reshape(8, 128)
-    rows = came[:, :, :, :, 64:]
+    branch = came[:, :, 0].astype(f32).sum(axis=1)
+    branch = jnp.concatenate([branch[0], branch[1]], axis=1)
+    rows = jnp.where(upper, came[0, :, 1], came[1, :, 1])
+    gate_in = jnp.where(upper, came[1, :, 1], came[0, :, 1]).astype(f32).sum(axis=0)
     widened = rows.astype(f32)
-    squares = jnp.sum(widened * widened, axis=(0, 1, 2, 4))[:, None]
-    rows = rows.reshape(4, 2, 8, 8, 64)
-    rows = jnp.concatenate([rows[:, 0], rows[:, 1]], axis=3).reshape(32, 8, 128)
+    squares = jnp.sum(jnp.sum(widened * widened, axis=0), axis=1, keepdims=True)
     scaling = lax.rsqrt(squares / D + epsilon)
     state_first, branch_first, readout = gated_step(
         (branch * scaling).astype(bf16),
@@ -271,9 +277,7 @@
     mixed = mixed.astype(f32).sum(axis=0)
     first = (mixed + residual).astype(bf16)
 
-    gain = lax.dynamic_slice_in_dim(norm_gain[1], lax.axis_index(ZQ) * 128, 128)
-    scaled = (first.astype(f32) * gain).astype(bf16)
-    products = contract(scaled, 1, w_second, 1).astype(bf16)
+    products = contract(first, 1, w_second, 1).astype(bf16)
     products = [products[:, 128 * at : 128 * (at + 1)].reshape(8, 8, 128) for at in range(8)]
     own_rows = first.reshape(8, 8, 128)
     sent = jnp.stack(
@@ -308,18 +312,17 @@
         later[2],
         later[3],
     )
-    rows = lax.dynamic_slice_in_dim(rows.reshape(4, 8, 1, 8, 128), lax.axis_index("zh") // 2, 1)
     sent = jnp.stack(
         [
             jnp.broadcast_to(readout[None], (32, 8, 128)),
-            jnp.broadcast_to(rows[0], (8, 4, 8, 128)).reshape(32, 8, 128),
+            rows.reshape(4, 8, 8, 128).transpose(1, 0, 2, 3).reshape(32, 8, 128),
         ],
         axis=1,
     )
     came = exchange(sent.reshape(32, 16, 128), PLANE).reshape(32, 2, 8, 128)
     mixed = contract(w_last, 0, came[:, 0].reshape(256, 128), 1).astype(bf16)
     mixed = mixed.reshape(32, 4, 256)
-    own = (lax.axis_index(Z) & 7) * 16 + lax.axis_index("y") * 4
+    own = (lax.axis_index(Z) - FIRST_GATHER) % 32 * 4
     own = lax.broadcasted_iota(jnp.int32, (4, 128), 0) + own
     own = (own == lax.broadcasted_iota(jnp.int32, (4, 128), 1)).astype(bf16)
     residual = contract(own, 1, came[:, 1].reshape(256, 128), 1)

time: 204 us -> 210 us (1.029)
  starting transfers between devices: 126 us -> 135 us
  waiting for transfers between devices: 56.5 us -> 53 us
  local copies, waits for them, and re-layouts: 8.45 us -> 11.2 us
    all_to_all x5 -> x4, waiting for transfers between devices: 41 us -> 21.1 us  [exchange(): return lax.all_to_all(tiles, axes, 0, 0, tiled=True)]
    all_to_all x3, waiting for transfers between devices: 10 us -> 23 us  [exchange_far(): lax.all_to_all(tiles, axes, 0, 0, axis_index_groups=[order], tiled=True)]
    ppermute x9 -> x12, starting transfers between devices: 27 us -> 38.5 us  [passed(): lax.ppermute(piece, axis, [(at, at ^ flip) for at in range(lax.axis_size(...]
    ppermute x9 -> x12, waiting for transfers between devices: 5.56 us -> 8.82 us  [passed(): lax.ppermute(piece, axis, [(at, at ^ flip) for at in range(lax.axis_size(...]
    all_to_all x3, starting transfers between devices: 70 us -> 66.9 us  [exchange_far(): lax.all_to_all(tiles, axes, 0, 0, axis_index_groups=[order], tiled=True)]
    unnamed x23 -> x28, local copies, waits for them, and re-layouts: 0.12 us -> 2.91 us
    all_to_all x5 -> x4, starting transfers between devices: 29 us -> 29.3 us  [exchange(): return lax.all_to_all(tiles, axes, 0, 0, tiled=True)]
  transfers between devices with their start and end apart: 17 -> 19, of which waited for: 10 -> 10; matrix products, arithmetic and copies ran while one was open for 4% -> 2% of each run, Pallas kernels for 0% -> 0%
where the time goes in v8:
time: 210 us; the launch traced here: 209 us
  starting transfers between devices  135 us (64%)
  waiting for transfers between devices  53 us (25%)
  local copies, waits for them, and re-layouts  11.2 us (5%)
  other arithmetic  4.45 us (2%)
  matrix products  3.74 us (2%)
    all_to_all x3, starting transfers between devices, exchange_far(): lax.all_to_all(tiles, axes, 0, 0, axis_index_groups=[order], tiled=True)  66.9 us
    ppermute x12, starting transfers between devices, passed(): lax.ppermute(piece, axis, [(at, at ^ flip) for at in range(lax.axis_size(...  38.5 us
    all_to_all x4, starting transfers between devices, exchange(): return lax.all_to_all(tiles, axes, 0, 0, tiled=True)  29.3 us
    all_to_all x3, waiting for transfers between devices, exchange_far(): lax.all_to_all(tiles, axes, 0, 0, axis_index_groups=[order], tiled=True)  23 us
    all_to_all x4, waiting for transfers between devices, exchange(): return lax.all_to_all(tiles, axes, 0, 0, tiled=True)  21.1 us
    ppermute x12, waiting for transfers between devices, passed(): lax.ppermute(piece, axis, [(at, at ^ flip) for at in range(lax.axis_size(...  8.82 us
  transfers between devices with their start and end apart: 19, of which 10 were waited for; matrix products, arithmetic and copies ran while one was open for 2% of the time, Pallas kernels for 0%

profile of v8, /device:TPU:1, one launch (start us, length us, event | category | flops | bytes accessed | tf_op | source)
XLA Modules:
  0.0 209.0 jit_solution(902064746683070878)
XLA Ops:
  0.7 0.8 slice_bitcast_fusion.15
  1.5 0.8 fusion.72
  2.3 0.3 fusion
  2.7 0.7 copy-done.4
  3.4 0.7 copy-done.5
  4.4 0.6 copy-done.11
  5.2 0.6 copy-done.10
  6.6 5.5 %collective-permute-start = (bf16[352,128]{1,0:T(8,128)(2,1)S(1)}, bf16[352,128]{1,0:T(8,128)(2,1)S(1)}, u32[]{:S(2)}, u32[]{:S(2)}) collective-permute-start(bf16[352,128]{1,0:T(8,128)(2,1)S(1)} %get-tuple-element.38), channel_id=1, source_target_pairs={{0,24},{8,16},{16,8},{24,0},{1,25},{9,17},{17,9},{25,1},{2,26},{10... | collective-permute-start | bytes 270344 | tf_op jit(solution)/shard_map/ppermute | solution.py:46
  12.1 2.3 %collective-permute-start.1 = (bf16[352,128]{1,0:T(8,128)(2,1)S(1)}, bf16[352,128]{1,0:T(8,128)(2,1)S(1)}, u32[]{:S(2)}, u32[]{:S(2)}) collective-permute-start(bf16[352,128]{1,0:T(8,128)(2,1)S(1)} %get-tuple-element.37), channel_id=1, source_target_pairs={{0,16},{8,24},{16,0},{24,8},{1,17},{9,25},{17,1},{25,9},{2,18},{10... | collective-permute-start | bytes 270344 | tf_op jit(solution)/shard_map/ppermute | solution.py:46
  14.4 2.1 %collective-permute-start.2 = (bf16[352,128]{1,0:T(8,128)(2,1)S(1)}, bf16[352,128]{1,0:T(8,128)(2,1)S(1)}, u32[]{:S(2)}, u32[]{:S(2)}) collective-permute-start(bf16[352,128]{1,0:T(8,128)(2,1)S(1)} %get-tuple-element.36), channel_id=1, source_target_pairs={{0,8},{8,0},{16,24},{24,16},{1,9},{9,1},{17,25},{25,17},{2,10},{10... | collective-permute-start | bytes 270344 | tf_op jit(solution)/shard_map/ppermute | solution.py:46
  16.5 0.6 broadcast_in_dim.118
  17.2 28.5 %all-to-all-start = ((bf16[32,4,256]{2,1,0:T(4,128)(2,1)}), bf16[32,4,256]{2,1,0:T(4,128)(2,1)S(1)}, u32[]{:S(2)}, u32[]{:S(2)}) async-start(bf16[32,4,256]{2,1,0:T(4,128)(2,1)} %broadcast_in_dim.118), calls=%async_computation | async-start | bytes 131072 | tf_op jit(solution)/shard_map/all_to_all | solution.py:36
  45.8 13.8 %all-to-all-done = bf16[32,4,256]{2,1,0:T(4,128)(2,1)S(1)} async-done(((bf16[32,4,256]{2,1,0:T(4,128)(2,1)}), bf16[32,4,256]{2,1,0:T(4,128)(2,1)S(1)}, u32[]{:S(2)}, u32[]{:S(2)}) %all-to-all-start) | async-done | bytes 65568 | tf_op jit(solution)/shard_map/all_to_all | solution.py:36
  59.6 0.1 fusion.2
  59.9 0.2 select_bitcast_fusion.9
  60.3 0.8 copy.68
  61.1 10.8 %all-to-all-start.1 = ((bf16[64,16,128]{2,1,0:T(8,128)(2,1)}), bf16[64,16,128]{2,1,0:T(8,128)(2,1)S(1)}, u32[]{:S(2)}, u32[]{:S(2)}) async-start(bf16[64,16,128]{2,1,0:T(8,128)(2,1)} %bitcast.75), calls=%async_computation.1 | async-start | bytes 524288 | tf_op jit(solution)/shard_map/all_to_all | solution.py:30
  71.9 0.3 fusion.1
  72.4 3.4 %collective-permute-start.3 = (bf16[256,128]{1,0:T(8,128)(2,1)S(1)}, bf16[256,128]{1,0:T(8,128)(2,1)S(1)}, u32[]{:S(2)}, u32[]{:S(2)}) collective-permute-start(bf16[256,128]{1,0:T(8,128)(2,1)S(1)} %get-tuple-element.39), channel_id=1, source_target_pairs={{0,32},{32,0},{64,96},{96,64},{1,33},{33,1},{65,97},{97,65},{2,34}... | collective-permute-start | bytes 196616 | tf_op jit(solution)/shard_map/ppermute | solution.py:46
  76.2 1.7 collective-permute-done.3
  78.5 3.1 %all-to-all-done.1 = bf16[64,16,128]{2,1,0:T(8,128)(2,1)S(1)} async-done(((bf16[64,16,128]{2,1,0:T(8,128)(2,1)}), bf16[64,16,128]{2,1,0:T(8,128)(2,1)S(1)}, u32[]{:S(2)}, u32[]{:S(2)}) %all-to-all-start.1) | async-done | bytes 262176 | tf_op jit(solution)/shard_map/all_to_all | solution.py:30
  81.6 0.1 convert_reduce_fusion.4
  81.8 0.1 fusion.73
  82.0 0.1 fusion.74
  82.1 0.2 fusion.27
  82.3 0.2 fusion.109
  82.5 0.7 maximum_bitcast_fusion
  83.2 4.0 %all-to-all-start.2 = ((bf16[32,16,128]{2,1,0:T(8,128)(2,1)}), bf16[32,16,128]{2,1,0:T(8,128)(2,1)S(1)}, u32[]{:S(2)}, u32[]{:S(2)}) async-start(bf16[32,16,128]{2,1,0:T(8,128)(2,1)} %maximum_bitcast_fusion), calls=%async_computation.2 | async-start | bytes 262144 | tf_op jit(solution)/shard_map/all_to_all | solution.py:30
  87.2 4.3 %collective-permute-start.5 = (bf16[256,128]{1,0:T(8,128)(2,1)S(1)}, bf16[256,128]{1,0:T(8,128)(2,1)S(1)}, u32[]{:S(2)}, u32[]{:S(2)}) collective-permute-start(bf16[256,128]{1,0:T(8,128)(2,1)S(1)} %get-tuple-element.40), channel_id=1, source_target_pairs={{0,64},{32,96},{64,0},{96,32},{1,65},{33,97},{65,1},{97,33},{2,66}... | collective-permute-start | bytes 196616 | tf_op jit(solution)/shard_map/ppermute | solution.py:46
  91.5 3.0 %collective-permute-start.4 = (bf16[256,128]{1,0:T(8,128)(2,1)S(1)}, bf16[256,128]{1,0:T(8,128)(2,1)S(1)}, u32[]{:S(2)}, u32[]{:S(2)}) collective-permute-start(bf16[256,128]{1,0:T(8,128)(2,1)S(1)} %get-tuple-element.41), channel_id=1, source_target_pairs={{0,96},{32,64},{64,32},{96,0},{1,97},{33,65},{65,33},{97,1},{2,98}... | collective-permute-start | bytes 196616 | tf_op jit(solution)/shard_map/ppermute | solution.py:46
  94.5 0.3 fusion.3
  94.9 1.5 collective-permute-done.5
  96.4 1.9 collective-permute-done.4
  98.5 0.2 convolution_convert_fusion.7
  98.6 0.7 broadcast_in_dim.119
  99.3 21.1 %all-to-all-start.3 = ((bf16[8,64,128]{2,1,0:T(8,128)(2,1)}), bf16[8,64,128]{2,1,0:T(8,128)(2,1)S(1)}, u32[]{:S(2)}, u32[]{:S(2)}) async-start(bf16[8,64,128]{2,1,0:T(8,128)(2,1)} %broadcast_in_dim.119), calls=%async_computation.3 | async-start | bytes 262144 | tf_op jit(solution)/shard_map/all_to_all | solution.py:36
  120.6 4.0 %collective-permute-start.6 = (bf16[416,128]{1,0:T(8,128)(2,1)S(1)}, bf16[416,128]{1,0:T(8,128)(2,1)S(1)}, u32[]{:S(2)}, u32[]{:S(2)}) collective-permute-start(bf16[416,128]{1,0:T(8,128)(2,1)S(1)} %get-tuple-element.35), channel_id=1, source_target_pairs={{0,24},{8,16},{16,8},{24,0},{1,25},{9,17},{17,9},{25,1},{2,26},{10... | collective-permute-start | bytes 319496 | tf_op jit(solution)/shard_map/ppermute | solution.py:46
  124.6 2.4 %collective-permute-start.7 = (bf16[416,128]{1,0:T(8,128)(2,1)S(1)}, bf16[416,128]{1,0:T(8,128)(2,1)S(1)}, u32[]{:S(2)}, u32[]{:S(2)}) collective-permute-start(bf16[416,128]{1,0:T(8,128)(2,1)S(1)} %get-tuple-element.34), channel_id=1, source_target_pairs={{0,16},{8,24},{16,0},{24,8},{1,17},{9,25},{17,1},{25,9},{2,18},{10... | collective-permute-start | bytes 319496 | tf_op jit(solution)/shard_map/ppermute | solution.py:46
  127.0 2.6 %collective-permute-start.8 = (bf16[416,128]{1,0:T(8,128)(2,1)S(1)}, bf16[416,128]{1,0:T(8,128)(2,1)S(1)}, u32[]{:S(2)}, u32[]{:S(2)}) collective-permute-start(bf16[416,128]{1,0:T(8,128)(2,1)S(1)} %get-tuple-element.33), channel_id=1, source_target_pairs={{0,8},{8,0},{16,24},{24,16},{1,9},{9,1},{17,25},{25,17},{2,10},{10... | collective-permute-start | bytes 319496 | tf_op jit(solution)/shard_map/ppermute | solution.py:46
  129.6 2.3 %collective-permute-done.7 = bf16[416,128]{1,0:T(8,128)(2,1)S(1)} collective-permute-done((bf16[416,128]{1,0:T(8,128)(2,1)S(1)}, bf16[416,128]{1,0:T(8,128)(2,1)S(1)}, u32[]{:S(2)}, u32[]{:S(2)}) %collective-permute-start.7) | collective-permute-done | bytes 106528 | tf_op jit(solution)/shard_map/ppermute | solution.py:46
  131.9 1.4 collective-permute-done.8
  133.5 0.2 convolution_convert_fusion
  133.8 0.7 copy.77
  134.6 8.6 %all-to-all-start.4 = ((bf16[32,32,128]{2,1,0:T(8,128)(2,1)}), bf16[32,32,128]{2,1,0:T(8,128)(2,1)S(1)}, u32[]{:S(2)}, u32[]{:S(2)}) async-start(bf16[32,32,128]{2,1,0:T(8,128)(2,1)} %bitcast.134), calls=%async_computation.4 | async-start | bytes 524288 | tf_op jit(solution)/shard_map/all_to_all | solution.py:30
  143.4 10.8 %all-to-all-done.4 = bf16[32,32,128]{2,1,0:T(8,128)(2,1)S(1)} async-done(((bf16[32,32,128]{2,1,0:T(8,128)(2,1)}), bf16[32,32,128]{2,1,0:T(8,128)(2,1)S(1)}, u32[]{:S(2)}, u32[]{:S(2)}) %all-to-all-start.4) | async-done | bytes 262176 | tf_op jit(solution)/shard_map/all_to_all | solution.py:30
  154.3 0.1 multiply_reduce_fusion
  154.5 0.1 fusion.76
  154.7 0.1 fusion.79
  154.9 0.1 fusion.15
  155.1 0.2 fusion.116
  155.5 3.8 %collective-permute-start.9 = (f32[8,128]{1,0:T(8,128)S(1)}, f32[8,128]{1,0:T(8,128)S(1)}, u32[]{:S(2)}, u32[]{:S(2)}) collective-permute-start(f32[8,128]{1,0:T(8,128)S(1)} %get-tuple-element.91), channel_id=1, source_target_pairs={{0,24},{8,16},{16,8},{24,0},{1,25},{9,17},{17,9},{25,1},{2,26},{10... | collective-permute-start | bytes 12296 | tf_op jit(solution)/shard_map/ppermute | solution.py:46
  159.2 2.6 %collective-permute-start.10 = (f32[8,128]{1,0:T(8,128)S(1)}, f32[8,128]{1,0:T(8,128)S(1)}, u32[]{:S(2)}, u32[]{:S(2)}) collective-permute-start(f32[8,128]{1,0:T(8,128)S(1)} %get-tuple-element.90), channel_id=1, source_target_pairs={{0,16},{8,24},{16,0},{24,8},{1,17},{9,25},{17,1},{25,9},{2,18},{10... | collective-permute-start | bytes 12296 | tf_op jit(solution)/shard_map/ppermute | solution.py:46
  161.8 2.6 %collective-permute-start.11 = (f32[8,128]{1,0:T(8,128)S(1)}, f32[8,128]{1,0:T(8,128)S(1)}, u32[]{:S(2)}, u32[]{:S(2)}) collective-permute-start(f32[8,128]{1,0:T(8,128)S(1)} %get-tuple-element.89), channel_id=1, source_target_pairs={{0,8},{8,0},{16,24},{24,16},{1,9},{9,1},{17,25},{25,17},{2,10},{10... | collective-permute-start | bytes 12296 | tf_op jit(solution)/shard_map/ppermute | solution.py:46
  164.5 0.7 copy_bitcast_fusion
  165.2 6.0 %all-to-all-start.5 = ((bf16[32,16,128]{2,1,0:T(8,128)(2,1)}), bf16[32,16,128]{2,1,0:T(8,128)(2,1)S(1)}, u32[]{:S(2)}, u32[]{:S(2)}) async-start(bf16[32,16,128]{2,1,0:T(8,128)(2,1)} %copy_bitcast_fusion), calls=%async_computation.5 | async-start | bytes 262144 | tf_op jit(solution)/shard_map/all_to_all | solution.py:30
  171.5 7.2 %all-to-all-done.5 = bf16[32,16,128]{2,1,0:T(8,128)(2,1)S(1)} async-done(((bf16[32,16,128]{2,1,0:T(8,128)(2,1)}), bf16[32,16,128]{2,1,0:T(8,128)(2,1)S(1)}, u32[]{:S(2)}, u32[]{:S(2)}) %all-to-all-start.5) | async-done | bytes 131104 | tf_op jit(solution)/shard_map/all_to_all | solution.py:30
  178.8 0.2 convolution_convert_fusion.2
  178.9 0.6 reshape.479
  179.6 17.3 %all-to-all-start.6 = ((bf16[32,4,256]{2,1,0:T(4,128)(2,1)}), bf16[32,4,256]{2,1,0:T(4,128)(2,1)S(1)}, u32[]{:S(2)}, u32[]{:S(2)}) async-start(bf16[32,4,256]{2,1,0:T(4,128)(2,1)} %reshape.479), calls=%async_computation.6 | async-start | bytes 131072 | tf_op jit(solution)/shard_map/all_to_all | solution.py:36
  197.0 0.7 slice-done
  197.7 0.6 pad_maximum_fusion.19
  198.3 0.6 slice_bitcast_fusion.6
  198.9 9.3 %all-to-all-done.6 = bf16[32,4,256]{2,1,0:T(4,128)(2,1)S(1)} async-done(((bf16[32,4,256]{2,1,0:T(4,128)(2,1)}), bf16[32,4,256]{2,1,0:T(4,128)(2,1)S(1)}, u32[]{:S(2)}, u32[]{:S(2)}) %all-to-all-start.6) | async-done | bytes 65568 | tf_op jit(solution)/shard_map/all_to_all | solution.py:36
  208.3 0.8 fusion.28
  (164 shorter events, 4.3 us)
Async XLA Ops:
  0.6 5.6 %copy-start = (bf16[2,4,32]{2,1,0:T(4,128)(2,1)S(1)}, bf16[2,4,32]{2,1,0:T(4,128)(2,1)}, u32[]{:S(2)}) copy-start(bf16[2,4,32]{2,1,0:T(4,128)(2,1)} %param.19) | copy-start | bytes 1540
  0.6 0.8 copy-start.2
  0.7 0.8 copy-start.8
  2.7 0.8 copy-start.4
  3.4 0.8 copy-start.5
  4.4 0.7 copy-start.11
  4.4 0.8 copy-start.6
  5.1 0.7 copy-start.10
  5.2 0.9 copy-start.3
  6.2 137.0 %copy-start.1 = (bf16[2,32,3,32]{3,1,2,0:T(8,128)(2,1)}, bf16[2,32,3,32]{3,1,2,0:T(8,128)(2,1)S(1)}, u32[]{:S(2)}) copy-start(bf16[2,32,3,32]{3,1,2,0:T(8,128)(2,1)S(1)} %broadcast_select_fusion.13) | copy-start | bytes 36868
  6.6 39.1 %collective-permute-start = (bf16[352,128]{1,0:T(8,128)(2,1)S(1)}, bf16[352,128]{1,0:T(8,128)(2,1)S(1)}, u32[]{:S(2)}, u32[]{:S(2)}) collective-permute-start(bf16[352,128]{1,0:T(8,128)(2,1)S(1)} %get-tuple-element.38), channel_id=1, source_target_pairs={{0,24},{8,16},{16,8},{24,0},{1,25},{9,17},{17,9},{25,1},{2,26},{10... | collective-permute-start | bytes 270344 | tf_op jit(solution)/shard_map/ppermute | solution.py:46
  12.1 4.4 %copy-start.9 = (bf16[256,4]{0,1:T(4,128)(2,1)S(1)}, bf16[256,4]{0,1:T(4,128)(2,1)}, u32[]{:S(2)}) copy-start(bf16[256,4]{0,1:T(4,128)(2,1)} %param.12) | copy-start | bytes 6148
  12.1 33.6 %collective-permute-start.1 = (bf16[352,128]{1,0:T(8,128)(2,1)S(1)}, bf16[352,128]{1,0:T(8,128)(2,1)S(1)}, u32[]{:S(2)}, u32[]{:S(2)}) collective-permute-start(bf16[352,128]{1,0:T(8,128)(2,1)S(1)} %get-tuple-element.37), channel_id=1, source_target_pairs={{0,16},{8,24},{16,0},{24,8},{1,17},{9,25},{17,1},{25,9},{2,18},{10... | collective-permute-start | bytes 270344 | tf_op jit(solution)/shard_map/ppermute | solution.py:46
  14.4 31.3 %collective-permute-start.2 = (bf16[352,128]{1,0:T(8,128)(2,1)S(1)}, bf16[352,128]{1,0:T(8,128)(2,1)S(1)}, u32[]{:S(2)}, u32[]{:S(2)}) collective-permute-start(bf16[352,128]{1,0:T(8,128)(2,1)S(1)} %get-tuple-element.36), channel_id=1, source_target_pairs={{0,8},{8,0},{16,24},{24,16},{1,9},{9,1},{17,25},{25,17},{2,10},{10... | collective-permute-start | bytes 270344 | tf_op jit(solution)/shard_map/ppermute | solution.py:46
  17.2 42.4 %all-to-all-start = ((bf16[32,4,256]{2,1,0:T(4,128)(2,1)}), bf16[32,4,256]{2,1,0:T(4,128)(2,1)S(1)}, u32[]{:S(2)}, u32[]{:S(2)}) async-start(bf16[32,4,256]{2,1,0:T(4,128)(2,1)} %broadcast_in_dim.118), calls=%async_computation | async-start | bytes 131072 | tf_op jit(solution)/shard_map/all_to_all | solution.py:36
  61.1 20.5 %all-to-all-start.1 = ((bf16[64,16,128]{2,1,0:T(8,128)(2,1)}), bf16[64,16,128]{2,1,0:T(8,128)(2,1)S(1)}, u32[]{:S(2)}, u32[]{:S(2)}) async-start(bf16[64,16,128]{2,1,0:T(8,128)(2,1)} %bitcast.75), calls=%async_computation.1 | async-start | bytes 524288 | tf_op jit(solution)/shard_map/all_to_all | solution.py:30
  72.4 5.5 %collective-permute-start.3 = (bf16[256,128]{1,0:T(8,128)(2,1)S(1)}, bf16[256,128]{1,0:T(8,128)(2,1)S(1)}, u32[]{:S(2)}, u32[]{:S(2)}) collective-permute-start(bf16[256,128]{1,0:T(8,128)(2,1)S(1)} %get-tuple-element.39), channel_id=1, source_target_pairs={{0,32},{32,0},{64,96},{96,64},{1,33},{33,1},{65,97},{97,65},{2,34}... | collective-permute-start | bytes 196616 | tf_op jit(solution)/shard_map/ppermute | solution.py:46
  83.2 11.4 %copy-start.7 = (bf16[2,32,512]{2,1,0:T(8,128)(2,1)S(1)}, bf16[2,32,512]{2,1,0:T(8,128)(2,1)}, u32[]{:S(2)}) copy-start(bf16[2,32,512]{2,1,0:T(8,128)(2,1)} %param.23) | copy-start | bytes 196612
  83.2 15.3 %all-to-all-start.2 = ((bf16[32,16,128]{2,1,0:T(8,128)(2,1)}), bf16[32,16,128]{2,1,0:T(8,128)(2,1)S(1)}, u32[]{:S(2)}, u32[]{:S(2)}) async-start(bf16[32,16,128]{2,1,0:T(8,128)(2,1)} %maximum_bitcast_fusion), calls=%async_computation.2 | async-start | bytes 262144 | tf_op jit(solution)/shard_map/all_to_all | solution.py:30
  87.2 9.2 %collective-permute-start.5 = (bf16[256,128]{1,0:T(8,128)(2,1)S(1)}, bf16[256,128]{1,0:T(8,128)(2,1)S(1)}, u32[]{:S(2)}, u32[]{:S(2)}) collective-permute-start(bf16[256,128]{1,0:T(8,128)(2,1)S(1)} %get-tuple-element.40), channel_id=1, source_target_pairs={{0,64},{32,96},{64,0},{96,32},{1,65},{33,97},{65,1},{97,33},{2,66}... | collective-permute-start | bytes 196616 | tf_op jit(solution)/shard_map/ppermute | solution.py:46
  91.5 6.9 %collective-permute-start.4 = (bf16[256,128]{1,0:T(8,128)(2,1)S(1)}, bf16[256,128]{1,0:T(8,128)(2,1)S(1)}, u32[]{:S(2)}, u32[]{:S(2)}) collective-permute-start(bf16[256,128]{1,0:T(8,128)(2,1)S(1)} %get-tuple-element.41), channel_id=1, source_target_pairs={{0,96},{32,64},{64,32},{96,0},{1,97},{33,65},{65,33},{97,1},{2,98}... | collective-permute-start | bytes 196616 | tf_op jit(solution)/shard_map/ppermute | solution.py:46
  99.3 34.1 %all-to-all-start.3 = ((bf16[8,64,128]{2,1,0:T(8,128)(2,1)}), bf16[8,64,128]{2,1,0:T(8,128)(2,1)S(1)}, u32[]{:S(2)}, u32[]{:S(2)}) async-start(bf16[8,64,128]{2,1,0:T(8,128)(2,1)} %broadcast_in_dim.119), calls=%async_computation.3 | async-start | bytes 262144 | tf_op jit(solution)/shard_map/all_to_all | solution.py:36
  120.6 9.0 %collective-permute-start.6 = (bf16[416,128]{1,0:T(8,128)(2,1)S(1)}, bf16[416,128]{1,0:T(8,128)(2,1)S(1)}, u32[]{:S(2)}, u32[]{:S(2)}) collective-permute-start(bf16[416,128]{1,0:T(8,128)(2,1)S(1)} %get-tuple-element.35), channel_id=1, source_target_pairs={{0,24},{8,16},{16,8},{24,0},{1,25},{9,17},{17,9},{25,1},{2,26},{10... | collective-permute-start | bytes 319496 | tf_op jit(solution)/shard_map/ppermute | solution.py:46
  124.6 7.2 %collective-permute-start.7 = (bf16[416,128]{1,0:T(8,128)(2,1)S(1)}, bf16[416,128]{1,0:T(8,128)(2,1)S(1)}, u32[]{:S(2)}, u32[]{:S(2)}) collective-permute-start(bf16[416,128]{1,0:T(8,128)(2,1)S(1)} %get-tuple-element.34), channel_id=1, source_target_pairs={{0,16},{8,24},{16,0},{24,8},{1,17},{9,25},{17,1},{25,9},{2,18},{10... | collective-permute-start | bytes 319496 | tf_op jit(solution)/shard_map/ppermute | solution.py:46
  127.0 6.2 %collective-permute-start.8 = (bf16[416,128]{1,0:T(8,128)(2,1)S(1)}, bf16[416,128]{1,0:T(8,128)(2,1)S(1)}, u32[]{:S(2)}, u32[]{:S(2)}) collective-permute-start(bf16[416,128]{1,0:T(8,128)(2,1)S(1)} %get-tuple-element.33), channel_id=1, source_target_pairs={{0,8},{8,0},{16,24},{24,16},{1,9},{9,1},{17,25},{25,17},{2,10},{10... | collective-permute-start | bytes 319496 | tf_op jit(solution)/shard_map/ppermute | solution.py:46
  134.6 19.6 %all-to-all-start.4 = ((bf16[32,32,128]{2,1,0:T(8,128)(2,1)}), bf16[32,32,128]{2,1,0:T(8,128)(2,1)S(1)}, u32[]{:S(2)}, u32[]{:S(2)}) async-start(bf16[32,32,128]{2,1,0:T(8,128)(2,1)} %bitcast.134), calls=%async_computation.4 | async-start | bytes 524288 | tf_op jit(solution)/shard_map/all_to_all | solution.py:30
  155.5 15.7 %collective-permute-start.9 = (f32[8,128]{1,0:T(8,128)S(1)}, f32[8,128]{1,0:T(8,128)S(1)}, u32[]{:S(2)}, u32[]{:S(2)}) collective-permute-start(f32[8,128]{1,0:T(8,128)S(1)} %get-tuple-element.91), channel_id=1, source_target_pairs={{0,24},{8,16},{16,8},{24,0},{1,25},{9,17},{17,9},{25,1},{2,26},{10... | collective-permute-start | bytes 12296 | tf_op jit(solution)/shard_map/ppermute | solution.py:46
  159.2 12.0 %collective-permute-start.10 = (f32[8,128]{1,0:T(8,128)S(1)}, f32[8,128]{1,0:T(8,128)S(1)}, u32[]{:S(2)}, u32[]{:S(2)}) collective-permute-start(f32[8,128]{1,0:T(8,128)S(1)} %get-tuple-element.90), channel_id=1, source_target_pairs={{0,16},{8,24},{16,0},{24,8},{1,17},{9,25},{17,1},{25,9},{2,18},{10... | collective-permute-start | bytes 12296 | tf_op jit(solution)/shard_map/ppermute | solution.py:46
  161.8 9.4 %collective-permute-start.11 = (f32[8,128]{1,0:T(8,128)S(1)}, f32[8,128]{1,0:T(8,128)S(1)}, u32[]{:S(2)}, u32[]{:S(2)}) collective-permute-start(f32[8,128]{1,0:T(8,128)S(1)} %get-tuple-element.89), channel_id=1, source_target_pairs={{0,8},{8,0},{16,24},{24,16},{1,9},{9,1},{17,25},{25,17},{2,10},{10... | collective-permute-start | bytes 12296 | tf_op jit(solution)/shard_map/ppermute | solution.py:46
  165.2 13.6 %all-to-all-start.5 = ((bf16[32,16,128]{2,1,0:T(8,128)(2,1)}), bf16[32,16,128]{2,1,0:T(8,128)(2,1)S(1)}, u32[]{:S(2)}, u32[]{:S(2)}) async-start(bf16[32,16,128]{2,1,0:T(8,128)(2,1)} %copy_bitcast_fusion), calls=%async_computation.5 | async-start | bytes 262144 | tf_op jit(solution)/shard_map/all_to_all | solution.py:30
  179.6 28.6 %all-to-all-start.6 = ((bf16[32,4,256]{2,1,0:T(4,128)(2,1)}), bf16[32,4,256]{2,1,0:T(4,128)(2,1)S(1)}, u32[]{:S(2)}, u32[]{:S(2)}) async-start(bf16[32,4,256]{2,1,0:T(4,128)(2,1)} %reshape.479), calls=%async_computation.6 | async-start | bytes 131072 | tf_op jit(solution)/shard_map/all_to_all | solution.py:36
  196.9 0.8 slice-start

commit v9 on v8

--- a/solution.py
+++ b/solution.py
@@ -1,6 +1,8 @@
 import jax
 import jax.numpy as jnp
 from jax import lax
+from jax.experimental import pallas as pl
+from jax.experimental.pallas import tpu as pltpu
 from jax.sharding import Mesh
 from jax.sharding import PartitionSpec as P
 
@@ -48,7 +50,8 @@
 
 def traded(tiles, axis):
     here = lax.axis_index(axis)
-    pieces = [lax.dynamic_slice_in_dim(tiles, here ^ flip, 1)[0] for flip in range(4)]
+    tiles = tiles if isinstance(tiles, list) else [tiles] * 4
+    pieces = [lax.dynamic_slice_in_dim(tiles[flip], here ^ flip, 1)[0] for flip in range(4)]
     return pieces[:1] + [passed(pieces[flip], axis, flip) for flip in range(1, 4)]
 
 
@@ -56,13 +59,6 @@
     here = lax.axis_index(axis)
     pieces = [jnp.where((here & 1) == 1, pieces[k ^ 1], pieces[k]) for k in range(4)]
     return [jnp.where(here > 1, pieces[k ^ 2], pieces[k]) for k in range(4)]
-
-
-def parts_of(value):
-    coarse = lax.reduce_precision(value, 8, 7)
-    rest = value - coarse
-    middle = lax.reduce_precision(rest, 8, 7)
-    return [coarse.astype(bf16), middle.astype(bf16), (rest - middle).astype(bf16)]
 
 
 def whole_of(coarse, middle, fine):
@@ -79,6 +75,63 @@
     source = ((to % 128) // 4 + first) % 32 * 16 + to // 128 * 4 + to % 4
     chosen = (jnp.arange(width, dtype=jnp.int32)[:, None] == source[None, :]).astype(bf16)
     return contract(rows_by_feature, 1, chosen, 0).astype(bf16)
+
+
+def pack_kernel(branch, gate, out, in_gate, rec_gate, gain, state, window, taps, decay, packed, later):
+    row = lax.broadcasted_iota(jnp.int32, (8, 32), 0)
+    weights = [
+        (weight[layer].astype(f32) * gain[layer : layer + 1]).astype(bf16)
+        for layer in range(2)
+        for weight in (branch, gate)
+    ]
+    width = 512
+    to = lax.broadcasted_iota(jnp.int32, (width, width), 1)
+    source = (((to & 127) >> 2) + FIRST_GATHER & 31) * 16 + (to >> 7) * 4 + (to & 3)
+    chosen = lax.broadcasted_iota(jnp.int32, (width, width), 0) == source
+    chosen = jnp.where(chosen, 1.0, 0.0).astype(bf16)
+    weights = jnp.concatenate([*weights, out[0]], axis=0)
+    weights = jnp.dot(weights, chosen, preferred_element_type=f32).astype(bf16)
+
+    def split(value):
+        coarse = value.astype(bf16).astype(f32)
+        middle = (value - coarse).astype(bf16).astype(f32)
+        return [coarse, middle, value - coarse - middle]
+
+    rates = split(jnp.where((row & 1) == 0, decay[:1], decay[1:2]))
+    rates = jnp.where(row < 2, rates[0], jnp.where(row < 4, rates[1], rates[2]))
+    rates = jnp.where(row < 6, rates, 0.0)
+    tap_rows = jnp.concatenate([taps[0].astype(f32), taps[1].astype(f32)], axis=0)
+    none = jnp.zeros((32, 32), f32)
+    small = [part for layer in range(2) for part in split(state[layer])]
+    small = small + [jnp.concatenate([rates] * 4, axis=0), none]
+    small = small + [window[layer, tap].astype(f32) for layer in range(2) for tap in range(3)]
+    small = small + [jnp.concatenate([tap_rows] * 4, axis=0), none]
+    small = [jnp.concatenate(small[4 * at : 4 * at + 4], axis=1) for at in range(4)]
+    for y in range(4):
+        packed[y, :64] = weights[:64, 128 * y : 128 * (y + 1)]
+        for kind, weight in enumerate((in_gate, rec_gate)):
+            for half in range(2):
+                place = 64 + 32 * (2 * kind + half)
+                packed[y, place : place + 32] = weight[0, :, 128 * half : 128 * (half + 1)]
+        for q in range(4):
+            place = 192 + 32 * q
+            packed[y, place : place + 32] = weights[128:, 128 * q : 128 * (q + 1)]
+        later[y] = weights[64:128, 128 * y : 128 * (y + 1)]
+        for at in range(4):
+            place = 320 + 8 * at
+            packed[y, place : place + 8] = small[at][8 * y : 8 * (y + 1)].astype(bf16)
+
+
+def packed_for_y(*arrays):
+    return pl.pallas_call(
+        pack_kernel,
+        out_shape=[
+            jax.ShapeDtypeStruct((4, 352, 128), bf16),
+            jax.ShapeDtypeStruct((4, 64, 128), bf16),
+        ],
+        compiler_params=pltpu.CompilerParams(vmem_limit_bytes=8 * 2**20),
+        cost_estimate=pl.CostEstimate(flops=100_000_000, bytes_accessed=800_000, transcendentals=0),
+    )(*arrays)
 
 
 def gated_step(branch, gate_in, upper, history, taps, gates, decay, earlier):
@@ -122,65 +175,37 @@
 
     stream_t = everywhere(stream.T, Z, FIRST_GATHER).reshape(128, 256)
 
-    def scaled(weight, layer):
-        return (weight[layer].T.astype(f32) * norm_gain[layer]).astype(bf16)
-
-    def grouped(*weights):
-        rows = grouped_features(jnp.concatenate(weights), FIRST_GATHER)
-        return rows.reshape(-1, 4, 128).transpose(1, 0, 2)
-
-    first_weights = grouped(scaled(w_branch, 0), scaled(w_gate_branch, 0), w_out[0])
-    second_weights = grouped(scaled(w_branch, 1), scaled(w_gate_branch, 1))
-
-    gate_rows = (
-        jnp.stack([w_in_gate, w_rec_gate], axis=1)
-        .reshape(LAYERS, 2, 2, 128, 32)
-        .transpose(0, 1, 2, 4, 3)
-        .reshape(256, 128)
+    second_gate_rows = jnp.concatenate(
+        [
+            weight[1, 128 * half : 128 * (half + 1)].T
+            for weight in (w_in_gate, w_rec_gate)
+            for half in range(2)
+        ]
     )
     depth = TAPS - 1
-    needed = depth + 1 - jnp.arange(depth, dtype=jnp.int32)
-    living = lengths[None, :, None, None] >= needed[None, None, :, None]
-    history = jnp.where(living, prior_window, jnp.zeros_like(prior_window))
-    earlier = jnp.where(
-        lengths[None, :, None] >= 2, prior_state, jnp.zeros_like(prior_state)
-    )
-
-    def by_rows(groups):
-        packed = jnp.concatenate(groups, axis=1).reshape(4, 8, -1, 128)
-        return packed.transpose(0, 2, 1, 3).reshape(4, -1, 128)
-
-    def for_all(rows):
-        return jnp.broadcast_to(rows[None], (4, 8, 32)).reshape(32, 32)
-
-    decay = jnp.concatenate(
-        parts_of(jax.nn.log_sigmoid(decay_param)) + [jnp.zeros((2, 32), bf16)]
-    )
-    none = jnp.zeros((32, 32), bf16)
-    small = by_rows(
-        [part[layer] for layer in range(LAYERS) for part in parts_of(earlier)]
-        + [for_all(decay), none]
-    )
-    windows = by_rows(
-        [history[layer, :, tap] for layer in range(LAYERS) for tap in range(depth)]
-        + [for_all(conv_taps.reshape(8, 32)), none]
-    )
 
     def for_each(rows):
         return jnp.broadcast_to(rows.reshape(1, -1, 128), (4, rows.size // 128, 128))
 
-    near = jnp.concatenate(
-        [
-            first_weights[:, :64],
-            for_each(gate_rows[:128]),
-            for_each(first_weights[:, 64:]),
-            small,
-            windows,
-        ],
-        axis=1,
+    near, second_weights = packed_for_y(
+        w_branch.transpose(0, 2, 1),
+        w_gate_branch.transpose(0, 2, 1),
+        w_out,
+        w_in_gate.transpose(0, 2, 1),
+        w_rec_gate.transpose(0, 2, 1),
+        norm_gain,
+        prior_state,
+        prior_window.transpose(0, 2, 1, 3),
+        conv_taps,
+        decay_param,
     )
     near = jnp.stack(in_order(traded(near, "y"), "y"))
     w_first = near[:, :64].reshape(4, 2, 32, 128).transpose(1, 0, 2, 3).reshape(2, 128, 128)
+    index = lax.broadcasted_iota(jnp.int32, (128, 128), 0)
+    same = (index == lax.broadcasted_iota(jnp.int32, (128, 128), 1)).astype(bf16)
+    w_first = jnp.concatenate(
+        [w_first[0], jnp.where(upper, same, w_first[1]), jnp.where(upper, w_first[1], same)]
+    )
 
     def gates_of(rows):
         return (
@@ -198,11 +223,11 @@
         [
             near[:, 192:320].reshape(4, 4, 32, 128).transpose(1, 0, 2, 3).reshape(4, 128, 128),
             second_weights,
-            for_each(near[:, 336:]),
         ],
         axis=1,
     )
-    shared = traded(shared, ZQ)
+    with_windows = jnp.concatenate([shared, for_each(near[:, 336:])], axis=1)
+    shared = traded([shared, with_windows, shared, shared], ZQ)
     partner = by_group(shared[1][192:].reshape(4, 16, 128))
     windows = jnp.concatenate(
         [jnp.where(upper, partner, groups[8:]), jnp.where(upper, groups[8:], partner)], axis=2
@@ -211,7 +236,7 @@
     w_mid = jnp.concatenate([piece[:128] for piece in shared])
     later_rows = jnp.concatenate(
         [
-            for_each(gate_rows[128:]),
+            for_each(second_gate_rows),
             for_each(jnp.concatenate([piece[128:] for piece in shared])),
             grouped_features(w_out[1], FIRST_LAST).reshape(32, 4, 128).transpose(1, 0, 2),
         ],
@@ -227,26 +252,30 @@
     )
     w_last = later_rows[:, 384:].reshape(128, 128)
 
-    earlier_rows = [whole_of(*groups[3 * layer : 3 * layer + 3]) for layer in range(LAYERS)]
+    own_lengths = lax.dynamic_slice_in_dim(lengths, lax.axis_index("y") * 8, 8)[:, None]
+    earlier_rows = [
+        jnp.where(own_lengths >= 2, whole_of(*groups[3 * layer : 3 * layer + 3]), 0.0)
+        for layer in range(LAYERS)
+    ]
     decay = whole_of(groups[6][:2], groups[6][2:4], groups[6][4:6])[:, None]
-    history_rows = windows[:6].reshape(LAYERS, depth, 8, 256)
+    decay = jax.nn.log_sigmoid(decay)
+    needed = depth + 1 - jnp.arange(depth, dtype=jnp.int32)
+    history_rows = jnp.where(
+        own_lengths >= needed[:, None, None], windows[:6].reshape(LAYERS, depth, 8, 256), 0.0
+    )
     taps = windows[6].reshape(LAYERS, TAPS, 256)
 
-    products = [
-        contract(stream_t, 0, w_first[kind], 1).astype(bf16).reshape(8, 4, 8, 128)
-        for kind in range(2)
-    ]
-    products.append(stream_t.T.reshape(8, 4, 8, 128))
-    branch, gate_in, rows = [part.transpose(1, 0, 2, 3) for part in products]
+    products = contract(stream_t, 0, w_first, 1).astype(bf16)
+    products = products.reshape(8, 4, 8, 3, 128).transpose(3, 1, 0, 2, 4)
     sent = jnp.stack(
         [
-            jnp.stack([branch, jnp.where(upper, rows, gate_in)], axis=2),
-            jnp.stack([branch, jnp.where(upper, gate_in, rows)], axis=2),
+            jnp.stack([products[0], products[1]], axis=2),
+            jnp.stack([products[0], products[2]], axis=2),
         ]
     )
     came = exchange(sent.reshape(64, 16, 128), PAIRED_PLANE)
     came = came.reshape(2, 32, 2, 8, 128)
-    later = (history_rows[1], taps[1], decay[1], earlier_rows[1], history)
+    later = (history_rows[1], taps[1], decay[1], earlier_rows[1])
     branch = came[:, :, 0].astype(f32).sum(axis=1)
     branch = jnp.concatenate([branch[0], branch[1]], axis=1)
     rows = jnp.where(upper, came[0, :, 1], came[1, :, 1])
@@ -296,6 +325,7 @@
         ]
     )
     came = exchange(sent.reshape(32, 32, 128), ZQ + DP).reshape(32, 4, 8, 128)
+    came, state_first, branch_first = lax.optimization_barrier((came, state_first, branch_first))
     rows = came[:, 3]
     came = came[:, :3].astype(f32).sum(axis=0)
     widened = rows.astype(f32)
@@ -335,7 +365,9 @@
     kept = kept.reshape(4, 8, 4, 32).transpose(2, 0, 1, 3).reshape(4, 8, 128)
     kept = jnp.stack(in_order(traded(kept, "y"), "y"))
     kept = kept.reshape(4, 4, 8, 32).transpose(1, 0, 2, 3).reshape(2, LAYERS, 32, 32)
-    window = jnp.concatenate([later[4][:, :, 1:], kept[1].astype(bf16)[:, :, None]], axis=2)
+    living = lengths[None, :, None, None] >= needed[None, None, 1:, None]
+    history = jnp.where(living, prior_window[:, :, 1:], jnp.zeros_like(prior_window[:, :, 1:]))
+    window = jnp.concatenate([history, kept[1].astype(bf16)[:, :, None]], axis=2)
     return second.T, kept[0], window
 
 

time: 210 us -> 210 us (level)
    unnamed x28 -> x30, local copies, waits for them, and re-layouts: 2.91 us -> 6.21 us
where the time goes in v9:
time: 210 us; the launch traced here: 209 us
  starting transfers between devices  135 us (64%)
  waiting for transfers between devices  52.3 us (25%)
  local copies, waits for them, and re-layouts  12.4 us (6%)
  other arithmetic  3.67 us (2%)
  matrix products  2.99 us (1%)
    all_to_all x3, starting transfers between devices, exchange_far(): lax.all_to_all(tiles, axes, 0, 0, axis_index_groups=[order], tiled=True)  67 us
    ppermute x12, starting transfers between devices, passed(): lax.ppermute(piece, axis, [(at, at ^ flip) for at in range(lax.axis_size(...  38.5 us
    all_to_all x4, starting transfers between devices, exchange(): return lax.all_to_all(tiles, axes, 0, 0, tiled=True)  29.9 us
    all_to_all x3, waiting for transfers between devices, exchange_far(): lax.all_to_all(tiles, axes, 0, 0, axis_index_groups=[order], tiled=True)  22.7 us
    all_to_all x4, waiting for transfers between devices, exchange(): return lax.all_to_all(tiles, axes, 0, 0, tiled=True)  21 us
    ppermute x12, waiting for transfers between devices, passed(): lax.ppermute(piece, axis, [(at, at ^ flip) for at in range(lax.axis_size(...  8.67 us
    unnamed x30, local copies, waits for them, and re-layouts  6.21 us
  transfers between devices with their start and end apart: 19, of which 10 were waited for; matrix products, arithmetic and copies ran while one was open for 2% of the time, Pallas kernels for 0%

profile of v9, /device:TPU:1, one launch (start us, length us, event | category | flops | bytes accessed | tf_op | source)
XLA Modules:
  0.0 208.8 jit_solution(14509682799970858766)
XLA Ops:
  0.7 0.7 copy-done.2
  1.4 0.8 copy-done
  2.2 0.8 copy-done.3
  3.0 0.8 copy-done.5
  3.8 0.8 copy-done.6
  4.6 0.8 copy-done.7
  5.5 0.8 copy-done.9
  6.2 0.3 shard_map.139
  6.6 5.5 %collective-permute-start = (bf16[352,128]{1,0:T(8,128)(2,1)S(1)}, bf16[352,128]{1,0:T(8,128)(2,1)S(1)}, u32[]{:S(2)}, u32[]{:S(2)}) collective-permute-start(bf16[352,128]{1,0:T(8,128)(2,1)S(1)} %get-tuple-element.46), channel_id=1, source_target_pairs={{0,24},{8,16},{16,8},{24,0},{1,25},{9,17},{17,9},{25,1},{2,26},{10... | collective-permute-start | bytes 270344 | tf_op jit(solution)/shard_map/ppermute | solution.py:48
  12.1 2.3 %collective-permute-start.1 = (bf16[352,128]{1,0:T(8,128)(2,1)S(1)}, bf16[352,128]{1,0:T(8,128)(2,1)S(1)}, u32[]{:S(2)}, u32[]{:S(2)}) collective-permute-start(bf16[352,128]{1,0:T(8,128)(2,1)S(1)} %get-tuple-element.45), channel_id=1, source_target_pairs={{0,16},{8,24},{16,0},{24,8},{1,17},{9,25},{17,1},{25,9},{2,18},{10... | collective-permute-start | bytes 270344 | tf_op jit(solution)/shard_map/ppermute | solution.py:48
  14.3 2.1 %collective-permute-start.2 = (bf16[352,128]{1,0:T(8,128)(2,1)S(1)}, bf16[352,128]{1,0:T(8,128)(2,1)S(1)}, u32[]{:S(2)}, u32[]{:S(2)}) collective-permute-start(bf16[352,128]{1,0:T(8,128)(2,1)S(1)} %get-tuple-element.44), channel_id=1, source_target_pairs={{0,8},{8,0},{16,24},{24,16},{1,9},{9,1},{17,25},{25,17},{2,10},{10... | collective-permute-start | bytes 270344 | tf_op jit(solution)/shard_map/ppermute | solution.py:48
  16.5 0.6 broadcast_in_dim.86
  17.1 28.6 %all-to-all-start = ((bf16[32,4,256]{2,1,0:T(4,128)(2,1)}), bf16[32,4,256]{2,1,0:T(4,128)(2,1)S(1)}, u32[]{:S(2)}, u32[]{:S(2)}) async-start(bf16[32,4,256]{2,1,0:T(4,128)(2,1)} %broadcast_in_dim.86), calls=%async_computation | async-start | bytes 131072 | tf_op jit(solution)/shard_map/all_to_all | solution.py:38
  45.8 0.3 fusion.1
  46.1 0.6 copy-done.14
  47.0 12.7 %all-to-all-done = bf16[32,4,256]{2,1,0:T(4,128)(2,1)S(1)} async-done(((bf16[32,4,256]{2,1,0:T(4,128)(2,1)}), bf16[32,4,256]{2,1,0:T(4,128)(2,1)S(1)}, u32[]{:S(2)}, u32[]{:S(2)}) %all-to-all-start) | async-done | bytes 65568 | tf_op jit(solution)/shard_map/all_to_all | solution.py:38
  59.7 0.2 fusion
  59.9 0.2 copy.54
  60.2 0.8 copy.57
  60.9 10.8 %all-to-all-start.1 = ((bf16[64,16,128]{2,1,0:T(8,128)(2,1)}), bf16[64,16,128]{2,1,0:T(8,128)(2,1)S(1)}, u32[]{:S(2)}, u32[]{:S(2)}) async-start(bf16[64,16,128]{2,1,0:T(8,128)(2,1)} %bitcast.38), calls=%async_computation.1 | async-start | bytes 524288 | tf_op jit(solution)/shard_map/all_to_all | solution.py:32
  71.9 3.4 %collective-permute-start.3 = (bf16[256,128]{1,0:T(8,128)(2,1)S(1)}, bf16[256,128]{1,0:T(8,128)(2,1)S(1)}, u32[]{:S(2)}, u32[]{:S(2)}) collective-permute-start(bf16[256,128]{1,0:T(8,128)(2,1)S(1)} %fusion.43), channel_id=1, source_target_pairs={{0,32},{32,0},{64,96},{96,64},{1,33},{33,1},{65,97},{97,65},{2,34}... | collective-permute-start | bytes 196616 | tf_op jit(solution)/shard_map/ppermute | solution.py:48
  75.7 2.2 %collective-permute-done.3 = bf16[256,128]{1,0:T(8,128)(2,1)S(1)} collective-permute-done((bf16[256,128]{1,0:T(8,128)(2,1)S(1)}, bf16[256,128]{1,0:T(8,128)(2,1)S(1)}, u32[]{:S(2)}, u32[]{:S(2)}) %collective-permute-start.3) | collective-permute-done | bytes 65568 | tf_op jit(solution)/shard_map/ppermute | solution.py:48
  78.5 3.0 %all-to-all-done.1 = bf16[64,16,128]{2,1,0:T(8,128)(2,1)S(1)} async-done(((bf16[64,16,128]{2,1,0:T(8,128)(2,1)}), bf16[64,16,128]{2,1,0:T(8,128)(2,1)S(1)}, u32[]{:S(2)}, u32[]{:S(2)}) %all-to-all-start.1) | async-done | bytes 262176 | tf_op jit(solution)/shard_map/all_to_all | solution.py:32
  81.5 0.1 convert_reduce_fusion.4
  81.8 0.1 fusion.69
  81.9 0.1 fusion.70
  82.1 0.2 fusion.25
  82.2 0.2 fusion.111
  82.4 0.7 maximum_bitcast_fusion
  83.1 4.0 %all-to-all-start.2 = ((bf16[32,16,128]{2,1,0:T(8,128)(2,1)}), bf16[32,16,128]{2,1,0:T(8,128)(2,1)S(1)}, u32[]{:S(2)}, u32[]{:S(2)}) async-start(bf16[32,16,128]{2,1,0:T(8,128)(2,1)} %maximum_bitcast_fusion), calls=%async_computation.2 | async-start | bytes 262144 | tf_op jit(solution)/shard_map/all_to_all | solution.py:32
  87.2 4.3 %collective-permute-start.5 = (bf16[192,128]{1,0:T(8,128)(2,1)S(1)}, bf16[192,128]{1,0:T(8,128)(2,1)S(1)}, u32[]{:S(2)}, u32[]{:S(2)}) collective-permute-start(bf16[192,128]{1,0:T(8,128)(2,1)S(1)} %get-tuple-element.56), channel_id=1, source_target_pairs={{0,64},{32,96},{64,0},{96,32},{1,65},{33,97},{65,1},{97,33},{2,66}... | collective-permute-start | bytes 147464 | tf_op jit(solution)/shard_map/ppermute | solution.py:48
  91.5 3.0 %collective-permute-start.4 = (bf16[192,128]{1,0:T(8,128)(2,1)S(1)}, bf16[192,128]{1,0:T(8,128)(2,1)S(1)}, u32[]{:S(2)}, u32[]{:S(2)}) collective-permute-start(bf16[192,128]{1,0:T(8,128)(2,1)S(1)} %get-tuple-element.55), channel_id=1, source_target_pairs={{0,96},{32,64},{64,32},{96,0},{1,97},{33,65},{65,33},{97,1},{2,98}... | collective-permute-start | bytes 147464 | tf_op jit(solution)/shard_map/ppermute | solution.py:48
  94.6 1.0 collective-permute-done.5
  95.6 2.5 %collective-permute-done.4 = bf16[192,128]{1,0:T(8,128)(2,1)S(1)} collective-permute-done((bf16[192,128]{1,0:T(8,128)(2,1)S(1)}, bf16[192,128]{1,0:T(8,128)(2,1)S(1)}, u32[]{:S(2)}, u32[]{:S(2)}) %collective-permute-start.4) | collective-permute-done | bytes 49184 | tf_op jit(solution)/shard_map/ppermute | solution.py:48
  98.3 0.2 convolution_convert_fusion.4
  98.5 0.7 broadcast_in_dim.89
  99.1 21.1 %all-to-all-start.3 = ((bf16[8,64,128]{2,1,0:T(8,128)(2,1)}), bf16[8,64,128]{2,1,0:T(8,128)(2,1)S(1)}, u32[]{:S(2)}, u32[]{:S(2)}) async-start(bf16[8,64,128]{2,1,0:T(8,128)(2,1)} %broadcast_in_dim.89), calls=%async_computation.3 | async-start | bytes 262144 | tf_op jit(solution)/shard_map/all_to_all | solution.py:38
  120.4 3.7 %collective-permute-start.6 = (bf16[416,128]{1,0:T(8,128)(2,1)S(1)}, bf16[416,128]{1,0:T(8,128)(2,1)S(1)}, u32[]{:S(2)}, u32[]{:S(2)}) collective-permute-start(bf16[416,128]{1,0:T(8,128)(2,1)S(1)} %get-tuple-element.43), channel_id=1, source_target_pairs={{0,24},{8,16},{16,8},{24,0},{1,25},{9,17},{17,9},{25,1},{2,26},{10... | collective-permute-start | bytes 319496 | tf_op jit(solution)/shard_map/ppermute | solution.py:48
  124.1 2.4 %collective-permute-start.7 = (bf16[416,128]{1,0:T(8,128)(2,1)S(1)}, bf16[416,128]{1,0:T(8,128)(2,1)S(1)}, u32[]{:S(2)}, u32[]{:S(2)}) collective-permute-start(bf16[416,128]{1,0:T(8,128)(2,1)S(1)} %get-tuple-element.42), channel_id=1, source_target_pairs={{0,16},{8,24},{16,0},{24,8},{1,17},{9,25},{17,1},{25,9},{2,18},{10... | collective-permute-start | bytes 319496 | tf_op jit(solution)/shard_map/ppermute | solution.py:48
  126.4 2.9 %collective-permute-start.8 = (bf16[416,128]{1,0:T(8,128)(2,1)S(1)}, bf16[416,128]{1,0:T(8,128)(2,1)S(1)}, u32[]{:S(2)}, u32[]{:S(2)}) collective-permute-start(bf16[416,128]{1,0:T(8,128)(2,1)S(1)} %get-tuple-element.41), channel_id=1, source_target_pairs={{0,8},{8,0},{16,24},{24,16},{1,9},{9,1},{17,25},{25,17},{2,10},{10... | collective-permute-start | bytes 319496 | tf_op jit(solution)/shard_map/ppermute | solution.py:48
  129.4 1.8 collective-permute-done.7
  131.2 1.1 collective-permute-done.8
  132.6 0.2 convolution_convert_fusion.1
  132.9 0.7 copy.65
  133.7 9.1 %all-to-all-start.4 = ((bf16[32,32,128]{2,1,0:T(8,128)(2,1)}), bf16[32,32,128]{2,1,0:T(8,128)(2,1)S(1)}, u32[]{:S(2)}, u32[]{:S(2)}) async-start(bf16[32,32,128]{2,1,0:T(8,128)(2,1)} %bitcast.106), calls=%async_computation.4 | async-start | bytes 524288 | tf_op jit(solution)/shard_map/all_to_all | solution.py:32
  143.0 10.8 %all-to-all-done.4 = bf16[32,32,128]{2,1,0:T(8,128)(2,1)S(1)} async-done(((bf16[32,32,128]{2,1,0:T(8,128)(2,1)}), bf16[32,32,128]{2,1,0:T(8,128)(2,1)S(1)}, u32[]{:S(2)}, u32[]{:S(2)}) %all-to-all-start.4) | async-done | bytes 262176 | tf_op jit(solution)/shard_map/all_to_all | solution.py:32
  153.9 0.1 multiply_reduce_fusion
  154.2 0.1 fusion.72
  154.3 0.1 fusion.75
  154.7 0.1 fusion.13
  154.8 0.2 fusion.118
  155.3 3.8 %collective-permute-start.9 = (f32[8,128]{1,0:T(8,128)S(1)}, f32[8,128]{1,0:T(8,128)S(1)}, u32[]{:S(2)}, u32[]{:S(2)}) collective-permute-start(f32[8,128]{1,0:T(8,128)S(1)} %get-tuple-element.93), channel_id=1, source_target_pairs={{0,24},{8,16},{16,8},{24,0},{1,25},{9,17},{17,9},{25,1},{2,26},{10... | collective-permute-start | bytes 12296 | tf_op jit(solution)/shard_map/ppermute | solution.py:48
  159.1 2.8 %collective-permute-start.10 = (f32[8,128]{1,0:T(8,128)S(1)}, f32[8,128]{1,0:T(8,128)S(1)}, u32[]{:S(2)}, u32[]{:S(2)}) collective-permute-start(f32[8,128]{1,0:T(8,128)S(1)} %get-tuple-element.92), channel_id=1, source_target_pairs={{0,16},{8,24},{16,0},{24,8},{1,17},{9,25},{17,1},{25,9},{2,18},{10... | collective-permute-start | bytes 12296 | tf_op jit(solution)/shard_map/ppermute | solution.py:48
  161.9 2.4 %collective-permute-start.11 = (f32[8,128]{1,0:T(8,128)S(1)}, f32[8,128]{1,0:T(8,128)S(1)}, u32[]{:S(2)}, u32[]{:S(2)}) collective-permute-start(f32[8,128]{1,0:T(8,128)S(1)} %get-tuple-element.91), channel_id=1, source_target_pairs={{0,8},{8,0},{16,24},{24,16},{1,9},{9,1},{17,25},{25,17},{2,10},{10... | collective-permute-start | bytes 12296 | tf_op jit(solution)/shard_map/ppermute | solution.py:48
  164.3 0.7 copy_bitcast_fusion
  165.0 6.0 %all-to-all-start.5 = ((bf16[32,16,128]{2,1,0:T(8,128)(2,1)}), bf16[32,16,128]{2,1,0:T(8,128)(2,1)S(1)}, u32[]{:S(2)}, u32[]{:S(2)}) async-start(bf16[32,16,128]{2,1,0:T(8,128)(2,1)} %copy_bitcast_fusion), calls=%async_computation.5 | async-start | bytes 262144 | tf_op jit(solution)/shard_map/all_to_all | solution.py:32
  171.3 7.2 %all-to-all-done.5 = bf16[32,16,128]{2,1,0:T(8,128)(2,1)S(1)} async-done(((bf16[32,16,128]{2,1,0:T(8,128)(2,1)}), bf16[32,16,128]{2,1,0:T(8,128)(2,1)S(1)}, u32[]{:S(2)}, u32[]{:S(2)}) %all-to-all-start.5) | async-done | bytes 131104 | tf_op jit(solution)/shard_map/all_to_all | solution.py:32
  178.6 0.2 convolution_convert_fusion.2
  178.7 0.6 reshape.484
  179.4 17.3 %all-to-all-start.6 = ((bf16[32,4,256]{2,1,0:T(4,128)(2,1)}), bf16[32,4,256]{2,1,0:T(4,128)(2,1)S(1)}, u32[]{:S(2)}, u32[]{:S(2)}) async-start(bf16[32,4,256]{2,1,0:T(4,128)(2,1)} %reshape.484), calls=%async_computation.6 | async-start | bytes 131072 | tf_op jit(solution)/shard_map/all_to_all | solution.py:38
  196.7 0.6 pad_maximum_fusion.18
  197.3 0.6 slice_bitcast_fusion.9
  198.0 10.0 %all-to-all-done.6 = bf16[32,4,256]{2,1,0:T(4,128)(2,1)S(1)} async-done(((bf16[32,4,256]{2,1,0:T(4,128)(2,1)}), bf16[32,4,256]{2,1,0:T(4,128)(2,1)S(1)}, u32[]{:S(2)}, u32[]{:S(2)}) %all-to-all-start.6) | async-done | bytes 65568 | tf_op jit(solution)/shard_map/all_to_all | solution.py:38
  208.0 0.8 fusion.26
  (143 shorter events, 3.5 us)
Async XLA Ops:
  0.6 0.8 copy-start.2
  0.7 0.7 copy-start.10
  0.7 0.7 copy-start.11
  0.7 0.7 copy-start.12
  1.4 0.8 copy-start
  2.2 0.8 copy-start.3
  3.0 0.8 copy-start.5
  3.8 0.8 copy-start.6
  4.6 0.8 copy-start.7
  5.5 0.8 copy-start.9
  6.6 40.3 %collective-permute-start = (bf16[352,128]{1,0:T(8,128)(2,1)S(1)}, bf16[352,128]{1,0:T(8,128)(2,1)S(1)}, u32[]{:S(2)}, u32[]{:S(2)}) collective-permute-start(bf16[352,128]{1,0:T(8,128)(2,1)S(1)} %get-tuple-element.46), channel_id=1, source_target_pairs={{0,24},{8,16},{16,8},{24,0},{1,25},{9,17},{17,9},{25,1},{2,26},{10... | collective-permute-start | bytes 270344 | tf_op jit(solution)/shard_map/ppermute | solution.py:48
  12.0 4.4 %copy-start.13 = (bf16[256,4]{0,1:T(4,128)(2,1)S(1)}, bf16[256,4]{0,1:T(4,128)(2,1)}, u32[]{:S(2)}) copy-start(bf16[256,4]{0,1:T(4,128)(2,1)} %param.12) | copy-start | bytes 6148
  12.1 34.8 %collective-permute-start.1 = (bf16[352,128]{1,0:T(8,128)(2,1)S(1)}, bf16[352,128]{1,0:T(8,128)(2,1)S(1)}, u32[]{:S(2)}, u32[]{:S(2)}) collective-permute-start(bf16[352,128]{1,0:T(8,128)(2,1)S(1)} %get-tuple-element.45), channel_id=1, source_target_pairs={{0,16},{8,24},{16,0},{24,8},{1,17},{9,25},{17,1},{25,9},{2,18},{10... | collective-permute-start | bytes 270344 | tf_op jit(solution)/shard_map/ppermute | solution.py:48
  14.3 32.6 %collective-permute-start.2 = (bf16[352,128]{1,0:T(8,128)(2,1)S(1)}, bf16[352,128]{1,0:T(8,128)(2,1)S(1)}, u32[]{:S(2)}, u32[]{:S(2)}) collective-permute-start(bf16[352,128]{1,0:T(8,128)(2,1)S(1)} %get-tuple-element.44), channel_id=1, source_target_pairs={{0,8},{8,0},{16,24},{24,16},{1,9},{9,1},{17,25},{25,17},{2,10},{10... | collective-permute-start | bytes 270344 | tf_op jit(solution)/shard_map/ppermute | solution.py:48
  17.1 28.7 %copy-start.8 = (bf16[2,32,512]{2,1,0:T(8,128)(2,1)S(1)}, bf16[2,32,512]{2,1,0:T(8,128)(2,1)}, u32[]{:S(2)}) copy-start(bf16[2,32,512]{2,1,0:T(8,128)(2,1)} %out.1) | copy-start | bytes 196612
  17.1 42.5 %all-to-all-start = ((bf16[32,4,256]{2,1,0:T(4,128)(2,1)}), bf16[32,4,256]{2,1,0:T(4,128)(2,1)S(1)}, u32[]{:S(2)}, u32[]{:S(2)}) async-start(bf16[32,4,256]{2,1,0:T(4,128)(2,1)} %broadcast_in_dim.86), calls=%async_computation | async-start | bytes 131072 | tf_op jit(solution)/shard_map/all_to_all | solution.py:38
  46.1 0.7 copy-start.14
  60.9 20.6 %all-to-all-start.1 = ((bf16[64,16,128]{2,1,0:T(8,128)(2,1)}), bf16[64,16,128]{2,1,0:T(8,128)(2,1)S(1)}, u32[]{:S(2)}, u32[]{:S(2)}) async-start(bf16[64,16,128]{2,1,0:T(8,128)(2,1)} %bitcast.38), calls=%async_computation.1 | async-start | bytes 524288 | tf_op jit(solution)/shard_map/all_to_all | solution.py:32
  71.9 6.0 %collective-permute-start.3 = (bf16[256,128]{1,0:T(8,128)(2,1)S(1)}, bf16[256,128]{1,0:T(8,128)(2,1)S(1)}, u32[]{:S(2)}, u32[]{:S(2)}) collective-permute-start(bf16[256,128]{1,0:T(8,128)(2,1)S(1)} %fusion.43), channel_id=1, source_target_pairs={{0,32},{32,0},{64,96},{96,64},{1,33},{33,1},{65,97},{97,65},{2,34}... | collective-permute-start | bytes 196616 | tf_op jit(solution)/shard_map/ppermute | solution.py:48
  83.1 4.0 %copy-start.4 = (bf16[2,256,32]{1,2,0:T(8,128)(2,1)S(1)}, bf16[2,256,32]{1,2,0:T(8,128)(2,1)}, u32[]{:S(2)}) copy-start(bf16[2,256,32]{1,2,0:T(8,128)(2,1)} %param.21) | copy-start | bytes 98308
  83.1 15.2 %all-to-all-start.2 = ((bf16[32,16,128]{2,1,0:T(8,128)(2,1)}), bf16[32,16,128]{2,1,0:T(8,128)(2,1)S(1)}, u32[]{:S(2)}, u32[]{:S(2)}) async-start(bf16[32,16,128]{2,1,0:T(8,128)(2,1)} %maximum_bitcast_fusion), calls=%async_computation.2 | async-start | bytes 262144 | tf_op jit(solution)/shard_map/all_to_all | solution.py:32
  87.2 8.4 %collective-permute-start.5 = (bf16[192,128]{1,0:T(8,128)(2,1)S(1)}, bf16[192,128]{1,0:T(8,128)(2,1)S(1)}, u32[]{:S(2)}, u32[]{:S(2)}) collective-permute-start(bf16[192,128]{1,0:T(8,128)(2,1)S(1)} %get-tuple-element.56), channel_id=1, source_target_pairs={{0,64},{32,96},{64,0},{96,32},{1,65},{33,97},{65,1},{97,33},{2,66}... | collective-permute-start | bytes 147464 | tf_op jit(solution)/shard_map/ppermute | solution.py:48
  91.5 6.7 %collective-permute-start.4 = (bf16[192,128]{1,0:T(8,128)(2,1)S(1)}, bf16[192,128]{1,0:T(8,128)(2,1)S(1)}, u32[]{:S(2)}, u32[]{:S(2)}) collective-permute-start(bf16[192,128]{1,0:T(8,128)(2,1)S(1)} %get-tuple-element.55), channel_id=1, source_target_pairs={{0,96},{32,64},{64,32},{96,0},{1,97},{33,65},{65,33},{97,1},{2,98}... | collective-permute-start | bytes 147464 | tf_op jit(solution)/shard_map/ppermute | solution.py:48
  99.1 33.4 %all-to-all-start.3 = ((bf16[8,64,128]{2,1,0:T(8,128)(2,1)}), bf16[8,64,128]{2,1,0:T(8,128)(2,1)S(1)}, u32[]{:S(2)}, u32[]{:S(2)}) async-start(bf16[8,64,128]{2,1,0:T(8,128)(2,1)} %broadcast_in_dim.89), calls=%async_computation.3 | async-start | bytes 262144 | tf_op jit(solution)/shard_map/all_to_all | solution.py:38
  120.4 9.0 %collective-permute-start.6 = (bf16[416,128]{1,0:T(8,128)(2,1)S(1)}, bf16[416,128]{1,0:T(8,128)(2,1)S(1)}, u32[]{:S(2)}, u32[]{:S(2)}) collective-permute-start(bf16[416,128]{1,0:T(8,128)(2,1)S(1)} %get-tuple-element.43), channel_id=1, source_target_pairs={{0,24},{8,16},{16,8},{24,0},{1,25},{9,17},{17,9},{25,1},{2,26},{10... | collective-permute-start | bytes 319496 | tf_op jit(solution)/shard_map/ppermute | solution.py:48
  124.1 7.2 %collective-permute-start.7 = (bf16[416,128]{1,0:T(8,128)(2,1)S(1)}, bf16[416,128]{1,0:T(8,128)(2,1)S(1)}, u32[]{:S(2)}, u32[]{:S(2)}) collective-permute-start(bf16[416,128]{1,0:T(8,128)(2,1)S(1)} %get-tuple-element.42), channel_id=1, source_target_pairs={{0,16},{8,24},{16,0},{24,8},{1,17},{9,25},{17,1},{25,9},{2,18},{10... | collective-permute-start | bytes 319496 | tf_op jit(solution)/shard_map/ppermute | solution.py:48
  126.4 5.9 %collective-permute-start.8 = (bf16[416,128]{1,0:T(8,128)(2,1)S(1)}, bf16[416,128]{1,0:T(8,128)(2,1)S(1)}, u32[]{:S(2)}, u32[]{:S(2)}) collective-permute-start(bf16[416,128]{1,0:T(8,128)(2,1)S(1)} %get-tuple-element.41), channel_id=1, source_target_pairs={{0,8},{8,0},{16,24},{24,16},{1,9},{9,1},{17,25},{25,17},{2,10},{10... | collective-permute-start | bytes 319496 | tf_op jit(solution)/shard_map/ppermute | solution.py:48
  133.7 9.3 %copy-start.1 = (bf16[2,32,3,32]{3,1,2,0:T(8,128)(2,1)S(1)}, bf16[2,32,3,32]{3,1,2,0:T(8,128)(2,1)}, u32[]{:S(2)}) copy-start(bf16[2,32,3,32]{3,1,2,0:T(8,128)(2,1)} %param.15) | copy-start | bytes 36868
  133.7 20.2 %all-to-all-start.4 = ((bf16[32,32,128]{2,1,0:T(8,128)(2,1)}), bf16[32,32,128]{2,1,0:T(8,128)(2,1)S(1)}, u32[]{:S(2)}, u32[]{:S(2)}) async-start(bf16[32,32,128]{2,1,0:T(8,128)(2,1)} %bitcast.106), calls=%async_computation.4 | async-start | bytes 524288 | tf_op jit(solution)/shard_map/all_to_all | solution.py:32
  155.3 15.7 %collective-permute-start.9 = (f32[8,128]{1,0:T(8,128)S(1)}, f32[8,128]{1,0:T(8,128)S(1)}, u32[]{:S(2)}, u32[]{:S(2)}) collective-permute-start(f32[8,128]{1,0:T(8,128)S(1)} %get-tuple-element.93), channel_id=1, source_target_pairs={{0,24},{8,16},{16,8},{24,0},{1,25},{9,17},{17,9},{25,1},{2,26},{10... | collective-permute-start | bytes 12296 | tf_op jit(solution)/shard_map/ppermute | solution.py:48
  159.1 12.0 %collective-permute-start.10 = (f32[8,128]{1,0:T(8,128)S(1)}, f32[8,128]{1,0:T(8,128)S(1)}, u32[]{:S(2)}, u32[]{:S(2)}) collective-permute-start(f32[8,128]{1,0:T(8,128)S(1)} %get-tuple-element.92), channel_id=1, source_target_pairs={{0,16},{8,24},{16,0},{24,8},{1,17},{9,25},{17,1},{25,9},{2,18},{10... | collective-permute-start | bytes 12296 | tf_op jit(solution)/shard_map/ppermute | solution.py:48
  161.9 9.1 %collective-permute-start.11 = (f32[8,128]{1,0:T(8,128)S(1)}, f32[8,128]{1,0:T(8,128)S(1)}, u32[]{:S(2)}, u32[]{:S(2)}) collective-permute-start(f32[8,128]{1,0:T(8,128)S(1)} %get-tuple-element.91), channel_id=1, source_target_pairs={{0,8},{8,0},{16,24},{24,16},{1,9},{9,1},{17,25},{25,17},{2,10},{10... | collective-permute-start | bytes 12296 | tf_op jit(solution)/shard_map/ppermute | solution.py:48
  165.0 13.6 %all-to-all-start.5 = ((bf16[32,16,128]{2,1,0:T(8,128)(2,1)}), bf16[32,16,128]{2,1,0:T(8,128)(2,1)S(1)}, u32[]{:S(2)}, u32[]{:S(2)}) async-start(bf16[32,16,128]{2,1,0:T(8,128)(2,1)} %copy_bitcast_fusion), calls=%async_computation.5 | async-start | bytes 262144 | tf_op jit(solution)/shard_map/all_to_all | solution.py:32
  179.4 28.6 %all-to-all-start.6 = ((bf16[32,4,256]{2,1,0:T(4,128)(2,1)}), bf16[32,4,256]{2,1,0:T(4,128)(2,1)S(1)}, u32[]{:S(2)}, u32[]{:S(2)}) async-start(bf16[32,4,256]{2,1,0:T(4,128)(2,1)} %reshape.484), calls=%async_computation.6 | async-start | bytes 131072 | tf_op jit(solution)/shard_map/all_to_all | solution.py:38

commit v10 on v9

--- a/solution.py
+++ b/solution.py
@@ -18,9 +18,9 @@
 DP = ("x", "core")
 PLANE = ("x", "core", "y")
 PAIRED_PLANE = ("zl", "y", "x", "core")
-FIRST_GATHER = 24
-FIRST_REDUCE = 4
-FIRST_LAST = 20
+FIRST_GATHER = 22
+FIRST_REDUCE = 3
+FIRST_LAST = 18
 bf16 = jnp.bfloat16
 f32 = jnp.float32
 
@@ -300,8 +300,11 @@
     came = jnp.concatenate([came[at] for at in range(4)], axis=1)
     mixed = contract(came, 1, w_mid, 0).astype(bf16)
     mixed = everywhere(mixed, "zh", FIRST_REDUCE)
-    mixed, w_second, gates_second, w_last = lax.optimization_barrier(
-        (mixed, w_second, gates_second, w_last)
+    at_z = lax.axis_index(Z)
+    mixed, w_second, gates_second, w_last, state_first, branch_first, at_z = (
+        lax.optimization_barrier(
+            (mixed, w_second, gates_second, w_last, state_first, branch_first, at_z)
+        )
     )
     mixed = mixed.astype(f32).sum(axis=0)
     first = (mixed + residual).astype(bf16)
@@ -350,9 +353,12 @@
         axis=1,
     )
     came = exchange(sent.reshape(32, 16, 128), PLANE).reshape(32, 2, 8, 128)
+    came, lengths, prior_window, at_z = lax.optimization_barrier(
+        (came, lengths, prior_window, at_z)
+    )
     mixed = contract(w_last, 0, came[:, 0].reshape(256, 128), 1).astype(bf16)
     mixed = mixed.reshape(32, 4, 256)
-    own = (lax.axis_index(Z) - FIRST_GATHER) % 32 * 4
+    own = (at_z + (32 - FIRST_GATHER) & 31) * 4
     own = lax.broadcasted_iota(jnp.int32, (4, 128), 0) + own
     own = (own == lax.broadcasted_iota(jnp.int32, (4, 128), 1)).astype(bf16)
     residual = contract(own, 1, came[:, 1].reshape(256, 128), 1)
@@ -365,7 +371,7 @@
     kept = kept.reshape(4, 8, 4, 32).transpose(2, 0, 1, 3).reshape(4, 8, 128)
     kept = jnp.stack(in_order(traded(kept, "y"), "y"))
     kept = kept.reshape(4, 4, 8, 32).transpose(1, 0, 2, 3).reshape(2, LAYERS, 32, 32)
-    living = lengths[None, :, None, None] >= needed[None, None, 1:, None]
+    living = lengths[:, None, None] >= depth - jnp.arange(2, dtype=jnp.int32)[:, None]
     history = jnp.where(living, prior_window[:, :, 1:], jnp.zeros_like(prior_window[:, :, 1:]))
     window = jnp.concatenate([history, kept[1].astype(bf16)[:, :, None]], axis=2)
     return second.T, kept[0], window

time: 210 us -> 204 us (0.971)
  waiting for transfers between devices: 52.3 us -> 48.9 us
  local copies, waits for them, and re-layouts: 12.4 us -> 9.91 us
    all_to_all x3, waiting for transfers between devices: 22.7 us -> 18.4 us  [exchange_far(): lax.all_to_all(tiles, axes, 0, 0, axis_index_groups=[order], tiled=True)]
    unnamed x30 -> x24, local copies, waits for them, and re-layouts: 6.21 us -> 3.02 us
  transfers between devices with their start and end apart: 19 -> 19, of which waited for: 10 -> 9; matrix products, arithmetic and copies ran while one was open for 2% -> 3% of each run, Pallas kernels for 0% -> 0%
where the time goes in v10:
time: 204 us; the launch traced here: 203 us
  starting transfers between devices  136 us (67%)
  waiting for transfers between devices  48.9 us (24%)
  local copies, waits for them, and re-layouts  9.91 us (5%)
  other arithmetic  3.67 us (2%)
  matrix products  2.99 us (1%)
    all_to_all x3, starting transfers between devices, exchange_far(): lax.all_to_all(tiles, axes, 0, 0, axis_index_groups=[order], tiled=True)  66.2 us
    ppermute x12, starting transfers between devices, passed(): lax.ppermute(piece, axis, [(at, at ^ flip) for at in range(lax.axis_size(...  39.4 us
    all_to_all x4, starting transfers between devices, exchange(): return lax.all_to_all(tiles, axes, 0, 0, tiled=True)  30.2 us
    all_to_all x4, waiting for transfers between devices, exchange(): return lax.all_to_all(tiles, axes, 0, 0, tiled=True)  20.7 us
    all_to_all x3, waiting for transfers between devices, exchange_far(): lax.all_to_all(tiles, axes, 0, 0, axis_index_groups=[order], tiled=True)  18.4 us
    ppermute x12, waiting for transfers between devices, passed(): lax.ppermute(piece, axis, [(at, at ^ flip) for at in range(lax.axis_size(...  9.75 us
  transfers between devices with their start and end apart: 19, of which 9 were waited for; matrix products, arithmetic and copies ran while one was open for 3% of the time, Pallas kernels for 0%

profile of v10, /device:TPU:1, one launch (start us, length us, event | category | flops | bytes accessed | tf_op | source)
XLA Modules:
  0.0 203.2 jit_solution(8933928844686437590)
XLA Ops:
  0.6 1.4 broadcast_in_dim.54
  2.0 29.7 %all-to-all-start = ((bf16[32,4,256]{2,1,0:T(4,128)(2,1)}), bf16[32,4,256]{2,1,0:T(4,128)(2,1)S(1)}, u32[]{:S(2)}, u32[]{:S(2)}) async-start(bf16[32,4,256]{2,1,0:T(4,128)(2,1)} %broadcast_in_dim.54), calls=%async_computation | async-start | bytes 131072 | tf_op jit(solution)/shard_map/all_to_all | solution.py:38
  31.8 0.7 copy-done.1
  32.5 0.8 copy-done.4
  33.3 0.8 copy-done.5
  34.1 0.3 shard_map.139
  34.5 3.3 %collective-permute-start.2 = (bf16[352,128]{1,0:T(8,128)(2,1)S(1)}, bf16[352,128]{1,0:T(8,128)(2,1)S(1)}, u32[]{:S(2)}, u32[]{:S(2)}) collective-permute-start(bf16[352,128]{1,0:T(8,128)(2,1)S(1)} %get-tuple-element.58), channel_id=1, source_target_pairs={{0,8},{8,0},{16,24},{24,16},{1,9},{9,1},{17,25},{25,17},{2,10},{10... | collective-permute-start | bytes 270344 | tf_op jit(solution)/shard_map/ppermute | solution.py:48
  37.8 4.5 %collective-permute-start.1 = (bf16[352,128]{1,0:T(8,128)(2,1)S(1)}, bf16[352,128]{1,0:T(8,128)(2,1)S(1)}, u32[]{:S(2)}, u32[]{:S(2)}) collective-permute-start(bf16[352,128]{1,0:T(8,128)(2,1)S(1)} %get-tuple-element.59), channel_id=1, source_target_pairs={{0,16},{8,24},{16,0},{24,8},{1,17},{9,25},{17,1},{25,9},{2,18},{10... | collective-permute-start | bytes 270344 | tf_op jit(solution)/shard_map/ppermute | solution.py:48
  42.4 1.9 collective-permute-start
  44.4 0.3 fusion.1
  44.7 0.6 copy-done.11
  45.4 3.4 %collective-permute-done = bf16[352,128]{1,0:T(8,128)(2,1)S(1)} collective-permute-done((bf16[352,128]{1,0:T(8,128)(2,1)S(1)}, bf16[352,128]{1,0:T(8,128)(2,1)S(1)}, u32[]{:S(2)}, u32[]{:S(2)}) %collective-permute-start) | collective-permute-done | bytes 90144 | tf_op jit(solution)/shard_map/ppermute | solution.py:48
  49.0 0.2 fusion
  49.2 0.2 copy.54
  49.5 0.7 copy.57
  50.2 8.7 %all-to-all-start.1 = ((bf16[64,16,128]{2,1,0:T(8,128)(2,1)}), bf16[64,16,128]{2,1,0:T(8,128)(2,1)S(1)}, u32[]{:S(2)}, u32[]{:S(2)}) async-start(bf16[64,16,128]{2,1,0:T(8,128)(2,1)} %bitcast.38), calls=%async_computation.1 | async-start | bytes 524288 | tf_op jit(solution)/shard_map/all_to_all | solution.py:32
  59.0 0.1 reshape.456
  59.1 0.1 copy.61
  59.2 0.1 reshape.465
  59.5 3.4 %collective-permute-start.3 = (bf16[256,128]{1,0:T(8,128)(2,1)S(1)}, bf16[256,128]{1,0:T(8,128)(2,1)S(1)}, u32[]{:S(2)}, u32[]{:S(2)}) collective-permute-start(bf16[256,128]{1,0:T(8,128)(2,1)S(1)} %fusion.43), channel_id=1, source_target_pairs={{0,32},{32,0},{64,96},{96,64},{1,33},{33,1},{65,97},{97,65},{2,34}... | collective-permute-start | bytes 196616 | tf_op jit(solution)/shard_map/ppermute | solution.py:48
  62.9 2.0 collective-permute-done.3
  65.2 0.1 select_n.350
  65.4 0.1 select_n.352
  65.6 3.0 %all-to-all-done.1 = bf16[64,16,128]{2,1,0:T(8,128)(2,1)S(1)} async-done(((bf16[64,16,128]{2,1,0:T(8,128)(2,1)}), bf16[64,16,128]{2,1,0:T(8,128)(2,1)S(1)}, u32[]{:S(2)}, u32[]{:S(2)}) %all-to-all-start.1) | async-done | bytes 262176 | tf_op jit(solution)/shard_map/all_to_all | solution.py:32
  68.6 0.1 convert_reduce_fusion.4
  68.9 0.1 fusion.73
  69.0 0.1 fusion.74
  69.2 0.2 fusion.25
  69.3 0.2 fusion.115
  69.6 0.7 maximum_bitcast_fusion
  70.2 5.5 %all-to-all-start.2 = ((bf16[32,16,128]{2,1,0:T(8,128)(2,1)}), bf16[32,16,128]{2,1,0:T(8,128)(2,1)S(1)}, u32[]{:S(2)}, u32[]{:S(2)}) async-start(bf16[32,16,128]{2,1,0:T(8,128)(2,1)} %maximum_bitcast_fusion), calls=%async_computation.2 | async-start | bytes 262144 | tf_op jit(solution)/shard_map/all_to_all | solution.py:32
  75.7 5.1 %collective-permute-start.4 = (bf16[192,128]{1,0:T(8,128)(2,1)S(1)}, bf16[192,128]{1,0:T(8,128)(2,1)S(1)}, u32[]{:S(2)}, u32[]{:S(2)}) collective-permute-start(bf16[192,128]{1,0:T(8,128)(2,1)S(1)} %get-tuple-element.69), channel_id=1, source_target_pairs={{0,96},{32,64},{64,32},{96,0},{1,97},{33,65},{65,33},{97,1},{2,98}... | collective-permute-start | bytes 147464 | tf_op jit(solution)/shard_map/ppermute | solution.py:48
  80.9 1.9 collective-permute-start.5
  82.8 0.1 collective-permute-done.4
  82.9 4.2 %collective-permute-done.5 = bf16[192,128]{1,0:T(8,128)(2,1)S(1)} collective-permute-done((bf16[192,128]{1,0:T(8,128)(2,1)S(1)}, bf16[192,128]{1,0:T(8,128)(2,1)S(1)}, u32[]{:S(2)}, u32[]{:S(2)}) %collective-permute-start.5) | collective-permute-done | bytes 49184 | tf_op jit(solution)/shard_map/ppermute | solution.py:48
  87.4 3.1 %collective-permute-start.8 = (bf16[416,128]{1,0:T(8,128)(2,1)S(1)}, bf16[416,128]{1,0:T(8,128)(2,1)S(1)}, u32[]{:S(2)}, u32[]{:S(2)}) collective-permute-start(bf16[416,128]{1,0:T(8,128)(2,1)S(1)} %get-tuple-element.55), channel_id=1, source_target_pairs={{0,8},{8,0},{16,24},{24,16},{1,9},{9,1},{17,25},{25,17},{2,10},{10... | collective-permute-start | bytes 319496 | tf_op jit(solution)/shard_map/ppermute | solution.py:48
  90.6 4.4 %collective-permute-start.7 = (bf16[416,128]{1,0:T(8,128)(2,1)S(1)}, bf16[416,128]{1,0:T(8,128)(2,1)S(1)}, u32[]{:S(2)}, u32[]{:S(2)}) collective-permute-start(bf16[416,128]{1,0:T(8,128)(2,1)S(1)} %get-tuple-element.56), channel_id=1, source_target_pairs={{0,16},{8,24},{16,0},{24,8},{1,17},{9,25},{17,1},{25,9},{2,18},{10... | collective-permute-start | bytes 319496 | tf_op jit(solution)/shard_map/ppermute | solution.py:48
  95.0 2.0 collective-permute-start.6
  97.1 0.2 convolution_convert_fusion.4
  97.2 0.7 broadcast_in_dim.90
  97.9 16.3 %all-to-all-start.3 = ((bf16[8,64,128]{2,1,0:T(8,128)(2,1)}), bf16[8,64,128]{2,1,0:T(8,128)(2,1)S(1)}, u32[]{:S(2)}, u32[]{:S(2)}) async-start(bf16[8,64,128]{2,1,0:T(8,128)(2,1)} %broadcast_in_dim.90), calls=%async_computation.3 | async-start | bytes 262144 | tf_op jit(solution)/shard_map/all_to_all | solution.py:38
  114.4 11.4 %all-to-all-done.3 = bf16[8,64,128]{2,1,0:T(8,128)(2,1)S(1)} async-done(((bf16[8,64,128]{2,1,0:T(8,128)(2,1)}), bf16[8,64,128]{2,1,0:T(8,128)(2,1)S(1)}, u32[]{:S(2)}, u32[]{:S(2)}) %all-to-all-start.3) | async-done | bytes 131104 | tf_op jit(solution)/shard_map/all_to_all | solution.py:38
  125.8 0.2 convolution_convert_fusion.1
  126.1 0.7 copy.65
  126.9 10.0 %all-to-all-start.4 = ((bf16[32,32,128]{2,1,0:T(8,128)(2,1)}), bf16[32,32,128]{2,1,0:T(8,128)(2,1)S(1)}, u32[]{:S(2)}, u32[]{:S(2)}) async-start(bf16[32,32,128]{2,1,0:T(8,128)(2,1)} %bitcast.106), calls=%async_computation.4 | async-start | bytes 524288 | tf_op jit(solution)/shard_map/all_to_all | solution.py:32
  136.9 11.1 %all-to-all-done.4 = bf16[32,32,128]{2,1,0:T(8,128)(2,1)S(1)} async-done(((bf16[32,32,128]{2,1,0:T(8,128)(2,1)}), bf16[32,32,128]{2,1,0:T(8,128)(2,1)S(1)}, u32[]{:S(2)}, u32[]{:S(2)}) %all-to-all-start.4) | async-done | bytes 262176 | tf_op jit(solution)/shard_map/all_to_all | solution.py:32
  148.0 0.1 multiply_reduce_fusion
  148.3 0.1 fusion.76
  148.4 0.1 fusion.79
  148.8 0.1 fusion.13
  148.9 0.2 fusion.122
  149.4 1.9 collective-permute-start.11
  151.4 5.6 %collective-permute-start.10 = (f32[8,128]{1,0:T(8,128)S(1)}, f32[8,128]{1,0:T(8,128)S(1)}, u32[]{:S(2)}, u32[]{:S(2)}) collective-permute-start(f32[8,128]{1,0:T(8,128)S(1)} %get-tuple-element.106), channel_id=1, source_target_pairs={{0,16},{8,24},{16,0},{24,8},{1,17},{9,25},{17,1},{25,9},{2,18},{10... | collective-permute-start | bytes 12296 | tf_op jit(solution)/shard_map/ppermute | solution.py:48
  157.0 2.0 collective-permute-start.9
  159.1 0.7 copy_bitcast_fusion
  159.7 6.1 %all-to-all-start.5 = ((bf16[32,16,128]{2,1,0:T(8,128)(2,1)}), bf16[32,16,128]{2,1,0:T(8,128)(2,1)S(1)}, u32[]{:S(2)}, u32[]{:S(2)}) async-start(bf16[32,16,128]{2,1,0:T(8,128)(2,1)} %copy_bitcast_fusion), calls=%async_computation.5 | async-start | bytes 262144 | tf_op jit(solution)/shard_map/all_to_all | solution.py:32
  166.2 0.6 slice_bitcast_fusion.5
  166.8 6.6 %all-to-all-done.5 = bf16[32,16,128]{2,1,0:T(8,128)(2,1)S(1)} async-done(((bf16[32,16,128]{2,1,0:T(8,128)(2,1)}), bf16[32,16,128]{2,1,0:T(8,128)(2,1)S(1)}, u32[]{:S(2)}, u32[]{:S(2)}) %all-to-all-start.5) | async-done | bytes 131104 | tf_op jit(solution)/shard_map/all_to_all | solution.py:32
  173.4 0.2 convolution_convert_fusion.2
  173.6 0.7 reshape.478
  174.2 20.3 %all-to-all-start.6 = ((bf16[32,4,256]{2,1,0:T(4,128)(2,1)}), bf16[32,4,256]{2,1,0:T(4,128)(2,1)S(1)}, u32[]{:S(2)}, u32[]{:S(2)}) async-start(bf16[32,4,256]{2,1,0:T(4,128)(2,1)} %reshape.478), calls=%async_computation.6 | async-start | bytes 131072 | tf_op jit(solution)/shard_map/all_to_all | solution.py:38
  194.7 0.6 pad_maximum_fusion.18
  195.3 7.1 %all-to-all-done.6 = bf16[32,4,256]{2,1,0:T(4,128)(2,1)S(1)} async-done(((bf16[32,4,256]{2,1,0:T(4,128)(2,1)}), bf16[32,4,256]{2,1,0:T(4,128)(2,1)S(1)}, u32[]{:S(2)}, u32[]{:S(2)}) %all-to-all-start.6) | async-done | bytes 65568 | tf_op jit(solution)/shard_map/all_to_all | solution.py:38
  202.5 0.8 fusion.26
  (137 shorter events, 2.9 us)
Async XLA Ops:
  0.6 31.1 %copy-start.3 = (bf16[2,512,32]{1,2,0:T(8,128)(2,1)S(1)}, bf16[2,512,32]{1,2,0:T(8,128)(2,1)}, u32[]{:S(2)}) copy-start(bf16[2,512,32]{1,2,0:T(8,128)(2,1)} %param.17) | copy-start | bytes 196612
  2.0 29.8 %copy-start = (bf16[2,32,3,32]{3,1,2,0:T(8,128)(2,1)S(1)}, bf16[2,32,3,32]{3,1,2,0:T(8,128)(2,1)}, u32[]{:S(2)}) copy-start(bf16[2,32,3,32]{3,1,2,0:T(8,128)(2,1)} %param.15) | copy-start | bytes 36868
  2.0 29.8 %copy-start.2 = (bf16[2,256,32]{1,2,0:T(8,128)(2,1)S(1)}, bf16[2,256,32]{1,2,0:T(8,128)(2,1)}, u32[]{:S(2)}) copy-start(bf16[2,256,32]{1,2,0:T(8,128)(2,1)} %param.21) | copy-start | bytes 98308
  2.0 29.8 %copy-start.7 = (f32[2,32,32]{2,1,0:T(8,128)S(1)}, f32[2,32,32]{2,1,0:T(8,128)}, u32[]{:S(2)}) copy-start(f32[2,32,32]{2,1,0:T(8,128)} %state.1) | copy-start | bytes 24580
  2.0 46.9 %all-to-all-start = ((bf16[32,4,256]{2,1,0:T(4,128)(2,1)}), bf16[32,4,256]{2,1,0:T(4,128)(2,1)S(1)}, u32[]{:S(2)}, u32[]{:S(2)}) async-start(bf16[32,4,256]{2,1,0:T(4,128)(2,1)} %broadcast_in_dim.54), calls=%async_computation | async-start | bytes 131072 | tf_op jit(solution)/shard_map/all_to_all | solution.py:38
  31.7 0.8 copy-start.1
  31.7 0.7 copy-start.8
  31.7 0.7 copy-start.9
  31.7 0.7 copy-start.10
  32.4 0.8 copy-start.4
  33.3 0.8 copy-start.5
  34.5 9.9 %copy-start.6 = (bf16[2,32,512]{2,1,0:T(8,128)(2,1)S(1)}, bf16[2,32,512]{2,1,0:T(8,128)(2,1)}, u32[]{:S(2)}) copy-start(bf16[2,32,512]{2,1,0:T(8,128)(2,1)} %out.1) | copy-start | bytes 196612
  34.5 10.9 %collective-permute-start.2 = (bf16[352,128]{1,0:T(8,128)(2,1)S(1)}, bf16[352,128]{1,0:T(8,128)(2,1)S(1)}, u32[]{:S(2)}, u32[]{:S(2)}) collective-permute-start(bf16[352,128]{1,0:T(8,128)(2,1)S(1)} %get-tuple-element.58), channel_id=1, source_target_pairs={{0,8},{8,0},{16,24},{24,16},{1,9},{9,1},{17,25},{25,17},{2,10},{10... | collective-permute-start | bytes 270344 | tf_op jit(solution)/shard_map/ppermute | solution.py:48
  37.8 7.6 %collective-permute-start.1 = (bf16[352,128]{1,0:T(8,128)(2,1)S(1)}, bf16[352,128]{1,0:T(8,128)(2,1)S(1)}, u32[]{:S(2)}, u32[]{:S(2)}) collective-permute-start(bf16[352,128]{1,0:T(8,128)(2,1)S(1)} %get-tuple-element.59), channel_id=1, source_target_pairs={{0,16},{8,24},{16,0},{24,8},{1,17},{9,25},{17,1},{25,9},{2,18},{10... | collective-permute-start | bytes 270344 | tf_op jit(solution)/shard_map/ppermute | solution.py:48
  42.4 6.5 %collective-permute-start = (bf16[352,128]{1,0:T(8,128)(2,1)S(1)}, bf16[352,128]{1,0:T(8,128)(2,1)S(1)}, u32[]{:S(2)}, u32[]{:S(2)}) collective-permute-start(bf16[352,128]{1,0:T(8,128)(2,1)S(1)} %get-tuple-element.60), channel_id=1, source_target_pairs={{0,24},{8,16},{16,8},{24,0},{1,25},{9,17},{17,9},{25,1},{2,26},{10... | collective-permute-start | bytes 270344 | tf_op jit(solution)/shard_map/ppermute | solution.py:48
  44.7 0.7 copy-start.11
  50.2 18.4 %all-to-all-start.1 = ((bf16[64,16,128]{2,1,0:T(8,128)(2,1)}), bf16[64,16,128]{2,1,0:T(8,128)(2,1)S(1)}, u32[]{:S(2)}, u32[]{:S(2)}) async-start(bf16[64,16,128]{2,1,0:T(8,128)(2,1)} %bitcast.38), calls=%async_computation.1 | async-start | bytes 524288 | tf_op jit(solution)/shard_map/all_to_all | solution.py:32
  59.5 5.5 %collective-permute-start.3 = (bf16[256,128]{1,0:T(8,128)(2,1)S(1)}, bf16[256,128]{1,0:T(8,128)(2,1)S(1)}, u32[]{:S(2)}, u32[]{:S(2)}) collective-permute-start(bf16[256,128]{1,0:T(8,128)(2,1)S(1)} %fusion.43), channel_id=1, source_target_pairs={{0,32},{32,0},{64,96},{96,64},{1,33},{33,1},{65,97},{97,65},{2,34}... | collective-permute-start | bytes 196616 | tf_op jit(solution)/shard_map/ppermute | solution.py:48
  70.2 26.8 %all-to-all-start.2 = ((bf16[32,16,128]{2,1,0:T(8,128)(2,1)}), bf16[32,16,128]{2,1,0:T(8,128)(2,1)S(1)}, u32[]{:S(2)}, u32[]{:S(2)}) async-start(bf16[32,16,128]{2,1,0:T(8,128)(2,1)} %maximum_bitcast_fusion), calls=%async_computation.2 | async-start | bytes 262144 | tf_op jit(solution)/shard_map/all_to_all | solution.py:32
  75.7 7.2 %collective-permute-start.4 = (bf16[192,128]{1,0:T(8,128)(2,1)S(1)}, bf16[192,128]{1,0:T(8,128)(2,1)S(1)}, u32[]{:S(2)}, u32[]{:S(2)}) collective-permute-start(bf16[192,128]{1,0:T(8,128)(2,1)S(1)} %get-tuple-element.69), channel_id=1, source_target_pairs={{0,96},{32,64},{64,32},{96,0},{1,97},{33,65},{65,33},{97,1},{2,98}... | collective-permute-start | bytes 147464 | tf_op jit(solution)/shard_map/ppermute | solution.py:48
  80.9 6.3 %collective-permute-start.5 = (bf16[192,128]{1,0:T(8,128)(2,1)S(1)}, bf16[192,128]{1,0:T(8,128)(2,1)S(1)}, u32[]{:S(2)}, u32[]{:S(2)}) collective-permute-start(bf16[192,128]{1,0:T(8,128)(2,1)S(1)} %get-tuple-element.70), channel_id=1, source_target_pairs={{0,64},{32,96},{64,0},{96,32},{1,65},{33,97},{65,1},{97,33},{2,66}... | collective-permute-start | bytes 147464 | tf_op jit(solution)/shard_map/ppermute | solution.py:48
  87.4 26.7 %collective-permute-start.8 = (bf16[416,128]{1,0:T(8,128)(2,1)S(1)}, bf16[416,128]{1,0:T(8,128)(2,1)S(1)}, u32[]{:S(2)}, u32[]{:S(2)}) collective-permute-start(bf16[416,128]{1,0:T(8,128)(2,1)S(1)} %get-tuple-element.55), channel_id=1, source_target_pairs={{0,8},{8,0},{16,24},{24,16},{1,9},{9,1},{17,25},{25,17},{2,10},{10... | collective-permute-start | bytes 319496 | tf_op jit(solution)/shard_map/ppermute | solution.py:48
  90.6 23.6 %collective-permute-start.7 = (bf16[416,128]{1,0:T(8,128)(2,1)S(1)}, bf16[416,128]{1,0:T(8,128)(2,1)S(1)}, u32[]{:S(2)}, u32[]{:S(2)}) collective-permute-start(bf16[416,128]{1,0:T(8,128)(2,1)S(1)} %get-tuple-element.56), channel_id=1, source_target_pairs={{0,16},{8,24},{16,0},{24,8},{1,17},{9,25},{17,1},{25,9},{2,18},{10... | collective-permute-start | bytes 319496 | tf_op jit(solution)/shard_map/ppermute | solution.py:48
  95.0 19.2 %collective-permute-start.6 = (bf16[416,128]{1,0:T(8,128)(2,1)S(1)}, bf16[416,128]{1,0:T(8,128)(2,1)S(1)}, u32[]{:S(2)}, u32[]{:S(2)}) collective-permute-start(bf16[416,128]{1,0:T(8,128)(2,1)S(1)} %get-tuple-element.57), channel_id=1, source_target_pairs={{0,24},{8,16},{16,8},{24,0},{1,25},{9,17},{17,9},{25,1},{2,26},{10... | collective-permute-start | bytes 319496 | tf_op jit(solution)/shard_map/ppermute | solution.py:48
  97.9 27.9 %all-to-all-start.3 = ((bf16[8,64,128]{2,1,0:T(8,128)(2,1)}), bf16[8,64,128]{2,1,0:T(8,128)(2,1)S(1)}, u32[]{:S(2)}, u32[]{:S(2)}) async-start(bf16[8,64,128]{2,1,0:T(8,128)(2,1)} %broadcast_in_dim.90), calls=%async_computation.3 | async-start | bytes 262144 | tf_op jit(solution)/shard_map/all_to_all | solution.py:38
  126.9 21.1 %all-to-all-start.4 = ((bf16[32,32,128]{2,1,0:T(8,128)(2,1)}), bf16[32,32,128]{2,1,0:T(8,128)(2,1)S(1)}, u32[]{:S(2)}, u32[]{:S(2)}) async-start(bf16[32,32,128]{2,1,0:T(8,128)(2,1)} %bitcast.106), calls=%async_computation.4 | async-start | bytes 524288 | tf_op jit(solution)/shard_map/all_to_all | solution.py:32
  149.4 16.4 %collective-permute-start.11 = (f32[8,128]{1,0:T(8,128)S(1)}, f32[8,128]{1,0:T(8,128)S(1)}, u32[]{:S(2)}, u32[]{:S(2)}) collective-permute-start(f32[8,128]{1,0:T(8,128)S(1)} %get-tuple-element.105), channel_id=1, source_target_pairs={{0,8},{8,0},{16,24},{24,16},{1,9},{9,1},{17,25},{25,17},{2,10},{10... | collective-permute-start | bytes 12296 | tf_op jit(solution)/shard_map/ppermute | solution.py:48
  151.4 14.4 %collective-permute-start.10 = (f32[8,128]{1,0:T(8,128)S(1)}, f32[8,128]{1,0:T(8,128)S(1)}, u32[]{:S(2)}, u32[]{:S(2)}) collective-permute-start(f32[8,128]{1,0:T(8,128)S(1)} %get-tuple-element.106), channel_id=1, source_target_pairs={{0,16},{8,24},{16,0},{24,8},{1,17},{9,25},{17,1},{25,9},{2,18},{10... | collective-permute-start | bytes 12296 | tf_op jit(solution)/shard_map/ppermute | solution.py:48
  157.0 8.8 %collective-permute-start.9 = (f32[8,128]{1,0:T(8,128)S(1)}, f32[8,128]{1,0:T(8,128)S(1)}, u32[]{:S(2)}, u32[]{:S(2)}) collective-permute-start(f32[8,128]{1,0:T(8,128)S(1)} %get-tuple-element.107), channel_id=1, source_target_pairs={{0,24},{8,16},{16,8},{24,0},{1,25},{9,17},{17,9},{25,1},{2,26},{10... | collective-permute-start | bytes 12296 | tf_op jit(solution)/shard_map/ppermute | solution.py:48
  159.7 13.6 %all-to-all-start.5 = ((bf16[32,16,128]{2,1,0:T(8,128)(2,1)}), bf16[32,16,128]{2,1,0:T(8,128)(2,1)S(1)}, u32[]{:S(2)}, u32[]{:S(2)}) async-start(bf16[32,16,128]{2,1,0:T(8,128)(2,1)} %copy_bitcast_fusion), calls=%async_computation.5 | async-start | bytes 262144 | tf_op jit(solution)/shard_map/all_to_all | solution.py:32
  174.2 28.2 %all-to-all-start.6 = ((bf16[32,4,256]{2,1,0:T(4,128)(2,1)}), bf16[32,4,256]{2,1,0:T(4,128)(2,1)S(1)}, u32[]{:S(2)}, u32[]{:S(2)}) async-start(bf16[32,4,256]{2,1,0:T(4,128)(2,1)} %reshape.478), calls=%async_computation.6 | async-start | bytes 131072 | tf_op jit(solution)/shard_map/all_to_all | solution.py:38

commit v11 on v10

--- a/solution.py
+++ b/solution.py
@@ -139,14 +139,9 @@
         jnp.sum(history * taps[:3, None], axis=0) + branch.astype(f32) * taps[3]
     ).astype(bf16)
     half = BLOCK // 2
-    mapped = [
-        contract(convolved[:, :half], 1, gates[kind, 0], 1)
-        + contract(convolved[:, half:], 1, gates[kind, 1], 1)
-        for kind in range(2)
-    ]
+    mapped = jax.nn.sigmoid(contract(convolved, 1, gates, 1))
+    input_gate, recur_gate = mapped[:, :half], mapped[:, half:]
     own = jnp.where(upper, convolved[:, half:], convolved[:, :half])
-    input_gate = jax.nn.sigmoid(mapped[0])
-    recur_gate = jax.nn.sigmoid(mapped[1])
     log_keep = 8.0 * recur_gate * decay
     keeping = jnp.exp(log_keep)
     feeding = jnp.sqrt(-jnp.expm1(2.0 * log_keep))
@@ -208,9 +203,8 @@
     )
 
     def gates_of(rows):
-        return (
-            rows.reshape(4, 2, 2, 32, 128).transpose(1, 2, 0, 3, 4).reshape(2, 2, 128, 128)
-        )
+        rows = rows.reshape(4, 2, 2, 32, 128).transpose(1, 0, 3, 2, 4)
+        return rows.reshape(256, 256)
 
     gates = gates_of(near[:, 64:192])
 

time: 204 us -> 204 us (level)
  no operation moved by 1% of the time
where the time goes in v11:
time: 204 us; the launch traced here: 203 us
  starting transfers between devices  136 us (67%)
  waiting for transfers between devices  48.6 us (24%)
  local copies, waits for them, and re-layouts  10.1 us (5%)
  other arithmetic  3.89 us (2%)
  matrix products  2.11 us (1%)
    all_to_all x3, starting transfers between devices, exchange_far(): lax.all_to_all(tiles, axes, 0, 0, axis_index_groups=[order], tiled=True)  66.2 us
    ppermute x12, starting transfers between devices, passed(): lax.ppermute(piece, axis, [(at, at ^ flip) for at in range(lax.axis_size(...  39.4 us
    all_to_all x4, starting transfers between devices, exchange(): return lax.all_to_all(tiles, axes, 0, 0, tiled=True)  30.3 us
    all_to_all x4, waiting for transfers between devices, exchange(): return lax.all_to_all(tiles, axes, 0, 0, tiled=True)  20.7 us
    all_to_all x3, waiting for transfers between devices, exchange_far(): lax.all_to_all(tiles, axes, 0, 0, axis_index_groups=[order], tiled=True)  18.3 us
    ppermute x12, waiting for transfers between devices, passed(): lax.ppermute(piece, axis, [(at, at ^ flip) for at in range(lax.axis_size(...  9.65 us
  transfers between devices with their start and end apart: 19, of which 9 were waited for; matrix products, arithmetic and copies ran while one was open for 3% of the time, Pallas kernels for 0%

profile of v11, /device:TPU:1, one launch (start us, length us, event | category | flops | bytes accessed | tf_op | source)
XLA Modules:
  0.0 202.6 jit_solution(15951905574379211917)
XLA Ops:
  0.6 1.4 broadcast_in_dim.54
  2.0 29.7 %all-to-all-start = ((bf16[32,4,256]{2,1,0:T(4,128)(2,1)}), bf16[32,4,256]{2,1,0:T(4,128)(2,1)S(1)}, u32[]{:S(2)}, u32[]{:S(2)}) async-start(bf16[32,4,256]{2,1,0:T(4,128)(2,1)} %broadcast_in_dim.54), calls=%async_computation | async-start | bytes 131072 | tf_op jit(solution)/shard_map/all_to_all | solution.py:38
  31.8 0.7 copy-done.1
  32.5 0.8 copy-done.4
  33.3 0.8 copy-done.5
  34.1 0.3 shard_map.139
  34.5 3.3 %collective-permute-start.2 = (bf16[352,128]{1,0:T(8,128)(2,1)S(1)}, bf16[352,128]{1,0:T(8,128)(2,1)S(1)}, u32[]{:S(2)}, u32[]{:S(2)}) collective-permute-start(bf16[352,128]{1,0:T(8,128)(2,1)S(1)} %get-tuple-element.62), channel_id=1, source_target_pairs={{0,8},{8,0},{16,24},{24,16},{1,9},{9,1},{17,25},{25,17},{2,10},{10... | collective-permute-start | bytes 270344 | tf_op jit(solution)/shard_map/ppermute | solution.py:48
  37.8 4.5 %collective-permute-start.1 = (bf16[352,128]{1,0:T(8,128)(2,1)S(1)}, bf16[352,128]{1,0:T(8,128)(2,1)S(1)}, u32[]{:S(2)}, u32[]{:S(2)}) collective-permute-start(bf16[352,128]{1,0:T(8,128)(2,1)S(1)} %get-tuple-element.63), channel_id=1, source_target_pairs={{0,16},{8,24},{16,0},{24,8},{1,17},{9,25},{17,1},{25,9},{2,18},{10... | collective-permute-start | bytes 270344 | tf_op jit(solution)/shard_map/ppermute | solution.py:48
  42.4 1.9 collective-permute-start
  44.4 0.3 fusion.1
  44.7 0.6 copy-done.11
  45.4 3.4 %collective-permute-done = bf16[352,128]{1,0:T(8,128)(2,1)S(1)} collective-permute-done((bf16[352,128]{1,0:T(8,128)(2,1)S(1)}, bf16[352,128]{1,0:T(8,128)(2,1)S(1)}, u32[]{:S(2)}, u32[]{:S(2)}) %collective-permute-start) | collective-permute-done | bytes 90144 | tf_op jit(solution)/shard_map/ppermute | solution.py:48
  49.0 0.2 fusion
  49.2 0.2 copy.54
  49.5 0.7 copy.57
  50.2 8.7 %all-to-all-start.1 = ((bf16[64,16,128]{2,1,0:T(8,128)(2,1)}), bf16[64,16,128]{2,1,0:T(8,128)(2,1)S(1)}, u32[]{:S(2)}, u32[]{:S(2)}) async-start(bf16[64,16,128]{2,1,0:T(8,128)(2,1)} %bitcast.38), calls=%async_computation.1 | async-start | bytes 524288 | tf_op jit(solution)/shard_map/all_to_all | solution.py:32
  59.0 0.1 reshape.456
  59.1 0.1 copy.61
  59.2 0.1 reshape.465
  59.5 3.4 %collective-permute-start.3 = (bf16[256,128]{1,0:T(8,128)(2,1)S(1)}, bf16[256,128]{1,0:T(8,128)(2,1)S(1)}, u32[]{:S(2)}, u32[]{:S(2)}) collective-permute-start(bf16[256,128]{1,0:T(8,128)(2,1)S(1)} %fusion.27), channel_id=1, source_target_pairs={{0,32},{32,0},{64,96},{96,64},{1,33},{33,1},{65,97},{97,65},{2,34}... | collective-permute-start | bytes 196616 | tf_op jit(solution)/shard_map/ppermute | solution.py:48
  62.9 0.1 copy.60
  63.0 1.9 collective-permute-done.3
  65.0 0.1 reshape_reshape.3
  65.2 0.1 select_n.350
  65.4 0.1 select_n.352
  65.6 3.0 %all-to-all-done.1 = bf16[64,16,128]{2,1,0:T(8,128)(2,1)S(1)} async-done(((bf16[64,16,128]{2,1,0:T(8,128)(2,1)}), bf16[64,16,128]{2,1,0:T(8,128)(2,1)S(1)}, u32[]{:S(2)}, u32[]{:S(2)}) %all-to-all-start.1) | async-done | bytes 262176 | tf_op jit(solution)/shard_map/all_to_all | solution.py:32
  68.6 0.1 convert_reduce_fusion.4
  68.9 0.2 fusion.7
  69.1 0.1 fusion.87
  69.2 0.7 maximum_bitcast_fusion
  69.9 5.5 %all-to-all-start.2 = ((bf16[32,16,128]{2,1,0:T(8,128)(2,1)}), bf16[32,16,128]{2,1,0:T(8,128)(2,1)S(1)}, u32[]{:S(2)}, u32[]{:S(2)}) async-start(bf16[32,16,128]{2,1,0:T(8,128)(2,1)} %maximum_bitcast_fusion), calls=%async_computation.2 | async-start | bytes 262144 | tf_op jit(solution)/shard_map/all_to_all | solution.py:32
  75.4 5.1 %collective-permute-start.4 = (bf16[192,128]{1,0:T(8,128)(2,1)S(1)}, bf16[192,128]{1,0:T(8,128)(2,1)S(1)}, u32[]{:S(2)}, u32[]{:S(2)}) collective-permute-start(bf16[192,128]{1,0:T(8,128)(2,1)S(1)} %get-tuple-element.73), channel_id=1, source_target_pairs={{0,96},{32,64},{64,32},{96,0},{1,97},{33,65},{65,33},{97,1},{2,98}... | collective-permute-start | bytes 147464 | tf_op jit(solution)/shard_map/ppermute | solution.py:48
  80.5 1.9 collective-permute-start.5
  82.5 0.1 collective-permute-done.4
  82.6 4.2 %collective-permute-done.5 = bf16[192,128]{1,0:T(8,128)(2,1)S(1)} collective-permute-done((bf16[192,128]{1,0:T(8,128)(2,1)S(1)}, bf16[192,128]{1,0:T(8,128)(2,1)S(1)}, u32[]{:S(2)}, u32[]{:S(2)}) %collective-permute-start.5) | collective-permute-done | bytes 49184 | tf_op jit(solution)/shard_map/ppermute | solution.py:48
  87.1 3.1 %collective-permute-start.8 = (bf16[416,128]{1,0:T(8,128)(2,1)S(1)}, bf16[416,128]{1,0:T(8,128)(2,1)S(1)}, u32[]{:S(2)}, u32[]{:S(2)}) collective-permute-start(bf16[416,128]{1,0:T(8,128)(2,1)S(1)} %get-tuple-element.59), channel_id=1, source_target_pairs={{0,8},{8,0},{16,24},{24,16},{1,9},{9,1},{17,25},{25,17},{2,10},{10... | collective-permute-start | bytes 319496 | tf_op jit(solution)/shard_map/ppermute | solution.py:48
  90.3 4.4 %collective-permute-start.7 = (bf16[416,128]{1,0:T(8,128)(2,1)S(1)}, bf16[416,128]{1,0:T(8,128)(2,1)S(1)}, u32[]{:S(2)}, u32[]{:S(2)}) collective-permute-start(bf16[416,128]{1,0:T(8,128)(2,1)S(1)} %get-tuple-element.60), channel_id=1, source_target_pairs={{0,16},{8,24},{16,0},{24,8},{1,17},{9,25},{17,1},{25,9},{2,18},{10... | collective-permute-start | bytes 319496 | tf_op jit(solution)/shard_map/ppermute | solution.py:48
  94.7 2.0 %collective-permute-start.6 = (bf16[416,128]{1,0:T(8,128)(2,1)S(1)}, bf16[416,128]{1,0:T(8,128)(2,1)S(1)}, u32[]{:S(2)}, u32[]{:S(2)}) collective-permute-start(bf16[416,128]{1,0:T(8,128)(2,1)S(1)} %get-tuple-element.61), channel_id=1, source_target_pairs={{0,24},{8,16},{16,8},{24,0},{1,25},{9,17},{17,9},{25,1},{2,26},{10... | collective-permute-start | bytes 319496 | tf_op jit(solution)/shard_map/ppermute | solution.py:48
  96.7 0.2 convolution_convert_fusion.4
  96.9 0.7 broadcast_in_dim.90
  97.6 16.3 %all-to-all-start.3 = ((bf16[8,64,128]{2,1,0:T(8,128)(2,1)}), bf16[8,64,128]{2,1,0:T(8,128)(2,1)S(1)}, u32[]{:S(2)}, u32[]{:S(2)}) async-start(bf16[8,64,128]{2,1,0:T(8,128)(2,1)} %broadcast_in_dim.90), calls=%async_computation.3 | async-start | bytes 262144 | tf_op jit(solution)/shard_map/all_to_all | solution.py:38
  114.0 0.1 copy.64
  114.2 11.2 %all-to-all-done.3 = bf16[8,64,128]{2,1,0:T(8,128)(2,1)S(1)} async-done(((bf16[8,64,128]{2,1,0:T(8,128)(2,1)}), bf16[8,64,128]{2,1,0:T(8,128)(2,1)S(1)}, u32[]{:S(2)}, u32[]{:S(2)}) %all-to-all-start.3) | async-done | bytes 131104 | tf_op jit(solution)/shard_map/all_to_all | solution.py:38
  125.5 0.2 convolution_convert_fusion.1
  125.8 0.7 copy.65
  126.5 10.0 %all-to-all-start.4 = ((bf16[32,32,128]{2,1,0:T(8,128)(2,1)}), bf16[32,32,128]{2,1,0:T(8,128)(2,1)S(1)}, u32[]{:S(2)}, u32[]{:S(2)}) async-start(bf16[32,32,128]{2,1,0:T(8,128)(2,1)} %bitcast.100), calls=%async_computation.4 | async-start | bytes 524288 | tf_op jit(solution)/shard_map/all_to_all | solution.py:32
  136.6 11.1 %all-to-all-done.4 = bf16[32,32,128]{2,1,0:T(8,128)(2,1)S(1)} async-done(((bf16[32,32,128]{2,1,0:T(8,128)(2,1)}), bf16[32,32,128]{2,1,0:T(8,128)(2,1)S(1)}, u32[]{:S(2)}, u32[]{:S(2)}) %all-to-all-start.4) | async-done | bytes 262176 | tf_op jit(solution)/shard_map/all_to_all | solution.py:32
  147.6 0.1 multiply_reduce_fusion
  148.2 0.2 fusion.4
  148.3 0.1 fusion.94
  148.6 0.1 reshape.482
  148.8 1.9 collective-permute-start.11
  150.7 5.6 %collective-permute-start.10 = (f32[8,128]{1,0:T(8,128)S(1)}, f32[8,128]{1,0:T(8,128)S(1)}, u32[]{:S(2)}, u32[]{:S(2)}) collective-permute-start(f32[8,128]{1,0:T(8,128)S(1)} %get-tuple-element.110), channel_id=1, source_target_pairs={{0,16},{8,24},{16,0},{24,8},{1,17},{9,25},{17,1},{25,9},{2,18},{10... | collective-permute-start | bytes 12296 | tf_op jit(solution)/shard_map/ppermute | solution.py:48
  156.3 2.0 %collective-permute-start.9 = (f32[8,128]{1,0:T(8,128)S(1)}, f32[8,128]{1,0:T(8,128)S(1)}, u32[]{:S(2)}, u32[]{:S(2)}) collective-permute-start(f32[8,128]{1,0:T(8,128)S(1)} %get-tuple-element.111), channel_id=1, source_target_pairs={{0,24},{8,16},{16,8},{24,0},{1,25},{9,17},{17,9},{25,1},{2,26},{10... | collective-permute-start | bytes 12296 | tf_op jit(solution)/shard_map/ppermute | solution.py:48
  158.4 0.7 copy_bitcast_fusion.1
  159.1 6.1 %all-to-all-start.5 = ((bf16[32,16,128]{2,1,0:T(8,128)(2,1)}), bf16[32,16,128]{2,1,0:T(8,128)(2,1)S(1)}, u32[]{:S(2)}, u32[]{:S(2)}) async-start(bf16[32,16,128]{2,1,0:T(8,128)(2,1)} %copy_bitcast_fusion.1), calls=%async_computation.5 | async-start | bytes 262144 | tf_op jit(solution)/shard_map/all_to_all | solution.py:32
  165.5 0.6 slice_bitcast_fusion.5
  166.1 6.6 %all-to-all-done.5 = bf16[32,16,128]{2,1,0:T(8,128)(2,1)S(1)} async-done(((bf16[32,16,128]{2,1,0:T(8,128)(2,1)}), bf16[32,16,128]{2,1,0:T(8,128)(2,1)S(1)}, u32[]{:S(2)}, u32[]{:S(2)}) %all-to-all-start.5) | async-done | bytes 131104 | tf_op jit(solution)/shard_map/all_to_all | solution.py:32
  172.7 0.2 convolution_convert_fusion.2
  172.9 0.7 reshape.478
  173.5 20.3 %all-to-all-start.6 = ((bf16[32,4,256]{2,1,0:T(4,128)(2,1)}), bf16[32,4,256]{2,1,0:T(4,128)(2,1)S(1)}, u32[]{:S(2)}, u32[]{:S(2)}) async-start(bf16[32,4,256]{2,1,0:T(4,128)(2,1)} %reshape.478), calls=%async_computation.6 | async-start | bytes 131072 | tf_op jit(solution)/shard_map/all_to_all | solution.py:38
  194.0 0.6 pad_maximum_fusion.18
  194.6 7.1 %all-to-all-done.6 = bf16[32,4,256]{2,1,0:T(4,128)(2,1)S(1)} async-done(((bf16[32,4,256]{2,1,0:T(4,128)(2,1)}), bf16[32,4,256]{2,1,0:T(4,128)(2,1)S(1)}, u32[]{:S(2)}, u32[]{:S(2)}) %all-to-all-start.6) | async-done | bytes 65568 | tf_op jit(solution)/shard_map/all_to_all | solution.py:38
  201.8 0.8 fusion.8
  (134 shorter events, 2.7 us)
Async XLA Ops:
  0.6 31.1 %copy-start.3 = (bf16[2,512,32]{1,2,0:T(8,128)(2,1)S(1)}, bf16[2,512,32]{1,2,0:T(8,128)(2,1)}, u32[]{:S(2)}) copy-start(bf16[2,512,32]{1,2,0:T(8,128)(2,1)} %param.17) | copy-start | bytes 196612
  2.0 29.8 %copy-start = (bf16[2,32,3,32]{3,1,2,0:T(8,128)(2,1)S(1)}, bf16[2,32,3,32]{3,1,2,0:T(8,128)(2,1)}, u32[]{:S(2)}) copy-start(bf16[2,32,3,32]{3,1,2,0:T(8,128)(2,1)} %param.15) | copy-start | bytes 36868
  2.0 29.8 %copy-start.2 = (bf16[2,256,32]{1,2,0:T(8,128)(2,1)S(1)}, bf16[2,256,32]{1,2,0:T(8,128)(2,1)}, u32[]{:S(2)}) copy-start(bf16[2,256,32]{1,2,0:T(8,128)(2,1)} %param.21) | copy-start | bytes 98308
  2.0 29.8 %copy-start.7 = (f32[2,32,32]{2,1,0:T(8,128)S(1)}, f32[2,32,32]{2,1,0:T(8,128)}, u32[]{:S(2)}) copy-start(f32[2,32,32]{2,1,0:T(8,128)} %state.1) | copy-start | bytes 24580
  2.0 46.9 %all-to-all-start = ((bf16[32,4,256]{2,1,0:T(4,128)(2,1)}), bf16[32,4,256]{2,1,0:T(4,128)(2,1)S(1)}, u32[]{:S(2)}, u32[]{:S(2)}) async-start(bf16[32,4,256]{2,1,0:T(4,128)(2,1)} %broadcast_in_dim.54), calls=%async_computation | async-start | bytes 131072 | tf_op jit(solution)/shard_map/all_to_all | solution.py:38
  31.7 0.8 copy-start.1
  31.7 0.7 copy-start.8
  31.7 0.7 copy-start.9
  31.7 0.7 copy-start.10
  32.4 0.8 copy-start.4
  33.3 0.8 copy-start.5
  34.5 9.9 %copy-start.6 = (bf16[2,32,512]{2,1,0:T(8,128)(2,1)S(1)}, bf16[2,32,512]{2,1,0:T(8,128)(2,1)}, u32[]{:S(2)}) copy-start(bf16[2,32,512]{2,1,0:T(8,128)(2,1)} %out.1) | copy-start | bytes 196612
  34.5 10.9 %collective-permute-start.2 = (bf16[352,128]{1,0:T(8,128)(2,1)S(1)}, bf16[352,128]{1,0:T(8,128)(2,1)S(1)}, u32[]{:S(2)}, u32[]{:S(2)}) collective-permute-start(bf16[352,128]{1,0:T(8,128)(2,1)S(1)} %get-tuple-element.62), channel_id=1, source_target_pairs={{0,8},{8,0},{16,24},{24,16},{1,9},{9,1},{17,25},{25,17},{2,10},{10... | collective-permute-start | bytes 270344 | tf_op jit(solution)/shard_map/ppermute | solution.py:48
  37.8 7.6 %collective-permute-start.1 = (bf16[352,128]{1,0:T(8,128)(2,1)S(1)}, bf16[352,128]{1,0:T(8,128)(2,1)S(1)}, u32[]{:S(2)}, u32[]{:S(2)}) collective-permute-start(bf16[352,128]{1,0:T(8,128)(2,1)S(1)} %get-tuple-element.63), channel_id=1, source_target_pairs={{0,16},{8,24},{16,0},{24,8},{1,17},{9,25},{17,1},{25,9},{2,18},{10... | collective-permute-start | bytes 270344 | tf_op jit(solution)/shard_map/ppermute | solution.py:48
  42.4 6.5 %collective-permute-start = (bf16[352,128]{1,0:T(8,128)(2,1)S(1)}, bf16[352,128]{1,0:T(8,128)(2,1)S(1)}, u32[]{:S(2)}, u32[]{:S(2)}) collective-permute-start(bf16[352,128]{1,0:T(8,128)(2,1)S(1)} %get-tuple-element.64), channel_id=1, source_target_pairs={{0,24},{8,16},{16,8},{24,0},{1,25},{9,17},{17,9},{25,1},{2,26},{10... | collective-permute-start | bytes 270344 | tf_op jit(solution)/shard_map/ppermute | solution.py:48
  44.7 0.7 copy-start.11
  50.2 18.4 %all-to-all-start.1 = ((bf16[64,16,128]{2,1,0:T(8,128)(2,1)}), bf16[64,16,128]{2,1,0:T(8,128)(2,1)S(1)}, u32[]{:S(2)}, u32[]{:S(2)}) async-start(bf16[64,16,128]{2,1,0:T(8,128)(2,1)} %bitcast.38), calls=%async_computation.1 | async-start | bytes 524288 | tf_op jit(solution)/shard_map/all_to_all | solution.py:32
  59.5 5.5 %collective-permute-start.3 = (bf16[256,128]{1,0:T(8,128)(2,1)S(1)}, bf16[256,128]{1,0:T(8,128)(2,1)S(1)}, u32[]{:S(2)}, u32[]{:S(2)}) collective-permute-start(bf16[256,128]{1,0:T(8,128)(2,1)S(1)} %fusion.27), channel_id=1, source_target_pairs={{0,32},{32,0},{64,96},{96,64},{1,33},{33,1},{65,97},{97,65},{2,34}... | collective-permute-start | bytes 196616 | tf_op jit(solution)/shard_map/ppermute | solution.py:48
  69.9 26.8 %all-to-all-start.2 = ((bf16[32,16,128]{2,1,0:T(8,128)(2,1)}), bf16[32,16,128]{2,1,0:T(8,128)(2,1)S(1)}, u32[]{:S(2)}, u32[]{:S(2)}) async-start(bf16[32,16,128]{2,1,0:T(8,128)(2,1)} %maximum_bitcast_fusion), calls=%async_computation.2 | async-start | bytes 262144 | tf_op jit(solution)/shard_map/all_to_all | solution.py:32
  75.4 7.2 %collective-permute-start.4 = (bf16[192,128]{1,0:T(8,128)(2,1)S(1)}, bf16[192,128]{1,0:T(8,128)(2,1)S(1)}, u32[]{:S(2)}, u32[]{:S(2)}) collective-permute-start(bf16[192,128]{1,0:T(8,128)(2,1)S(1)} %get-tuple-element.73), channel_id=1, source_target_pairs={{0,96},{32,64},{64,32},{96,0},{1,97},{33,65},{65,33},{97,1},{2,98}... | collective-permute-start | bytes 147464 | tf_op jit(solution)/shard_map/ppermute | solution.py:48
  80.5 6.3 %collective-permute-start.5 = (bf16[192,128]{1,0:T(8,128)(2,1)S(1)}, bf16[192,128]{1,0:T(8,128)(2,1)S(1)}, u32[]{:S(2)}, u32[]{:S(2)}) collective-permute-start(bf16[192,128]{1,0:T(8,128)(2,1)S(1)} %get-tuple-element.74), channel_id=1, source_target_pairs={{0,64},{32,96},{64,0},{96,32},{1,65},{33,97},{65,1},{97,33},{2,66}... | collective-permute-start | bytes 147464 | tf_op jit(solution)/shard_map/ppermute | solution.py:48
  87.1 26.7 %collective-permute-start.8 = (bf16[416,128]{1,0:T(8,128)(2,1)S(1)}, bf16[416,128]{1,0:T(8,128)(2,1)S(1)}, u32[]{:S(2)}, u32[]{:S(2)}) collective-permute-start(bf16[416,128]{1,0:T(8,128)(2,1)S(1)} %get-tuple-element.59), channel_id=1, source_target_pairs={{0,8},{8,0},{16,24},{24,16},{1,9},{9,1},{17,25},{25,17},{2,10},{10... | collective-permute-start | bytes 319496 | tf_op jit(solution)/shard_map/ppermute | solution.py:48
  90.3 23.6 %collective-permute-start.7 = (bf16[416,128]{1,0:T(8,128)(2,1)S(1)}, bf16[416,128]{1,0:T(8,128)(2,1)S(1)}, u32[]{:S(2)}, u32[]{:S(2)}) collective-permute-start(bf16[416,128]{1,0:T(8,128)(2,1)S(1)} %get-tuple-element.60), channel_id=1, source_target_pairs={{0,16},{8,24},{16,0},{24,8},{1,17},{9,25},{17,1},{25,9},{2,18},{10... | collective-permute-start | bytes 319496 | tf_op jit(solution)/shard_map/ppermute | solution.py:48
  94.7 19.2 %collective-permute-start.6 = (bf16[416,128]{1,0:T(8,128)(2,1)S(1)}, bf16[416,128]{1,0:T(8,128)(2,1)S(1)}, u32[]{:S(2)}, u32[]{:S(2)}) collective-permute-start(bf16[416,128]{1,0:T(8,128)(2,1)S(1)} %get-tuple-element.61), channel_id=1, source_target_pairs={{0,24},{8,16},{16,8},{24,0},{1,25},{9,17},{17,9},{25,1},{2,26},{10... | collective-permute-start | bytes 319496 | tf_op jit(solution)/shard_map/ppermute | solution.py:48
  97.6 27.9 %all-to-all-start.3 = ((bf16[8,64,128]{2,1,0:T(8,128)(2,1)}), bf16[8,64,128]{2,1,0:T(8,128)(2,1)S(1)}, u32[]{:S(2)}, u32[]{:S(2)}) async-start(bf16[8,64,128]{2,1,0:T(8,128)(2,1)} %broadcast_in_dim.90), calls=%async_computation.3 | async-start | bytes 262144 | tf_op jit(solution)/shard_map/all_to_all | solution.py:38
  126.5 21.1 %all-to-all-start.4 = ((bf16[32,32,128]{2,1,0:T(8,128)(2,1)}), bf16[32,32,128]{2,1,0:T(8,128)(2,1)S(1)}, u32[]{:S(2)}, u32[]{:S(2)}) async-start(bf16[32,32,128]{2,1,0:T(8,128)(2,1)} %bitcast.100), calls=%async_computation.4 | async-start | bytes 524288 | tf_op jit(solution)/shard_map/all_to_all | solution.py:32
  148.8 16.4 %collective-permute-start.11 = (f32[8,128]{1,0:T(8,128)S(1)}, f32[8,128]{1,0:T(8,128)S(1)}, u32[]{:S(2)}, u32[]{:S(2)}) collective-permute-start(f32[8,128]{1,0:T(8,128)S(1)} %get-tuple-element.109), channel_id=1, source_target_pairs={{0,8},{8,0},{16,24},{24,16},{1,9},{9,1},{17,25},{25,17},{2,10},{10... | collective-permute-start | bytes 12296 | tf_op jit(solution)/shard_map/ppermute | solution.py:48
  150.7 14.4 %collective-permute-start.10 = (f32[8,128]{1,0:T(8,128)S(1)}, f32[8,128]{1,0:T(8,128)S(1)}, u32[]{:S(2)}, u32[]{:S(2)}) collective-permute-start(f32[8,128]{1,0:T(8,128)S(1)} %get-tuple-element.110), channel_id=1, source_target_pairs={{0,16},{8,24},{16,0},{24,8},{1,17},{9,25},{17,1},{25,9},{2,18},{10... | collective-permute-start | bytes 12296 | tf_op jit(solution)/shard_map/ppermute | solution.py:48
  156.3 8.8 %collective-permute-start.9 = (f32[8,128]{1,0:T(8,128)S(1)}, f32[8,128]{1,0:T(8,128)S(1)}, u32[]{:S(2)}, u32[]{:S(2)}) collective-permute-start(f32[8,128]{1,0:T(8,128)S(1)} %get-tuple-element.111), channel_id=1, source_target_pairs={{0,24},{8,16},{16,8},{24,0},{1,25},{9,17},{17,9},{25,1},{2,26},{10... | collective-permute-start | bytes 12296 | tf_op jit(solution)/shard_map/ppermute | solution.py:48
  159.1 13.6 %all-to-all-start.5 = ((bf16[32,16,128]{2,1,0:T(8,128)(2,1)}), bf16[32,16,128]{2,1,0:T(8,128)(2,1)S(1)}, u32[]{:S(2)}, u32[]{:S(2)}) async-start(bf16[32,16,128]{2,1,0:T(8,128)(2,1)} %copy_bitcast_fusion.1), calls=%async_computation.5 | async-start | bytes 262144 | tf_op jit(solution)/shard_map/all_to_all | solution.py:32
  173.5 28.2 %all-to-all-start.6 = ((bf16[32,4,256]{2,1,0:T(4,128)(2,1)}), bf16[32,4,256]{2,1,0:T(4,128)(2,1)S(1)}, u32[]{:S(2)}, u32[]{:S(2)}) async-start(bf16[32,4,256]{2,1,0:T(4,128)(2,1)} %reshape.478), calls=%async_computation.6 | async-start | bytes 131072 | tf_op jit(solution)/shard_map/all_to_all | solution.py:38

commit v12 on v11

--- a/solution.py
+++ b/solution.py
@@ -19,7 +19,7 @@
 PLANE = ("x", "core", "y")
 PAIRED_PLANE = ("zl", "y", "x", "core")
 FIRST_GATHER = 22
-FIRST_REDUCE = 3
+FIRST_REDUCE = 4
 FIRST_LAST = 18
 bf16 = jnp.bfloat16
 f32 = jnp.float32
@@ -185,9 +185,9 @@
     near, second_weights = packed_for_y(
         w_branch.transpose(0, 2, 1),
         w_gate_branch.transpose(0, 2, 1),
-        w_out,
-        w_in_gate.transpose(0, 2, 1),
-        w_rec_gate.transpose(0, 2, 1),
+        w_out[:1],
+        w_in_gate[:1].transpose(0, 2, 1),
+        w_rec_gate[:1].transpose(0, 2, 1),
         norm_gain,
         prior_state,
         prior_window.transpose(0, 2, 1, 3),

time: 204 us -> 203 us (level)
  starting transfers between devices: 136 us -> 139 us
    all_to_all x3, starting transfers between devices: 66.2 us -> 72 us  [exchange_far(): lax.all_to_all(tiles, axes, 0, 0, axis_index_groups=[order], tiled=True)]
    all_to_all x4, starting transfers between devices: 30.3 us -> 27.5 us  [exchange(): return lax.all_to_all(tiles, axes, 0, 0, tiled=True)]
where the time goes in v12:
time: 203 us; the launch traced here: 202 us
  starting transfers between devices  139 us (68%)
  waiting for transfers between devices  46.6 us (23%)
  local copies, waits for them, and re-layouts  8.53 us (4%)
  other arithmetic  3.9 us (2%)
  matrix products  2.11 us (1%)
    all_to_all x3, starting transfers between devices, exchange_far(): lax.all_to_all(tiles, axes, 0, 0, axis_index_groups=[order], tiled=True)  72 us
    ppermute x12, starting transfers between devices, passed(): lax.ppermute(piece, axis, [(at, at ^ flip) for at in range(lax.axis_size(...  39.2 us
    all_to_all x4, starting transfers between devices, exchange(): return lax.all_to_all(tiles, axes, 0, 0, tiled=True)  27.5 us
    all_to_all x4, waiting for transfers between devices, exchange(): return lax.all_to_all(tiles, axes, 0, 0, tiled=True)  20.7 us
    all_to_all x3, waiting for transfers between devices, exchange_far(): lax.all_to_all(tiles, axes, 0, 0, axis_index_groups=[order], tiled=True)  16.3 us
    ppermute x12, waiting for transfers between devices, passed(): lax.ppermute(piece, axis, [(at, at ^ flip) for at in range(lax.axis_size(...  9.66 us
  transfers between devices with their start and end apart: 19, of which 9 were waited for; matrix products, arithmetic and copies ran while one was open for 3% of the time, Pallas kernels for 0%

profile of v12, /device:TPU:1, one launch (start us, length us, event | category | flops | bytes accessed | tf_op | source)
XLA Modules:
  0.0 201.8 jit_solution(11076591122179224913)
XLA Ops:
  0.6 1.4 broadcast_in_dim.54
  2.0 29.7 %all-to-all-start = ((bf16[32,4,256]{2,1,0:T(4,128)(2,1)}), bf16[32,4,256]{2,1,0:T(4,128)(2,1)S(1)}, u32[]{:S(2)}, u32[]{:S(2)}) async-start(bf16[32,4,256]{2,1,0:T(4,128)(2,1)} %broadcast_in_dim.54), calls=%async_computation | async-start | bytes 131072 | tf_op jit(solution)/shard_map/all_to_all | solution.py:38
  31.9 0.5 copy-done.4
  32.4 0.1 copy-done.3
  32.5 0.1 copy-done.1
  32.6 0.3 shard_map.139
  32.9 3.2 %collective-permute-start.2 = (bf16[352,128]{1,0:T(8,128)(2,1)S(1)}, bf16[352,128]{1,0:T(8,128)(2,1)S(1)}, u32[]{:S(2)}, u32[]{:S(2)}) collective-permute-start(bf16[352,128]{1,0:T(8,128)(2,1)S(1)} %get-tuple-element.62), channel_id=1, source_target_pairs={{0,8},{8,0},{16,24},{24,16},{1,9},{9,1},{17,25},{25,17},{2,10},{10... | collective-permute-start | bytes 270344 | tf_op jit(solution)/shard_map/ppermute | solution.py:48
  36.1 4.5 %collective-permute-start.1 = (bf16[352,128]{1,0:T(8,128)(2,1)S(1)}, bf16[352,128]{1,0:T(8,128)(2,1)S(1)}, u32[]{:S(2)}, u32[]{:S(2)}) collective-permute-start(bf16[352,128]{1,0:T(8,128)(2,1)S(1)} %get-tuple-element.63), channel_id=1, source_target_pairs={{0,16},{8,24},{16,0},{24,8},{1,17},{9,25},{17,1},{25,9},{2,18},{10... | collective-permute-start | bytes 270344 | tf_op jit(solution)/shard_map/ppermute | solution.py:48
  40.7 1.9 collective-permute-start
  42.7 0.3 fusion.1
  43.0 0.6 copy-done.10
  43.7 3.4 %collective-permute-done = bf16[352,128]{1,0:T(8,128)(2,1)S(1)} collective-permute-done((bf16[352,128]{1,0:T(8,128)(2,1)S(1)}, bf16[352,128]{1,0:T(8,128)(2,1)S(1)}, u32[]{:S(2)}, u32[]{:S(2)}) %collective-permute-start) | collective-permute-done | bytes 90144 | tf_op jit(solution)/shard_map/ppermute | solution.py:48
  47.3 0.2 fusion
  47.5 0.2 copy.54
  47.8 0.7 copy.57
  48.5 8.7 %all-to-all-start.1 = ((bf16[64,16,128]{2,1,0:T(8,128)(2,1)}), bf16[64,16,128]{2,1,0:T(8,128)(2,1)S(1)}, u32[]{:S(2)}, u32[]{:S(2)}) async-start(bf16[64,16,128]{2,1,0:T(8,128)(2,1)} %bitcast.38), calls=%async_computation.1 | async-start | bytes 524288 | tf_op jit(solution)/shard_map/all_to_all | solution.py:32
  57.3 0.1 reshape.456
  57.4 0.1 copy.61
  57.5 0.1 reshape.465
  57.8 3.4 %collective-permute-start.3 = (bf16[256,128]{1,0:T(8,128)(2,1)S(1)}, bf16[256,128]{1,0:T(8,128)(2,1)S(1)}, u32[]{:S(2)}, u32[]{:S(2)}) collective-permute-start(bf16[256,128]{1,0:T(8,128)(2,1)S(1)} %fusion.27), channel_id=1, source_target_pairs={{0,32},{32,0},{64,96},{96,64},{1,33},{33,1},{65,97},{97,65},{2,34}... | collective-permute-start | bytes 196616 | tf_op jit(solution)/shard_map/ppermute | solution.py:48
  61.2 0.1 copy.60
  61.3 1.9 collective-permute-done.3
  63.3 0.1 reshape_reshape.3
  63.5 0.1 select_n.350
  63.7 0.1 select_n.352
  63.9 3.0 %all-to-all-done.1 = bf16[64,16,128]{2,1,0:T(8,128)(2,1)S(1)} async-done(((bf16[64,16,128]{2,1,0:T(8,128)(2,1)}), bf16[64,16,128]{2,1,0:T(8,128)(2,1)S(1)}, u32[]{:S(2)}, u32[]{:S(2)}) %all-to-all-start.1) | async-done | bytes 262176 | tf_op jit(solution)/shard_map/all_to_all | solution.py:32
  66.9 0.1 convert_reduce_fusion.4
  67.2 0.2 fusion.7
  67.4 0.1 fusion.87
  67.5 0.7 maximum_bitcast_fusion
  68.2 5.5 %all-to-all-start.2 = ((bf16[32,16,128]{2,1,0:T(8,128)(2,1)}), bf16[32,16,128]{2,1,0:T(8,128)(2,1)S(1)}, u32[]{:S(2)}, u32[]{:S(2)}) async-start(bf16[32,16,128]{2,1,0:T(8,128)(2,1)} %maximum_bitcast_fusion), calls=%async_computation.2 | async-start | bytes 262144 | tf_op jit(solution)/shard_map/all_to_all | solution.py:32
  73.7 5.1 %collective-permute-start.4 = (bf16[192,128]{1,0:T(8,128)(2,1)S(1)}, bf16[192,128]{1,0:T(8,128)(2,1)S(1)}, u32[]{:S(2)}, u32[]{:S(2)}) collective-permute-start(bf16[192,128]{1,0:T(8,128)(2,1)S(1)} %get-tuple-element.73), channel_id=1, source_target_pairs={{0,96},{32,64},{64,32},{96,0},{1,97},{33,65},{65,33},{97,1},{2,98}... | collective-permute-start | bytes 147464 | tf_op jit(solution)/shard_map/ppermute | solution.py:48
  78.8 1.9 collective-permute-start.5
  80.8 0.1 collective-permute-done.4
  80.9 4.2 %collective-permute-done.5 = bf16[192,128]{1,0:T(8,128)(2,1)S(1)} collective-permute-done((bf16[192,128]{1,0:T(8,128)(2,1)S(1)}, bf16[192,128]{1,0:T(8,128)(2,1)S(1)}, u32[]{:S(2)}, u32[]{:S(2)}) %collective-permute-start.5) | collective-permute-done | bytes 49184 | tf_op jit(solution)/shard_map/ppermute | solution.py:48
  85.4 3.1 %collective-permute-start.8 = (bf16[416,128]{1,0:T(8,128)(2,1)S(1)}, bf16[416,128]{1,0:T(8,128)(2,1)S(1)}, u32[]{:S(2)}, u32[]{:S(2)}) collective-permute-start(bf16[416,128]{1,0:T(8,128)(2,1)S(1)} %get-tuple-element.59), channel_id=1, source_target_pairs={{0,8},{8,0},{16,24},{24,16},{1,9},{9,1},{17,25},{25,17},{2,10},{10... | collective-permute-start | bytes 319496 | tf_op jit(solution)/shard_map/ppermute | solution.py:48
  88.6 4.4 %collective-permute-start.7 = (bf16[416,128]{1,0:T(8,128)(2,1)S(1)}, bf16[416,128]{1,0:T(8,128)(2,1)S(1)}, u32[]{:S(2)}, u32[]{:S(2)}) collective-permute-start(bf16[416,128]{1,0:T(8,128)(2,1)S(1)} %get-tuple-element.60), channel_id=1, source_target_pairs={{0,16},{8,24},{16,0},{24,8},{1,17},{9,25},{17,1},{25,9},{2,18},{10... | collective-permute-start | bytes 319496 | tf_op jit(solution)/shard_map/ppermute | solution.py:48
  93.0 2.0 %collective-permute-start.6 = (bf16[416,128]{1,0:T(8,128)(2,1)S(1)}, bf16[416,128]{1,0:T(8,128)(2,1)S(1)}, u32[]{:S(2)}, u32[]{:S(2)}) collective-permute-start(bf16[416,128]{1,0:T(8,128)(2,1)S(1)} %get-tuple-element.61), channel_id=1, source_target_pairs={{0,24},{8,16},{16,8},{24,0},{1,25},{9,17},{17,9},{25,1},{2,26},{10... | collective-permute-start | bytes 319496 | tf_op jit(solution)/shard_map/ppermute | solution.py:48
  95.1 0.2 convolution_convert_fusion.4
  95.2 0.7 broadcast_in_dim.90
  95.9 21.1 %all-to-all-start.3 = ((bf16[8,64,128]{2,1,0:T(8,128)(2,1)}), bf16[8,64,128]{2,1,0:T(8,128)(2,1)S(1)}, u32[]{:S(2)}, u32[]{:S(2)}) async-start(bf16[8,64,128]{2,1,0:T(8,128)(2,1)} %broadcast_in_dim.90), calls=%async_computation.3 | async-start | bytes 262144 | tf_op jit(solution)/shard_map/all_to_all | solution.py:38
  117.2 0.1 copy.64
  117.3 9.2 %all-to-all-done.3 = bf16[8,64,128]{2,1,0:T(8,128)(2,1)S(1)} async-done(((bf16[8,64,128]{2,1,0:T(8,128)(2,1)}), bf16[8,64,128]{2,1,0:T(8,128)(2,1)S(1)}, u32[]{:S(2)}, u32[]{:S(2)}) %all-to-all-start.3) | async-done | bytes 131104 | tf_op jit(solution)/shard_map/all_to_all | solution.py:38
  126.6 0.2 convolution_convert_fusion.1
  126.9 0.7 copy.65
  127.6 7.2 %all-to-all-start.4 = ((bf16[32,32,128]{2,1,0:T(8,128)(2,1)}), bf16[32,32,128]{2,1,0:T(8,128)(2,1)S(1)}, u32[]{:S(2)}, u32[]{:S(2)}) async-start(bf16[32,32,128]{2,1,0:T(8,128)(2,1)} %bitcast.100), calls=%async_computation.4 | async-start | bytes 524288 | tf_op jit(solution)/shard_map/all_to_all | solution.py:32
  134.9 11.1 %all-to-all-done.4 = bf16[32,32,128]{2,1,0:T(8,128)(2,1)S(1)} async-done(((bf16[32,32,128]{2,1,0:T(8,128)(2,1)}), bf16[32,32,128]{2,1,0:T(8,128)(2,1)S(1)}, u32[]{:S(2)}, u32[]{:S(2)}) %all-to-all-start.4) | async-done | bytes 262176 | tf_op jit(solution)/shard_map/all_to_all | solution.py:32
  146.0 0.1 multiply_reduce_fusion
  146.5 0.2 fusion.4
  146.7 0.1 fusion.94
  146.9 0.1 reshape.482
  147.1 1.9 collective-permute-start.11
  149.0 5.6 %collective-permute-start.10 = (f32[8,128]{1,0:T(8,128)S(1)}, f32[8,128]{1,0:T(8,128)S(1)}, u32[]{:S(2)}, u32[]{:S(2)}) collective-permute-start(f32[8,128]{1,0:T(8,128)S(1)} %get-tuple-element.110), channel_id=1, source_target_pairs={{0,16},{8,24},{16,0},{24,8},{1,17},{9,25},{17,1},{25,9},{2,18},{10... | collective-permute-start | bytes 12296 | tf_op jit(solution)/shard_map/ppermute | solution.py:48
  154.7 2.0 %collective-permute-start.9 = (f32[8,128]{1,0:T(8,128)S(1)}, f32[8,128]{1,0:T(8,128)S(1)}, u32[]{:S(2)}, u32[]{:S(2)}) collective-permute-start(f32[8,128]{1,0:T(8,128)S(1)} %get-tuple-element.111), channel_id=1, source_target_pairs={{0,24},{8,16},{16,8},{24,0},{1,25},{9,17},{17,9},{25,1},{2,26},{10... | collective-permute-start | bytes 12296 | tf_op jit(solution)/shard_map/ppermute | solution.py:48
  156.7 0.7 copy_bitcast_fusion.1
  157.4 6.1 %all-to-all-start.5 = ((bf16[32,16,128]{2,1,0:T(8,128)(2,1)}), bf16[32,16,128]{2,1,0:T(8,128)(2,1)S(1)}, u32[]{:S(2)}, u32[]{:S(2)}) async-start(bf16[32,16,128]{2,1,0:T(8,128)(2,1)} %copy_bitcast_fusion.1), calls=%async_computation.5 | async-start | bytes 262144 | tf_op jit(solution)/shard_map/all_to_all | solution.py:32
  163.8 0.6 slice_bitcast_fusion.5
  164.4 6.6 %all-to-all-done.5 = bf16[32,16,128]{2,1,0:T(8,128)(2,1)S(1)} async-done(((bf16[32,16,128]{2,1,0:T(8,128)(2,1)}), bf16[32,16,128]{2,1,0:T(8,128)(2,1)S(1)}, u32[]{:S(2)}, u32[]{:S(2)}) %all-to-all-start.5) | async-done | bytes 131104 | tf_op jit(solution)/shard_map/all_to_all | solution.py:32
  171.0 0.2 convolution_convert_fusion.2
  171.2 0.7 reshape.478
  171.9 21.2 %all-to-all-start.6 = ((bf16[32,4,256]{2,1,0:T(4,128)(2,1)}), bf16[32,4,256]{2,1,0:T(4,128)(2,1)S(1)}, u32[]{:S(2)}, u32[]{:S(2)}) async-start(bf16[32,4,256]{2,1,0:T(4,128)(2,1)} %reshape.478), calls=%async_computation.6 | async-start | bytes 131072 | tf_op jit(solution)/shard_map/all_to_all | solution.py:38
  193.2 0.6 pad_maximum_fusion.18
  193.9 7.1 %all-to-all-done.6 = bf16[32,4,256]{2,1,0:T(4,128)(2,1)S(1)} async-done(((bf16[32,4,256]{2,1,0:T(4,128)(2,1)}), bf16[32,4,256]{2,1,0:T(4,128)(2,1)S(1)}, u32[]{:S(2)}, u32[]{:S(2)}) %all-to-all-start.6) | async-done | bytes 65568 | tf_op jit(solution)/shard_map/all_to_all | solution.py:38
  201.0 0.8 fusion.8
  (134 shorter events, 2.7 us)
Async XLA Ops:
  0.6 31.1 %copy-start.9 = (bf16[2,32,512]{2,1,0:T(8,128)(2,1)S(1)}, bf16[2,32,512]{2,1,0:T(8,128)(2,1)}, u32[]{:S(2)}) copy-start(bf16[2,32,512]{2,1,0:T(8,128)(2,1)} %param.23) | copy-start | bytes 196612
  2.0 29.8 %copy-start.7 = (bf16[2,256,32]{1,2,0:T(8,128)(2,1)S(1)}, bf16[2,256,32]{1,2,0:T(8,128)(2,1)}, u32[]{:S(2)}) copy-start(bf16[2,256,32]{1,2,0:T(8,128)(2,1)} %param.21) | copy-start | bytes 98308
  2.0 29.8 %copy-start.8 = (bf16[2,256,32]{1,2,0:T(8,128)(2,1)S(1)}, bf16[2,256,32]{1,2,0:T(8,128)(2,1)}, u32[]{:S(2)}) copy-start(bf16[2,256,32]{1,2,0:T(8,128)(2,1)} %param.20) | copy-start | bytes 98308
  2.0 29.8 %copy-start.2 = (bf16[2,512,32]{1,2,0:T(8,128)(2,1)S(1)}, bf16[2,512,32]{1,2,0:T(8,128)(2,1)}, u32[]{:S(2)}) copy-start(bf16[2,512,32]{1,2,0:T(8,128)(2,1)} %param.18) | copy-start | bytes 196612
  2.0 45.3 %all-to-all-start = ((bf16[32,4,256]{2,1,0:T(4,128)(2,1)}), bf16[32,4,256]{2,1,0:T(4,128)(2,1)S(1)}, u32[]{:S(2)}, u32[]{:S(2)}) async-start(bf16[32,4,256]{2,1,0:T(4,128)(2,1)} %broadcast_in_dim.54), calls=%async_computation | async-start | bytes 131072 | tf_op jit(solution)/shard_map/all_to_all | solution.py:38
  31.7 0.7 copy-start.4
  31.7 0.8 copy-start.3
  31.7 0.8 copy-start.1
  31.8 0.8 copy-start
  31.8 0.8 copy-start.5
  31.8 0.8 copy-start.6
  32.9 10.8 %collective-permute-start.2 = (bf16[352,128]{1,0:T(8,128)(2,1)S(1)}, bf16[352,128]{1,0:T(8,128)(2,1)S(1)}, u32[]{:S(2)}, u32[]{:S(2)}) collective-permute-start(bf16[352,128]{1,0:T(8,128)(2,1)S(1)} %get-tuple-element.62), channel_id=1, source_target_pairs={{0,8},{8,0},{16,24},{24,16},{1,9},{9,1},{17,25},{25,17},{2,10},{10... | collective-permute-start | bytes 270344 | tf_op jit(solution)/shard_map/ppermute | solution.py:48
  36.1 7.6 %collective-permute-start.1 = (bf16[352,128]{1,0:T(8,128)(2,1)S(1)}, bf16[352,128]{1,0:T(8,128)(2,1)S(1)}, u32[]{:S(2)}, u32[]{:S(2)}) collective-permute-start(bf16[352,128]{1,0:T(8,128)(2,1)S(1)} %get-tuple-element.63), channel_id=1, source_target_pairs={{0,16},{8,24},{16,0},{24,8},{1,17},{9,25},{17,1},{25,9},{2,18},{10... | collective-permute-start | bytes 270344 | tf_op jit(solution)/shard_map/ppermute | solution.py:48
  40.7 6.5 %collective-permute-start = (bf16[352,128]{1,0:T(8,128)(2,1)S(1)}, bf16[352,128]{1,0:T(8,128)(2,1)S(1)}, u32[]{:S(2)}, u32[]{:S(2)}) collective-permute-start(bf16[352,128]{1,0:T(8,128)(2,1)S(1)} %get-tuple-element.64), channel_id=1, source_target_pairs={{0,24},{8,16},{16,8},{24,0},{1,25},{9,17},{17,9},{25,1},{2,26},{10... | collective-permute-start | bytes 270344 | tf_op jit(solution)/shard_map/ppermute | solution.py:48
  43.0 0.7 copy-start.10
  48.5 18.4 %all-to-all-start.1 = ((bf16[64,16,128]{2,1,0:T(8,128)(2,1)}), bf16[64,16,128]{2,1,0:T(8,128)(2,1)S(1)}, u32[]{:S(2)}, u32[]{:S(2)}) async-start(bf16[64,16,128]{2,1,0:T(8,128)(2,1)} %bitcast.38), calls=%async_computation.1 | async-start | bytes 524288 | tf_op jit(solution)/shard_map/all_to_all | solution.py:32
  57.8 5.5 %collective-permute-start.3 = (bf16[256,128]{1,0:T(8,128)(2,1)S(1)}, bf16[256,128]{1,0:T(8,128)(2,1)S(1)}, u32[]{:S(2)}, u32[]{:S(2)}) collective-permute-start(bf16[256,128]{1,0:T(8,128)(2,1)S(1)} %fusion.27), channel_id=1, source_target_pairs={{0,32},{32,0},{64,96},{96,64},{1,33},{33,1},{65,97},{97,65},{2,34}... | collective-permute-start | bytes 196616 | tf_op jit(solution)/shard_map/ppermute | solution.py:48
  68.2 26.8 %all-to-all-start.2 = ((bf16[32,16,128]{2,1,0:T(8,128)(2,1)}), bf16[32,16,128]{2,1,0:T(8,128)(2,1)S(1)}, u32[]{:S(2)}, u32[]{:S(2)}) async-start(bf16[32,16,128]{2,1,0:T(8,128)(2,1)} %maximum_bitcast_fusion), calls=%async_computation.2 | async-start | bytes 262144 | tf_op jit(solution)/shard_map/all_to_all | solution.py:32
  73.7 7.2 %collective-permute-start.4 = (bf16[192,128]{1,0:T(8,128)(2,1)S(1)}, bf16[192,128]{1,0:T(8,128)(2,1)S(1)}, u32[]{:S(2)}, u32[]{:S(2)}) collective-permute-start(bf16[192,128]{1,0:T(8,128)(2,1)S(1)} %get-tuple-element.73), channel_id=1, source_target_pairs={{0,96},{32,64},{64,32},{96,0},{1,97},{33,65},{65,33},{97,1},{2,98}... | collective-permute-start | bytes 147464 | tf_op jit(solution)/shard_map/ppermute | solution.py:48
  78.8 6.3 %collective-permute-start.5 = (bf16[192,128]{1,0:T(8,128)(2,1)S(1)}, bf16[192,128]{1,0:T(8,128)(2,1)S(1)}, u32[]{:S(2)}, u32[]{:S(2)}) collective-permute-start(bf16[192,128]{1,0:T(8,128)(2,1)S(1)} %get-tuple-element.74), channel_id=1, source_target_pairs={{0,64},{32,96},{64,0},{96,32},{1,65},{33,97},{65,1},{97,33},{2,66}... | collective-permute-start | bytes 147464 | tf_op jit(solution)/shard_map/ppermute | solution.py:48
  85.4 31.5 %collective-permute-start.8 = (bf16[416,128]{1,0:T(8,128)(2,1)S(1)}, bf16[416,128]{1,0:T(8,128)(2,1)S(1)}, u32[]{:S(2)}, u32[]{:S(2)}) collective-permute-start(bf16[416,128]{1,0:T(8,128)(2,1)S(1)} %get-tuple-element.59), channel_id=1, source_target_pairs={{0,8},{8,0},{16,24},{24,16},{1,9},{9,1},{17,25},{25,17},{2,10},{10... | collective-permute-start | bytes 319496 | tf_op jit(solution)/shard_map/ppermute | solution.py:48
  88.6 28.4 %collective-permute-start.7 = (bf16[416,128]{1,0:T(8,128)(2,1)S(1)}, bf16[416,128]{1,0:T(8,128)(2,1)S(1)}, u32[]{:S(2)}, u32[]{:S(2)}) collective-permute-start(bf16[416,128]{1,0:T(8,128)(2,1)S(1)} %get-tuple-element.60), channel_id=1, source_target_pairs={{0,16},{8,24},{16,0},{24,8},{1,17},{9,25},{17,1},{25,9},{2,18},{10... | collective-permute-start | bytes 319496 | tf_op jit(solution)/shard_map/ppermute | solution.py:48
  93.0 24.0 %collective-permute-start.6 = (bf16[416,128]{1,0:T(8,128)(2,1)S(1)}, bf16[416,128]{1,0:T(8,128)(2,1)S(1)}, u32[]{:S(2)}, u32[]{:S(2)}) collective-permute-start(bf16[416,128]{1,0:T(8,128)(2,1)S(1)} %get-tuple-element.61), channel_id=1, source_target_pairs={{0,24},{8,16},{16,8},{24,0},{1,25},{9,17},{17,9},{25,1},{2,26},{10... | collective-permute-start | bytes 319496 | tf_op jit(solution)/shard_map/ppermute | solution.py:48
  95.9 30.6 %all-to-all-start.3 = ((bf16[8,64,128]{2,1,0:T(8,128)(2,1)}), bf16[8,64,128]{2,1,0:T(8,128)(2,1)S(1)}, u32[]{:S(2)}, u32[]{:S(2)}) async-start(bf16[8,64,128]{2,1,0:T(8,128)(2,1)} %broadcast_in_dim.90), calls=%async_computation.3 | async-start | bytes 262144 | tf_op jit(solution)/shard_map/all_to_all | solution.py:38
  127.6 18.3 %all-to-all-start.4 = ((bf16[32,32,128]{2,1,0:T(8,128)(2,1)}), bf16[32,32,128]{2,1,0:T(8,128)(2,1)S(1)}, u32[]{:S(2)}, u32[]{:S(2)}) async-start(bf16[32,32,128]{2,1,0:T(8,128)(2,1)} %bitcast.100), calls=%async_computation.4 | async-start | bytes 524288 | tf_op jit(solution)/shard_map/all_to_all | solution.py:32
  147.1 16.4 %collective-permute-start.11 = (f32[8,128]{1,0:T(8,128)S(1)}, f32[8,128]{1,0:T(8,128)S(1)}, u32[]{:S(2)}, u32[]{:S(2)}) collective-permute-start(f32[8,128]{1,0:T(8,128)S(1)} %get-tuple-element.109), channel_id=1, source_target_pairs={{0,8},{8,0},{16,24},{24,16},{1,9},{9,1},{17,25},{25,17},{2,10},{10... | collective-permute-start | bytes 12296 | tf_op jit(solution)/shard_map/ppermute | solution.py:48
  149.0 14.4 %collective-permute-start.10 = (f32[8,128]{1,0:T(8,128)S(1)}, f32[8,128]{1,0:T(8,128)S(1)}, u32[]{:S(2)}, u32[]{:S(2)}) collective-permute-start(f32[8,128]{1,0:T(8,128)S(1)} %get-tuple-element.110), channel_id=1, source_target_pairs={{0,16},{8,24},{16,0},{24,8},{1,17},{9,25},{17,1},{25,9},{2,18},{10... | collective-permute-start | bytes 12296 | tf_op jit(solution)/shard_map/ppermute | solution.py:48
  154.7 8.8 %collective-permute-start.9 = (f32[8,128]{1,0:T(8,128)S(1)}, f32[8,128]{1,0:T(8,128)S(1)}, u32[]{:S(2)}, u32[]{:S(2)}) collective-permute-start(f32[8,128]{1,0:T(8,128)S(1)} %get-tuple-element.111), channel_id=1, source_target_pairs={{0,24},{8,16},{16,8},{24,0},{1,25},{9,17},{17,9},{25,1},{2,26},{10... | collective-permute-start | bytes 12296 | tf_op jit(solution)/shard_map/ppermute | solution.py:48
  157.4 13.6 %all-to-all-start.5 = ((bf16[32,16,128]{2,1,0:T(8,128)(2,1)}), bf16[32,16,128]{2,1,0:T(8,128)(2,1)S(1)}, u32[]{:S(2)}, u32[]{:S(2)}) async-start(bf16[32,16,128]{2,1,0:T(8,128)(2,1)} %copy_bitcast_fusion.1), calls=%async_computation.5 | async-start | bytes 262144 | tf_op jit(solution)/shard_map/all_to_all | solution.py:32
  171.9 29.1 %all-to-all-start.6 = ((bf16[32,4,256]{2,1,0:T(4,128)(2,1)}), bf16[32,4,256]{2,1,0:T(4,128)(2,1)S(1)}, u32[]{:S(2)}, u32[]{:S(2)}) async-start(bf16[32,4,256]{2,1,0:T(4,128)(2,1)} %reshape.478), calls=%async_computation.6 | async-start | bytes 131072 | tf_op jit(solution)/shard_map/all_to_all | solution.py:38
